TPU v7x, 128 devices: a whole 4x4x4 slice. The times are simulated.
128 devices in a mesh: sp: 16 (over z, x), tp: 8 (over y, core).
Axes of the slice: x: 4, y: 4, z: 4, core: 2. Of those that a mesh axis runs over, the one named last changes fastest.
Arguments:
- tokens: bfloat16 [2048, 1024], P('sp', 'tp'), may hold values from -6 to 6
- norm_gain: float32 [3, 1024], replicated, may hold values from 0.1 to 1.9
- w_query: bfloat16 [3, 1024, 1024], P(None, 'sp', 'tp'), may hold values from -0.1875 to 0.1875
- w_key: bfloat16 [3, 1024, 1024], P(None, 'sp', 'tp'), may hold values from -0.1875 to 0.1875
- w_value: bfloat16 [3, 1024, 1024], P(None, 'sp', 'tp'), may hold values from -0.1875 to 0.1875
- w_out: bfloat16 [3, 1024, 1024], P(None, 'tp', 'sp'), may hold values from -0.5625 to 0.5625
- offset_bias: float32 [3, 16, 8, 16], P(None, 'tp'), may hold values from -3 to 3
- documents: int32 [2048], P('sp'), may hold values from 0 to 15, never falling along the last dimension, each value on 1 to 256 neighbouring positions
Outputs:
- mixed: bfloat16 [2048, 1024], P('sp', 'tp')
Inputs may be any that keep to these rules, and one draw needn't show every extreme that they name: `documents`: document numbers never fall along the token order, start at 0, and each document has 1 to 256 tokens.
All inputs are finite; a program needn't handle non-finite values.
Results may differ from a plain program's by a relative error of at most 0.02.
Values may be sent and summed in bfloat16 or wider, within the bound.
No kernel may reach another device: no remote copies, remote signals or barrier semaphores. Data moves between devices by JAX's collectives and lax.ppermute only.
A program may use at most 64 MiB of HBM per device.

v0:
```python
import jax
import jax.numpy as jnp
from jax import lax
from jax.sharding import Mesh
from jax.sharding import PartitionSpec as P

HEAD_DIM = 64
WIN_ROWS = 8
WIN_COLS = 16
LAYERS = 3
GRID_W = 32
TP = ("tp_0", "tp_1")


EPS = 1e-06


def with_halo(shard, sides, width, wrap):
    for axis, dim in sides:
        count, length = lax.axis_size(axis), shard.shape[dim]
        up = [(i, (i + 1) % count) for i in range(count if wrap else count - 1)]
        down = [(j, i) for i, j in up]
        last = lax.slice_in_dim(shard, length - width, length, axis=dim)
        leading = lax.slice_in_dim(shard, 0, width, axis=dim)
        before = lax.ppermute(last, axis, up)
        after = lax.ppermute(leading, axis, down)
        shard = jnp.concatenate([before, shard, after], axis=dim)
    return shard


def laid_out(blocks, dim):
    dims = list(blocks.shape[1:])
    dims[dim] *= blocks.shape[0]
    return jnp.moveaxis(blocks, 0, dim).reshape(dims)


def gather_together(arrays, axis, dims):
    ravelled = jnp.concatenate([a.reshape(-1) for a in arrays])
    lines, at, done = lax.all_gather(ravelled, axis), 0, []
    for a, dim in zip(arrays, dims):
        blocks = lines[:, at : at + a.size].reshape(-1, *a.shape)
        done.append(laid_out(blocks, dim))
        at += a.size
    return tuple(done)


def stacked_from(shard, axes, sequence):
    blocks = shard[None]
    for k in sequence:
        blocks = lax.all_gather(blocks, axes[k], axis=0, tiled=True)
    current = [lax.axis_size(axes[k]) for k in reversed(sequence)]
    blocks = blocks.reshape(*current, *shard.shape)
    turned = sorted(range(len(sequence)), key=lambda place: sequence[len(sequence) - 1 - place])
    return blocks.transpose(*turned, *range(len(sequence), blocks.ndim)).reshape(-1, *shard.shape)


def whole_of(shard, axes, sequence, dim):
    return laid_out(stacked_from(shard, axes, sequence), dim)


def rms_rows(stream, gain_row):
    values = stream.astype(jnp.float32)
    mean_sq = jnp.mean(values * values, axis=-1, keepdims=True)
    return (values * lax.rsqrt(mean_sq + EPS) * gain_row).astype(jnp.bfloat16)


def head_norm(heads_raw):
    values = heads_raw.astype(jnp.float32)
    mean_sq = jnp.mean(values * values, axis=-1, keepdims=True)
    return (values * lax.rsqrt(mean_sq + EPS)).astype(jnp.bfloat16)


def attend(queries, fringe, seg_own, seg_fringe, bias_layer):
    row_count, grid_width, head_count, head_width = queries.shape
    key_rows = jnp.stack(
        [fringe[row_lag : row_lag + row_count] for row_lag in range(WIN_ROWS)], axis=1
    )
    seg_rows = jnp.stack(
        [seg_fringe[row_lag : row_lag + row_count] for row_lag in range(WIN_ROWS)], axis=1
    )
    key_part = key_rows[..., :head_width]
    value_part = key_rows[..., head_width:]
    scores = jnp.einsum(
        "rchd,rjkhd->rhcjk", queries, key_part, preferred_element_type=jnp.float32
    ) * head_width ** (-0.5)
    column = jnp.arange(grid_width)
    col_offset = column[None, :] - column[:, None] + WIN_COLS // 2
    inside = (col_offset >= 0) & (col_offset < WIN_COLS)
    bias_table = bias_layer[:, :, jnp.clip(col_offset, 0, WIN_COLS - 1)]
    scores = scores + jnp.transpose(bias_table, (0, 2, 1, 3))[None]
    same_doc = seg_rows[:, None, None, :, :] == seg_own[:, None, :, None, None]
    allowed = same_doc & inside[None, None, :, None, :]
    scores = jnp.where(allowed, scores, -1e30)
    flat = scores.reshape(row_count, head_count, grid_width, WIN_ROWS * grid_width)
    attn_probs = jax.nn.softmax(flat, axis=-1).astype(jnp.bfloat16)
    attn_probs = attn_probs.reshape(row_count, head_count, grid_width, WIN_ROWS, grid_width)
    mixed_heads = jnp.einsum(
        "rhcjk,rjkhd->rchd", attn_probs, value_part, preferred_element_type=jnp.float32
    )
    return mixed_heads.astype(jnp.bfloat16)


def local(tokens, norm_gain, w_query, w_key, w_value, w_out, offset_bias, documents):
    token_count = tokens.shape[0]
    row_count = token_count // GRID_W
    reach_rows = WIN_ROWS // 2
    head_count = offset_bias.shape[1]
    seg_own = (documents + 1).reshape(row_count, GRID_W)
    seg_fringe = with_halo(seg_own, (("sp", 0),), reach_rows, False)
    collected = gather_together((w_query, w_key, w_value, w_out), "sp", (1, 1, 1, 2))
    stream = tokens
    for layer_index in range(LAYERS):
        gathered = whole_of(stream, ("tp_0", "tp_1"), (0, 1), 1)
        normed = rms_rows(gathered, norm_gain[layer_index])
        query_raw = jnp.dot(normed, collected[0][layer_index], preferred_element_type=jnp.float32)
        key_raw = jnp.dot(normed, collected[1][layer_index], preferred_element_type=jnp.float32)
        value_raw = jnp.dot(normed, collected[2][layer_index], preferred_element_type=jnp.float32)
        query_heads = head_norm(
            query_raw.astype(jnp.bfloat16).reshape(row_count, GRID_W, head_count, HEAD_DIM)
        )
        key_heads = head_norm(
            key_raw.astype(jnp.bfloat16).reshape(row_count, GRID_W, head_count, HEAD_DIM)
        )
        value_heads = value_raw.astype(jnp.bfloat16).reshape(
            row_count, GRID_W, head_count, HEAD_DIM
        )
        key_value = jnp.concatenate([key_heads, value_heads], axis=-1)
        fringe = with_halo(key_value, (("sp", 0),), reach_rows, False)
        attended = attend(query_heads, fringe, seg_own, seg_fringe, offset_bias[layer_index])
        attended = attended.reshape(token_count, head_count * HEAD_DIM)
        partial_sums = jnp.dot(
            attended, collected[3][layer_index], preferred_element_type=jnp.float32
        )
        stream = (
            lax.psum_scatter(partial_sums.astype(jnp.bfloat16), TP, scatter_dimension=1, tiled=True)
            .astype(jnp.float32)
            .astype(jnp.bfloat16)
        )
    return stream


def solution(mesh):
    torus = Mesh(mesh.devices.reshape(mesh.shape["sp"], 4, 2), ("sp", "tp_0", "tp_1"))
    return jax.shard_map(
        local,
        mesh=torus,
        in_specs=(
            P("sp", TP),
            P(),
            P(None, "sp", TP),
            P(None, "sp", TP),
            P(None, "sp", TP),
            P(None, TP, "sp"),
            P(None, TP, None, None),
            P("sp"),
        ),
        out_specs=P("sp", TP),
        check_vma=False,
    )
```

profile of v0, /device:TPU:33, one launch (start us, length us, event | category | flops | bytes accessed | tf_op | source)
XLA Modules:
  0.0 245.7 jit_solution(3143307342069625789)
XLA Ops:
  6.5 0.9 copy.207
  7.6 1.6 pad_maximum_fusion
  10.0 3.1 %collective-permute-start.2 = (s32[4,32]{1,0:T(4,128)S(1)}, s32[4,32]{1,0:T(4,128)S(1)}, u32[]{:S(2)}, u32[]{:S(2)}) collective-permute-start(s32[4,32]{1,0:T(4,128)S(1)} %reshape.364), channel_id=1, source_target_pairs={{0,8},{8,16},{16,24},{24,32},{32,40},{40,48},{48,56},{56,64},{64,7... | collective-permute-start | bytes 1544 | tf_op jit(solution)/shard_map/ppermute | solution.py:25
  13.1 4.3 %collective-permute-start.3 = (s32[4,32]{1,0:T(4,128)S(1)}, s32[4,32]{1,0:T(4,128)S(1)}, u32[]{:S(2)}, u32[]{:S(2)}) collective-permute-start(s32[4,32]{1,0:T(4,128)S(1)} %reshape.364), channel_id=1, source_target_pairs={{8,0},{16,8},{24,16},{32,24},{40,32},{48,40},{56,48},{64,56},{72,6... | collective-permute-start | bytes 1544 | tf_op jit(solution)/shard_map/ppermute | solution.py:26
  17.4 9.8 %all-gather = bf16[512,128]{1,0:T(8,128)(2,1)S(1)} all-gather(bf16[128,128]{1,0:T(8,128)(2,1)} %param.8), channel_id=2, replica_groups=mesh['sp'=16,'tp_0'=4,'tp_1'=2] {'tp_0'}, dimensions={0}, use_global_device_ids=true | all-gather | bytes 163840 | tf_op jit(solution)/shard_map/all_gather | solution.py:50
  27.2 5.7 %all_gather.25 = bf16[8,128,128]{2,1,0:T(8,128)(2,1)S(1)} all-gather(bf16[4,128,128]{2,1,0:T(8,128)(2,1)S(1)} %bitcast.377), channel_id=1, replica_groups=mesh['sp'=16,'tp_0'=4,'tp_1'=2] {'tp_1'}, dimensions={0}, use_global_device_ids=true | all-gather | bytes 393216 | tf_op jit(solution)/shard_map/all_gather | solution.py:50
  35.0 3.5 %gather_fusion = f32[1024,2,8]{2,1,0:T(2,128)S(1)} fusion(f32[2,8,16]{1,0,2:T(2,128)S(1)} %bitcast.325, s32[1024]{0:T(1024)S(1)} %broadcast_clamp_fusion), kind=kCustom, calls=%fused_computation | custom fusion | bytes 135168 | tf_op jit(solution)/shard_map/gather | solution.py:89
  38.5 1.3 copy.224
  40.2 17.0 %all-gather.6.cloned.1.call-done = bf16[1572864]{0:T(1024)(128)(2,1)} async-done(((bf16[98304]{0:T(1024)(128)(2,1)}), bf16[1572864]{0:T(1024)(128)(2,1)}) %all-gather.6.cloned.1.call-update) | async-done | bytes 3145744 | tf_op jit(solution)/shard_map/all_gather | solution.py:39
  57.3 2.8 %reshape.409 = bf16[16,98304]{1,0:T(8,128)(2,1)S(1)} reshape(bf16[1572864]{0:T(1024)(128)(2,1)} %all-gather.6.cloned.1.call-done) | data formatting | bytes 6291456 | tf_op jit(solution)/shard_map/all_gather | solution.py:39
  60.0 1.5 fusion.69
  65.4 1.6 pad_maximum_fusion.4
  67.0 2.2 collective-permute-start
  69.3 5.1 %collective-permute-start.1 = (bf16[4,32,2,128]{3,1,2,0:T(8,128)(2,1)}, bf16[4,32,2,128]{3,1,2,0:T(8,128)(2,1)}, u32[]{:S(2)}, u32[]{:S(2)}) collective-permute-start(bf16[4,32,2,128]{3,1,2,0:T(8,128)(2,1)} %pad_maximum_fusion.4), channel_id=1, source_target_pairs={{8,0},{16,8},{24,16},{32,24},{40,32},{48,40},{56,48},{64,56},{72,6... | collective-permute-start | bytes 196616 | tf_op jit(solution)/shard_map/ppermute | solution.py:26
  76.1 1.7 reshape.367
  77.9 0.9 fusion.70
  79.0 1.3 copy.227
  81.2 1.0 pad_maximum_fusion.1
  85.9 3.5 %gather_fusion.1 = f32[1024,2,8]{2,1,0:T(2,128)S(1)} fusion(f32[2,8,16]{1,0,2:T(2,128)S(1)} %bitcast.326, s32[1024]{0:T(1024)S(1)} %broadcast_clamp_fusion), kind=kCustom, calls=%fused_computation.1 | custom fusion | bytes 135168 | tf_op jit(solution)/shard_map/gather | solution.py:89
  90.4 23.9 %reduce-scatter.10.cloned.1.call-done = bf16[128,128]{1,0:T(8,128)(2,1)} async-done(((bf16[1024,128]{1,0:T(8,128)(2,1)}), bf16[128,128]{1,0:T(8,128)(2,1)}) %reduce-scatter.10.cloned.1.call-update) | async-done | bytes 32784
  115.1 10.1 %all-gather.2 = bf16[512,128]{1,0:T(8,128)(2,1)S(1)} all-gather(bf16[128,128]{1,0:T(8,128)(2,1)S(1)} %copy.277), channel_id=4, replica_groups=mesh['sp'=16,'tp_0'=4,'tp_1'=2] {'tp_0'}, dimensions={0}, use_global_device_ids=true | all-gather | bytes 163840 | tf_op jit(solution)/shard_map/all_gather | solution.py:50
  125.2 6.8 %all_gather.29 = bf16[8,128,128]{2,1,0:T(8,128)(2,1)S(1)} all-gather(bf16[4,128,128]{2,1,0:T(8,128)(2,1)S(1)} %bitcast.375), channel_id=1, replica_groups=mesh['sp'=16,'tp_0'=4,'tp_1'=2] {'tp_1'}, dimensions={0}, use_global_device_ids=true | all-gather | bytes 393216 | tf_op jit(solution)/shard_map/all_gather | solution.py:50
  134.0 3.2 %collective-permute-start.4 = (bf16[4,32,2,128]{3,1,2,0:T(8,128)(2,1)S(1)}, bf16[4,32,2,128]{3,1,2,0:T(8,128)(2,1)S(1)}, u32[]{:S(2)}, u32[]{:S(2)}) collective-permute-start(bf16[4,32,2,128]{3,1,2,0:T(8,128)(2,1)S(1)} %pad_maximum_fusion.5), channel_id=1, source_target_pairs={{0,8},{8,16},{16,24},{24,32},{32,40},{40,48},{48,56},{56,64},{64,7... | collective-permute-start | bytes 196616 | tf_op jit(solution)/shard_map/ppermute | solution.py:25
  137.1 4.4 %collective-permute-start.5 = (bf16[4,32,2,128]{3,1,2,0:T(8,128)(2,1)S(1)}, bf16[4,32,2,128]{3,1,2,0:T(8,128)(2,1)S(1)}, u32[]{:S(2)}, u32[]{:S(2)}) collective-permute-start(bf16[4,32,2,128]{3,1,2,0:T(8,128)(2,1)S(1)} %pad_maximum_fusion.5), channel_id=1, source_target_pairs={{8,0},{16,8},{24,16},{32,24},{40,32},{48,40},{56,48},{64,56},{72,6... | collective-permute-start | bytes 196616 | tf_op jit(solution)/shard_map/ppermute | solution.py:26
  145.7 3.5 %gather_fusion.2 = f32[1024,2,8]{2,1,0:T(2,128)S(1)} fusion(f32[2,8,16]{1,0,2:T(2,128)S(1)} %bitcast.324, s32[1024]{0:T(1024)S(1)} %broadcast_clamp_fusion), kind=kCustom, calls=%fused_computation.2 | custom fusion | bytes 135168 | tf_op jit(solution)/shard_map/gather | solution.py:89
  150.2 25.9 %reduce-scatter.12.cloned.1.call-done = bf16[128,128]{1,0:T(8,128)(2,1)} async-done(((bf16[1024,128]{1,0:T(8,128)(2,1)}), bf16[128,128]{1,0:T(8,128)(2,1)}) %reduce-scatter.12.cloned.1.call-update) | async-done | bytes 32784
  176.9 10.1 %all-gather.3 = bf16[512,128]{1,0:T(8,128)(2,1)S(1)} all-gather(bf16[128,128]{1,0:T(8,128)(2,1)S(1)} %copy.279), channel_id=5, replica_groups=mesh['sp'=16,'tp_0'=4,'tp_1'=2] {'tp_0'}, dimensions={0}, use_global_device_ids=true | all-gather | bytes 163840 | tf_op jit(solution)/shard_map/all_gather | solution.py:50
  187.0 6.8 %all_gather.31 = bf16[8,128,128]{2,1,0:T(8,128)(2,1)S(1)} all-gather(bf16[4,128,128]{2,1,0:T(8,128)(2,1)S(1)} %bitcast.376), channel_id=1, replica_groups=mesh['sp'=16,'tp_0'=4,'tp_1'=2] {'tp_1'}, dimensions={0}, use_global_device_ids=true | all-gather | bytes 393216 | tf_op jit(solution)/shard_map/all_gather | solution.py:50
  195.7 3.2 %collective-permute-start.6 = (bf16[4,32,2,128]{3,1,2,0:T(8,128)(2,1)S(1)}, bf16[4,32,2,128]{3,1,2,0:T(8,128)(2,1)S(1)}, u32[]{:S(2)}, u32[]{:S(2)}) collective-permute-start(bf16[4,32,2,128]{3,1,2,0:T(8,128)(2,1)S(1)} %pad_maximum_fusion.6), channel_id=1, source_target_pairs={{0,8},{8,16},{16,24},{24,32},{32,40},{40,48},{48,56},{56,64},{64,7... | collective-permute-start | bytes 196616 | tf_op jit(solution)/shard_map/ppermute | solution.py:25
  198.9 4.2 %collective-permute-start.7 = (bf16[4,32,2,128]{3,1,2,0:T(8,128)(2,1)S(1)}, bf16[4,32,2,128]{3,1,2,0:T(8,128)(2,1)S(1)}, u32[]{:S(2)}, u32[]{:S(2)}) collective-permute-start(bf16[4,32,2,128]{3,1,2,0:T(8,128)(2,1)S(1)} %pad_maximum_fusion.6), channel_id=1, source_target_pairs={{8,0},{16,8},{24,16},{32,24},{40,32},{48,40},{56,48},{64,56},{72,6... | collective-permute-start | bytes 196616 | tf_op jit(solution)/shard_map/ppermute | solution.py:26
  207.2 30.5 %reduce-scatter.14.cloned.1.call-done = bf16[128,128]{1,0:T(8,128)(2,1)} async-done(((bf16[1024,128]{1,0:T(8,128)(2,1)}), bf16[128,128]{1,0:T(8,128)(2,1)}) %reduce-scatter.14.cloned.1.call-update) | async-done | bytes 32784
  237.7 1.5 copy.281
  (195 shorter events, 28.5 us)
Async XLA Ops:
  6.5 26.7 %copy-start.16 = (f32[3,1024]{1,0:T(4,128)S(1)}, f32[3,1024]{1,0:T(4,128)}, u32[]{:S(2)}) copy-start(f32[3,1024]{1,0:T(4,128)} %param.9) | copy-start | bytes 36868
  6.5 27.3 %copy-start.14 = (f32[3,2,8,16]{3,2,1,0:T(8,128)S(1)}, f32[3,2,8,16]{3,2,1,0:T(8,128)}, u32[]{:S(2)}) copy-start(f32[3,2,8,16]{3,2,1,0:T(8,128)} %param.14) | copy-start | bytes 9220
  6.5 50.7 %all-gather.6.cloned.1.call-start = ((), (), s32[]{:S(2)}) async-start(), calls=%async_computation.3 | async-start | bytes 3342336 | tf_op jit(solution)/shard_map/all_gather | solution.py:39
  9.2 105.1 %reduce-scatter.10.cloned.1.call-start = ((), (), s32[]{:S(2)}) async-start(), calls=%async_computation.4 | async-start | bytes 294912
  10.0 29.9 %collective-permute-start.2 = (s32[4,32]{1,0:T(4,128)S(1)}, s32[4,32]{1,0:T(4,128)S(1)}, u32[]{:S(2)}, u32[]{:S(2)}) collective-permute-start(s32[4,32]{1,0:T(4,128)S(1)} %reshape.364), channel_id=1, source_target_pairs={{0,8},{8,16},{16,24},{24,32},{32,40},{40,48},{48,56},{56,64},{64,7... | collective-permute-start | bytes 1544 | tf_op jit(solution)/shard_map/ppermute | solution.py:25
  13.1 26.8 %collective-permute-start.3 = (s32[4,32]{1,0:T(4,128)S(1)}, s32[4,32]{1,0:T(4,128)S(1)}, u32[]{:S(2)}, u32[]{:S(2)}) collective-permute-start(s32[4,32]{1,0:T(4,128)S(1)} %reshape.364), channel_id=1, source_target_pairs={{8,0},{16,8},{24,16},{32,24},{40,32},{48,40},{56,48},{64,56},{72,6... | collective-permute-start | bytes 1544 | tf_op jit(solution)/shard_map/ppermute | solution.py:26
  61.5 2.5 %copy-start.1 = (bf16[2,8,192,128]{3,1,2,0:T(8,128)(2,1)S(1)}, bf16[2,8,192,128]{3,1,2,0:T(8,128)(2,1)}, u32[]{:S(2)}) copy-start(bf16[2,8,192,128]{3,1,2,0:T(8,128)(2,1)} %get-tuple-element.7) | copy-start | bytes 2359300
  62.5 11.9 %copy-start = (bf16[2,8,192,128]{3,1,2,0:T(8,128)(2,1)S(1)}, bf16[2,8,192,128]{3,1,2,0:T(8,128)(2,1)}, u32[]{:S(2)}) copy-start(bf16[2,8,192,128]{3,1,2,0:T(8,128)(2,1)} %get-tuple-element.6) | copy-start | bytes 2359300
  64.1 12.0 %copy-start.2 = (bf16[16,24576]{1,0:T(8,128)(2,1)S(1)}, bf16[16,24576]{1,0:T(8,128)(2,1)}, u32[]{:S(2)}) copy-start(bf16[16,24576]{1,0:T(8,128)(2,1)} %get-tuple-element.5) | copy-start | bytes 2359300
  65.4 9.0 %copy-start.11 = (bf16[4,32,2,64]{3,1,2,0:T(8,128)(2,1)}, bf16[4,32,2,64]{3,1,2,0:T(8,128)(2,1)S(1)}, u32[]{:S(2)}) copy-start(bf16[4,32,2,64]{3,1,2,0:T(8,128)(2,1)S(1)} %copy.211) | copy-start | bytes 98308
  67.0 13.3 %collective-permute-start = (bf16[4,32,2,128]{3,1,2,0:T(8,128)(2,1)}, bf16[4,32,2,128]{3,1,2,0:T(8,128)(2,1)}, u32[]{:S(2)}, u32[]{:S(2)}) collective-permute-start(bf16[4,32,2,128]{3,1,2,0:T(8,128)(2,1)} %pad_maximum_fusion.4), channel_id=1, source_target_pairs={{0,8},{8,16},{16,24},{24,32},{32,40},{40,48},{48,56},{56,64},{64,7... | collective-permute-start | bytes 196616 | tf_op jit(solution)/shard_map/ppermute | solution.py:25
  69.3 11.9 %collective-permute-start.1 = (bf16[4,32,2,128]{3,1,2,0:T(8,128)(2,1)}, bf16[4,32,2,128]{3,1,2,0:T(8,128)(2,1)}, u32[]{:S(2)}, u32[]{:S(2)}) collective-permute-start(bf16[4,32,2,128]{3,1,2,0:T(8,128)(2,1)} %pad_maximum_fusion.4), channel_id=1, source_target_pairs={{8,0},{16,8},{24,16},{32,24},{40,32},{48,40},{56,48},{64,56},{72,6... | collective-permute-start | bytes 196616 | tf_op jit(solution)/shard_map/ppermute | solution.py:26
  76.1 5.0 %copy-start.10 = (bf16[4,32,2,64]{3,1,2,0:T(8,128)(2,1)S(1)}, bf16[4,32,2,64]{3,1,2,0:T(8,128)(2,1)}, u32[]{:S(2)}) copy-start(bf16[4,32,2,64]{3,1,2,0:T(8,128)(2,1)} %fusion.35) | copy-start | bytes 98308
  76.1 5.0 %copy-start.12 = (bf16[4,32,2,64]{3,1,2,0:T(8,128)(2,1)S(1)}, bf16[4,32,2,64]{3,1,2,0:T(8,128)(2,1)}, u32[]{:S(2)}) copy-start(bf16[4,32,2,64]{3,1,2,0:T(8,128)(2,1)} %copy-done.11) | copy-start | bytes 98308
  77.9 5.3 %copy-start.3 = (f32[32,32,2,8]{0,1,3,2:T(8,128)S(1)}, f32[32,32,2,8]{0,1,3,2:T(8,128)}, u32[]{:S(2)}) copy-start(f32[32,32,2,8]{0,1,3,2:T(8,128)} %copy.224) | copy-start | bytes 196612
  83.8 1.9 copy-start.13
  84.9 47.4 %copy-start.15 = (f32[1,1024]{1,0:T(1,128)S(1)}, f32[1,1024]{1,0:T(1,128)}, u32[]{:S(2)}) copy-start(f32[1,1024]{1,0:T(1,128)} %get-tuple-element.32) | copy-start | bytes 12292
  85.7 90.3 %reduce-scatter.12.cloned.1.call-start = ((), (), s32[]{:S(2)}) async-start(), calls=%async_computation.5 | async-start | bytes 294912
  89.4 43.2 %copy-start.7 = (bf16[1,16,64,128]{3,2,0,1:T(8,128)(2,1)S(1)}, bf16[1,16,64,128]{3,2,0,1:T(8,128)(2,1)}, u32[]{:S(2)}) copy-start(bf16[1,16,64,128]{3,2,0,1:T(8,128)(2,1)} %get-tuple-element.16) | copy-start | bytes 786436
  90.1 43.3 %copy-start.8 = (bf16[1,16,64,128]{3,2,0,1:T(8,128)(2,1)S(1)}, bf16[1,16,64,128]{3,2,0,1:T(8,128)(2,1)}, u32[]{:S(2)}) copy-start(bf16[1,16,64,128]{3,2,0,1:T(8,128)(2,1)} %get-tuple-element.19) | copy-start | bytes 786436
  125.2 16.3 %copy-start.9 = (bf16[1,16,64,128]{3,2,0,1:T(8,128)(2,1)S(1)}, bf16[1,16,64,128]{3,2,0,1:T(8,128)(2,1)}, u32[]{:S(2)}) copy-start(bf16[1,16,64,128]{3,2,0,1:T(8,128)(2,1)} %get-tuple-element.13) | copy-start | bytes 786436
  134.0 8.5 %collective-permute-start.4 = (bf16[4,32,2,128]{3,1,2,0:T(8,128)(2,1)S(1)}, bf16[4,32,2,128]{3,1,2,0:T(8,128)(2,1)S(1)}, u32[]{:S(2)}, u32[]{:S(2)}) collective-permute-start(bf16[4,32,2,128]{3,1,2,0:T(8,128)(2,1)S(1)} %pad_maximum_fusion.5), channel_id=1, source_target_pairs={{0,8},{8,16},{16,24},{24,32},{32,40},{40,48},{48,56},{56,64},{64,7... | collective-permute-start | bytes 196616 | tf_op jit(solution)/shard_map/ppermute | solution.py:25
  137.1 5.6 %collective-permute-start.5 = (bf16[4,32,2,128]{3,1,2,0:T(8,128)(2,1)S(1)}, bf16[4,32,2,128]{3,1,2,0:T(8,128)(2,1)S(1)}, u32[]{:S(2)}, u32[]{:S(2)}) collective-permute-start(bf16[4,32,2,128]{3,1,2,0:T(8,128)(2,1)S(1)} %pad_maximum_fusion.5), channel_id=1, source_target_pairs={{8,0},{16,8},{24,16},{32,24},{40,32},{48,40},{56,48},{64,56},{72,6... | collective-permute-start | bytes 196616 | tf_op jit(solution)/shard_map/ppermute | solution.py:26
  145.5 92.2 %reduce-scatter.14.cloned.1.call-start = ((), (), s32[]{:S(2)}) async-start(), calls=%async_computation.6 | async-start | bytes 294912
  149.2 45.1 %copy-start.4 = (bf16[1,16,64,128]{3,2,0,1:T(8,128)(2,1)S(1)}, bf16[1,16,64,128]{3,2,0,1:T(8,128)(2,1)}, u32[]{:S(2)}) copy-start(bf16[1,16,64,128]{3,2,0,1:T(8,128)(2,1)} %get-tuple-element.15) | copy-start | bytes 786436
  149.9 45.3 %copy-start.5 = (bf16[1,16,64,128]{3,2,0,1:T(8,128)(2,1)S(1)}, bf16[1,16,64,128]{3,2,0,1:T(8,128)(2,1)}, u32[]{:S(2)}) copy-start(bf16[1,16,64,128]{3,2,0,1:T(8,128)(2,1)} %get-tuple-element.18) | copy-start | bytes 786436
  187.0 16.1 %copy-start.6 = (bf16[1,16,64,128]{3,2,0,1:T(8,128)(2,1)S(1)}, bf16[1,16,64,128]{3,2,0,1:T(8,128)(2,1)}, u32[]{:S(2)}) copy-start(bf16[1,16,64,128]{3,2,0,1:T(8,128)(2,1)} %get-tuple-element.12) | copy-start | bytes 786436
  195.7 8.3 %collective-permute-start.6 = (bf16[4,32,2,128]{3,1,2,0:T(8,128)(2,1)S(1)}, bf16[4,32,2,128]{3,1,2,0:T(8,128)(2,1)S(1)}, u32[]{:S(2)}, u32[]{:S(2)}) collective-permute-start(bf16[4,32,2,128]{3,1,2,0:T(8,128)(2,1)S(1)} %pad_maximum_fusion.6), channel_id=1, source_target_pairs={{0,8},{8,16},{16,24},{24,32},{32,40},{40,48},{48,56},{56,64},{64,7... | collective-permute-start | bytes 196616 | tf_op jit(solution)/shard_map/ppermute | solution.py:25
  198.9 5.5 %collective-permute-start.7 = (bf16[4,32,2,128]{3,1,2,0:T(8,128)(2,1)S(1)}, bf16[4,32,2,128]{3,1,2,0:T(8,128)(2,1)S(1)}, u32[]{:S(2)}, u32[]{:S(2)}) collective-permute-start(bf16[4,32,2,128]{3,1,2,0:T(8,128)(2,1)S(1)} %pad_maximum_fusion.6), channel_id=1, source_target_pairs={{8,0},{16,8},{24,16},{32,24},{40,32},{48,40},{56,48},{64,56},{72,6... | collective-permute-start | bytes 196616 | tf_op jit(solution)/shard_map/ppermute | solution.py:26
Sparse Core Ops, SparseCore 0:
  9.5 47.7 all-gather.5
  85.8 28.3 reduce-scatter.9
  145.7 30.3 reduce-scatter.11
  207.4 30.3 reduce-scatter.13
where the time goes:
time: 250 us; the launch traced here: 246 us
  waiting for transfers between devices  98 us (39%)
  blocking collectives  49.4 us (20%)
  local copies, waits for them, and re-layouts  38.1 us (15%)
  starting transfers between devices  29.9 us (12%)
  between operations  14.2 us (6%)
  other arithmetic  10.2 us (4%)
  matrix products  6.03 us (2%)
    unnamed x7, waiting for transfers between devices  80.3 us
    all_gather x6, blocking collectives, stacked_from(): blocks = lax.all_gather(blocks, axes[k], axis=0, tiled=True)  49.4 us
    ppermute x4, starting transfers between devices, with_halo(): after = lax.ppermute(leading, axis, down)  18.1 us
    all_gather x1, waiting for transfers between devices, gather_together(): lines, at, done = (lax.all_gather(ravelled, axis), 0, [])  17 us
    gather x6, local copies, waits for them, and re-layouts, attend(): bias_table = bias_layer[:, :, jnp.clip(col_offset, 0, WIN_COLS - 1)]  13.4 us
    ppermute x4, starting transfers between devices, with_halo(): before = lax.ppermute(last, axis, up)  11.7 us
    unnamed x75, local copies, waits for them, and re-layouts  9.4 us
  transfers between devices with their start and end apart: 12, of which 6 were waited for; matrix products, arithmetic and copies ran while one was open for 10% of the time, Pallas kernels for 0%

commit v1 on v0

v1 whole, which is shorter than its diff:
```python
import jax
import jax.numpy as jnp
from jax import lax
from jax.experimental import pallas as pl
from jax.experimental.pallas import tpu as pltpu
from jax.sharding import Mesh
from jax.sharding import PartitionSpec as P

HEAD_DIM = 64
WIN_ROWS = 8
WIN_COLS = 16
LAYERS = 3
GRID_W = 32
SP = ("z", "x")
TP = ("y", "c")
EPS = 1e-06
F32 = jnp.float32
BF16 = jnp.bfloat16
NT = (((1,), (1,)), ((), ()))


def turn(k):
    return [(i, (i + k) % 4) for i in range(4)]


def spread(a, axis):
    return [lax.ppermute(a, axis, turn(k)) for k in (1, 3, 2)]


def in_order(a, three):
    return [a, three[0], three[2], three[1]]


def swap(a):
    return lax.ppermute(a, "c", [(0, 1), (1, 0)])


def from_before(a):
    return lax.ppermute(a, SP, [(i, i + 1) for i in range(15)])


def from_after(a):
    return lax.ppermute(a, SP, [(i + 1, i) for i in range(15)])


def behind(axis, k):
    return (lax.axis_index(axis) + (4 - k)) & 3


def ahead(axis, k):
    return (lax.axis_index(axis) + k) & 3


def call(body, outs, *args, scratch=(), name=None):
    return pl.pallas_call(
        body,
        out_shape=outs,
        scratch_shapes=list(scratch),
        name=name,
        compiler_params=pltpu.CompilerParams(vmem_limit_bytes=24 * 1024 * 1024),
    )(*args)


def shaped(*shape, dtype=BF16):
    return jax.ShapeDtypeStruct(shape, dtype)


def pack_body(wq, wk, wv, wo, tokens, docs, first, rest, payload):
    for layer in range(LAYERS):
        into = first if layer == 0 else rest.at[layer - 1]
        into[:, 0:128] = wq[layer]
        into[:, 128:256] = wk[layer]
        into[:, 256:384] = wv[layer]
        into[:, 384:512] = wo[layer].astype(F32).T.astype(BF16)
    payload[0:128, :] = tokens[...]
    payload[128:144, :] = jnp.broadcast_to((docs[...] + 1).astype(F32).astype(BF16), (16, 128))


def table_body(rows, before, own, after, table):
    own_docs = own[128:144, :].astype(F32)[0:1]
    query_docs = jnp.broadcast_to(own_docs, (128, 128)).T
    key_docs = jnp.concatenate(
        [before[128:144, :].astype(F32)[0:1], own_docs, after[128:144, :].astype(F32)[0:1]], axis=1
    )
    same = jnp.concatenate([query_docs] * 3, axis=1) == key_docs
    r = lax.broadcasted_iota(jnp.int32, (128, 384), 0)
    m = lax.broadcasted_iota(jnp.int32, (128, 384), 1)
    lag = (m >> 5) - (r >> 5)
    off = (m & 31) - (r & 31) + WIN_COLS // 2
    allowed = same & (lag >= 0) & (lag < WIN_ROWS) & (off >= 0) & (off < WIN_COLS)
    for n in range(2 * LAYERS):
        line = jnp.broadcast_to(rows[n : n + 1, :], (GRID_W, 256))
        line = pltpu.roll(line, 256 - WIN_COLS // 2, 1, stride=1, stride_axis=0)
        line = jnp.concatenate([line, jnp.zeros((GRID_W, 128), F32)], axis=1)
        block = jnp.concatenate(
            [line] + [pltpu.roll(line, 32 * q, 1) for q in range(1, 4)], axis=0
        )
        table[n] = jnp.where(allowed, block, -1e30)


def normed_heads(raw):
    values = raw.astype(BF16).astype(F32)
    squares = values * values
    low = lax.broadcasted_iota(jnp.int32, values.shape, 1) < HEAD_DIM
    first = jnp.sum(jnp.where(low, squares, 0.0), axis=1, keepdims=True)
    second = jnp.sum(jnp.where(low, 0.0, squares), axis=1, keepdims=True)
    scale = jnp.where(
        low,
        lax.rsqrt(first * (1.0 / HEAD_DIM) + EPS),
        lax.rsqrt(second * (1.0 / HEAD_DIM) + EPS),
    )
    return (values * scale).astype(BF16)


def fill_weights(parts, weights, lo, hi):
    for kz in range(4):
        for kx in range(4):
            block = behind("z", kz) * 4 + behind("x", kx)
            weights[pl.ds(pl.multiple_of(block * 64, 64), 64), :] = parts[kz][kx, :, lo:hi]


def finish_heads(acc, q, kv):
    q[...] = normed_heads(acc[:, 0:128])
    kv[:, 0:128] = normed_heads(acc[:, 128:256])
    kv[:, 128:256] = acc[:, 256:384].astype(BF16)


def heads_first_body(own, partner, gain, w0, w1, w2, w3, q, kv, weights):
    fill_weights((w0, w1, w2, w3), weights, 0, 384)
    c = lax.axis_index("c")
    total = jnp.zeros((384, 128), F32)
    for k in range(4):
        for part in (own, partner):
            values = part[k].astype(F32)
            total = total + values * values
    scale = lax.rsqrt(jnp.sum(total, axis=1, keepdims=True) * (1.0 / 1024) + EPS)
    acc = jnp.zeros((384, 384), F32)
    for k in range(4):
        for part, core in ((own, c), (partner, 1 - c)):
            block = behind("y", k) * 2 + core
            gains = gain[pl.ds(block, 1), :]
            normed = (part[k].astype(F32) * scale * gains).astype(BF16)
            rows = weights[pl.ds(pl.multiple_of(block * 128, 128), 128), :]
            acc = acc + jnp.dot(normed, rows, preferred_element_type=F32)
    q[...] = normed_heads(acc[128:256, 0:128])
    kv[:, 0:128] = normed_heads(acc[:, 128:256])
    kv[:, 128:256] = acc[:, 256:384].astype(BF16)


def heads_pieces_body(x0, x1, x2, x3, gain, w0, w1, w2, w3, q, kv, weights):
    fill_weights((w0, w1, w2, w3), weights, 0, 384)
    pieces = [x[...].astype(F32) for x in (x0, x1, x2, x3)]
    total = sum(p * p for p in pieces)
    scale = lax.rsqrt(jnp.sum(total, axis=1, keepdims=True) * (1.0 / 1024) + EPS)
    acc = jnp.zeros((128, 384), F32)
    for k in range(4):
        block = behind("y", k)
        normed = (pieces[k] * scale * gain[block]).astype(BF16)
        rows = weights[pl.ds(pl.multiple_of(block * 256, 256), 256), :]
        acc = acc + jnp.dot(normed, rows, preferred_element_type=F32)
    finish_heads(acc, q, kv)


def heads_whole_body(mine, theirs, gain, w0, w1, w2, w3, q, kv, weights):
    fill_weights((w0, w1, w2, w3), weights, 0, 384)
    stream = (mine[...].astype(F32) + theirs[...].astype(F32)).astype(BF16).astype(F32)
    scale = lax.rsqrt(jnp.sum(stream * stream, axis=1, keepdims=True) * (1.0 / 1024) + EPS)
    normed = (stream * scale * gain[...]).astype(BF16)
    acc = jnp.dot(normed, weights[...], preferred_element_type=F32)
    finish_heads(acc, q, kv)


def attend(q, keys_values, table):
    queries = q[...]
    low = lax.broadcasted_iota(jnp.int32, (128, 128), 1) < HEAD_DIM
    results = []
    for h in range(2):
        mine = jnp.where(low if h == 0 else ~low, queries, jnp.zeros_like(queries))
        weights, total = [], 0.0
        for b, (keys, _) in enumerate(keys_values):
            scores = lax.dot_general(mine, keys, NT, preferred_element_type=F32)
            scores = scores * HEAD_DIM**-0.5 + table[h, :, b * 128 : (b + 1) * 128]
            grown = jnp.exp(scores)
            weights.append(grown)
            total = total + jnp.sum(grown, axis=1, keepdims=True)
        share = 1.0 / total
        out = 0.0
        for grown, (_, values) in zip(weights, keys_values):
            probs = (grown * share).astype(BF16)
            out = out + jnp.dot(probs, values, preferred_element_type=F32)
        results.append(out)
    return jnp.where(low, results[0], results[1]).astype(BF16)


def attend_scatter_body(q, before, own, after, table, w0, w1, w2, w3, kept, s1, s2, s3, weights):
    fill_weights((w0, w1, w2, w3), weights, 384, 512)
    parts = [(p[:, 0:128], p[:, 128:256]) for p in (before, own, after)]
    attended = attend(q, parts, table)
    for k, into in enumerate((kept, s1, s2, s3)):
        rows = weights[pl.ds(pl.multiple_of(ahead("y", k) * 256, 256), 256), :]
        share = lax.dot_general(attended, rows, NT, preferred_element_type=F32)
        into[...] = share.astype(into.dtype)


def attend_first_body(q, kv, table, *rest):
    attend_scatter_body(q, kv.at[0:128], kv.at[128:256], kv.at[256:384], table, *rest)


def attend_body(q, before, own, after, table, out):
    parts = [(p[:, 0:128], p[:, 128:256]) for p in (before, own, after)]
    out[...] = attend(q, parts, table)


def extract_body(w0, w1, w2, w3, out):
    fill_weights((w0, w1, w2, w3), out, 384, 512)


def project_body(a0, a1, a2, a3, w0, w1, w2, w3, out):
    acc = 0.0
    for a, w in ((a0, w0), (a1, w1), (a2, w2), (a3, w3)):
        acc = acc + lax.dot_general(a[...], w[...], NT, preferred_element_type=F32)
    out[...] = acc.astype(BF16)


def sum_body(kept, r1, r2, r3, out):
    out[...] = kept[...] + r1[...].astype(F32) + r2[...].astype(F32) + r3[...].astype(F32)


def pair_sum_body(mine, theirs, out):
    out[...] = (mine[...] + theirs[...]).astype(BF16)


def split_body(kept, r1, r2, r3, mine, theirs):
    c = lax.axis_index("c")
    for into, core in ((mine, c), (theirs, 1 - c)):
        at = pl.ds(pl.multiple_of(core * 128, 128), 128)
        into[...] = (
            kept[:, at] + r1[:, at].astype(F32) + r2[:, at].astype(F32) + r3[:, at].astype(F32)
        )


def scattered(q_and_kv, body, table, weights):
    outs = [shaped(128, 256, dtype=F32)] + [shaped(128, 256)] * 3
    kept, s1, s2, s3 = call(
        body, outs, *q_and_kv, table, *weights,
        scratch=[pltpu.VMEM((1024, 128), BF16)], name="attend_scatter",
    )
    r3 = lax.ppermute(s3, "y", turn(3))
    r1 = lax.ppermute(s1, "y", turn(1))
    r2 = lax.ppermute(s2, "y", turn(2))
    return kept, r1, r2, r3


def local(tokens, norm_gain, w_query, w_key, w_value, w_out, offset_bias, documents):
    first, rest, payload = call(
        pack_body,
        [shaped(64, 512), shaped(2, 64, 512), shaped(144, 128)],
        w_query, w_key, w_value, w_out, tokens, documents.reshape(1, 128), name="pack",
    )
    heads_scratch = [pltpu.VMEM((1024, 384), BF16)]
    first_x = jnp.stack(in_order(first, spread(first, "x")))
    before = from_before(payload)
    after = from_after(payload)
    weights0 = in_order(first_x, spread(first_x, "z"))

    near = jnp.concatenate([before[0:128], tokens, after[0:128]], axis=0)
    near_y = jnp.stack(in_order(near, spread(near, "y")))
    near_partner = swap(near_y)

    rest_x = in_order(rest, spread(rest, "x"))
    layer1_x = jnp.stack([r[0] for r in rest_x])
    layer2_x = jnp.stack([r[1] for r in rest_x])

    rows = jnp.pad(offset_bias, ((0, 0), (0, 0), (0, 0), (0, 16))).reshape(6, 256)
    table = call(
        table_body, shaped(6, 128, 384, dtype=F32), rows, before, payload, after, name="table"
    )

    q, kv = call(
        heads_first_body, [shaped(128, 128), shaped(384, 256)],
        near_y, near_partner, norm_gain[0].reshape(8, 128), *weights0,
        scratch=heads_scratch, name="heads0",
    )
    weights1 = in_order(layer1_x, spread(layer1_x, "z"))
    kept, r1, r2, r3 = scattered((q, kv), attend_first_body, table[0:2], weights0)
    half = call(sum_body, shaped(128, 256, dtype=F32), kept, r1, r2, r3, name="sum0")
    stream = call(pair_sum_body, shaped(128, 256), half, swap(half), name="pair0")
    pieces = in_order(stream, spread(stream, "y"))

    q, kv = call(
        heads_pieces_body, [shaped(128, 128), shaped(128, 256)],
        *pieces, norm_gain[1].reshape(4, 1, 256), *weights1,
        scratch=heads_scratch, name="heads1",
    )
    out1 = call(extract_body, shaped(1024, 128), *weights1, name="extract1")
    out1_y = in_order(out1, spread(out1, "y"))
    weights2 = in_order(layer2_x, spread(layer2_x, "z"))
    attended = call(
        attend_body, shaped(128, 128), q, from_before(kv), kv, from_after(kv), table[2:4],
        name="attend1",
    )
    attended_y = in_order(attended, spread(attended, "y"))
    share = call(project_body, shaped(128, 1024), *attended_y, *out1_y, name="project1")
    q, kv = call(
        heads_whole_body, [shaped(128, 128), shaped(128, 256)],
        share, swap(share), norm_gain[2].reshape(1, 1024), *weights2,
        scratch=heads_scratch, name="heads2",
    )
    kept, r1, r2, r3 = scattered(
        (q, from_before(kv), kv, from_after(kv)), attend_scatter_body, table[4:6], weights2
    )
    mine, theirs = call(
        split_body, [shaped(128, 128, dtype=F32)] * 2, kept, r1, r2, r3, name="split2"
    )
    return call(pair_sum_body, shaped(128, 128), mine, swap(theirs), name="pair2")


def solution(mesh):
    torus = Mesh(mesh.devices.reshape(4, 4, 4, 2), ("z", "x", "y", "c"))
    return jax.shard_map(
        local,
        mesh=torus,
        in_specs=(
            P(SP, TP),
            P(),
            P(None, SP, TP),
            P(None, SP, TP),
            P(None, SP, TP),
            P(None, TP, SP),
            P(None, TP, None, None),
            P(SP),
        ),
        out_specs=P(SP, TP),
        check_vma=False,
    )
```

time: 250 us -> 135 us (0.54)
  the two profiles are of different devices: /device:TPU:33 before, /device:TPU:31 now
where the time goes in v1:
time: 135 us; the launch traced here: 134 us
  starting transfers between devices  81.8 us (61%)
  waiting for transfers between devices  37.8 us (28%)
  Pallas kernels  6.72 us (5%)
  local copies, waits for them, and re-layouts  6.5 us (5%)
    ppermute x27, starting transfers between devices, spread(): return [lax.ppermute(a, axis, turn(k)) for k in (1, 3, 2)]  35 us
    ppermute x4, starting transfers between devices, swap(): return lax.ppermute(a, 'c', [(0, 1), (1, 0)])  21.3 us
    ppermute x27, waiting for transfers between devices, spread(): return [lax.ppermute(a, axis, turn(k)) for k in (1, 3, 2)]  17.3 us
    ppermute x3, starting transfers between devices, from_before(): return lax.ppermute(a, SP, [(i, i + 1) for i in range(15)])  9.69 us
    ppermute x3, waiting for transfers between devices, from_after(): return lax.ppermute(a, SP, [(i + 1, i) for i in range(15)])  8.92 us
    ppermute x3, starting transfers between devices, from_after(): return lax.ppermute(a, SP, [(i + 1, i) for i in range(15)])  7.2 us
    pallas_call x14, Pallas kernels, call(): pl.pallas_call(body, out_shape=outs, scratch_shapes=list(scratch), name=n...  6.72 us
    ppermute x2, starting transfers between devices, scattered(): r1 = lax.ppermute(s1, 'y', turn(1))  6.28 us
  transfers between devices with their start and end apart: 43, of which 15 were waited for; matrix products, arithmetic and copies ran while one was open for 2% of the time, Pallas kernels for 3%

profile of v1, /device:TPU:31, one launch (start us, length us, event | category | flops | bytes accessed | tf_op | source)
XLA Modules:
  0.0 134.1 jit_solution(11951311372699165260)
XLA Ops:
  4.8 3.5 %collective-permute-start = (bf16[144,128]{1,0:T(8,128)(2,1)S(1)}, bf16[144,128]{1,0:T(8,128)(2,1)S(1)}, u32[]{:S(2)}, u32[]{:S(2)}) collective-permute-start(bf16[144,128]{1,0:T(8,128)(2,1)S(1)} %get-tuple-element.24.own), channel_id=1, source_target_pairs={{0,8},{8,16},{16,24},{24,32},{32,40},{40,48},{48,56},{56,64},{64,7... | collective-permute-start | bytes 110600 | tf_op jit(solution)/shard_map/ppermute | solution.py:39
  8.3 1.9 %collective-permute-start.1 = (bf16[144,128]{1,0:T(8,128)(2,1)S(1)}, bf16[144,128]{1,0:T(8,128)(2,1)S(1)}, u32[]{:S(2)}, u32[]{:S(2)}) collective-permute-start(bf16[144,128]{1,0:T(8,128)(2,1)S(1)} %get-tuple-element.24.own), channel_id=1, source_target_pairs={{8,0},{16,8},{24,16},{32,24},{40,32},{48,40},{56,48},{64,56},{72,6... | collective-permute-start | bytes 110600 | tf_op jit(solution)/shard_map/ppermute | solution.py:43
  10.3 2.2 %collective-permute-start.7 = (bf16[64,512]{1,0:T(8,128)(2,1)S(1)}, bf16[64,512]{1,0:T(8,128)(2,1)S(1)}, u32[]{:S(2)}, u32[]{:S(2)}) collective-permute-start(bf16[64,512]{1,0:T(8,128)(2,1)S(1)} %get-tuple-element.25), channel_id=1, source_target_pairs={{0,16},{8,24},{16,0},{24,8},{1,17},{9,25},{17,1},{25,9},{2,18},{10... | collective-permute-start | bytes 196616 | tf_op jit(solution)/shard_map/ppermute | solution.py:27
  14.2 2.7 %collective-permute-start.19 = (bf16[2,64,512]{2,1,0:T(8,128)(2,1)S(1)}, bf16[2,64,512]{2,1,0:T(8,128)(2,1)S(1)}, u32[]{:S(2)}, u32[]{:S(2)}) collective-permute-start(bf16[2,64,512]{2,1,0:T(8,128)(2,1)S(1)} %get-tuple-element.32), channel_id=1, source_target_pairs={{0,8},{8,16},{16,24},{24,0},{1,9},{9,17},{17,25},{25,1},{2,10},{10... | collective-permute-start | bytes 393224 | tf_op jit(solution)/shard_map/ppermute | solution.py:27
  19.4 2.2 %collective-permute-start.3 = (bf16[384,128]{1,0:T(8,128)(2,1)S(1)}, bf16[384,128]{1,0:T(8,128)(2,1)S(1)}, u32[]{:S(2)}, u32[]{:S(2)}) collective-permute-start(bf16[384,128]{1,0:T(8,128)(2,1)S(1)} %get-tuple-element.55), channel_id=1, source_target_pairs={{0,4},{2,6},{4,0},{6,2},{1,5},{3,7},{5,1},{7,3},{8,12},{10,14},{12... | collective-permute-start | bytes 294920 | tf_op jit(solution)/shard_map/ppermute | solution.py:27
  22.3 4.0 %collective-permute-start.10 = (bf16[4,64,512]{2,1,0:T(8,128)(2,1)S(1)}, bf16[4,64,512]{2,1,0:T(8,128)(2,1)S(1)}, u32[]{:S(2)}, u32[]{:S(2)}) collective-permute-start(bf16[4,64,512]{2,1,0:T(8,128)(2,1)S(1)} %pad_maximum_fusion.1.w0.rest_0_), channel_id=1, source_target_pairs={{0,64},{32,96},{64,0},{96,32},{1,65},{33,97},{65,1},{97,33},{2,66}... | collective-permute-start | bytes 786440 | tf_op jit(solution)/shard_map/ppermute | solution.py:27
  27.9 4.7 %collective-permute-start.5 = (bf16[4,384,128]{2,1,0:T(8,128)(2,1)S(1)}, bf16[4,384,128]{2,1,0:T(8,128)(2,1)S(1)}, u32[]{:S(2)}, u32[]{:S(2)}) collective-permute-start(bf16[4,384,128]{2,1,0:T(8,128)(2,1)S(1)} %pad_maximum_fusion.own), channel_id=1, source_target_pairs={{0,1},{1,0},{2,3},{3,2},{4,5},{5,4},{6,7},{7,6},{8,9},{9,8},{10,11... | collective-permute-start | bytes 1179656 | tf_op jit(solution)/shard_map/ppermute | solution.py:35
  33.5 3.3 %collective-permute-start.23 = (bf16[4,64,512]{2,1,0:T(8,128)(2,1)S(1)}, bf16[4,64,512]{2,1,0:T(8,128)(2,1)S(1)}, u32[]{:S(2)}, u32[]{:S(2)}) collective-permute-start(bf16[4,64,512]{2,1,0:T(8,128)(2,1)S(1)} %pad_maximum_fusion.2.w0), channel_id=1, source_target_pairs={{0,64},{32,96},{64,0},{96,32},{1,65},{33,97},{65,1},{97,33},{2,66}... | collective-permute-start | bytes 786440 | tf_op jit(solution)/shard_map/ppermute | solution.py:27
  37.1 3.4 %collective-permute-start.24 = (bf16[4,64,512]{2,1,0:T(8,128)(2,1)S(1)}, bf16[4,64,512]{2,1,0:T(8,128)(2,1)S(1)}, u32[]{:S(2)}, u32[]{:S(2)}) collective-permute-start(bf16[4,64,512]{2,1,0:T(8,128)(2,1)S(1)} %pad_maximum_fusion.2.w0), channel_id=1, source_target_pairs={{0,96},{32,0},{64,32},{96,64},{1,97},{33,1},{65,33},{97,65},{2,98}... | collective-permute-start | bytes 786440 | tf_op jit(solution)/shard_map/ppermute | solution.py:27
  42.6 4.2 %collective-permute-start.12 = (bf16[128,256]{1,0:T(8,128)(2,1)S(1)}, bf16[128,256]{1,0:T(8,128)(2,1)S(1)}, u32[]{:S(2)}, u32[]{:S(2)}) collective-permute-start(bf16[128,256]{1,0:T(8,128)(2,1)S(1)} %get-tuple-element.29), channel_id=1, source_target_pairs={{0,2},{2,4},{4,6},{6,0},{1,3},{3,5},{5,7},{7,1},{8,10},{10,12},{12... | collective-permute-start | bytes 196616 | tf_op jit(solution)/shard_map/ppermute | solution.py:249
  48.6 2.9 %collective-permute-done.13.r2 = bf16[128,256]{1,0:T(8,128)(2,1)S(1)} collective-permute-done((bf16[128,256]{1,0:T(8,128)(2,1)S(1)}, bf16[128,256]{1,0:T(8,128)(2,1)S(1)}, u32[]{:S(2)}, u32[]{:S(2)}) %collective-permute-start.13) | collective-permute-done | bytes 65568 | tf_op jit(solution)/shard_map/ppermute | solution.py:250
  51.4 2.4 %collective-permute-done.14.r3 = bf16[128,256]{1,0:T(8,128)(2,1)S(1)} collective-permute-done((bf16[128,256]{1,0:T(8,128)(2,1)S(1)}, bf16[128,256]{1,0:T(8,128)(2,1)S(1)}, u32[]{:S(2)}, u32[]{:S(2)}) %collective-permute-start.14) | collective-permute-done | bytes 65568 | tf_op jit(solution)/shard_map/ppermute | solution.py:248
  53.8 4.8 %collective-permute-start.15 = (f32[128,256]{1,0:T(8,128)S(1)}, f32[128,256]{1,0:T(8,128)S(1)}, u32[]{:S(2)}, u32[]{:S(2)}) collective-permute-start(f32[128,256]{1,0:T(8,128)S(1)} %sum0.1.mine), channel_id=1, source_target_pairs={{0,1},{1,0},{2,3},{3,2},{4,5},{5,4},{6,7},{7,6},{8,9},{9,8},{10,11... | collective-permute-start | bytes 393224 | tf_op jit(solution)/shard_map/ppermute | solution.py:35
  58.8 1.8 %collective-permute-start.30 = (bf16[1024,128]{1,0:T(8,128)(2,1)S(1)}, bf16[1024,128]{1,0:T(8,128)(2,1)S(1)}, u32[]{:S(2)}, u32[]{:S(2)}) collective-permute-start(bf16[1024,128]{1,0:T(8,128)(2,1)S(1)} %extract1.1.w0), channel_id=1, source_target_pairs={{0,2},{2,4},{4,6},{6,0},{1,3},{3,5},{5,7},{7,1},{8,10},{10,12},{12... | collective-permute-start | bytes 786440 | tf_op jit(solution)/shard_map/ppermute | solution.py:27
  62.2 3.5 %collective-permute-start.17 = (bf16[128,256]{1,0:T(8,128)(2,1)S(1)}, bf16[128,256]{1,0:T(8,128)(2,1)S(1)}, u32[]{:S(2)}, u32[]{:S(2)}) collective-permute-start(bf16[128,256]{1,0:T(8,128)(2,1)S(1)} %pair0.1.x0), channel_id=1, source_target_pairs={{0,4},{2,6},{4,0},{6,2},{1,5},{3,7},{5,1},{7,3},{8,12},{10,14},{12... | collective-permute-start | bytes 196616 | tf_op jit(solution)/shard_map/ppermute | solution.py:27
  65.7 2.4 %collective-permute-done.16.x1 = bf16[128,256]{1,0:T(8,128)(2,1)S(1)} collective-permute-done((bf16[128,256]{1,0:T(8,128)(2,1)S(1)}, bf16[128,256]{1,0:T(8,128)(2,1)S(1)}, u32[]{:S(2)}, u32[]{:S(2)}) %collective-permute-start.16) | collective-permute-done | bytes 65568 | tf_op jit(solution)/shard_map/ppermute | solution.py:27
  68.2 8.7 %collective-permute-done.17.x2 = bf16[128,256]{1,0:T(8,128)(2,1)S(1)} collective-permute-done((bf16[128,256]{1,0:T(8,128)(2,1)S(1)}, bf16[128,256]{1,0:T(8,128)(2,1)S(1)}, u32[]{:S(2)}, u32[]{:S(2)}) %collective-permute-start.17) | collective-permute-done | bytes 65568 | tf_op jit(solution)/shard_map/ppermute | solution.py:27
  76.8 2.7 %collective-permute-done.18.x3 = bf16[128,256]{1,0:T(8,128)(2,1)S(1)} collective-permute-done((bf16[128,256]{1,0:T(8,128)(2,1)S(1)}, bf16[128,256]{1,0:T(8,128)(2,1)S(1)}, u32[]{:S(2)}, u32[]{:S(2)}) %collective-permute-start.18) | collective-permute-done | bytes 65568 | tf_op jit(solution)/shard_map/ppermute | solution.py:27
  80.1 4.3 %collective-permute-start.25 = (bf16[128,256]{1,0:T(8,128)(2,1)S(1)}, bf16[128,256]{1,0:T(8,128)(2,1)S(1)}, u32[]{:S(2)}, u32[]{:S(2)}) collective-permute-start(bf16[128,256]{1,0:T(8,128)(2,1)S(1)} %get-tuple-element.34.own), channel_id=1, source_target_pairs={{0,8},{8,16},{16,24},{24,32},{32,40},{40,48},{48,56},{56,64},{64,7... | collective-permute-start | bytes 196616 | tf_op jit(solution)/shard_map/ppermute | solution.py:39
  84.4 1.9 %collective-permute-start.26 = (bf16[128,256]{1,0:T(8,128)(2,1)S(1)}, bf16[128,256]{1,0:T(8,128)(2,1)S(1)}, u32[]{:S(2)}, u32[]{:S(2)}) collective-permute-start(bf16[128,256]{1,0:T(8,128)(2,1)S(1)} %get-tuple-element.34.own), channel_id=1, source_target_pairs={{8,0},{16,8},{24,16},{32,24},{40,32},{48,40},{56,48},{64,56},{72,6... | collective-permute-start | bytes 196616 | tf_op jit(solution)/shard_map/ppermute | solution.py:43
  86.4 5.2 %collective-permute-done.26.after = bf16[128,256]{1,0:T(8,128)(2,1)S(1)} collective-permute-done((bf16[128,256]{1,0:T(8,128)(2,1)S(1)}, bf16[128,256]{1,0:T(8,128)(2,1)S(1)}, u32[]{:S(2)}, u32[]{:S(2)}) %collective-permute-start.26) | collective-permute-done | bytes 65568 | tf_op jit(solution)/shard_map/ppermute | solution.py:43
  94.5 1.8 %collective-permute-start.34 = (bf16[4,64,512]{2,1,0:T(8,128)(2,1)S(1)}, bf16[4,64,512]{2,1,0:T(8,128)(2,1)S(1)}, u32[]{:S(2)}, u32[]{:S(2)}) collective-permute-start(bf16[4,64,512]{2,1,0:T(8,128)(2,1)S(1)} %pad_maximum_fusion.3.w0), channel_id=1, source_target_pairs={{0,32},{32,64},{64,96},{96,0},{1,33},{33,65},{65,97},{97,1},{2,34}... | collective-permute-start | bytes 786440 | tf_op jit(solution)/shard_map/ppermute | solution.py:27
  96.4 2.5 %collective-permute-start.36 = (bf16[4,64,512]{2,1,0:T(8,128)(2,1)S(1)}, bf16[4,64,512]{2,1,0:T(8,128)(2,1)S(1)}, u32[]{:S(2)}, u32[]{:S(2)}) collective-permute-start(bf16[4,64,512]{2,1,0:T(8,128)(2,1)S(1)} %pad_maximum_fusion.3.w0), channel_id=1, source_target_pairs={{0,96},{32,0},{64,32},{96,64},{1,97},{33,1},{65,33},{97,65},{2,98}... | collective-permute-start | bytes 786440 | tf_op jit(solution)/shard_map/ppermute | solution.py:27
  99.3 4.9 %collective-permute-start.33 = (bf16[128,1024]{1,0:T(8,128)(2,1)S(1)}, bf16[128,1024]{1,0:T(8,128)(2,1)S(1)}, u32[]{:S(2)}, u32[]{:S(2)}) collective-permute-start(bf16[128,1024]{1,0:T(8,128)(2,1)S(1)} %project1.1.mine), channel_id=1, source_target_pairs={{0,1},{1,0},{2,3},{3,2},{4,5},{5,4},{6,7},{7,6},{8,9},{9,8},{10,11... | collective-permute-start | bytes 786440 | tf_op jit(solution)/shard_map/ppermute | solution.py:35
  105.0 1.9 %collective-permute-done.36.w3 = bf16[4,64,512]{2,1,0:T(8,128)(2,1)S(1)} collective-permute-done((bf16[4,64,512]{2,1,0:T(8,128)(2,1)S(1)}, bf16[4,64,512]{2,1,0:T(8,128)(2,1)S(1)}, u32[]{:S(2)}, u32[]{:S(2)}) %collective-permute-start.36) | collective-permute-done | bytes 262176 | tf_op jit(solution)/shard_map/ppermute | solution.py:27
  107.5 1.9 %collective-permute-start.37 = (bf16[128,256]{1,0:T(8,128)(2,1)S(1)}, bf16[128,256]{1,0:T(8,128)(2,1)S(1)}, u32[]{:S(2)}, u32[]{:S(2)}) collective-permute-start(bf16[128,256]{1,0:T(8,128)(2,1)S(1)} %get-tuple-element.36.own), channel_id=1, source_target_pairs={{0,8},{8,16},{16,24},{24,32},{32,40},{40,48},{48,56},{56,64},{64,7... | collective-permute-start | bytes 196616 | tf_op jit(solution)/shard_map/ppermute | solution.py:39
  109.4 3.4 %collective-permute-start.38 = (bf16[128,256]{1,0:T(8,128)(2,1)S(1)}, bf16[128,256]{1,0:T(8,128)(2,1)S(1)}, u32[]{:S(2)}, u32[]{:S(2)}) collective-permute-start(bf16[128,256]{1,0:T(8,128)(2,1)S(1)} %get-tuple-element.36.own), channel_id=1, source_target_pairs={{8,0},{16,8},{24,16},{32,24},{40,32},{48,40},{56,48},{64,56},{72,6... | collective-permute-start | bytes 196616 | tf_op jit(solution)/shard_map/ppermute | solution.py:43
  112.8 3.7 %collective-permute-done.38.after = bf16[128,256]{1,0:T(8,128)(2,1)S(1)} collective-permute-done((bf16[128,256]{1,0:T(8,128)(2,1)S(1)}, bf16[128,256]{1,0:T(8,128)(2,1)S(1)}, u32[]{:S(2)}, u32[]{:S(2)}) %collective-permute-start.38) | collective-permute-done | bytes 65568 | tf_op jit(solution)/shard_map/ppermute | solution.py:43
  117.5 2.1 %collective-permute-start.39 = (bf16[128,256]{1,0:T(8,128)(2,1)S(1)}, bf16[128,256]{1,0:T(8,128)(2,1)S(1)}, u32[]{:S(2)}, u32[]{:S(2)}) collective-permute-start(bf16[128,256]{1,0:T(8,128)(2,1)S(1)} %get-tuple-element.38), channel_id=1, source_target_pairs={{0,2},{2,4},{4,6},{6,0},{1,3},{3,5},{5,7},{7,1},{8,10},{10,12},{12... | collective-permute-start | bytes 196616 | tf_op jit(solution)/shard_map/ppermute | solution.py:249
  119.6 1.8 %collective-permute-start.40 = (bf16[128,256]{1,0:T(8,128)(2,1)S(1)}, bf16[128,256]{1,0:T(8,128)(2,1)S(1)}, u32[]{:S(2)}, u32[]{:S(2)}) collective-permute-start(bf16[128,256]{1,0:T(8,128)(2,1)S(1)} %get-tuple-element.39), channel_id=1, source_target_pairs={{0,4},{2,6},{4,0},{6,2},{1,5},{3,7},{5,1},{7,3},{8,12},{10,14},{12... | collective-permute-start | bytes 196616 | tf_op jit(solution)/shard_map/ppermute | solution.py:250
  121.3 2.8 %collective-permute-done.40.r2 = bf16[128,256]{1,0:T(8,128)(2,1)S(1)} collective-permute-done((bf16[128,256]{1,0:T(8,128)(2,1)S(1)}, bf16[128,256]{1,0:T(8,128)(2,1)S(1)}, u32[]{:S(2)}, u32[]{:S(2)}) %collective-permute-start.40) | collective-permute-done | bytes 65568 | tf_op jit(solution)/shard_map/ppermute | solution.py:250
  125.7 6.9 %collective-permute-start.42 = (f32[128,128]{1,0:T(8,128)S(1)}, f32[128,128]{1,0:T(8,128)S(1)}, u32[]{:S(2)}, u32[]{:S(2)}) collective-permute-start(f32[128,128]{1,0:T(8,128)S(1)} %get-tuple-element.42), channel_id=1, source_target_pairs={{0,1},{1,0},{2,3},{3,2},{4,5},{5,4},{6,7},{7,6},{8,9},{9,8},{10,11... | collective-permute-start | bytes 196616 | tf_op jit(solution)/shard_map/ppermute | solution.py:35
  (94 shorter events, 27.3 us)
Async XLA Ops:
  4.8 9.4 %collective-permute-start = (bf16[144,128]{1,0:T(8,128)(2,1)S(1)}, bf16[144,128]{1,0:T(8,128)(2,1)S(1)}, u32[]{:S(2)}, u32[]{:S(2)}) collective-permute-start(bf16[144,128]{1,0:T(8,128)(2,1)S(1)} %get-tuple-element.24.own), channel_id=1, source_target_pairs={{0,8},{8,16},{16,24},{24,32},{32,40},{40,48},{48,56},{56,64},{64,7... | collective-permute-start | bytes 110600 | tf_op jit(solution)/shard_map/ppermute | solution.py:39
  8.3 8.6 %collective-permute-start.1 = (bf16[144,128]{1,0:T(8,128)(2,1)S(1)}, bf16[144,128]{1,0:T(8,128)(2,1)S(1)}, u32[]{:S(2)}, u32[]{:S(2)}) collective-permute-start(bf16[144,128]{1,0:T(8,128)(2,1)S(1)} %get-tuple-element.24.own), channel_id=1, source_target_pairs={{8,0},{16,8},{24,16},{32,24},{40,32},{48,40},{56,48},{64,56},{72,6... | collective-permute-start | bytes 110600 | tf_op jit(solution)/shard_map/ppermute | solution.py:43
  10.2 8.3 %collective-permute-start.6 = (bf16[64,512]{1,0:T(8,128)(2,1)S(1)}, bf16[64,512]{1,0:T(8,128)(2,1)S(1)}, u32[]{:S(2)}, u32[]{:S(2)}) collective-permute-start(bf16[64,512]{1,0:T(8,128)(2,1)S(1)} %get-tuple-element.25), channel_id=1, source_target_pairs={{0,8},{8,16},{16,24},{24,0},{1,9},{9,17},{17,25},{25,1},{2,10},{10... | collective-permute-start | bytes 196616 | tf_op jit(solution)/shard_map/ppermute | solution.py:27
  10.3 9.0 %collective-permute-start.7 = (bf16[64,512]{1,0:T(8,128)(2,1)S(1)}, bf16[64,512]{1,0:T(8,128)(2,1)S(1)}, u32[]{:S(2)}, u32[]{:S(2)}) collective-permute-start(bf16[64,512]{1,0:T(8,128)(2,1)S(1)} %get-tuple-element.25), channel_id=1, source_target_pairs={{0,16},{8,24},{16,0},{24,8},{1,17},{9,25},{17,1},{25,9},{2,18},{10... | collective-permute-start | bytes 196616 | tf_op jit(solution)/shard_map/ppermute | solution.py:27
  12.5 6.8 %collective-permute-start.8 = (bf16[64,512]{1,0:T(8,128)(2,1)S(1)}, bf16[64,512]{1,0:T(8,128)(2,1)S(1)}, u32[]{:S(2)}, u32[]{:S(2)}) collective-permute-start(bf16[64,512]{1,0:T(8,128)(2,1)S(1)} %get-tuple-element.25), channel_id=1, source_target_pairs={{0,24},{8,0},{16,8},{24,16},{1,25},{9,1},{17,9},{25,17},{2,26},{10... | collective-permute-start | bytes 196616 | tf_op jit(solution)/shard_map/ppermute | solution.py:27
  14.2 7.4 %collective-permute-start.19 = (bf16[2,64,512]{2,1,0:T(8,128)(2,1)S(1)}, bf16[2,64,512]{2,1,0:T(8,128)(2,1)S(1)}, u32[]{:S(2)}, u32[]{:S(2)}) collective-permute-start(bf16[2,64,512]{2,1,0:T(8,128)(2,1)S(1)} %get-tuple-element.32), channel_id=1, source_target_pairs={{0,8},{8,16},{16,24},{24,0},{1,9},{9,17},{17,25},{25,1},{2,10},{10... | collective-permute-start | bytes 393224 | tf_op jit(solution)/shard_map/ppermute | solution.py:27
  18.5 14.1 %collective-permute-start.21 = (bf16[2,64,512]{2,1,0:T(8,128)(2,1)S(1)}, bf16[2,64,512]{2,1,0:T(8,128)(2,1)S(1)}, u32[]{:S(2)}, u32[]{:S(2)}) collective-permute-start(bf16[2,64,512]{2,1,0:T(8,128)(2,1)S(1)} %get-tuple-element.32), channel_id=1, source_target_pairs={{0,24},{8,0},{16,8},{24,16},{1,25},{9,1},{17,9},{25,17},{2,26},{10... | collective-permute-start | bytes 393224 | tf_op jit(solution)/shard_map/ppermute | solution.py:27
  19.4 6.9 %collective-permute-start.2 = (bf16[384,128]{1,0:T(8,128)(2,1)S(1)}, bf16[384,128]{1,0:T(8,128)(2,1)S(1)}, u32[]{:S(2)}, u32[]{:S(2)}) collective-permute-start(bf16[384,128]{1,0:T(8,128)(2,1)S(1)} %get-tuple-element.55), channel_id=1, source_target_pairs={{0,2},{2,4},{4,6},{6,0},{1,3},{3,5},{5,7},{7,1},{8,10},{10,12},{12... | collective-permute-start | bytes 294920 | tf_op jit(solution)/shard_map/ppermute | solution.py:27
  19.4 8.0 %collective-permute-start.3 = (bf16[384,128]{1,0:T(8,128)(2,1)S(1)}, bf16[384,128]{1,0:T(8,128)(2,1)S(1)}, u32[]{:S(2)}, u32[]{:S(2)}) collective-permute-start(bf16[384,128]{1,0:T(8,128)(2,1)S(1)} %get-tuple-element.55), channel_id=1, source_target_pairs={{0,4},{2,6},{4,0},{6,2},{1,5},{3,7},{5,1},{7,3},{8,12},{10,14},{12... | collective-permute-start | bytes 294920 | tf_op jit(solution)/shard_map/ppermute | solution.py:27
  21.7 6.2 %collective-permute-start.4 = (bf16[384,128]{1,0:T(8,128)(2,1)S(1)}, bf16[384,128]{1,0:T(8,128)(2,1)S(1)}, u32[]{:S(2)}, u32[]{:S(2)}) collective-permute-start(bf16[384,128]{1,0:T(8,128)(2,1)S(1)} %get-tuple-element.55), channel_id=1, source_target_pairs={{0,6},{2,0},{4,2},{6,4},{1,7},{3,1},{5,3},{7,5},{8,14},{10,8},{12,... | collective-permute-start | bytes 294920 | tf_op jit(solution)/shard_map/ppermute | solution.py:27
  22.3 11.2 %collective-permute-start.10 = (bf16[4,64,512]{2,1,0:T(8,128)(2,1)S(1)}, bf16[4,64,512]{2,1,0:T(8,128)(2,1)S(1)}, u32[]{:S(2)}, u32[]{:S(2)}) collective-permute-start(bf16[4,64,512]{2,1,0:T(8,128)(2,1)S(1)} %pad_maximum_fusion.1.w0.rest_0_), channel_id=1, source_target_pairs={{0,64},{32,96},{64,0},{96,32},{1,65},{33,97},{65,1},{97,33},{2,66}... | collective-permute-start | bytes 786440 | tf_op jit(solution)/shard_map/ppermute | solution.py:27
  26.3 10.7 %collective-permute-start.11 = (bf16[4,64,512]{2,1,0:T(8,128)(2,1)S(1)}, bf16[4,64,512]{2,1,0:T(8,128)(2,1)S(1)}, u32[]{:S(2)}, u32[]{:S(2)}) collective-permute-start(bf16[4,64,512]{2,1,0:T(8,128)(2,1)S(1)} %pad_maximum_fusion.1.w0.rest_0_), channel_id=1, source_target_pairs={{0,96},{32,0},{64,32},{96,64},{1,97},{33,1},{65,33},{97,65},{2,98}... | collective-permute-start | bytes 786440 | tf_op jit(solution)/shard_map/ppermute | solution.py:27
  27.4 13.1 %collective-permute-start.9 = (bf16[4,64,512]{2,1,0:T(8,128)(2,1)S(1)}, bf16[4,64,512]{2,1,0:T(8,128)(2,1)S(1)}, u32[]{:S(2)}, u32[]{:S(2)}) collective-permute-start(bf16[4,64,512]{2,1,0:T(8,128)(2,1)S(1)} %pad_maximum_fusion.1.w0.rest_0_), channel_id=1, source_target_pairs={{0,32},{32,64},{64,96},{96,0},{1,33},{33,65},{65,97},{97,1},{2,34}... | collective-permute-start | bytes 786440 | tf_op jit(solution)/shard_map/ppermute | solution.py:27
  27.9 12.7 %collective-permute-start.5 = (bf16[4,384,128]{2,1,0:T(8,128)(2,1)S(1)}, bf16[4,384,128]{2,1,0:T(8,128)(2,1)S(1)}, u32[]{:S(2)}, u32[]{:S(2)}) collective-permute-start(bf16[4,384,128]{2,1,0:T(8,128)(2,1)S(1)} %pad_maximum_fusion.own), channel_id=1, source_target_pairs={{0,1},{1,0},{2,3},{3,2},{4,5},{5,4},{6,7},{7,6},{8,9},{9,8},{10,11... | collective-permute-start | bytes 1179656 | tf_op jit(solution)/shard_map/ppermute | solution.py:35
  32.6 26.0 %collective-permute-start.22 = (bf16[4,64,512]{2,1,0:T(8,128)(2,1)S(1)}, bf16[4,64,512]{2,1,0:T(8,128)(2,1)S(1)}, u32[]{:S(2)}, u32[]{:S(2)}) collective-permute-start(bf16[4,64,512]{2,1,0:T(8,128)(2,1)S(1)} %pad_maximum_fusion.2.w0), channel_id=1, source_target_pairs={{0,32},{32,64},{64,96},{96,0},{1,33},{33,65},{65,97},{97,1},{2,34}... | collective-permute-start | bytes 786440 | tf_op jit(solution)/shard_map/ppermute | solution.py:27
  33.5 25.2 %collective-permute-start.23 = (bf16[4,64,512]{2,1,0:T(8,128)(2,1)S(1)}, bf16[4,64,512]{2,1,0:T(8,128)(2,1)S(1)}, u32[]{:S(2)}, u32[]{:S(2)}) collective-permute-start(bf16[4,64,512]{2,1,0:T(8,128)(2,1)S(1)} %pad_maximum_fusion.2.w0), channel_id=1, source_target_pairs={{0,64},{32,96},{64,0},{96,32},{1,65},{33,97},{65,1},{97,33},{2,66}... | collective-permute-start | bytes 786440 | tf_op jit(solution)/shard_map/ppermute | solution.py:27
  37.1 21.6 %collective-permute-start.24 = (bf16[4,64,512]{2,1,0:T(8,128)(2,1)S(1)}, bf16[4,64,512]{2,1,0:T(8,128)(2,1)S(1)}, u32[]{:S(2)}, u32[]{:S(2)}) collective-permute-start(bf16[4,64,512]{2,1,0:T(8,128)(2,1)S(1)} %pad_maximum_fusion.2.w0), channel_id=1, source_target_pairs={{0,96},{32,0},{64,32},{96,64},{1,97},{33,1},{65,33},{97,65},{2,98}... | collective-permute-start | bytes 786440 | tf_op jit(solution)/shard_map/ppermute | solution.py:27
  53.8 6.7 %collective-permute-start.15 = (f32[128,256]{1,0:T(8,128)S(1)}, f32[128,256]{1,0:T(8,128)S(1)}, u32[]{:S(2)}, u32[]{:S(2)}) collective-permute-start(f32[128,256]{1,0:T(8,128)S(1)} %sum0.1.mine), channel_id=1, source_target_pairs={{0,1},{1,0},{2,3},{3,2},{4,5},{5,4},{6,7},{7,6},{8,9},{9,8},{10,11... | collective-permute-start | bytes 393224 | tf_op jit(solution)/shard_map/ppermute | solution.py:35
  58.8 35.1 %collective-permute-start.30 = (bf16[1024,128]{1,0:T(8,128)(2,1)S(1)}, bf16[1024,128]{1,0:T(8,128)(2,1)S(1)}, u32[]{:S(2)}, u32[]{:S(2)}) collective-permute-start(bf16[1024,128]{1,0:T(8,128)(2,1)S(1)} %extract1.1.w0), channel_id=1, source_target_pairs={{0,2},{2,4},{4,6},{6,0},{1,3},{3,5},{5,7},{7,1},{8,10},{10,12},{12... | collective-permute-start | bytes 786440 | tf_op jit(solution)/shard_map/ppermute | solution.py:27
  60.6 7.6 %collective-permute-start.16 = (bf16[128,256]{1,0:T(8,128)(2,1)S(1)}, bf16[128,256]{1,0:T(8,128)(2,1)S(1)}, u32[]{:S(2)}, u32[]{:S(2)}) collective-permute-start(bf16[128,256]{1,0:T(8,128)(2,1)S(1)} %pair0.1.x0), channel_id=1, source_target_pairs={{0,2},{2,4},{4,6},{6,0},{1,3},{3,5},{5,7},{7,1},{8,10},{10,12},{12... | collective-permute-start | bytes 196616 | tf_op jit(solution)/shard_map/ppermute | solution.py:27
  61.5 33.1 %collective-permute-start.31 = (bf16[1024,128]{1,0:T(8,128)(2,1)S(1)}, bf16[1024,128]{1,0:T(8,128)(2,1)S(1)}, u32[]{:S(2)}, u32[]{:S(2)}) collective-permute-start(bf16[1024,128]{1,0:T(8,128)(2,1)S(1)} %extract1.1.w0), channel_id=1, source_target_pairs={{0,4},{2,6},{4,0},{6,2},{1,5},{3,7},{5,1},{7,3},{8,12},{10,14},{12... | collective-permute-start | bytes 786440 | tf_op jit(solution)/shard_map/ppermute | solution.py:27
  62.2 34.2 %collective-permute-start.32 = (bf16[1024,128]{1,0:T(8,128)(2,1)S(1)}, bf16[1024,128]{1,0:T(8,128)(2,1)S(1)}, u32[]{:S(2)}, u32[]{:S(2)}) collective-permute-start(bf16[1024,128]{1,0:T(8,128)(2,1)S(1)} %extract1.1.w0), channel_id=1, source_target_pairs={{0,6},{2,0},{4,2},{6,4},{1,7},{3,1},{5,3},{7,5},{8,14},{10,8},{12,... | collective-permute-start | bytes 786440 | tf_op jit(solution)/shard_map/ppermute | solution.py:27
  62.2 14.7 %collective-permute-start.17 = (bf16[128,256]{1,0:T(8,128)(2,1)S(1)}, bf16[128,256]{1,0:T(8,128)(2,1)S(1)}, u32[]{:S(2)}, u32[]{:S(2)}) collective-permute-start(bf16[128,256]{1,0:T(8,128)(2,1)S(1)} %pair0.1.x0), channel_id=1, source_target_pairs={{0,4},{2,6},{4,0},{6,2},{1,5},{3,7},{5,1},{7,3},{8,12},{10,14},{12... | collective-permute-start | bytes 196616 | tf_op jit(solution)/shard_map/ppermute | solution.py:27
  68.1 11.4 %collective-permute-start.18 = (bf16[128,256]{1,0:T(8,128)(2,1)S(1)}, bf16[128,256]{1,0:T(8,128)(2,1)S(1)}, u32[]{:S(2)}, u32[]{:S(2)}) collective-permute-start(bf16[128,256]{1,0:T(8,128)(2,1)S(1)} %pair0.1.x0), channel_id=1, source_target_pairs={{0,6},{2,0},{4,2},{6,4},{1,7},{3,1},{5,3},{7,5},{8,14},{10,8},{12,... | collective-permute-start | bytes 196616 | tf_op jit(solution)/shard_map/ppermute | solution.py:27
  80.1 6.3 %collective-permute-start.25 = (bf16[128,256]{1,0:T(8,128)(2,1)S(1)}, bf16[128,256]{1,0:T(8,128)(2,1)S(1)}, u32[]{:S(2)}, u32[]{:S(2)}) collective-permute-start(bf16[128,256]{1,0:T(8,128)(2,1)S(1)} %get-tuple-element.34.own), channel_id=1, source_target_pairs={{0,8},{8,16},{16,24},{24,32},{32,40},{40,48},{48,56},{56,64},{64,7... | collective-permute-start | bytes 196616 | tf_op jit(solution)/shard_map/ppermute | solution.py:39
  84.4 7.1 %collective-permute-start.26 = (bf16[128,256]{1,0:T(8,128)(2,1)S(1)}, bf16[128,256]{1,0:T(8,128)(2,1)S(1)}, u32[]{:S(2)}, u32[]{:S(2)}) collective-permute-start(bf16[128,256]{1,0:T(8,128)(2,1)S(1)} %get-tuple-element.34.own), channel_id=1, source_target_pairs={{8,0},{16,8},{24,16},{32,24},{40,32},{48,40},{56,48},{64,56},{72,6... | collective-permute-start | bytes 196616 | tf_op jit(solution)/shard_map/ppermute | solution.py:43
  94.5 9.6 %collective-permute-start.34 = (bf16[4,64,512]{2,1,0:T(8,128)(2,1)S(1)}, bf16[4,64,512]{2,1,0:T(8,128)(2,1)S(1)}, u32[]{:S(2)}, u32[]{:S(2)}) collective-permute-start(bf16[4,64,512]{2,1,0:T(8,128)(2,1)S(1)} %pad_maximum_fusion.3.w0), channel_id=1, source_target_pairs={{0,32},{32,64},{64,96},{96,0},{1,33},{33,65},{65,97},{97,1},{2,34}... | collective-permute-start | bytes 786440 | tf_op jit(solution)/shard_map/ppermute | solution.py:27
  96.4 8.6 %collective-permute-start.35 = (bf16[4,64,512]{2,1,0:T(8,128)(2,1)S(1)}, bf16[4,64,512]{2,1,0:T(8,128)(2,1)S(1)}, u32[]{:S(2)}, u32[]{:S(2)}) collective-permute-start(bf16[4,64,512]{2,1,0:T(8,128)(2,1)S(1)} %pad_maximum_fusion.3.w0), channel_id=1, source_target_pairs={{0,64},{32,96},{64,0},{96,32},{1,65},{33,97},{65,1},{97,33},{2,66}... | collective-permute-start | bytes 786440 | tf_op jit(solution)/shard_map/ppermute | solution.py:27
  96.4 10.5 %collective-permute-start.36 = (bf16[4,64,512]{2,1,0:T(8,128)(2,1)S(1)}, bf16[4,64,512]{2,1,0:T(8,128)(2,1)S(1)}, u32[]{:S(2)}, u32[]{:S(2)}) collective-permute-start(bf16[4,64,512]{2,1,0:T(8,128)(2,1)S(1)} %pad_maximum_fusion.3.w0), channel_id=1, source_target_pairs={{0,96},{32,0},{64,32},{96,64},{1,97},{33,1},{65,33},{97,65},{2,98}... | collective-permute-start | bytes 786440 | tf_op jit(solution)/shard_map/ppermute | solution.py:27
  99.3 7.6 %collective-permute-start.33 = (bf16[128,1024]{1,0:T(8,128)(2,1)S(1)}, bf16[128,1024]{1,0:T(8,128)(2,1)S(1)}, u32[]{:S(2)}, u32[]{:S(2)}) collective-permute-start(bf16[128,1024]{1,0:T(8,128)(2,1)S(1)} %project1.1.mine), channel_id=1, source_target_pairs={{0,1},{1,0},{2,3},{3,2},{4,5},{5,4},{6,7},{7,6},{8,9},{9,8},{10,11... | collective-permute-start | bytes 786440 | tf_op jit(solution)/shard_map/ppermute | solution.py:35
  109.4 7.1 %collective-permute-start.38 = (bf16[128,256]{1,0:T(8,128)(2,1)S(1)}, bf16[128,256]{1,0:T(8,128)(2,1)S(1)}, u32[]{:S(2)}, u32[]{:S(2)}) collective-permute-start(bf16[128,256]{1,0:T(8,128)(2,1)S(1)} %get-tuple-element.36.own), channel_id=1, source_target_pairs={{8,0},{16,8},{24,16},{32,24},{40,32},{48,40},{56,48},{64,56},{72,6... | collective-permute-start | bytes 196616 | tf_op jit(solution)/shard_map/ppermute | solution.py:43
  125.7 7.8 %collective-permute-start.42 = (f32[128,128]{1,0:T(8,128)S(1)}, f32[128,128]{1,0:T(8,128)S(1)}, u32[]{:S(2)}, u32[]{:S(2)}) collective-permute-start(f32[128,128]{1,0:T(8,128)S(1)} %get-tuple-element.42), channel_id=1, source_target_pairs={{0,1},{1,0},{2,3},{3,2},{4,5},{5,4},{6,7},{7,6},{8,9},{9,8},{10,11... | collective-permute-start | bytes 196616 | tf_op jit(solution)/shard_map/ppermute | solution.py:35
  (16 other events, 57.2 us)

commit v2 on v1

v2 whole, which is shorter than its diff:
```python
import jax
import jax.numpy as jnp
from jax import lax
from jax.experimental import pallas as pl
from jax.experimental.pallas import tpu as pltpu
from jax.sharding import Mesh
from jax.sharding import PartitionSpec as P

HEAD_DIM = 64
WIN_ROWS = 8
WIN_COLS = 16
LAYERS = 3
GRID_W = 32
SP = ("z", "x")
TP = ("y", "c")
EPS = 1e-06
F32 = jnp.float32
BF16 = jnp.bfloat16
NT = (((1,), (1,)), ((), ()))


def turn(k):
    return [(i, (i + k) % 4) for i in range(4)]


def spread(a, axis):
    return [lax.ppermute(a, axis, turn(k)) for k in (1, 3, 2)]


def in_order(a, three):
    return [a, three[0], three[2], three[1]]


def gather_rows(a):
    many = a if a.ndim == 3 else jnp.broadcast_to(a[None], (16,) + a.shape)
    return lax.all_to_all(many, SP, 0, 0, tiled=True).reshape(1024, 512)


def after_this(a, done):
    return lax.optimization_barrier((a, done))[0]


def swap(a):
    return lax.ppermute(a, "c", [(0, 1), (1, 0)])


def from_before(a):
    return lax.ppermute(a, SP, [(i, i + 1) for i in range(15)])


def from_after(a):
    return lax.ppermute(a, SP, [(i + 1, i) for i in range(15)])


def behind(axis, k):
    return (lax.axis_index(axis) + (4 - k)) & 3


def ahead(axis, k):
    return (lax.axis_index(axis) + k) & 3


def call(body, outs, *args, scratch=(), name=None, **specs):
    return pl.pallas_call(
        body,
        out_shape=outs,
        **specs,
        scratch_shapes=list(scratch),
        name=name,
        compiler_params=pltpu.CompilerParams(vmem_limit_bytes=24 * 1024 * 1024),
    )(*args)


def shaped(*shape, dtype=BF16):
    return jax.ShapeDtypeStruct(shape, dtype)


def pack_body(
    wq, wk, wv, wo, tokens, docs, first, rest, payload, wq_in, wk_in, wv_in, wo_in, docs_in, sems
):
    pairs = ((wq, wq_in), (wk, wk_in), (wv, wv_in), (wo, wo_in), (docs, docs_in))
    pairs = pairs + ((tokens, payload.at[0:128]),)
    copies = [pltpu.make_async_copy(a, b, sems.at[n]) for n, (a, b) in enumerate(pairs)]
    for copy in copies:
        copy.start()
    for copy in copies:
        copy.wait()
    whole = jnp.concatenate([wq_in[0], wk_in[0], wv_in[0], wo_in[0]], axis=1)
    for n in range(16):
        first[n] = whole
    for layer in (1, 2):
        for n, part in enumerate((wq_in, wk_in, wv_in, wo_in)):
            rest[layer - 1, :, n * 128 : n * 128 + 128] = part[layer]
    payload[128:144, :] = jnp.broadcast_to((docs_in[...] + 1).astype(F32).astype(BF16), (16, 128))


def table_body(bias, before, own, after, table, wide):
    own_docs = own[128:144, :].astype(F32)[0:1]
    query_docs = jnp.broadcast_to(own_docs, (128, 128)).T
    key_docs = jnp.concatenate(
        [before[128:144, :].astype(F32)[0:1], own_docs, after[128:144, :].astype(F32)[0:1]], axis=1
    )
    same = jnp.concatenate([query_docs] * 3, axis=1) == key_docs
    r = lax.broadcasted_iota(jnp.int32, (128, 384), 0)
    m = lax.broadcasted_iota(jnp.int32, (128, 384), 1)
    lag = (m >> 5) - (r >> 5)
    off = (m & 31) - (r & 31) + WIN_COLS // 2
    allowed = same & (lag >= 0) & (lag < WIN_ROWS) & (off >= 0) & (off < WIN_COLS)
    wide[...] = jnp.zeros((8, 256), F32)
    for n in range(2 * LAYERS):
        for lag_row in range(WIN_ROWS):
            at = lag_row * GRID_W
            wide[n : n + 1, at : at + WIN_COLS] = bias[n // 2, n % 2, lag_row : lag_row + 1, :]
    for n in range(2 * LAYERS):
        line = jnp.broadcast_to(wide[n : n + 1, :], (GRID_W, 256))
        line = pltpu.roll(line, 256 - WIN_COLS // 2, 1, stride=1, stride_axis=0)
        line = jnp.concatenate([line, jnp.zeros((GRID_W, 128), F32)], axis=1)
        block = jnp.concatenate(
            [line] + [pltpu.roll(line, 32 * q, 1) for q in range(1, 4)], axis=0
        )
        table[n] = jnp.where(allowed, block, -1e30)


def normed_heads(raw):
    values = raw.astype(BF16).astype(F32)
    squares = values * values
    low = lax.broadcasted_iota(jnp.int32, values.shape, 1) < HEAD_DIM
    first = jnp.sum(jnp.where(low, squares, 0.0), axis=1, keepdims=True)
    second = jnp.sum(jnp.where(low, 0.0, squares), axis=1, keepdims=True)
    scale = jnp.where(
        low,
        lax.rsqrt(first * (1.0 / HEAD_DIM) + EPS),
        lax.rsqrt(second * (1.0 / HEAD_DIM) + EPS),
    )
    return (values * scale).astype(BF16)


def finish_heads(acc, q, kv):
    q[...] = normed_heads(acc[:, 0:128])
    kv[:, 0:128] = normed_heads(acc[:, 128:256])
    kv[:, 128:256] = acc[:, 256:384].astype(BF16)


def heads_first_body(own, partner, gain, weights, q, kv):
    c = lax.axis_index("c")
    total = jnp.zeros((384, 128), F32)
    for k in range(4):
        for part in (own, partner):
            values = part[k].astype(F32)
            total = total + values * values
    scale = lax.rsqrt(jnp.sum(total, axis=1, keepdims=True) * (1.0 / 1024) + EPS)
    acc = jnp.zeros((384, 384), F32)
    for k in range(4):
        for part, core in ((own, c), (partner, 1 - c)):
            block = behind("y", k) * 2 + core
            gains = gain[0:1, pl.ds(pl.multiple_of(block * 128, 128), 128)]
            normed = (part[k].astype(F32) * scale * gains).astype(BF16)
            rows = weights[pl.ds(pl.multiple_of(block * 128, 128), 128), 0:384]
            acc = acc + jnp.dot(normed, rows, preferred_element_type=F32)
    q[...] = normed_heads(acc[128:256, 0:128])
    kv[:, 0:128] = normed_heads(acc[:, 128:256])
    kv[:, 128:256] = acc[:, 256:384].astype(BF16)


def heads_pieces_body(x0, x1, x2, x3, gain, weights, q, kv):
    pieces = [x[...].astype(F32) for x in (x0, x1, x2, x3)]
    total = sum(p * p for p in pieces)
    scale = lax.rsqrt(jnp.sum(total, axis=1, keepdims=True) * (1.0 / 1024) + EPS)
    acc = jnp.zeros((128, 384), F32)
    for k in range(4):
        block = behind("y", k)
        at = pl.ds(pl.multiple_of(block * 256, 256), 256)
        normed = (pieces[k] * scale * gain[1:2, at]).astype(BF16)
        rows = weights[at, 0:384]
        acc = acc + jnp.dot(normed, rows, preferred_element_type=F32)
    finish_heads(acc, q, kv)


def heads_whole_body(mine, theirs, gain, weights, q, kv):
    stream = (mine[...].astype(F32) + theirs[...].astype(F32)).astype(BF16).astype(F32)
    scale = lax.rsqrt(jnp.sum(stream * stream, axis=1, keepdims=True) * (1.0 / 1024) + EPS)
    normed = (stream * scale * gain[2:3, :]).astype(BF16)
    acc = jnp.dot(normed, weights[:, 0:384], preferred_element_type=F32)
    finish_heads(acc, q, kv)


def attend(q, keys_values, table):
    queries = q[...]
    low = lax.broadcasted_iota(jnp.int32, (128, 128), 1) < HEAD_DIM
    results = []
    for h in range(2):
        mine = jnp.where(low if h == 0 else ~low, queries, jnp.zeros_like(queries))
        weights, total = [], 0.0
        for b, (keys, _) in enumerate(keys_values):
            scores = lax.dot_general(mine, keys, NT, preferred_element_type=F32)
            scores = scores * HEAD_DIM**-0.5 + table[h, :, b * 128 : (b + 1) * 128]
            grown = jnp.exp(scores)
            weights.append(grown)
            total = total + jnp.sum(grown, axis=1, keepdims=True)
        share = 1.0 / total
        out = 0.0
        for grown, (_, values) in zip(weights, keys_values):
            probs = (grown * share).astype(BF16)
            out = out + jnp.dot(probs, values, preferred_element_type=F32)
        results.append(out)
    return jnp.where(low, results[0], results[1]).astype(BF16)


def attend_scatter_body(q, before, own, after, table, weights, kept, s1, s2, s3, *, layer):
    parts = [(p[:, 0:128], p[:, 128:256]) for p in (before, own, after)]
    attended = attend(q, parts, table.at[2 * layer : 2 * layer + 2])
    for k, into in enumerate((kept, s1, s2, s3)):
        rows = weights[pl.ds(pl.multiple_of(ahead("y", k) * 256, 256), 256), 384:512]
        share = lax.dot_general(attended, rows, NT, preferred_element_type=F32)
        into[...] = share.astype(into.dtype)


def attend_first_body(q, kv, *rest):
    attend_scatter_body(q, kv.at[0:128], kv.at[128:256], kv.at[256:384], *rest, layer=0)


def attend_last_body(*refs):
    attend_scatter_body(*refs, layer=2)


def attend_body(q, before, own, after, table, out):
    parts = [(p[:, 0:128], p[:, 128:256]) for p in (before, own, after)]
    out[...] = attend(q, parts, table.at[2:4])


def project_body(a0, a1, a2, a3, w, out):
    acc = 0.0
    for k, a in enumerate((a0, a1, a2, a3)):
        acc = acc + lax.dot_general(a[...], w[behind("y", k)], NT, preferred_element_type=F32)
    out[...] = acc.astype(BF16)


def sum_body(kept, r1, r2, r3, out):
    out[...] = kept[...] + r1[...].astype(F32) + r2[...].astype(F32) + r3[...].astype(F32)


def pair_sum_body(mine, theirs, out):
    out[...] = (mine[...] + theirs[...]).astype(BF16)


def split_body(kept, r1, r2, r3, mine, theirs):
    c = lax.axis_index("c")
    for into, core in ((mine, c), (theirs, 1 - c)):
        at = pl.ds(pl.multiple_of(core * 128, 128), 128)
        into[...] = (
            kept[:, at] + r1[:, at].astype(F32) + r2[:, at].astype(F32) + r3[:, at].astype(F32)
        )


def scattered(body, *args):
    outs = [shaped(128, 256, dtype=F32)] + [shaped(128, 256)] * 3
    kept, s1, s2, s3 = call(body, outs, *args, name="attend_scatter")
    r1 = lax.ppermute(s1, "y", turn(1))
    r3 = lax.ppermute(s3, "y", turn(3))
    r2 = lax.ppermute(s2, "y", turn(2))
    return kept, r1, r2, r3


def local(tokens, norm_gain, w_query, w_key, w_value, w_out, offset_bias, documents):
    hbm = pl.BlockSpec(memory_space=pltpu.HBM)
    first, rest, payload = call(
        pack_body,
        [shaped(16, 64, 512), shaped(2, 64, 512), shaped(144, 128)],
        *[
            pltpu.with_memory_space_constraint(a, pltpu.HBM)
            for a in (
                w_query,
                w_key,
                w_value,
                jnp.swapaxes(w_out, 1, 2),
                tokens,
                documents.reshape(1, 128),
            )
        ],
        name="pack",
        in_specs=[hbm] * 6,
        scratch=[pltpu.VMEM((3, 64, 128), BF16)] * 4
        + [pltpu.VMEM((1, 128), jnp.int32), pltpu.SemaphoreType.DMA((6,))],
    )
    weights0 = gather_rows(first)
    before = from_before(payload)
    after = from_after(payload)
    near = jnp.concatenate([before[0:128], payload[0:128], after[0:128]], axis=0)
    near_y = jnp.stack(in_order(near, spread(near, "y")))
    table = call(
        table_body, shaped(6, 128, 384, dtype=F32), offset_bias, before, payload, after,
        scratch=[pltpu.VMEM((8, 256), F32)], name="table",
    )
    near_partner = swap(after_this(near_y, table))

    q, kv = call(
        heads_first_body, [shaped(128, 128), shaped(384, 256)],
        near_y, near_partner, norm_gain, weights0, name="heads0",
    )
    weights1 = gather_rows(after_this(rest[0], q))
    kept, r1, r2, r3 = scattered(attend_first_body, q, kv, table, weights0)
    half = call(sum_body, shaped(128, 256, dtype=F32), kept, r1, r2, r3, name="sum0")
    stream = call(pair_sum_body, shaped(128, 256), half, swap(half), name="pair0")
    pieces = in_order(stream, spread(stream, "y"))

    q, kv = call(
        heads_pieces_body, [shaped(128, 128), shaped(128, 256)],
        *pieces, norm_gain, weights1, name="heads1",
    )
    out1 = jnp.broadcast_to(after_this(weights1, q)[None, :, 384:512], (4, 1024, 128))
    out1_y = lax.all_to_all(out1, "y", 0, 0, tiled=True)
    before, after = from_before(kv), from_after(kv)
    weights2 = gather_rows(after_this(rest[1], (before, after)))
    attended = call(attend_body, shaped(128, 128), q, before, kv, after, table, name="attend1")
    attended_y = in_order(attended, spread(attended, "y"))
    share = call(project_body, shaped(128, 1024), *attended_y, out1_y, name="project1")
    q, kv = call(
        heads_whole_body, [shaped(128, 128), shaped(128, 256)],
        share, swap(share), norm_gain, weights2, name="heads2",
    )
    before, after = from_before(kv), from_after(kv)
    kept, r1, r2, r3 = scattered(attend_last_body, q, before, kv, after, table, weights2)
    mine, theirs = call(
        split_body, [shaped(128, 128, dtype=F32)] * 2, kept, r1, r2, r3, name="split2"
    )
    return call(pair_sum_body, shaped(128, 128), mine, swap(theirs), name="pair2")


def solution(mesh):
    torus = Mesh(mesh.devices.reshape(4, 4, 4, 2), ("z", "x", "y", "c"))
    return jax.shard_map(
        local,
        mesh=torus,
        in_specs=(
            P(SP, TP),
            P(),
            P(None, SP, TP),
            P(None, SP, TP),
            P(None, SP, TP),
            P(None, TP, SP),
            P(None, TP, None, None),
            P(SP),
        ),
        out_specs=P(SP, TP),
        check_vma=False,
    )
```

time: 135 us -> 130 us (0.963)
  the two profiles are of different devices: /device:TPU:31 before, /device:TPU:33 now
where the time goes in v2:
time: 130 us
  starting transfers between devices  70.2 us (54%)
  waiting for transfers between devices  46.7 us (36%)
  Pallas kernels  8.41 us (6%)
  local copies, waits for them, and re-layouts  3.99 us (3%)
    all_to_all x3, starting transfers between devices, gather_rows(): return lax.all_to_all(many, SP, 0, 0, tiled=True).reshape(1024, 512)  18.9 us
    ppermute x3, waiting for transfers between devices, from_before(): return lax.ppermute(a, SP, [(i, i + 1) for i in range(15)])  15.6 us
    ppermute x4, starting transfers between devices, swap(): return lax.ppermute(a, 'c', [(0, 1), (1, 0)])  13 us
    ppermute x3, starting transfers between devices, from_after(): return lax.ppermute(a, SP, [(i + 1, i) for i in range(15)])  11.7 us
    ppermute x9, waiting for transfers between devices, spread(): return [lax.ppermute(a, axis, turn(k)) for k in (1, 3, 2)]  11.5 us
    ppermute x9, starting transfers between devices, spread(): return [lax.ppermute(a, axis, turn(k)) for k in (1, 3, 2)]  9.97 us
    pallas_call x13, Pallas kernels, call(): pl.pallas_call(body, out_shape=outs, **specs, scratch_shapes=list(scratch...  8.41 us
    ppermute x3, starting transfers between devices, from_before(): return lax.ppermute(a, SP, [(i, i + 1) for i in range(15)])  6.02 us
  transfers between devices with their start and end apart: 29, of which 22 were waited for; matrix products, arithmetic and copies ran while one was open for 1% of the time, Pallas kernels for 2%

profile of v2, /device:TPU:33, one launch (start us, length us, event | category | flops | bytes accessed | tf_op | source)
XLA Modules:
  0.0 129.6 jit_solution(9195430255987942963)
XLA Ops:
  0.0 2.0 %pack.1 = (bf16[16,64,512]{2,1,0:T(8,128)(2,1)}, bf16[2,64,512]{2,1,0:T(8,128)(2,1)S(1)}, bf16[144,128]{1,0:T(8,128)(2,1)S(1)}) custom-call(bf16[3,64,128]{2,1,0:T(8,128)(2,1)} %wq.1, bf16[3,64,128]{2,1,0:T(8,128)(2,1)} %wk.1, bf16[3,64,128]{2,1,0:T(8,128)(2,1)} %wv.1, bf16[3,64,128]{2,1,0:T(8,128)(2,1)} %bitcast.23, bf16[128,128]{1,0:T(8,128)(2,1)} %tokens.1, ...), custom_call_target="tpu_custom_call" | custom-call | tf_op jit(solution)/shard_map/pack/pallas_call | solution.py:64
  2.1 7.3 %all-to-all-start = ((bf16[16,64,512]{2,1,0:T(8,128)(2,1)}), bf16[16,64,512]{2,1,0:T(8,128)(2,1)S(1)}, u32[]{:S(2)}, u32[]{:S(2)}) async-start(bf16[16,64,512]{2,1,0:T(8,128)(2,1)} %get-tuple-element.30), calls=%async_computation | async-start | bytes 2097152 | tf_op jit(solution)/shard_map/all_to_all | solution.py:36
  9.4 4.3 %collective-permute-start.1 = (bf16[144,128]{1,0:T(8,128)(2,1)S(1)}, bf16[144,128]{1,0:T(8,128)(2,1)S(1)}, u32[]{:S(2)}, u32[]{:S(2)}) collective-permute-start(bf16[144,128]{1,0:T(8,128)(2,1)S(1)} %get-tuple-element.28.own), channel_id=1, source_target_pairs={{8,0},{16,8},{24,16},{32,24},{40,32},{48,40},{56,48},{64,56},{72,6... | collective-permute-start | bytes 110600 | tf_op jit(solution)/shard_map/ppermute | solution.py:52
  13.7 1.9 %collective-permute-start = (bf16[144,128]{1,0:T(8,128)(2,1)S(1)}, bf16[144,128]{1,0:T(8,128)(2,1)S(1)}, u32[]{:S(2)}, u32[]{:S(2)}) collective-permute-start(bf16[144,128]{1,0:T(8,128)(2,1)S(1)} %get-tuple-element.28.own), channel_id=1, source_target_pairs={{0,8},{8,16},{16,24},{24,32},{32,40},{40,48},{48,56},{56,64},{64,7... | collective-permute-start | bytes 110600 | tf_op jit(solution)/shard_map/ppermute | solution.py:48
  15.6 5.9 %collective-permute-done.1.after = bf16[144,128]{1,0:T(8,128)(2,1)S(1)} collective-permute-done((bf16[144,128]{1,0:T(8,128)(2,1)S(1)}, bf16[144,128]{1,0:T(8,128)(2,1)S(1)}, u32[]{:S(2)}, u32[]{:S(2)}) %collective-permute-start.1) | collective-permute-done | bytes 36896 | tf_op jit(solution)/shard_map/ppermute | solution.py:52
  21.6 5.2 %collective-permute-done.before = bf16[144,128]{1,0:T(8,128)(2,1)S(1)} collective-permute-done((bf16[144,128]{1,0:T(8,128)(2,1)S(1)}, bf16[144,128]{1,0:T(8,128)(2,1)S(1)}, u32[]{:S(2)}, u32[]{:S(2)}) %collective-permute-start) | collective-permute-done | bytes 36896 | tf_op jit(solution)/shard_map/ppermute | solution.py:48
  26.8 3.0 %collective-permute-start.3 = (bf16[384,128]{1,0:T(8,128)(2,1)S(1)}, bf16[384,128]{1,0:T(8,128)(2,1)S(1)}, u32[]{:S(2)}, u32[]{:S(2)}) collective-permute-start(bf16[384,128]{1,0:T(8,128)(2,1)S(1)} %get-tuple-element.54), channel_id=1, source_target_pairs={{0,4},{2,6},{4,0},{6,2},{1,5},{3,7},{5,1},{7,3},{8,12},{10,14},{12... | collective-permute-start | bytes 294920 | tf_op jit(solution)/shard_map/ppermute | solution.py:27
  30.2 2.3 %collective-permute-start.4 = (bf16[384,128]{1,0:T(8,128)(2,1)S(1)}, bf16[384,128]{1,0:T(8,128)(2,1)S(1)}, u32[]{:S(2)}, u32[]{:S(2)}) collective-permute-start(bf16[384,128]{1,0:T(8,128)(2,1)S(1)} %get-tuple-element.54), channel_id=1, source_target_pairs={{0,6},{2,0},{4,2},{6,4},{1,7},{3,1},{5,3},{7,5},{8,14},{10,8},{12,... | collective-permute-start | bytes 294920 | tf_op jit(solution)/shard_map/ppermute | solution.py:27
  33.0 2.1 %collective-permute-done.2 = bf16[384,128]{1,0:T(8,128)(2,1)S(1)} collective-permute-done((bf16[384,128]{1,0:T(8,128)(2,1)S(1)}, bf16[384,128]{1,0:T(8,128)(2,1)S(1)}, u32[]{:S(2)}, u32[]{:S(2)}) %collective-permute-start.2) | collective-permute-done | bytes 98336 | tf_op jit(solution)/shard_map/ppermute | solution.py:27
  39.8 4.8 %all-to-all-start.1 = ((bf16[16,64,512]{2,1,0:T(8,128)(2,1)}), bf16[16,64,512]{2,1,0:T(8,128)(2,1)S(1)}, u32[]{:S(2)}, u32[]{:S(2)}) async-start(bf16[16,64,512]{2,1,0:T(8,128)(2,1)} %broadcast_in_dim.6), calls=%async_computation.1 | async-start | bytes 2097152 | tf_op jit(solution)/shard_map/all_to_all | solution.py:36
  46.5 3.4 %collective-permute-start.7 = (bf16[128,256]{1,0:T(8,128)(2,1)S(1)}, bf16[128,256]{1,0:T(8,128)(2,1)S(1)}, u32[]{:S(2)}, u32[]{:S(2)}) collective-permute-start(bf16[128,256]{1,0:T(8,128)(2,1)S(1)} %get-tuple-element.35), channel_id=1, source_target_pairs={{0,4},{2,6},{4,0},{6,2},{1,5},{3,7},{5,1},{7,3},{8,12},{10,14},{12... | collective-permute-start | bytes 196616 | tf_op jit(solution)/shard_map/ppermute | solution.py:260
  50.6 1.9 %collective-permute-done.7.r2 = bf16[128,256]{1,0:T(8,128)(2,1)S(1)} collective-permute-done((bf16[128,256]{1,0:T(8,128)(2,1)S(1)}, bf16[128,256]{1,0:T(8,128)(2,1)S(1)}, u32[]{:S(2)}, u32[]{:S(2)}) %collective-permute-start.7) | collective-permute-done | bytes 65568 | tf_op jit(solution)/shard_map/ppermute | solution.py:260
  53.4 2.3 %collective-permute-start.9 = (f32[128,256]{1,0:T(8,128)S(1)}, f32[128,256]{1,0:T(8,128)S(1)}, u32[]{:S(2)}, u32[]{:S(2)}) collective-permute-start(f32[128,256]{1,0:T(8,128)S(1)} %sum0.1.mine), channel_id=1, source_target_pairs={{0,1},{1,0},{2,3},{3,2},{4,5},{5,4},{6,7},{7,6},{8,9},{9,8},{10,11... | collective-permute-start | bytes 393224 | tf_op jit(solution)/shard_map/ppermute | solution.py:44
  58.8 1.3 %collective-permute-done.12.x3 = bf16[128,256]{1,0:T(8,128)(2,1)S(1)} collective-permute-done((bf16[128,256]{1,0:T(8,128)(2,1)S(1)}, bf16[128,256]{1,0:T(8,128)(2,1)S(1)}, u32[]{:S(2)}, u32[]{:S(2)}) %collective-permute-start.12) | collective-permute-done | bytes 65568 | tf_op jit(solution)/shard_map/ppermute | solution.py:27
  60.2 2.1 %collective-permute-done.11.x2 = bf16[128,256]{1,0:T(8,128)(2,1)S(1)} collective-permute-done((bf16[128,256]{1,0:T(8,128)(2,1)S(1)}, bf16[128,256]{1,0:T(8,128)(2,1)S(1)}, u32[]{:S(2)}, u32[]{:S(2)}) %collective-permute-start.11) | collective-permute-done | bytes 65568 | tf_op jit(solution)/shard_map/ppermute | solution.py:27
  62.3 1.7 %collective-permute-done.10.x1 = bf16[128,256]{1,0:T(8,128)(2,1)S(1)} collective-permute-done((bf16[128,256]{1,0:T(8,128)(2,1)S(1)}, bf16[128,256]{1,0:T(8,128)(2,1)S(1)}, u32[]{:S(2)}, u32[]{:S(2)}) %collective-permute-start.10) | collective-permute-done | bytes 65568 | tf_op jit(solution)/shard_map/ppermute | solution.py:27
  65.7 3.6 %all-to-all-start.2 = ((bf16[4,1024,128]{2,1,0:T(8,128)(2,1)}), bf16[4,1024,128]{2,1,0:T(8,128)(2,1)S(1)}, u32[]{:S(2)}, u32[]{:S(2)}) async-start(bf16[4,1024,128]{2,1,0:T(8,128)(2,1)} %broadcast_in_dim.7), calls=%async_computation.2 | async-start | bytes 2097152 | tf_op jit(solution)/shard_map/all_to_all | solution.py:311
  69.3 4.3 %collective-permute-start.14 = (bf16[128,256]{1,0:T(8,128)(2,1)S(1)}, bf16[128,256]{1,0:T(8,128)(2,1)S(1)}, u32[]{:S(2)}, u32[]{:S(2)}) collective-permute-start(bf16[128,256]{1,0:T(8,128)(2,1)S(1)} %get-tuple-element.40.own), channel_id=1, source_target_pairs={{8,0},{16,8},{24,16},{32,24},{40,32},{48,40},{56,48},{64,56},{72,6... | collective-permute-start | bytes 196616 | tf_op jit(solution)/shard_map/ppermute | solution.py:52
  73.6 1.9 %collective-permute-start.13 = (bf16[128,256]{1,0:T(8,128)(2,1)S(1)}, bf16[128,256]{1,0:T(8,128)(2,1)S(1)}, u32[]{:S(2)}, u32[]{:S(2)}) collective-permute-start(bf16[128,256]{1,0:T(8,128)(2,1)S(1)} %get-tuple-element.40.own), channel_id=1, source_target_pairs={{0,8},{8,16},{16,24},{24,32},{32,40},{40,48},{48,56},{56,64},{64,7... | collective-permute-start | bytes 196616 | tf_op jit(solution)/shard_map/ppermute | solution.py:48
  75.6 5.5 %collective-permute-done.13.before = bf16[128,256]{1,0:T(8,128)(2,1)S(1)} collective-permute-done((bf16[128,256]{1,0:T(8,128)(2,1)S(1)}, bf16[128,256]{1,0:T(8,128)(2,1)S(1)}, u32[]{:S(2)}, u32[]{:S(2)}) %collective-permute-start.13) | collective-permute-done | bytes 65568 | tf_op jit(solution)/shard_map/ppermute | solution.py:48
  81.0 2.3 %all-to-all-done.2.w = bf16[4,1024,128]{2,1,0:T(8,128)(2,1)S(1)} async-done(((bf16[4,1024,128]{2,1,0:T(8,128)(2,1)}), bf16[4,1024,128]{2,1,0:T(8,128)(2,1)S(1)}, u32[]{:S(2)}, u32[]{:S(2)}) %all-to-all-start.2) | async-done | bytes 1048608 | tf_op jit(solution)/shard_map/all_to_all | solution.py:311
  84.4 6.7 %all-to-all-start.3 = ((bf16[16,64,512]{2,1,0:T(8,128)(2,1)}), bf16[16,64,512]{2,1,0:T(8,128)(2,1)S(1)}, u32[]{:S(2)}, u32[]{:S(2)}) async-start(bf16[16,64,512]{2,1,0:T(8,128)(2,1)} %broadcast_in_dim.8), calls=%async_computation.3 | async-start | bytes 2097152 | tf_op jit(solution)/shard_map/all_to_all | solution.py:36
  94.7 2.4 %collective-permute-done.16.a2 = bf16[128,128]{1,0:T(8,128)(2,1)S(1)} collective-permute-done((bf16[128,128]{1,0:T(8,128)(2,1)S(1)}, bf16[128,128]{1,0:T(8,128)(2,1)S(1)}, u32[]{:S(2)}, u32[]{:S(2)}) %collective-permute-start.16) | collective-permute-done | bytes 32800 | tf_op jit(solution)/shard_map/ppermute | solution.py:27
  97.1 1.2 collective-permute-done.15.a1
  98.8 4.2 %collective-permute-start.18 = (bf16[128,1024]{1,0:T(8,128)(2,1)S(1)}, bf16[128,1024]{1,0:T(8,128)(2,1)S(1)}, u32[]{:S(2)}, u32[]{:S(2)}) collective-permute-start(bf16[128,1024]{1,0:T(8,128)(2,1)S(1)} %project1.1.mine), channel_id=1, source_target_pairs={{0,1},{1,0},{2,3},{3,2},{4,5},{5,4},{6,7},{7,6},{8,9},{9,8},{10,11... | collective-permute-start | bytes 786440 | tf_op jit(solution)/shard_map/ppermute | solution.py:44
  104.2 1.2 all-to-all-done.3
  105.9 3.1 %collective-permute-start.20 = (bf16[128,256]{1,0:T(8,128)(2,1)S(1)}, bf16[128,256]{1,0:T(8,128)(2,1)S(1)}, u32[]{:S(2)}, u32[]{:S(2)}) collective-permute-start(bf16[128,256]{1,0:T(8,128)(2,1)S(1)} %get-tuple-element.44.refs_2_), channel_id=1, source_target_pairs={{8,0},{16,8},{24,16},{32,24},{40,32},{48,40},{56,48},{64,56},{72,6... | collective-permute-start | bytes 196616 | tf_op jit(solution)/shard_map/ppermute | solution.py:52
  109.0 2.2 %collective-permute-start.19 = (bf16[128,256]{1,0:T(8,128)(2,1)S(1)}, bf16[128,256]{1,0:T(8,128)(2,1)S(1)}, u32[]{:S(2)}, u32[]{:S(2)}) collective-permute-start(bf16[128,256]{1,0:T(8,128)(2,1)S(1)} %get-tuple-element.44.refs_2_), channel_id=1, source_target_pairs={{0,8},{8,16},{16,24},{24,32},{32,40},{40,48},{48,56},{56,64},{64,7... | collective-permute-start | bytes 196616 | tf_op jit(solution)/shard_map/ppermute | solution.py:48
  111.2 4.9 %collective-permute-done.19.refs_1_ = bf16[128,256]{1,0:T(8,128)(2,1)S(1)} collective-permute-done((bf16[128,256]{1,0:T(8,128)(2,1)S(1)}, bf16[128,256]{1,0:T(8,128)(2,1)S(1)}, u32[]{:S(2)}, u32[]{:S(2)}) %collective-permute-start.19) | collective-permute-done | bytes 65568 | tf_op jit(solution)/shard_map/ppermute | solution.py:48
  117.2 1.7 %collective-permute-start.22 = (bf16[128,256]{1,0:T(8,128)(2,1)S(1)}, bf16[128,256]{1,0:T(8,128)(2,1)S(1)}, u32[]{:S(2)}, u32[]{:S(2)}) collective-permute-start(bf16[128,256]{1,0:T(8,128)(2,1)S(1)} %get-tuple-element.47), channel_id=1, source_target_pairs={{0,4},{2,6},{4,0},{6,2},{1,5},{3,7},{5,1},{7,3},{8,12},{10,14},{12... | collective-permute-start | bytes 196616 | tf_op jit(solution)/shard_map/ppermute | solution.py:260
  119.8 2.3 %collective-permute-done.21.r1 = bf16[128,256]{1,0:T(8,128)(2,1)S(1)} collective-permute-done((bf16[128,256]{1,0:T(8,128)(2,1)S(1)}, bf16[128,256]{1,0:T(8,128)(2,1)S(1)}, u32[]{:S(2)}, u32[]{:S(2)}) %collective-permute-start.21) | collective-permute-done | bytes 65568 | tf_op jit(solution)/shard_map/ppermute | solution.py:258
  122.8 5.3 %collective-permute-start.24 = (f32[128,128]{1,0:T(8,128)S(1)}, f32[128,128]{1,0:T(8,128)S(1)}, u32[]{:S(2)}, u32[]{:S(2)}) collective-permute-start(f32[128,128]{1,0:T(8,128)S(1)} %get-tuple-element.50), channel_id=1, source_target_pairs={{0,1},{1,0},{2,3},{3,2},{4,5},{5,4},{6,7},{7,6},{8,9},{9,8},{10,11... | collective-permute-start | bytes 196616 | tf_op jit(solution)/shard_map/ppermute | solution.py:44
  (55 shorter events, 24.8 us)
Async XLA Ops:
  2.0 30.4 %copy-start.1 = (f32[3,2,8,16]{3,2,1,0:T(8,128)S(1)}, f32[3,2,8,16]{3,2,1,0:T(8,128)}, u32[]{:S(2)}) copy-start(f32[3,2,8,16]{3,2,1,0:T(8,128)} %bias.1) | copy-start | bytes 9220
  2.1 35.7 %all-to-all-start = ((bf16[16,64,512]{2,1,0:T(8,128)(2,1)}), bf16[16,64,512]{2,1,0:T(8,128)(2,1)S(1)}, u32[]{:S(2)}, u32[]{:S(2)}) async-start(bf16[16,64,512]{2,1,0:T(8,128)(2,1)} %get-tuple-element.30), calls=%async_computation | async-start | bytes 2097152 | tf_op jit(solution)/shard_map/all_to_all | solution.py:36
  9.4 12.2 %collective-permute-start.1 = (bf16[144,128]{1,0:T(8,128)(2,1)S(1)}, bf16[144,128]{1,0:T(8,128)(2,1)S(1)}, u32[]{:S(2)}, u32[]{:S(2)}) collective-permute-start(bf16[144,128]{1,0:T(8,128)(2,1)S(1)} %get-tuple-element.28.own), channel_id=1, source_target_pairs={{8,0},{16,8},{24,16},{32,24},{40,32},{48,40},{56,48},{64,56},{72,6... | collective-permute-start | bytes 110600 | tf_op jit(solution)/shard_map/ppermute | solution.py:52
  13.7 13.1 %collective-permute-start = (bf16[144,128]{1,0:T(8,128)(2,1)S(1)}, bf16[144,128]{1,0:T(8,128)(2,1)S(1)}, u32[]{:S(2)}, u32[]{:S(2)}) collective-permute-start(bf16[144,128]{1,0:T(8,128)(2,1)S(1)} %get-tuple-element.28.own), channel_id=1, source_target_pairs={{0,8},{8,16},{16,24},{24,32},{32,40},{40,48},{48,56},{56,64},{64,7... | collective-permute-start | bytes 110600 | tf_op jit(solution)/shard_map/ppermute | solution.py:48
  26.8 11.0 %copy-start = (f32[3,1024]{1,0:T(4,128)S(1)}, f32[3,1024]{1,0:T(4,128)}, u32[]{:S(2)}) copy-start(f32[3,1024]{1,0:T(4,128)} %gain.5) | copy-start | bytes 36868
  26.8 6.2 %collective-permute-start.3 = (bf16[384,128]{1,0:T(8,128)(2,1)S(1)}, bf16[384,128]{1,0:T(8,128)(2,1)S(1)}, u32[]{:S(2)}, u32[]{:S(2)}) collective-permute-start(bf16[384,128]{1,0:T(8,128)(2,1)S(1)} %get-tuple-element.54), channel_id=1, source_target_pairs={{0,4},{2,6},{4,0},{6,2},{1,5},{3,7},{5,1},{7,3},{8,12},{10,14},{12... | collective-permute-start | bytes 294920 | tf_op jit(solution)/shard_map/ppermute | solution.py:27
  29.8 5.4 %collective-permute-start.2 = (bf16[384,128]{1,0:T(8,128)(2,1)S(1)}, bf16[384,128]{1,0:T(8,128)(2,1)S(1)}, u32[]{:S(2)}, u32[]{:S(2)}) collective-permute-start(bf16[384,128]{1,0:T(8,128)(2,1)S(1)} %get-tuple-element.54), channel_id=1, source_target_pairs={{0,2},{2,4},{4,6},{6,0},{1,3},{3,5},{5,7},{7,1},{8,10},{10,12},{12... | collective-permute-start | bytes 294920 | tf_op jit(solution)/shard_map/ppermute | solution.py:27
  30.2 5.0 %collective-permute-start.4 = (bf16[384,128]{1,0:T(8,128)(2,1)S(1)}, bf16[384,128]{1,0:T(8,128)(2,1)S(1)}, u32[]{:S(2)}, u32[]{:S(2)}) collective-permute-start(bf16[384,128]{1,0:T(8,128)(2,1)S(1)} %get-tuple-element.54), channel_id=1, source_target_pairs={{0,6},{2,0},{4,2},{6,4},{1,7},{3,1},{5,3},{7,5},{8,14},{10,8},{12,... | collective-permute-start | bytes 294920 | tf_op jit(solution)/shard_map/ppermute | solution.py:27
  35.2 2.5 %collective-permute-start.5 = (bf16[4,384,128]{2,1,0:T(8,128)(2,1)S(1)}, bf16[4,384,128]{2,1,0:T(8,128)(2,1)S(1)}, u32[]{:S(2)}, u32[]{:S(2)}) collective-permute-start(bf16[4,384,128]{2,1,0:T(8,128)(2,1)S(1)} %pad_maximum_fusion.own), channel_id=1, source_target_pairs={{0,1},{1,0},{2,3},{3,2},{4,5},{5,4},{6,7},{7,6},{8,9},{9,8},{10,11... | collective-permute-start | bytes 1179656 | tf_op jit(solution)/shard_map/ppermute | solution.py:44
  39.8 24.1 %all-to-all-start.1 = ((bf16[16,64,512]{2,1,0:T(8,128)(2,1)}), bf16[16,64,512]{2,1,0:T(8,128)(2,1)S(1)}, u32[]{:S(2)}, u32[]{:S(2)}) async-start(bf16[16,64,512]{2,1,0:T(8,128)(2,1)} %broadcast_in_dim.6), calls=%async_computation.1 | async-start | bytes 2097152 | tf_op jit(solution)/shard_map/all_to_all | solution.py:36
  45.6 4.9 %collective-permute-start.6 = (bf16[128,256]{1,0:T(8,128)(2,1)S(1)}, bf16[128,256]{1,0:T(8,128)(2,1)S(1)}, u32[]{:S(2)}, u32[]{:S(2)}) collective-permute-start(bf16[128,256]{1,0:T(8,128)(2,1)S(1)} %get-tuple-element.34), channel_id=1, source_target_pairs={{0,2},{2,4},{4,6},{6,0},{1,3},{3,5},{5,7},{7,1},{8,10},{10,12},{12... | collective-permute-start | bytes 196616 | tf_op jit(solution)/shard_map/ppermute | solution.py:258
  46.5 6.0 %collective-permute-start.7 = (bf16[128,256]{1,0:T(8,128)(2,1)S(1)}, bf16[128,256]{1,0:T(8,128)(2,1)S(1)}, u32[]{:S(2)}, u32[]{:S(2)}) collective-permute-start(bf16[128,256]{1,0:T(8,128)(2,1)S(1)} %get-tuple-element.35), channel_id=1, source_target_pairs={{0,4},{2,6},{4,0},{6,2},{1,5},{3,7},{5,1},{7,3},{8,12},{10,14},{12... | collective-permute-start | bytes 196616 | tf_op jit(solution)/shard_map/ppermute | solution.py:260
  49.8 3.5 %collective-permute-start.8 = (bf16[128,256]{1,0:T(8,128)(2,1)S(1)}, bf16[128,256]{1,0:T(8,128)(2,1)S(1)}, u32[]{:S(2)}, u32[]{:S(2)}) collective-permute-start(bf16[128,256]{1,0:T(8,128)(2,1)S(1)} %get-tuple-element.36), channel_id=1, source_target_pairs={{0,6},{2,0},{4,2},{6,4},{1,7},{3,1},{5,3},{7,5},{8,14},{10,8},{12,... | collective-permute-start | bytes 196616 | tf_op jit(solution)/shard_map/ppermute | solution.py:259
  53.4 3.3 %collective-permute-start.9 = (f32[128,256]{1,0:T(8,128)S(1)}, f32[128,256]{1,0:T(8,128)S(1)}, u32[]{:S(2)}, u32[]{:S(2)}) collective-permute-start(f32[128,256]{1,0:T(8,128)S(1)} %sum0.1.mine), channel_id=1, source_target_pairs={{0,1},{1,0},{2,3},{3,2},{4,5},{5,4},{6,7},{7,6},{8,9},{9,8},{10,11... | collective-permute-start | bytes 393224 | tf_op jit(solution)/shard_map/ppermute | solution.py:44
  56.7 3.5 %collective-permute-start.12 = (bf16[128,256]{1,0:T(8,128)(2,1)S(1)}, bf16[128,256]{1,0:T(8,128)(2,1)S(1)}, u32[]{:S(2)}, u32[]{:S(2)}) collective-permute-start(bf16[128,256]{1,0:T(8,128)(2,1)S(1)} %pair0.1.x0), channel_id=1, source_target_pairs={{0,6},{2,0},{4,2},{6,4},{1,7},{3,1},{5,3},{7,5},{8,14},{10,8},{12,... | collective-permute-start | bytes 196616 | tf_op jit(solution)/shard_map/ppermute | solution.py:27
  57.7 4.6 %collective-permute-start.11 = (bf16[128,256]{1,0:T(8,128)(2,1)S(1)}, bf16[128,256]{1,0:T(8,128)(2,1)S(1)}, u32[]{:S(2)}, u32[]{:S(2)}) collective-permute-start(bf16[128,256]{1,0:T(8,128)(2,1)S(1)} %pair0.1.x0), channel_id=1, source_target_pairs={{0,4},{2,6},{4,0},{6,2},{1,5},{3,7},{5,1},{7,3},{8,12},{10,14},{12... | collective-permute-start | bytes 196616 | tf_op jit(solution)/shard_map/ppermute | solution.py:27
  58.1 5.9 %collective-permute-start.10 = (bf16[128,256]{1,0:T(8,128)(2,1)S(1)}, bf16[128,256]{1,0:T(8,128)(2,1)S(1)}, u32[]{:S(2)}, u32[]{:S(2)}) collective-permute-start(bf16[128,256]{1,0:T(8,128)(2,1)S(1)} %pair0.1.x0), channel_id=1, source_target_pairs={{0,2},{2,4},{4,6},{6,0},{1,3},{3,5},{5,7},{7,1},{8,10},{10,12},{12... | collective-permute-start | bytes 196616 | tf_op jit(solution)/shard_map/ppermute | solution.py:27
  65.7 17.7 %copy-start.2 = (bf16[64,512]{1,0:T(8,128)(2,1)S(1)}, bf16[64,512]{1,0:T(8,128)(2,1)}, u32[]{:S(2)}) copy-start(bf16[64,512]{1,0:T(8,128)(2,1)} %get-tuple-element.42) | copy-start | bytes 196612
  65.7 17.7 %all-to-all-start.2 = ((bf16[4,1024,128]{2,1,0:T(8,128)(2,1)}), bf16[4,1024,128]{2,1,0:T(8,128)(2,1)S(1)}, u32[]{:S(2)}, u32[]{:S(2)}) async-start(bf16[4,1024,128]{2,1,0:T(8,128)(2,1)} %broadcast_in_dim.7), calls=%async_computation.2 | async-start | bytes 2097152 | tf_op jit(solution)/shard_map/all_to_all | solution.py:311
  69.3 6.3 %collective-permute-start.14 = (bf16[128,256]{1,0:T(8,128)(2,1)S(1)}, bf16[128,256]{1,0:T(8,128)(2,1)S(1)}, u32[]{:S(2)}, u32[]{:S(2)}) collective-permute-start(bf16[128,256]{1,0:T(8,128)(2,1)S(1)} %get-tuple-element.40.own), channel_id=1, source_target_pairs={{8,0},{16,8},{24,16},{32,24},{40,32},{48,40},{56,48},{64,56},{72,6... | collective-permute-start | bytes 196616 | tf_op jit(solution)/shard_map/ppermute | solution.py:52
  73.6 7.4 %collective-permute-start.13 = (bf16[128,256]{1,0:T(8,128)(2,1)S(1)}, bf16[128,256]{1,0:T(8,128)(2,1)S(1)}, u32[]{:S(2)}, u32[]{:S(2)}) collective-permute-start(bf16[128,256]{1,0:T(8,128)(2,1)S(1)} %get-tuple-element.40.own), channel_id=1, source_target_pairs={{0,8},{8,16},{16,24},{24,32},{32,40},{40,48},{48,56},{56,64},{64,7... | collective-permute-start | bytes 196616 | tf_op jit(solution)/shard_map/ppermute | solution.py:48
  84.4 20.9 %all-to-all-start.3 = ((bf16[16,64,512]{2,1,0:T(8,128)(2,1)}), bf16[16,64,512]{2,1,0:T(8,128)(2,1)S(1)}, u32[]{:S(2)}, u32[]{:S(2)}) async-start(bf16[16,64,512]{2,1,0:T(8,128)(2,1)} %broadcast_in_dim.8), calls=%async_computation.3 | async-start | bytes 2097152 | tf_op jit(solution)/shard_map/all_to_all | solution.py:36
  91.9 2.8 %collective-permute-start.17 = (bf16[128,128]{1,0:T(8,128)(2,1)S(1)}, bf16[128,128]{1,0:T(8,128)(2,1)S(1)}, u32[]{:S(2)}, u32[]{:S(2)}) collective-permute-start(bf16[128,128]{1,0:T(8,128)(2,1)S(1)} %attend1.1.a0), channel_id=1, source_target_pairs={{0,6},{2,0},{4,2},{6,4},{1,7},{3,1},{5,3},{7,5},{8,14},{10,8},{12,... | collective-permute-start | bytes 98312 | tf_op jit(solution)/shard_map/ppermute | solution.py:27
  92.9 4.3 %collective-permute-start.16 = (bf16[128,128]{1,0:T(8,128)(2,1)S(1)}, bf16[128,128]{1,0:T(8,128)(2,1)S(1)}, u32[]{:S(2)}, u32[]{:S(2)}) collective-permute-start(bf16[128,128]{1,0:T(8,128)(2,1)S(1)} %attend1.1.a0), channel_id=1, source_target_pairs={{0,4},{2,6},{4,0},{6,2},{1,5},{3,7},{5,1},{7,3},{8,12},{10,14},{12... | collective-permute-start | bytes 98312 | tf_op jit(solution)/shard_map/ppermute | solution.py:27
  94.0 4.3 %collective-permute-start.15 = (bf16[128,128]{1,0:T(8,128)(2,1)S(1)}, bf16[128,128]{1,0:T(8,128)(2,1)S(1)}, u32[]{:S(2)}, u32[]{:S(2)}) collective-permute-start(bf16[128,128]{1,0:T(8,128)(2,1)S(1)} %attend1.1.a0), channel_id=1, source_target_pairs={{0,2},{2,4},{4,6},{6,0},{1,3},{3,5},{5,7},{7,1},{8,10},{10,12},{12... | collective-permute-start | bytes 98312 | tf_op jit(solution)/shard_map/ppermute | solution.py:27
  98.8 5.4 %collective-permute-start.18 = (bf16[128,1024]{1,0:T(8,128)(2,1)S(1)}, bf16[128,1024]{1,0:T(8,128)(2,1)S(1)}, u32[]{:S(2)}, u32[]{:S(2)}) collective-permute-start(bf16[128,1024]{1,0:T(8,128)(2,1)S(1)} %project1.1.mine), channel_id=1, source_target_pairs={{0,1},{1,0},{2,3},{3,2},{4,5},{5,4},{6,7},{7,6},{8,9},{9,8},{10,11... | collective-permute-start | bytes 786440 | tf_op jit(solution)/shard_map/ppermute | solution.py:44
  105.9 5.3 %collective-permute-start.20 = (bf16[128,256]{1,0:T(8,128)(2,1)S(1)}, bf16[128,256]{1,0:T(8,128)(2,1)S(1)}, u32[]{:S(2)}, u32[]{:S(2)}) collective-permute-start(bf16[128,256]{1,0:T(8,128)(2,1)S(1)} %get-tuple-element.44.refs_2_), channel_id=1, source_target_pairs={{8,0},{16,8},{24,16},{32,24},{40,32},{48,40},{56,48},{64,56},{72,6... | collective-permute-start | bytes 196616 | tf_op jit(solution)/shard_map/ppermute | solution.py:52
  109.0 7.1 %collective-permute-start.19 = (bf16[128,256]{1,0:T(8,128)(2,1)S(1)}, bf16[128,256]{1,0:T(8,128)(2,1)S(1)}, u32[]{:S(2)}, u32[]{:S(2)}) collective-permute-start(bf16[128,256]{1,0:T(8,128)(2,1)S(1)} %get-tuple-element.44.refs_2_), channel_id=1, source_target_pairs={{0,8},{8,16},{16,24},{24,32},{32,40},{40,48},{48,56},{56,64},{64,7... | collective-permute-start | bytes 196616 | tf_op jit(solution)/shard_map/ppermute | solution.py:48
  117.1 5.1 %collective-permute-start.21 = (bf16[128,256]{1,0:T(8,128)(2,1)S(1)}, bf16[128,256]{1,0:T(8,128)(2,1)S(1)}, u32[]{:S(2)}, u32[]{:S(2)}) collective-permute-start(bf16[128,256]{1,0:T(8,128)(2,1)S(1)} %get-tuple-element.46), channel_id=1, source_target_pairs={{0,2},{2,4},{4,6},{6,0},{1,3},{3,5},{5,7},{7,1},{8,10},{10,12},{12... | collective-permute-start | bytes 196616 | tf_op jit(solution)/shard_map/ppermute | solution.py:258
  117.2 5.0 %collective-permute-start.22 = (bf16[128,256]{1,0:T(8,128)(2,1)S(1)}, bf16[128,256]{1,0:T(8,128)(2,1)S(1)}, u32[]{:S(2)}, u32[]{:S(2)}) collective-permute-start(bf16[128,256]{1,0:T(8,128)(2,1)S(1)} %get-tuple-element.47), channel_id=1, source_target_pairs={{0,4},{2,6},{4,0},{6,2},{1,5},{3,7},{5,1},{7,3},{8,12},{10,14},{12... | collective-permute-start | bytes 196616 | tf_op jit(solution)/shard_map/ppermute | solution.py:260
  118.9 3.9 %collective-permute-start.23 = (bf16[128,256]{1,0:T(8,128)(2,1)S(1)}, bf16[128,256]{1,0:T(8,128)(2,1)S(1)}, u32[]{:S(2)}, u32[]{:S(2)}) collective-permute-start(bf16[128,256]{1,0:T(8,128)(2,1)S(1)} %get-tuple-element.48), channel_id=1, source_target_pairs={{0,6},{2,0},{4,2},{6,4},{1,7},{3,1},{5,3},{7,5},{8,14},{10,8},{12,... | collective-permute-start | bytes 196616 | tf_op jit(solution)/shard_map/ppermute | solution.py:259
  122.8 6.2 %collective-permute-start.24 = (f32[128,128]{1,0:T(8,128)S(1)}, f32[128,128]{1,0:T(8,128)S(1)}, u32[]{:S(2)}, u32[]{:S(2)}) collective-permute-start(f32[128,128]{1,0:T(8,128)S(1)} %get-tuple-element.50), channel_id=1, source_target_pairs={{0,1},{1,0},{2,3},{3,2},{4,5},{5,4},{6,7},{7,6},{8,9},{9,8},{10,11... | collective-permute-start | bytes 196616 | tf_op jit(solution)/shard_map/ppermute | solution.py:44

commit v3 on v2

--- a/solution.py
+++ b/solution.py
@@ -1,3 +1,5 @@
+import functools
+
 import jax
 import jax.numpy as jnp
 from jax import lax
@@ -32,8 +34,7 @@
 
 
 def gather_rows(a):
-    many = a if a.ndim == 3 else jnp.broadcast_to(a[None], (16,) + a.shape)
-    return lax.all_to_all(many, SP, 0, 0, tiled=True).reshape(1024, 512)
+    return lax.all_to_all(a, SP, 0, 0, tiled=True).reshape(1024, 512)
 
 
 def after_this(a, done):
@@ -94,7 +95,10 @@
     payload[128:144, :] = jnp.broadcast_to((docs_in[...] + 1).astype(F32).astype(BF16), (16, 128))
 
 
-def table_body(bias, before, own, after, table, wide):
+def table_body(bias, before, own, after, rest, table, many1, many2, wide):
+    for n in range(16):
+        many1[n] = rest[0]
+        many2[n] = rest[1]
     own_docs = own[128:144, :].astype(F32)[0:1]
     query_docs = jnp.broadcast_to(own_docs, (128, 128)).T
     key_docs = jnp.concatenate(
@@ -162,7 +166,7 @@
     kv[:, 128:256] = acc[:, 256:384].astype(BF16)
 
 
-def heads_pieces_body(x0, x1, x2, x3, gain, weights, q, kv):
+def heads_pieces_body(x0, x1, x2, x3, gain, weights, q, kv, *, layer):
     pieces = [x[...].astype(F32) for x in (x0, x1, x2, x3)]
     total = sum(p * p for p in pieces)
     scale = lax.rsqrt(jnp.sum(total, axis=1, keepdims=True) * (1.0 / 1024) + EPS)
@@ -170,17 +174,9 @@
     for k in range(4):
         block = behind("y", k)
         at = pl.ds(pl.multiple_of(block * 256, 256), 256)
-        normed = (pieces[k] * scale * gain[1:2, at]).astype(BF16)
+        normed = (pieces[k] * scale * gain[layer : layer + 1, at]).astype(BF16)
         rows = weights[at, 0:384]
         acc = acc + jnp.dot(normed, rows, preferred_element_type=F32)
-    finish_heads(acc, q, kv)
-
-
-def heads_whole_body(mine, theirs, gain, weights, q, kv):
-    stream = (mine[...].astype(F32) + theirs[...].astype(F32)).astype(BF16).astype(F32)
-    scale = lax.rsqrt(jnp.sum(stream * stream, axis=1, keepdims=True) * (1.0 / 1024) + EPS)
-    normed = (stream * scale * gain[2:3, :]).astype(BF16)
-    acc = jnp.dot(normed, weights[:, 0:384], preferred_element_type=F32)
     finish_heads(acc, q, kv)
 
 
@@ -219,22 +215,6 @@
     attend_scatter_body(q, kv.at[0:128], kv.at[128:256], kv.at[256:384], *rest, layer=0)
 
 
-def attend_last_body(*refs):
-    attend_scatter_body(*refs, layer=2)
-
-
-def attend_body(q, before, own, after, table, out):
-    parts = [(p[:, 0:128], p[:, 128:256]) for p in (before, own, after)]
-    out[...] = attend(q, parts, table.at[2:4])
-
-
-def project_body(a0, a1, a2, a3, w, out):
-    acc = 0.0
-    for k, a in enumerate((a0, a1, a2, a3)):
-        acc = acc + lax.dot_general(a[...], w[behind("y", k)], NT, preferred_element_type=F32)
-    out[...] = acc.astype(BF16)
-
-
 def sum_body(kept, r1, r2, r3, out):
     out[...] = kept[...] + r1[...].astype(F32) + r2[...].astype(F32) + r3[...].astype(F32)
 
@@ -282,13 +262,14 @@
         scratch=[pltpu.VMEM((3, 64, 128), BF16)] * 4
         + [pltpu.VMEM((1, 128), jnp.int32), pltpu.SemaphoreType.DMA((6,))],
     )
-    weights0 = gather_rows(first)
     before = from_before(payload)
     after = from_after(payload)
+    weights0 = gather_rows(after_this(first, (before, after)))
     near = jnp.concatenate([before[0:128], payload[0:128], after[0:128]], axis=0)
     near_y = jnp.stack(in_order(near, spread(near, "y")))
-    table = call(
-        table_body, shaped(6, 128, 384, dtype=F32), offset_bias, before, payload, after,
+    table, many1, many2 = call(
+        table_body, [shaped(6, 128, 384, dtype=F32)] + [shaped(16, 64, 512)] * 2,
+        offset_bias, before, payload, after, rest,
         scratch=[pltpu.VMEM((8, 256), F32)], name="table",
     )
     near_partner = swap(after_this(near_y, table))
@@ -297,33 +278,26 @@
         heads_first_body, [shaped(128, 128), shaped(384, 256)],
         near_y, near_partner, norm_gain, weights0, name="heads0",
     )
-    weights1 = gather_rows(after_this(rest[0], q))
-    kept, r1, r2, r3 = scattered(attend_first_body, q, kv, table, weights0)
-    half = call(sum_body, shaped(128, 256, dtype=F32), kept, r1, r2, r3, name="sum0")
-    stream = call(pair_sum_body, shaped(128, 256), half, swap(half), name="pair0")
-    pieces = in_order(stream, spread(stream, "y"))
-
-    q, kv = call(
-        heads_pieces_body, [shaped(128, 128), shaped(128, 256)],
-        *pieces, norm_gain, weights1, name="heads1",
-    )
-    out1 = jnp.broadcast_to(after_this(weights1, q)[None, :, 384:512], (4, 1024, 128))
-    out1_y = lax.all_to_all(out1, "y", 0, 0, tiled=True)
-    before, after = from_before(kv), from_after(kv)
-    weights2 = gather_rows(after_this(rest[1], (before, after)))
-    attended = call(attend_body, shaped(128, 128), q, before, kv, after, table, name="attend1")
-    attended_y = in_order(attended, spread(attended, "y"))
-    share = call(project_body, shaped(128, 1024), *attended_y, out1_y, name="project1")
-    q, kv = call(
-        heads_whole_body, [shaped(128, 128), shaped(128, 256)],
-        share, swap(share), norm_gain, weights2, name="heads2",
-    )
-    before, after = from_before(kv), from_after(kv)
-    kept, r1, r2, r3 = scattered(attend_last_body, q, before, kv, after, table, weights2)
+    weights = weights0
+    body, args = attend_first_body, (q, kv)
+    for layer, many in ((1, many1), (2, many2)):
+        kept, r1, r2, r3 = scattered(body, *args, table, weights)
+        weights = gather_rows(after_this(many, kept))
+        half = call(sum_body, shaped(128, 256, dtype=F32), kept, r1, r2, r3, name="sum")
+        stream = call(pair_sum_body, shaped(128, 256), half, swap(half), name="pair")
+        pieces = in_order(stream, spread(stream, "y"))
+        q, kv = call(
+            functools.partial(heads_pieces_body, layer=layer),
+            [shaped(128, 128), shaped(128, 256)],
+            *pieces, norm_gain, weights, name="heads",
+        )
+        body = functools.partial(attend_scatter_body, layer=layer)
+        args = (q, from_before(kv), kv, from_after(kv))
+    kept, r1, r2, r3 = scattered(body, *args, table, weights)
     mine, theirs = call(
-        split_body, [shaped(128, 128, dtype=F32)] * 2, kept, r1, r2, r3, name="split2"
-    )
-    return call(pair_sum_body, shaped(128, 128), mine, swap(theirs), name="pair2")
+        split_body, [shaped(128, 128, dtype=F32)] * 2, kept, r1, r2, r3, name="split"
+    )
+    return call(pair_sum_body, shaped(128, 128), mine, swap(theirs), name="pair_last")
 
 
 def solution(mesh):

time: 130 us -> 123 us (0.946)
  local copies, waits for them, and re-layouts: 3.99 us -> 0.02 us
  waiting for transfers between devices: 46.7 us -> 42.9 us
    all_to_all x4 -> x3, starting transfers between devices: 22.5 us -> 15.2 us  [gather_rows(): return lax.all_to_all(a, SP, 0, 0, tiled=True).reshape(1024, 512)]
    ppermute x3, waiting for transfers between devices: 5.94 us -> 0.01 us  [from_after(): return lax.ppermute(a, SP, [(i + 1, i) for i in range(15)])]
    broadcast_in_dim x3 -> x0, local copies, waits for them, and re-layouts: 3.3 us -> none  [the longest x2 2.18 us: gather_rows(): many = a if a.ndim == 3 else jnp.broadcast_to(a[None], (16,) + a.shape)]
    ppermute x2 -> x3, starting transfers between devices: 0.93 us -> 3.75 us  [scattered(): r3 = lax.ppermute(s3, 'y', turn(3))]
    all_to_all x4 -> x3, waiting for transfers between devices: 3.51 us -> 1.14 us  [gather_rows(): return lax.all_to_all(a, SP, 0, 0, tiled=True).reshape(1024, 512)]
    ppermute x9, starting transfers between devices: 9.97 us -> 11.8 us  [spread(): return [lax.ppermute(a, axis, turn(k)) for k in (1, 3, 2)]]
    ppermute x4, starting transfers between devices: 13 us -> 14.7 us  [swap(): return lax.ppermute(a, 'c', [(0, 1), (1, 0)])]
    ppermute x9, waiting for transfers between devices: 11.5 us -> 13.2 us  [spread(): return [lax.ppermute(a, axis, turn(k)) for k in (1, 3, 2)]]
  transfers between devices with their start and end apart: 29 -> 31, of which waited for: 22 -> 22; matrix products, arithmetic and copies ran while one was open for 1% -> 0% of each run, Pallas kernels for 2% -> 2%
where the time goes in v3:
time: 123 us
  starting transfers between devices  70 us (57%)
  waiting for transfers between devices  42.9 us (35%)
  Pallas kernels  9.49 us (8%)
    ppermute x3, waiting for transfers between devices, from_before(): return lax.ppermute(a, SP, [(i, i + 1) for i in range(15)])  15.2 us
    all_to_all x3, starting transfers between devices, gather_rows(): return lax.all_to_all(a, SP, 0, 0, tiled=True).reshape(1024, 512)  15.2 us
    ppermute x4, starting transfers between devices, swap(): return lax.ppermute(a, 'c', [(0, 1), (1, 0)])  14.7 us
    ppermute x9, waiting for transfers between devices, spread(): return [lax.ppermute(a, axis, turn(k)) for k in (1, 3, 2)]  13.2 us
    ppermute x3, starting transfers between devices, from_after(): return lax.ppermute(a, SP, [(i + 1, i) for i in range(15)])  12.5 us
    ppermute x9, starting transfers between devices, spread(): return [lax.ppermute(a, axis, turn(k)) for k in (1, 3, 2)]  11.8 us
    pallas_call x14, Pallas kernels, call(): pl.pallas_call(body, out_shape=outs, **specs, scratch_shapes=list(scratch...  9.49 us
    ppermute x3, starting transfers between devices, from_before(): return lax.ppermute(a, SP, [(i, i + 1) for i in range(15)])  5.76 us
  transfers between devices with their start and end apart: 31, of which 22 were waited for; matrix products, arithmetic and copies ran while one was open for 0% of the time, Pallas kernels for 2%

profile of v3, /device:TPU:33, one launch (start us, length us, event | category | flops | bytes accessed | tf_op | source)
XLA Modules:
  0.0 122.7 jit_solution(10622433584765311330)
XLA Ops:
  0.0 2.0 %pack.1 = (bf16[16,64,512]{2,1,0:T(8,128)(2,1)}, bf16[2,64,512]{2,1,0:T(8,128)(2,1)S(1)}, bf16[144,128]{1,0:T(8,128)(2,1)S(1)}) custom-call(bf16[3,64,128]{2,1,0:T(8,128)(2,1)} %wq.1, bf16[3,64,128]{2,1,0:T(8,128)(2,1)} %wk.1, bf16[3,64,128]{2,1,0:T(8,128)(2,1)} %wv.1, bf16[3,64,128]{2,1,0:T(8,128)(2,1)} %bitcast.19, bf16[128,128]{1,0:T(8,128)(2,1)} %tokens.1, ...), custom_call_target="tpu_custom_call" | custom-call | tf_op jit(solution)/shard_map/pack/pallas_call | solution.py:65
  2.1 3.9 %collective-permute-start.1 = (bf16[144,128]{1,0:T(8,128)(2,1)S(1)}, bf16[144,128]{1,0:T(8,128)(2,1)S(1)}, u32[]{:S(2)}, u32[]{:S(2)}) collective-permute-start(bf16[144,128]{1,0:T(8,128)(2,1)S(1)} %get-tuple-element.35.own), channel_id=1, source_target_pairs={{8,0},{16,8},{24,16},{32,24},{40,32},{48,40},{56,48},{64,56},{72,6... | collective-permute-start | bytes 110600 | tf_op jit(solution)/shard_map/ppermute | solution.py:53
  6.0 1.9 %collective-permute-start = (bf16[144,128]{1,0:T(8,128)(2,1)S(1)}, bf16[144,128]{1,0:T(8,128)(2,1)S(1)}, u32[]{:S(2)}, u32[]{:S(2)}) collective-permute-start(bf16[144,128]{1,0:T(8,128)(2,1)S(1)} %get-tuple-element.35.own), channel_id=1, source_target_pairs={{0,8},{8,16},{16,24},{24,32},{32,40},{40,48},{48,56},{56,64},{64,7... | collective-permute-start | bytes 110600 | tf_op jit(solution)/shard_map/ppermute | solution.py:49
  7.9 4.9 %collective-permute-done.before = bf16[144,128]{1,0:T(8,128)(2,1)S(1)} collective-permute-done((bf16[144,128]{1,0:T(8,128)(2,1)S(1)}, bf16[144,128]{1,0:T(8,128)(2,1)S(1)}, u32[]{:S(2)}, u32[]{:S(2)}) %collective-permute-start) | collective-permute-done | bytes 36896 | tf_op jit(solution)/shard_map/ppermute | solution.py:49
  12.8 5.3 %all-to-all-start = ((bf16[16,64,512]{2,1,0:T(8,128)(2,1)}), bf16[16,64,512]{2,1,0:T(8,128)(2,1)S(1)}, u32[]{:S(2)}, u32[]{:S(2)}) async-start(bf16[16,64,512]{2,1,0:T(8,128)(2,1)} %get-tuple-element.40), calls=%async_computation | async-start | bytes 2097152 | tf_op jit(solution)/shard_map/all_to_all | solution.py:37
  18.2 3.0 %collective-permute-start.3 = (bf16[384,128]{1,0:T(8,128)(2,1)S(1)}, bf16[384,128]{1,0:T(8,128)(2,1)S(1)}, u32[]{:S(2)}, u32[]{:S(2)}) collective-permute-start(bf16[384,128]{1,0:T(8,128)(2,1)S(1)} %get-tuple-element.66), channel_id=1, source_target_pairs={{0,4},{2,6},{4,0},{6,2},{1,5},{3,7},{5,1},{7,3},{8,12},{10,14},{12... | collective-permute-start | bytes 294920 | tf_op jit(solution)/shard_map/ppermute | solution.py:29
  21.6 2.3 %collective-permute-start.4 = (bf16[384,128]{1,0:T(8,128)(2,1)S(1)}, bf16[384,128]{1,0:T(8,128)(2,1)S(1)}, u32[]{:S(2)}, u32[]{:S(2)}) collective-permute-start(bf16[384,128]{1,0:T(8,128)(2,1)S(1)} %get-tuple-element.66), channel_id=1, source_target_pairs={{0,6},{2,0},{4,2},{6,4},{1,7},{3,1},{5,3},{7,5},{8,14},{10,8},{12,... | collective-permute-start | bytes 294920 | tf_op jit(solution)/shard_map/ppermute | solution.py:29
  23.9 1.9 %table.1 = (f32[6,128,384]{2,1,0:T(8,128)S(1)}, bf16[16,64,512]{2,1,0:T(8,128)(2,1)}, bf16[16,64,512]{2,1,0:T(8,128)(2,1)}) custom-call(f32[3,2,8,16]{3,2,1,0:T(8,128)S(1)} %copy-done.1, bf16[144,128]{1,0:T(8,128)(2,1)S(1)} %collective-permute-done.before, bf16[144,128]{1,0:T(8,128)(2,1)S(1)} %get-tuple-element.35.own, ...), custom_call_target="tpu_custom_call" | custom-call | tf_op jit(solution)/shard_map/table/pallas_call | solution.py:65
  27.3 2.8 %collective-permute-start.5 = (bf16[4,384,128]{2,1,0:T(8,128)(2,1)S(1)}, bf16[4,384,128]{2,1,0:T(8,128)(2,1)S(1)}, u32[]{:S(2)}, u32[]{:S(2)}) collective-permute-start(bf16[4,384,128]{2,1,0:T(8,128)(2,1)S(1)} %pad_maximum_fusion.own), channel_id=1, source_target_pairs={{0,1},{1,0},{2,3},{3,2},{4,5},{5,4},{6,7},{7,6},{8,9},{9,8},{10,11... | collective-permute-start | bytes 1179656 | tf_op jit(solution)/shard_map/ppermute | solution.py:45
  34.5 5.5 %all-to-all-start.1 = ((bf16[16,64,512]{2,1,0:T(8,128)(2,1)}), bf16[16,64,512]{2,1,0:T(8,128)(2,1)S(1)}, u32[]{:S(2)}, u32[]{:S(2)}) async-start(bf16[16,64,512]{2,1,0:T(8,128)(2,1)} %get-tuple-element.48), calls=%async_computation.1 | async-start | bytes 2097152 | tf_op jit(solution)/shard_map/all_to_all | solution.py:37
  40.9 3.3 %collective-permute-start.7 = (bf16[128,256]{1,0:T(8,128)(2,1)S(1)}, bf16[128,256]{1,0:T(8,128)(2,1)S(1)}, u32[]{:S(2)}, u32[]{:S(2)}) collective-permute-start(bf16[128,256]{1,0:T(8,128)(2,1)S(1)} %get-tuple-element.45), channel_id=1, source_target_pairs={{0,4},{2,6},{4,0},{6,2},{1,5},{3,7},{5,1},{7,3},{8,12},{10,14},{12... | collective-permute-start | bytes 196616 | tf_op jit(solution)/shard_map/ppermute | solution.py:240
  44.7 1.9 %collective-permute-done.7.r2 = bf16[128,256]{1,0:T(8,128)(2,1)S(1)} collective-permute-done((bf16[128,256]{1,0:T(8,128)(2,1)S(1)}, bf16[128,256]{1,0:T(8,128)(2,1)S(1)}, u32[]{:S(2)}, u32[]{:S(2)}) %collective-permute-start.7) | collective-permute-done | bytes 65568 | tf_op jit(solution)/shard_map/ppermute | solution.py:240
  47.7 4.1 %collective-permute-start.9 = (f32[128,256]{1,0:T(8,128)S(1)}, f32[128,256]{1,0:T(8,128)S(1)}, u32[]{:S(2)}, u32[]{:S(2)}) collective-permute-start(f32[128,256]{1,0:T(8,128)S(1)} %sum.2.mine), channel_id=1, source_target_pairs={{0,1},{1,0},{2,3},{3,2},{4,5},{5,4},{6,7},{7,6},{8,9},{9,8},{10,11... | collective-permute-start | bytes 393224 | tf_op jit(solution)/shard_map/ppermute | solution.py:45
  52.8 2.4 %collective-permute-start.12 = (bf16[128,256]{1,0:T(8,128)(2,1)S(1)}, bf16[128,256]{1,0:T(8,128)(2,1)S(1)}, u32[]{:S(2)}, u32[]{:S(2)}) collective-permute-start(bf16[128,256]{1,0:T(8,128)(2,1)S(1)} %pair.2.x0), channel_id=1, source_target_pairs={{0,6},{2,0},{4,2},{6,4},{1,7},{3,1},{5,3},{7,5},{8,14},{10,8},{12,... | collective-permute-start | bytes 196616 | tf_op jit(solution)/shard_map/ppermute | solution.py:29
  55.8 2.2 %collective-permute-done.12.x3 = bf16[128,256]{1,0:T(8,128)(2,1)S(1)} collective-permute-done((bf16[128,256]{1,0:T(8,128)(2,1)S(1)}, bf16[128,256]{1,0:T(8,128)(2,1)S(1)}, u32[]{:S(2)}, u32[]{:S(2)}) %collective-permute-start.12) | collective-permute-done | bytes 65568 | tf_op jit(solution)/shard_map/ppermute | solution.py:29
  59.7 1.8 %collective-permute-done.10.x1 = bf16[128,256]{1,0:T(8,128)(2,1)S(1)} collective-permute-done((bf16[128,256]{1,0:T(8,128)(2,1)S(1)}, bf16[128,256]{1,0:T(8,128)(2,1)S(1)}, u32[]{:S(2)}, u32[]{:S(2)}) %collective-permute-start.10) | collective-permute-done | bytes 65568 | tf_op jit(solution)/shard_map/ppermute | solution.py:29
  62.1 4.3 %collective-permute-start.14 = (bf16[128,256]{1,0:T(8,128)(2,1)S(1)}, bf16[128,256]{1,0:T(8,128)(2,1)S(1)}, u32[]{:S(2)}, u32[]{:S(2)}) collective-permute-start(bf16[128,256]{1,0:T(8,128)(2,1)S(1)} %get-tuple-element.50.own), channel_id=1, source_target_pairs={{8,0},{16,8},{24,16},{32,24},{40,32},{48,40},{56,48},{64,56},{72,6... | collective-permute-start | bytes 196616 | tf_op jit(solution)/shard_map/ppermute | solution.py:53
  66.4 1.9 %collective-permute-start.13 = (bf16[128,256]{1,0:T(8,128)(2,1)S(1)}, bf16[128,256]{1,0:T(8,128)(2,1)S(1)}, u32[]{:S(2)}, u32[]{:S(2)}) collective-permute-start(bf16[128,256]{1,0:T(8,128)(2,1)S(1)} %get-tuple-element.50.own), channel_id=1, source_target_pairs={{0,8},{8,16},{16,24},{24,32},{32,40},{40,48},{48,56},{56,64},{64,7... | collective-permute-start | bytes 196616 | tf_op jit(solution)/shard_map/ppermute | solution.py:49
  68.3 5.2 %collective-permute-done.13.before = bf16[128,256]{1,0:T(8,128)(2,1)S(1)} collective-permute-done((bf16[128,256]{1,0:T(8,128)(2,1)S(1)}, bf16[128,256]{1,0:T(8,128)(2,1)S(1)}, u32[]{:S(2)}, u32[]{:S(2)}) %collective-permute-start.13) | collective-permute-done | bytes 65568 | tf_op jit(solution)/shard_map/ppermute | solution.py:49
  74.4 4.3 %all-to-all-start.2 = ((bf16[16,64,512]{2,1,0:T(8,128)(2,1)}), bf16[16,64,512]{2,1,0:T(8,128)(2,1)S(1)}, u32[]{:S(2)}, u32[]{:S(2)}) async-start(bf16[16,64,512]{2,1,0:T(8,128)(2,1)} %get-tuple-element.56), calls=%async_computation.2 | async-start | bytes 2097152 | tf_op jit(solution)/shard_map/all_to_all | solution.py:37
  81.4 2.3 %collective-permute-done.15.r1 = bf16[128,256]{1,0:T(8,128)(2,1)S(1)} collective-permute-done((bf16[128,256]{1,0:T(8,128)(2,1)S(1)}, bf16[128,256]{1,0:T(8,128)(2,1)S(1)}, u32[]{:S(2)}, u32[]{:S(2)}) %collective-permute-start.15) | collective-permute-done | bytes 65568 | tf_op jit(solution)/shard_map/ppermute | solution.py:238
  84.7 4.0 %collective-permute-start.18 = (f32[128,256]{1,0:T(8,128)S(1)}, f32[128,256]{1,0:T(8,128)S(1)}, u32[]{:S(2)}, u32[]{:S(2)}) collective-permute-start(f32[128,256]{1,0:T(8,128)S(1)} %sum.3.mine), channel_id=1, source_target_pairs={{0,1},{1,0},{2,3},{3,2},{4,5},{5,4},{6,7},{7,6},{8,9},{9,8},{10,11... | collective-permute-start | bytes 393224 | tf_op jit(solution)/shard_map/ppermute | solution.py:45
  89.7 2.5 %collective-permute-start.21 = (bf16[128,256]{1,0:T(8,128)(2,1)S(1)}, bf16[128,256]{1,0:T(8,128)(2,1)S(1)}, u32[]{:S(2)}, u32[]{:S(2)}) collective-permute-start(bf16[128,256]{1,0:T(8,128)(2,1)S(1)} %pair.3.x0), channel_id=1, source_target_pairs={{0,6},{2,0},{4,2},{6,4},{1,7},{3,1},{5,3},{7,5},{8,14},{10,8},{12,... | collective-permute-start | bytes 196616 | tf_op jit(solution)/shard_map/ppermute | solution.py:29
  92.8 2.2 %collective-permute-done.21.x3 = bf16[128,256]{1,0:T(8,128)(2,1)S(1)} collective-permute-done((bf16[128,256]{1,0:T(8,128)(2,1)S(1)}, bf16[128,256]{1,0:T(8,128)(2,1)S(1)}, u32[]{:S(2)}, u32[]{:S(2)}) %collective-permute-start.21) | collective-permute-done | bytes 65568 | tf_op jit(solution)/shard_map/ppermute | solution.py:29
  95.1 1.7 %collective-permute-done.20.x2 = bf16[128,256]{1,0:T(8,128)(2,1)S(1)} collective-permute-done((bf16[128,256]{1,0:T(8,128)(2,1)S(1)}, bf16[128,256]{1,0:T(8,128)(2,1)S(1)}, u32[]{:S(2)}, u32[]{:S(2)}) %collective-permute-start.20) | collective-permute-done | bytes 65568 | tf_op jit(solution)/shard_map/ppermute | solution.py:29
  96.8 2.0 %collective-permute-done.19.x1 = bf16[128,256]{1,0:T(8,128)(2,1)S(1)} collective-permute-done((bf16[128,256]{1,0:T(8,128)(2,1)S(1)}, bf16[128,256]{1,0:T(8,128)(2,1)S(1)}, u32[]{:S(2)}, u32[]{:S(2)}) %collective-permute-start.19) | collective-permute-done | bytes 65568 | tf_op jit(solution)/shard_map/ppermute | solution.py:29
  99.3 4.3 %collective-permute-start.23 = (bf16[128,256]{1,0:T(8,128)(2,1)S(1)}, bf16[128,256]{1,0:T(8,128)(2,1)S(1)}, u32[]{:S(2)}, u32[]{:S(2)}) collective-permute-start(bf16[128,256]{1,0:T(8,128)(2,1)S(1)} %get-tuple-element.58.own), channel_id=1, source_target_pairs={{8,0},{16,8},{24,16},{32,24},{40,32},{48,40},{56,48},{64,56},{72,6... | collective-permute-start | bytes 196616 | tf_op jit(solution)/shard_map/ppermute | solution.py:53
  103.6 1.9 %collective-permute-start.22 = (bf16[128,256]{1,0:T(8,128)(2,1)S(1)}, bf16[128,256]{1,0:T(8,128)(2,1)S(1)}, u32[]{:S(2)}, u32[]{:S(2)}) collective-permute-start(bf16[128,256]{1,0:T(8,128)(2,1)S(1)} %get-tuple-element.58.own), channel_id=1, source_target_pairs={{0,8},{8,16},{16,24},{24,32},{32,40},{40,48},{48,56},{56,64},{64,7... | collective-permute-start | bytes 196616 | tf_op jit(solution)/shard_map/ppermute | solution.py:49
  105.5 5.2 %collective-permute-done.22.before = bf16[128,256]{1,0:T(8,128)(2,1)S(1)} collective-permute-done((bf16[128,256]{1,0:T(8,128)(2,1)S(1)}, bf16[128,256]{1,0:T(8,128)(2,1)S(1)}, u32[]{:S(2)}, u32[]{:S(2)}) %collective-permute-start.22) | collective-permute-done | bytes 65568 | tf_op jit(solution)/shard_map/ppermute | solution.py:49
  112.6 1.8 %collective-permute-start.26 = (bf16[128,256]{1,0:T(8,128)(2,1)S(1)}, bf16[128,256]{1,0:T(8,128)(2,1)S(1)}, u32[]{:S(2)}, u32[]{:S(2)}) collective-permute-start(bf16[128,256]{1,0:T(8,128)(2,1)S(1)} %get-tuple-element.62), channel_id=1, source_target_pairs={{0,6},{2,0},{4,2},{6,4},{1,7},{3,1},{5,3},{7,5},{8,14},{10,8},{12,... | collective-permute-start | bytes 196616 | tf_op jit(solution)/shard_map/ppermute | solution.py:239
  114.5 2.3 %collective-permute-done.24.r1 = bf16[128,256]{1,0:T(8,128)(2,1)S(1)} collective-permute-done((bf16[128,256]{1,0:T(8,128)(2,1)S(1)}, bf16[128,256]{1,0:T(8,128)(2,1)S(1)}, u32[]{:S(2)}, u32[]{:S(2)}) %collective-permute-start.24) | collective-permute-done | bytes 65568 | tf_op jit(solution)/shard_map/ppermute | solution.py:238
  117.4 3.8 %collective-permute-start.27 = (f32[128,128]{1,0:T(8,128)S(1)}, f32[128,128]{1,0:T(8,128)S(1)}, u32[]{:S(2)}, u32[]{:S(2)}) collective-permute-start(f32[128,128]{1,0:T(8,128)S(1)} %get-tuple-element.64), channel_id=1, source_target_pairs={{0,1},{1,0},{2,3},{3,2},{4,5},{5,4},{6,7},{7,6},{8,9},{9,8},{10,11... | collective-permute-start | bytes 196616 | tf_op jit(solution)/shard_map/ppermute | solution.py:45
  (53 shorter events, 23.4 us)
Async XLA Ops:
  2.1 5.9 %collective-permute-start.1 = (bf16[144,128]{1,0:T(8,128)(2,1)S(1)}, bf16[144,128]{1,0:T(8,128)(2,1)S(1)}, u32[]{:S(2)}, u32[]{:S(2)}) collective-permute-start(bf16[144,128]{1,0:T(8,128)(2,1)S(1)} %get-tuple-element.35.own), channel_id=1, source_target_pairs={{8,0},{16,8},{24,16},{32,24},{40,32},{48,40},{56,48},{64,56},{72,6... | collective-permute-start | bytes 110600 | tf_op jit(solution)/shard_map/ppermute | solution.py:53
  6.0 6.8 %collective-permute-start = (bf16[144,128]{1,0:T(8,128)(2,1)S(1)}, bf16[144,128]{1,0:T(8,128)(2,1)S(1)}, u32[]{:S(2)}, u32[]{:S(2)}) collective-permute-start(bf16[144,128]{1,0:T(8,128)(2,1)S(1)} %get-tuple-element.35.own), channel_id=1, source_target_pairs={{0,8},{8,16},{16,24},{24,32},{32,40},{40,48},{48,56},{56,64},{64,7... | collective-permute-start | bytes 110600 | tf_op jit(solution)/shard_map/ppermute | solution.py:49
  12.8 19.8 %all-to-all-start = ((bf16[16,64,512]{2,1,0:T(8,128)(2,1)}), bf16[16,64,512]{2,1,0:T(8,128)(2,1)S(1)}, u32[]{:S(2)}, u32[]{:S(2)}) async-start(bf16[16,64,512]{2,1,0:T(8,128)(2,1)} %get-tuple-element.40), calls=%async_computation | async-start | bytes 2097152 | tf_op jit(solution)/shard_map/all_to_all | solution.py:37
  18.1 14.5 %copy-start = (f32[3,1024]{1,0:T(4,128)S(1)}, f32[3,1024]{1,0:T(4,128)}, u32[]{:S(2)}) copy-start(f32[3,1024]{1,0:T(4,128)} %gain.5) | copy-start | bytes 36868
  18.2 7.5 %collective-permute-start.3 = (bf16[384,128]{1,0:T(8,128)(2,1)S(1)}, bf16[384,128]{1,0:T(8,128)(2,1)S(1)}, u32[]{:S(2)}, u32[]{:S(2)}) collective-permute-start(bf16[384,128]{1,0:T(8,128)(2,1)S(1)} %get-tuple-element.66), channel_id=1, source_target_pairs={{0,4},{2,6},{4,0},{6,2},{1,5},{3,7},{5,1},{7,3},{8,12},{10,14},{12... | collective-permute-start | bytes 294920 | tf_op jit(solution)/shard_map/ppermute | solution.py:29
  21.2 6.0 %collective-permute-start.2 = (bf16[384,128]{1,0:T(8,128)(2,1)S(1)}, bf16[384,128]{1,0:T(8,128)(2,1)S(1)}, u32[]{:S(2)}, u32[]{:S(2)}) collective-permute-start(bf16[384,128]{1,0:T(8,128)(2,1)S(1)} %get-tuple-element.66), channel_id=1, source_target_pairs={{0,2},{2,4},{4,6},{6,0},{1,3},{3,5},{5,7},{7,1},{8,10},{10,12},{12... | collective-permute-start | bytes 294920 | tf_op jit(solution)/shard_map/ppermute | solution.py:29
  21.6 5.6 %collective-permute-start.4 = (bf16[384,128]{1,0:T(8,128)(2,1)S(1)}, bf16[384,128]{1,0:T(8,128)(2,1)S(1)}, u32[]{:S(2)}, u32[]{:S(2)}) collective-permute-start(bf16[384,128]{1,0:T(8,128)(2,1)S(1)} %get-tuple-element.66), channel_id=1, source_target_pairs={{0,6},{2,0},{4,2},{6,4},{1,7},{3,1},{5,3},{7,5},{8,14},{10,8},{12,... | collective-permute-start | bytes 294920 | tf_op jit(solution)/shard_map/ppermute | solution.py:29
  27.3 4.2 %collective-permute-start.5 = (bf16[4,384,128]{2,1,0:T(8,128)(2,1)S(1)}, bf16[4,384,128]{2,1,0:T(8,128)(2,1)S(1)}, u32[]{:S(2)}, u32[]{:S(2)}) collective-permute-start(bf16[4,384,128]{2,1,0:T(8,128)(2,1)S(1)} %pad_maximum_fusion.own), channel_id=1, source_target_pairs={{0,1},{1,0},{2,3},{3,2},{4,5},{5,4},{6,7},{7,6},{8,9},{9,8},{10,11... | collective-permute-start | bytes 1179656 | tf_op jit(solution)/shard_map/ppermute | solution.py:45
  34.5 27.0 %all-to-all-start.1 = ((bf16[16,64,512]{2,1,0:T(8,128)(2,1)}), bf16[16,64,512]{2,1,0:T(8,128)(2,1)S(1)}, u32[]{:S(2)}, u32[]{:S(2)}) async-start(bf16[16,64,512]{2,1,0:T(8,128)(2,1)} %get-tuple-element.48), calls=%async_computation.1 | async-start | bytes 2097152 | tf_op jit(solution)/shard_map/all_to_all | solution.py:37
  40.1 4.6 %collective-permute-start.6 = (bf16[128,256]{1,0:T(8,128)(2,1)S(1)}, bf16[128,256]{1,0:T(8,128)(2,1)S(1)}, u32[]{:S(2)}, u32[]{:S(2)}) collective-permute-start(bf16[128,256]{1,0:T(8,128)(2,1)S(1)} %get-tuple-element.44), channel_id=1, source_target_pairs={{0,2},{2,4},{4,6},{6,0},{1,3},{3,5},{5,7},{7,1},{8,10},{10,12},{12... | collective-permute-start | bytes 196616 | tf_op jit(solution)/shard_map/ppermute | solution.py:238
  40.9 5.7 %collective-permute-start.7 = (bf16[128,256]{1,0:T(8,128)(2,1)S(1)}, bf16[128,256]{1,0:T(8,128)(2,1)S(1)}, u32[]{:S(2)}, u32[]{:S(2)}) collective-permute-start(bf16[128,256]{1,0:T(8,128)(2,1)S(1)} %get-tuple-element.45), channel_id=1, source_target_pairs={{0,4},{2,6},{4,0},{6,2},{1,5},{3,7},{5,1},{7,3},{8,12},{10,14},{12... | collective-permute-start | bytes 196616 | tf_op jit(solution)/shard_map/ppermute | solution.py:240
  44.2 3.4 %collective-permute-start.8 = (bf16[128,256]{1,0:T(8,128)(2,1)S(1)}, bf16[128,256]{1,0:T(8,128)(2,1)S(1)}, u32[]{:S(2)}, u32[]{:S(2)}) collective-permute-start(bf16[128,256]{1,0:T(8,128)(2,1)S(1)} %get-tuple-element.46), channel_id=1, source_target_pairs={{0,6},{2,0},{4,2},{6,4},{1,7},{3,1},{5,3},{7,5},{8,14},{10,8},{12,... | collective-permute-start | bytes 196616 | tf_op jit(solution)/shard_map/ppermute | solution.py:239
  47.7 5.1 %collective-permute-start.9 = (f32[128,256]{1,0:T(8,128)S(1)}, f32[128,256]{1,0:T(8,128)S(1)}, u32[]{:S(2)}, u32[]{:S(2)}) collective-permute-start(f32[128,256]{1,0:T(8,128)S(1)} %sum.2.mine), channel_id=1, source_target_pairs={{0,1},{1,0},{2,3},{3,2},{4,5},{5,4},{6,7},{7,6},{8,9},{9,8},{10,11... | collective-permute-start | bytes 393224 | tf_op jit(solution)/shard_map/ppermute | solution.py:45
  52.8 5.3 %collective-permute-start.12 = (bf16[128,256]{1,0:T(8,128)(2,1)S(1)}, bf16[128,256]{1,0:T(8,128)(2,1)S(1)}, u32[]{:S(2)}, u32[]{:S(2)}) collective-permute-start(bf16[128,256]{1,0:T(8,128)(2,1)S(1)} %pair.2.x0), channel_id=1, source_target_pairs={{0,6},{2,0},{4,2},{6,4},{1,7},{3,1},{5,3},{7,5},{8,14},{10,8},{12,... | collective-permute-start | bytes 196616 | tf_op jit(solution)/shard_map/ppermute | solution.py:29
  55.1 4.6 %collective-permute-start.11 = (bf16[128,256]{1,0:T(8,128)(2,1)S(1)}, bf16[128,256]{1,0:T(8,128)(2,1)S(1)}, u32[]{:S(2)}, u32[]{:S(2)}) collective-permute-start(bf16[128,256]{1,0:T(8,128)(2,1)S(1)} %pair.2.x0), channel_id=1, source_target_pairs={{0,4},{2,6},{4,0},{6,2},{1,5},{3,7},{5,1},{7,3},{8,12},{10,14},{12... | collective-permute-start | bytes 196616 | tf_op jit(solution)/shard_map/ppermute | solution.py:29
  55.1 6.4 %collective-permute-start.10 = (bf16[128,256]{1,0:T(8,128)(2,1)S(1)}, bf16[128,256]{1,0:T(8,128)(2,1)S(1)}, u32[]{:S(2)}, u32[]{:S(2)}) collective-permute-start(bf16[128,256]{1,0:T(8,128)(2,1)S(1)} %pair.2.x0), channel_id=1, source_target_pairs={{0,2},{2,4},{4,6},{6,0},{1,3},{3,5},{5,7},{7,1},{8,10},{10,12},{12... | collective-permute-start | bytes 196616 | tf_op jit(solution)/shard_map/ppermute | solution.py:29
  62.1 6.2 %collective-permute-start.14 = (bf16[128,256]{1,0:T(8,128)(2,1)S(1)}, bf16[128,256]{1,0:T(8,128)(2,1)S(1)}, u32[]{:S(2)}, u32[]{:S(2)}) collective-permute-start(bf16[128,256]{1,0:T(8,128)(2,1)S(1)} %get-tuple-element.50.own), channel_id=1, source_target_pairs={{8,0},{16,8},{24,16},{32,24},{40,32},{48,40},{56,48},{64,56},{72,6... | collective-permute-start | bytes 196616 | tf_op jit(solution)/shard_map/ppermute | solution.py:53
  66.4 7.1 %collective-permute-start.13 = (bf16[128,256]{1,0:T(8,128)(2,1)S(1)}, bf16[128,256]{1,0:T(8,128)(2,1)S(1)}, u32[]{:S(2)}, u32[]{:S(2)}) collective-permute-start(bf16[128,256]{1,0:T(8,128)(2,1)S(1)} %get-tuple-element.50.own), channel_id=1, source_target_pairs={{0,8},{8,16},{16,24},{24,32},{32,40},{40,48},{48,56},{56,64},{64,7... | collective-permute-start | bytes 196616 | tf_op jit(solution)/shard_map/ppermute | solution.py:49
  74.4 24.4 %all-to-all-start.2 = ((bf16[16,64,512]{2,1,0:T(8,128)(2,1)}), bf16[16,64,512]{2,1,0:T(8,128)(2,1)S(1)}, u32[]{:S(2)}, u32[]{:S(2)}) async-start(bf16[16,64,512]{2,1,0:T(8,128)(2,1)} %get-tuple-element.56), calls=%async_computation.2 | async-start | bytes 2097152 | tf_op jit(solution)/shard_map/all_to_all | solution.py:37
  78.8 5.0 %collective-permute-start.15 = (bf16[128,256]{1,0:T(8,128)(2,1)S(1)}, bf16[128,256]{1,0:T(8,128)(2,1)S(1)}, u32[]{:S(2)}, u32[]{:S(2)}) collective-permute-start(bf16[128,256]{1,0:T(8,128)(2,1)S(1)} %get-tuple-element.52), channel_id=1, source_target_pairs={{0,2},{2,4},{4,6},{6,0},{1,3},{3,5},{5,7},{7,1},{8,10},{10,12},{12... | collective-permute-start | bytes 196616 | tf_op jit(solution)/shard_map/ppermute | solution.py:238
  78.8 5.0 %collective-permute-start.16 = (bf16[128,256]{1,0:T(8,128)(2,1)S(1)}, bf16[128,256]{1,0:T(8,128)(2,1)S(1)}, u32[]{:S(2)}, u32[]{:S(2)}) collective-permute-start(bf16[128,256]{1,0:T(8,128)(2,1)S(1)} %get-tuple-element.53), channel_id=1, source_target_pairs={{0,4},{2,6},{4,0},{6,2},{1,5},{3,7},{5,1},{7,3},{8,12},{10,14},{12... | collective-permute-start | bytes 196616 | tf_op jit(solution)/shard_map/ppermute | solution.py:240
  79.9 4.8 %collective-permute-start.17 = (bf16[128,256]{1,0:T(8,128)(2,1)S(1)}, bf16[128,256]{1,0:T(8,128)(2,1)S(1)}, u32[]{:S(2)}, u32[]{:S(2)}) collective-permute-start(bf16[128,256]{1,0:T(8,128)(2,1)S(1)} %get-tuple-element.54), channel_id=1, source_target_pairs={{0,6},{2,0},{4,2},{6,4},{1,7},{3,1},{5,3},{7,5},{8,14},{10,8},{12,... | collective-permute-start | bytes 196616 | tf_op jit(solution)/shard_map/ppermute | solution.py:239
  84.7 5.0 %collective-permute-start.18 = (f32[128,256]{1,0:T(8,128)S(1)}, f32[128,256]{1,0:T(8,128)S(1)}, u32[]{:S(2)}, u32[]{:S(2)}) collective-permute-start(f32[128,256]{1,0:T(8,128)S(1)} %sum.3.mine), channel_id=1, source_target_pairs={{0,1},{1,0},{2,3},{3,2},{4,5},{5,4},{6,7},{7,6},{8,9},{9,8},{10,11... | collective-permute-start | bytes 393224 | tf_op jit(solution)/shard_map/ppermute | solution.py:45
  89.7 5.4 %collective-permute-start.21 = (bf16[128,256]{1,0:T(8,128)(2,1)S(1)}, bf16[128,256]{1,0:T(8,128)(2,1)S(1)}, u32[]{:S(2)}, u32[]{:S(2)}) collective-permute-start(bf16[128,256]{1,0:T(8,128)(2,1)S(1)} %pair.3.x0), channel_id=1, source_target_pairs={{0,6},{2,0},{4,2},{6,4},{1,7},{3,1},{5,3},{7,5},{8,14},{10,8},{12,... | collective-permute-start | bytes 196616 | tf_op jit(solution)/shard_map/ppermute | solution.py:29
  92.1 4.6 %collective-permute-start.20 = (bf16[128,256]{1,0:T(8,128)(2,1)S(1)}, bf16[128,256]{1,0:T(8,128)(2,1)S(1)}, u32[]{:S(2)}, u32[]{:S(2)}) collective-permute-start(bf16[128,256]{1,0:T(8,128)(2,1)S(1)} %pair.3.x0), channel_id=1, source_target_pairs={{0,4},{2,6},{4,0},{6,2},{1,5},{3,7},{5,1},{7,3},{8,12},{10,14},{12... | collective-permute-start | bytes 196616 | tf_op jit(solution)/shard_map/ppermute | solution.py:29
  92.6 6.2 %collective-permute-start.19 = (bf16[128,256]{1,0:T(8,128)(2,1)S(1)}, bf16[128,256]{1,0:T(8,128)(2,1)S(1)}, u32[]{:S(2)}, u32[]{:S(2)}) collective-permute-start(bf16[128,256]{1,0:T(8,128)(2,1)S(1)} %pair.3.x0), channel_id=1, source_target_pairs={{0,2},{2,4},{4,6},{6,0},{1,3},{3,5},{5,7},{7,1},{8,10},{10,12},{12... | collective-permute-start | bytes 196616 | tf_op jit(solution)/shard_map/ppermute | solution.py:29
  99.3 6.2 %collective-permute-start.23 = (bf16[128,256]{1,0:T(8,128)(2,1)S(1)}, bf16[128,256]{1,0:T(8,128)(2,1)S(1)}, u32[]{:S(2)}, u32[]{:S(2)}) collective-permute-start(bf16[128,256]{1,0:T(8,128)(2,1)S(1)} %get-tuple-element.58.own), channel_id=1, source_target_pairs={{8,0},{16,8},{24,16},{32,24},{40,32},{48,40},{56,48},{64,56},{72,6... | collective-permute-start | bytes 196616 | tf_op jit(solution)/shard_map/ppermute | solution.py:53
  103.6 7.1 %collective-permute-start.22 = (bf16[128,256]{1,0:T(8,128)(2,1)S(1)}, bf16[128,256]{1,0:T(8,128)(2,1)S(1)}, u32[]{:S(2)}, u32[]{:S(2)}) collective-permute-start(bf16[128,256]{1,0:T(8,128)(2,1)S(1)} %get-tuple-element.58.own), channel_id=1, source_target_pairs={{0,8},{8,16},{16,24},{24,32},{32,40},{40,48},{48,56},{56,64},{64,7... | collective-permute-start | bytes 196616 | tf_op jit(solution)/shard_map/ppermute | solution.py:49
  111.7 5.1 %collective-permute-start.24 = (bf16[128,256]{1,0:T(8,128)(2,1)S(1)}, bf16[128,256]{1,0:T(8,128)(2,1)S(1)}, u32[]{:S(2)}, u32[]{:S(2)}) collective-permute-start(bf16[128,256]{1,0:T(8,128)(2,1)S(1)} %get-tuple-element.60), channel_id=1, source_target_pairs={{0,2},{2,4},{4,6},{6,0},{1,3},{3,5},{5,7},{7,1},{8,10},{10,12},{12... | collective-permute-start | bytes 196616 | tf_op jit(solution)/shard_map/ppermute | solution.py:238
  111.7 5.0 %collective-permute-start.25 = (bf16[128,256]{1,0:T(8,128)(2,1)S(1)}, bf16[128,256]{1,0:T(8,128)(2,1)S(1)}, u32[]{:S(2)}, u32[]{:S(2)}) collective-permute-start(bf16[128,256]{1,0:T(8,128)(2,1)S(1)} %get-tuple-element.61), channel_id=1, source_target_pairs={{0,4},{2,6},{4,0},{6,2},{1,5},{3,7},{5,1},{7,3},{8,12},{10,14},{12... | collective-permute-start | bytes 196616 | tf_op jit(solution)/shard_map/ppermute | solution.py:240
  112.6 4.7 %collective-permute-start.26 = (bf16[128,256]{1,0:T(8,128)(2,1)S(1)}, bf16[128,256]{1,0:T(8,128)(2,1)S(1)}, u32[]{:S(2)}, u32[]{:S(2)}) collective-permute-start(bf16[128,256]{1,0:T(8,128)(2,1)S(1)} %get-tuple-element.62), channel_id=1, source_target_pairs={{0,6},{2,0},{4,2},{6,4},{1,7},{3,1},{5,3},{7,5},{8,14},{10,8},{12,... | collective-permute-start | bytes 196616 | tf_op jit(solution)/shard_map/ppermute | solution.py:239
  117.4 4.7 %collective-permute-start.27 = (f32[128,128]{1,0:T(8,128)S(1)}, f32[128,128]{1,0:T(8,128)S(1)}, u32[]{:S(2)}, u32[]{:S(2)}) collective-permute-start(f32[128,128]{1,0:T(8,128)S(1)} %get-tuple-element.64), channel_id=1, source_target_pairs={{0,1},{1,0},{2,3},{3,2},{4,5},{5,4},{6,7},{7,6},{8,9},{9,8},{10,11... | collective-permute-start | bytes 196616 | tf_op jit(solution)/shard_map/ppermute | solution.py:45
  (1 other events, 11.0 us)

commit v4 on v3

--- a/solution.py
+++ b/solution.py
@@ -34,7 +34,7 @@
 
 
 def gather_rows(a):
-    return lax.all_to_all(a, SP, 0, 0, tiled=True).reshape(1024, 512)
+    return lax.all_gather(a, SP, axis=0, tiled=True)
 
 
 def after_this(a, done):
@@ -77,7 +77,8 @@
 
 
 def pack_body(
-    wq, wk, wv, wo, tokens, docs, first, rest, payload, wq_in, wk_in, wv_in, wo_in, docs_in, sems
+    wq, wk, wv, wo, tokens, docs, first, second, third, payload,
+    wq_in, wk_in, wv_in, wo_in, docs_in, sems
 ):
     pairs = ((wq, wq_in), (wk, wk_in), (wv, wv_in), (wo, wo_in), (docs, docs_in))
     pairs = pairs + ((tokens, payload.at[0:128]),)
@@ -86,19 +87,13 @@
         copy.start()
     for copy in copies:
         copy.wait()
-    whole = jnp.concatenate([wq_in[0], wk_in[0], wv_in[0], wo_in[0]], axis=1)
-    for n in range(16):
-        first[n] = whole
-    for layer in (1, 2):
+    for layer, into in enumerate((first, second, third)):
         for n, part in enumerate((wq_in, wk_in, wv_in, wo_in)):
-            rest[layer - 1, :, n * 128 : n * 128 + 128] = part[layer]
+            into[:, n * 128 : n * 128 + 128] = part[layer]
     payload[128:144, :] = jnp.broadcast_to((docs_in[...] + 1).astype(F32).astype(BF16), (16, 128))
 
 
-def table_body(bias, before, own, after, rest, table, many1, many2, wide):
-    for n in range(16):
-        many1[n] = rest[0]
-        many2[n] = rest[1]
+def table_body(bias, before, own, after, table, wide):
     own_docs = own[128:144, :].astype(F32)[0:1]
     query_docs = jnp.broadcast_to(own_docs, (128, 128)).T
     key_docs = jnp.concatenate(
@@ -243,9 +238,9 @@
 
 def local(tokens, norm_gain, w_query, w_key, w_value, w_out, offset_bias, documents):
     hbm = pl.BlockSpec(memory_space=pltpu.HBM)
-    first, rest, payload = call(
+    first, second, third, payload = call(
         pack_body,
-        [shaped(16, 64, 512), shaped(2, 64, 512), shaped(144, 128)],
+        [shaped(64, 512)] * 3 + [shaped(144, 128)],
         *[
             pltpu.with_memory_space_constraint(a, pltpu.HBM)
             for a in (
@@ -264,12 +259,11 @@
     )
     before = from_before(payload)
     after = from_after(payload)
-    weights0 = gather_rows(after_this(first, (before, after)))
+    weights0, weights1, weights2 = [gather_rows(a) for a in (first, second, third)]
     near = jnp.concatenate([before[0:128], payload[0:128], after[0:128]], axis=0)
     near_y = jnp.stack(in_order(near, spread(near, "y")))
-    table, many1, many2 = call(
-        table_body, [shaped(6, 128, 384, dtype=F32)] + [shaped(16, 64, 512)] * 2,
-        offset_bias, before, payload, after, rest,
+    table = call(
+        table_body, shaped(6, 128, 384, dtype=F32), offset_bias, before, payload, after,
         scratch=[pltpu.VMEM((8, 256), F32)], name="table",
     )
     near_partner = swap(after_this(near_y, table))
@@ -280,9 +274,9 @@
     )
     weights = weights0
     body, args = attend_first_body, (q, kv)
-    for layer, many in ((1, many1), (2, many2)):
+    for layer, next_weights in ((1, weights1), (2, weights2)):
         kept, r1, r2, r3 = scattered(body, *args, table, weights)
-        weights = gather_rows(after_this(many, kept))
+        weights = next_weights
         half = call(sum_body, shaped(128, 256, dtype=F32), kept, r1, r2, r3, name="sum")
         stream = call(pair_sum_body, shaped(128, 256), half, swap(half), name="pair")
         pieces = in_order(stream, spread(stream, "y"))

time: 123 us -> 174 us (1.41); the launches traced: 123 us -> 171 us
  waiting for transfers between devices: 42.9 us -> 79.2 us
  between operations: 0.22 us -> 13.3 us
  local copies, waits for them, and re-layouts: 0.02 us -> 4.62 us
  starting transfers between devices: 70 us -> 66.3 us
    all_gather x0 -> x3, waiting for transfers between devices: none -> 61.5 us  [gather_rows(): return lax.all_gather(a, SP, axis=0, tiled=True)]
    ppermute x3, waiting for transfers between devices: 15.2 us -> 0.01 us  [from_before(): return lax.ppermute(a, SP, [(i, i + 1) for i in range(15)])]
    all_to_all x3 -> x0, starting transfers between devices: 15.2 us -> none  [gather_rows(): return lax.all_to_all(a, SP, 0, 0, tiled=True).reshape(1024, 512)]
    ppermute x9, waiting for transfers between devices: 13.2 us -> 2.01 us  [spread(): return [lax.ppermute(a, axis, turn(k)) for k in (1, 3, 2)]]
    ppermute x3, waiting for transfers between devices: 4.75 us -> 0.01 us  [scattered(): r1 = lax.ppermute(s1, 'y', turn(1))]
    unnamed x4 -> x12, local copies, waits for them, and re-layouts: 0.01 us -> 4.61 us
    ppermute x3, waiting for transfers between devices: 0.01 us -> 3.6 us  [from_after(): return lax.ppermute(a, SP, [(i + 1, i) for i in range(15)])]
    ppermute x3, starting transfers between devices: 0.9 us -> 3.81 us  [scattered(): r1 = lax.ppermute(s1, 'y', turn(1))]
  transfers between devices with their start and end apart: 31 -> 31, of which waited for: 22 -> 18; matrix products, arithmetic and copies ran while one was open for 0% -> 0% of each run, Pallas kernels for 2% -> 2%
where the time goes in v4:
time: 174 us; the launch traced here: 171 us
  waiting for transfers between devices  79.2 us (46%)
  starting transfers between devices  66.3 us (38%)
  between operations  13.3 us (8%)
  Pallas kernels  7.77 us (4%)
  local copies, waits for them, and re-layouts  4.62 us (3%)
    all_gather x3, waiting for transfers between devices, gather_rows(): return lax.all_gather(a, SP, axis=0, tiled=True)  61.5 us
    ppermute x4, starting transfers between devices, swap(): return lax.ppermute(a, 'c', [(0, 1), (1, 0)])  17.1 us
    ppermute x3, starting transfers between devices, from_after(): return lax.ppermute(a, SP, [(i + 1, i) for i in range(15)])  15.1 us
    ppermute x9, starting transfers between devices, spread(): return [lax.ppermute(a, axis, turn(k)) for k in (1, 3, 2)]  12.3 us
    pallas_call x14, Pallas kernels, call(): pl.pallas_call(body, out_shape=outs, **specs, scratch_shapes=list(scratch...  7.77 us
    ppermute x3, starting transfers between devices, scattered(): r2 = lax.ppermute(s2, 'y', turn(2))  7.32 us
    ppermute x3, starting transfers between devices, from_before(): return lax.ppermute(a, SP, [(i, i + 1) for i in range(15)])  7.09 us
    unnamed x12, local copies, waits for them, and re-layouts  4.61 us
  transfers between devices with their start and end apart: 31, of which 18 were waited for; matrix products, arithmetic and copies ran while one was open for 0% of the time, Pallas kernels for 2%

profile of v4, /device:TPU:33, one launch (start us, length us, event | category | flops | bytes accessed | tf_op | source)
XLA Modules:
  0.0 171.2 jit_solution(11931507900109411508)
XLA Ops:
  6.5 1.6 pack.1
  9.7 3.1 %collective-permute-start = (bf16[144,128]{1,0:T(8,128)(2,1)S(1)}, bf16[144,128]{1,0:T(8,128)(2,1)S(1)}, u32[]{:S(2)}, u32[]{:S(2)}) collective-permute-start(bf16[144,128]{1,0:T(8,128)(2,1)S(1)} %get-tuple-element.30.own), channel_id=1, source_target_pairs={{0,8},{8,16},{16,24},{24,32},{32,40},{40,48},{48,56},{56,64},{64,7... | collective-permute-start | bytes 110600 | tf_op jit(solution)/shard_map/ppermute | solution.py:49
  12.8 4.3 %collective-permute-start.1 = (bf16[144,128]{1,0:T(8,128)(2,1)S(1)}, bf16[144,128]{1,0:T(8,128)(2,1)S(1)}, u32[]{:S(2)}, u32[]{:S(2)}) collective-permute-start(bf16[144,128]{1,0:T(8,128)(2,1)S(1)} %get-tuple-element.30.own), channel_id=1, source_target_pairs={{8,0},{16,8},{24,16},{32,24},{40,32},{48,40},{56,48},{64,56},{72,6... | collective-permute-start | bytes 110600 | tf_op jit(solution)/shard_map/ppermute | solution.py:53
  18.2 1.4 collective-permute-start.2
  19.5 2.6 %collective-permute-start.3 = (bf16[384,128]{1,0:T(8,128)(2,1)S(1)}, bf16[384,128]{1,0:T(8,128)(2,1)S(1)}, u32[]{:S(2)}, u32[]{:S(2)}) collective-permute-start(bf16[384,128]{1,0:T(8,128)(2,1)S(1)} %get-tuple-element.56), channel_id=1, source_target_pairs={{0,4},{2,6},{4,0},{6,2},{1,5},{3,7},{5,1},{7,3},{8,12},{10,14},{12... | collective-permute-start | bytes 294920 | tf_op jit(solution)/shard_map/ppermute | solution.py:29
  25.2 1.3 collective-permute-done.4
  26.6 2.7 %collective-permute-start.5 = (bf16[4,384,128]{2,1,0:T(8,128)(2,1)S(1)}, bf16[4,384,128]{2,1,0:T(8,128)(2,1)S(1)}, u32[]{:S(2)}, u32[]{:S(2)}) collective-permute-start(bf16[4,384,128]{2,1,0:T(8,128)(2,1)S(1)} %pad_maximum_fusion.own), channel_id=1, source_target_pairs={{0,1},{1,0},{2,3},{3,2},{4,5},{5,4},{6,7},{7,6},{8,9},{9,8},{10,11... | collective-permute-start | bytes 1179656 | tf_op jit(solution)/shard_map/ppermute | solution.py:45
  29.3 1.3 collective-permute-done.5.partner
  30.6 21.2 %all-gather.4.cloned.1.call-done.weights.rest_1_ = bf16[1024,512]{1,0:T(8,128)(2,1)} async-done(((bf16[64,512]{1,0:T(8,128)(2,1)}), bf16[1024,512]{1,0:T(8,128)(2,1)}) %all-gather.4.cloned.1.call-update) | async-done | bytes 1048592 | tf_op jit(solution)/shard_map/all_gather | solution.py:37
  51.8 1.2 copy-done
  55.2 1.3 collective-permute-start.6
  56.5 2.4 %collective-permute-start.7 = (bf16[128,256]{1,0:T(8,128)(2,1)S(1)}, bf16[128,256]{1,0:T(8,128)(2,1)S(1)}, u32[]{:S(2)}, u32[]{:S(2)}) collective-permute-start(bf16[128,256]{1,0:T(8,128)(2,1)S(1)} %get-tuple-element.37), channel_id=1, source_target_pairs={{0,4},{2,6},{4,0},{6,2},{1,5},{3,7},{5,1},{7,3},{8,12},{10,14},{12... | collective-permute-start | bytes 196616 | tf_op jit(solution)/shard_map/ppermute | solution.py:235
  62.3 4.0 %collective-permute-start.9 = (f32[128,256]{1,0:T(8,128)S(1)}, f32[128,256]{1,0:T(8,128)S(1)}, u32[]{:S(2)}, u32[]{:S(2)}) collective-permute-start(f32[128,256]{1,0:T(8,128)S(1)} %sum.2.mine), channel_id=1, source_target_pairs={{0,1},{1,0},{2,3},{3,2},{4,5},{5,4},{6,7},{7,6},{8,9},{9,8},{10,11... | collective-permute-start | bytes 393224 | tf_op jit(solution)/shard_map/ppermute | solution.py:45
  67.7 3.2 %collective-permute-start.11 = (bf16[128,256]{1,0:T(8,128)(2,1)S(1)}, bf16[128,256]{1,0:T(8,128)(2,1)S(1)}, u32[]{:S(2)}, u32[]{:S(2)}) collective-permute-start(bf16[128,256]{1,0:T(8,128)(2,1)S(1)} %pair.2.x0), channel_id=1, source_target_pairs={{0,4},{2,6},{4,0},{6,2},{1,5},{3,7},{5,1},{7,3},{8,12},{10,14},{12... | collective-permute-start | bytes 196616 | tf_op jit(solution)/shard_map/ppermute | solution.py:29
  70.9 24.7 %all-gather.6.cloned.1.call-done.weights = bf16[1024,512]{1,0:T(8,128)(2,1)} async-done(((bf16[64,512]{1,0:T(8,128)(2,1)}), bf16[1024,512]{1,0:T(8,128)(2,1)}) %all-gather.6.cloned.1.call-update) | async-done | bytes 1048592 | tf_op jit(solution)/shard_map/all_gather | solution.py:37
  95.7 1.2 copy-done.3
  97.4 2.0 %collective-permute-start.13 = (bf16[128,256]{1,0:T(8,128)(2,1)S(1)}, bf16[128,256]{1,0:T(8,128)(2,1)S(1)}, u32[]{:S(2)}, u32[]{:S(2)}) collective-permute-start(bf16[128,256]{1,0:T(8,128)(2,1)S(1)} %get-tuple-element.41.own), channel_id=1, source_target_pairs={{0,8},{8,16},{16,24},{24,32},{32,40},{40,48},{48,56},{56,64},{64,7... | collective-permute-start | bytes 196616 | tf_op jit(solution)/shard_map/ppermute | solution.py:49
  99.4 5.4 %collective-permute-start.14 = (bf16[128,256]{1,0:T(8,128)(2,1)S(1)}, bf16[128,256]{1,0:T(8,128)(2,1)S(1)}, u32[]{:S(2)}, u32[]{:S(2)}) collective-permute-start(bf16[128,256]{1,0:T(8,128)(2,1)S(1)} %get-tuple-element.41.own), channel_id=1, source_target_pairs={{8,0},{16,8},{24,16},{32,24},{40,32},{48,40},{56,48},{64,56},{72,6... | collective-permute-start | bytes 196616 | tf_op jit(solution)/shard_map/ppermute | solution.py:53
  104.8 1.3 collective-permute-done.14.after
  107.1 1.3 collective-permute-start.15
  108.3 2.4 %collective-permute-start.16 = (bf16[128,256]{1,0:T(8,128)(2,1)S(1)}, bf16[128,256]{1,0:T(8,128)(2,1)S(1)}, u32[]{:S(2)}, u32[]{:S(2)}) collective-permute-start(bf16[128,256]{1,0:T(8,128)(2,1)S(1)} %get-tuple-element.44), channel_id=1, source_target_pairs={{0,4},{2,6},{4,0},{6,2},{1,5},{3,7},{5,1},{7,3},{8,12},{10,14},{12... | collective-permute-start | bytes 196616 | tf_op jit(solution)/shard_map/ppermute | solution.py:235
  114.2 5.1 %collective-permute-start.18 = (f32[128,256]{1,0:T(8,128)S(1)}, f32[128,256]{1,0:T(8,128)S(1)}, u32[]{:S(2)}, u32[]{:S(2)}) collective-permute-start(f32[128,256]{1,0:T(8,128)S(1)} %sum.3.mine), channel_id=1, source_target_pairs={{0,1},{1,0},{2,3},{3,2},{4,5},{5,4},{6,7},{7,6},{8,9},{9,8},{10,11... | collective-permute-start | bytes 393224 | tf_op jit(solution)/shard_map/ppermute | solution.py:45
  120.7 3.2 %collective-permute-start.20 = (bf16[128,256]{1,0:T(8,128)(2,1)S(1)}, bf16[128,256]{1,0:T(8,128)(2,1)S(1)}, u32[]{:S(2)}, u32[]{:S(2)}) collective-permute-start(bf16[128,256]{1,0:T(8,128)(2,1)S(1)} %pair.3.x0), channel_id=1, source_target_pairs={{0,4},{2,6},{4,0},{6,2},{1,5},{3,7},{5,1},{7,3},{8,12},{10,14},{12... | collective-permute-start | bytes 196616 | tf_op jit(solution)/shard_map/ppermute | solution.py:29
  123.9 15.6 %all-gather.8.cloned.1.call-done.weights = bf16[1024,512]{1,0:T(8,128)(2,1)} async-done(((bf16[64,512]{1,0:T(8,128)(2,1)}), bf16[1024,512]{1,0:T(8,128)(2,1)}) %all-gather.8.cloned.1.call-update) | async-done | bytes 1048592 | tf_op jit(solution)/shard_map/all_gather | solution.py:37
  139.6 1.2 copy-done.2
  141.3 2.0 %collective-permute-start.22 = (bf16[128,256]{1,0:T(8,128)(2,1)S(1)}, bf16[128,256]{1,0:T(8,128)(2,1)S(1)}, u32[]{:S(2)}, u32[]{:S(2)}) collective-permute-start(bf16[128,256]{1,0:T(8,128)(2,1)S(1)} %get-tuple-element.48.own), channel_id=1, source_target_pairs={{0,8},{8,16},{16,24},{24,32},{32,40},{40,48},{48,56},{56,64},{64,7... | collective-permute-start | bytes 196616 | tf_op jit(solution)/shard_map/ppermute | solution.py:49
  143.3 5.4 %collective-permute-start.23 = (bf16[128,256]{1,0:T(8,128)(2,1)S(1)}, bf16[128,256]{1,0:T(8,128)(2,1)S(1)}, u32[]{:S(2)}, u32[]{:S(2)}) collective-permute-start(bf16[128,256]{1,0:T(8,128)(2,1)S(1)} %get-tuple-element.48.own), channel_id=1, source_target_pairs={{8,0},{16,8},{24,16},{32,24},{40,32},{48,40},{56,48},{64,56},{72,6... | collective-permute-start | bytes 196616 | tf_op jit(solution)/shard_map/ppermute | solution.py:53
  148.7 1.3 collective-permute-done.23.after
  150.9 1.3 collective-permute-start.24
  152.2 2.4 %collective-permute-start.25 = (bf16[128,256]{1,0:T(8,128)(2,1)S(1)}, bf16[128,256]{1,0:T(8,128)(2,1)S(1)}, u32[]{:S(2)}, u32[]{:S(2)}) collective-permute-start(bf16[128,256]{1,0:T(8,128)(2,1)S(1)} %get-tuple-element.51), channel_id=1, source_target_pairs={{0,4},{2,6},{4,0},{6,2},{1,5},{3,7},{5,1},{7,3},{8,12},{10,14},{12... | collective-permute-start | bytes 196616 | tf_op jit(solution)/shard_map/ppermute | solution.py:235
  155.8 1.2 collective-permute-done.25.r2
  157.8 5.4 %collective-permute-start.27 = (f32[128,128]{1,0:T(8,128)S(1)}, f32[128,128]{1,0:T(8,128)S(1)}, u32[]{:S(2)}, u32[]{:S(2)}) collective-permute-start(f32[128,128]{1,0:T(8,128)S(1)} %get-tuple-element.54), channel_id=1, source_target_pairs={{0,1},{1,0},{2,3},{3,2},{4,5},{5,4},{6,7},{7,6},{8,9},{9,8},{10,11... | collective-permute-start | bytes 196616 | tf_op jit(solution)/shard_map/ppermute | solution.py:45
  (64 shorter events, 23.8 us)
Async XLA Ops:
  6.5 45.3 %all-gather.4.cloned.1.call-start = ((), (), s32[]{:S(2)}) async-start(), calls=%async_computation | async-start | bytes 1114112 | tf_op jit(solution)/shard_map/all_gather | solution.py:37
  8.2 87.4 %all-gather.6.cloned.1.call-start = ((), (), s32[]{:S(2)}) async-start(), calls=%async_computation.1 | async-start | bytes 1114112 | tf_op jit(solution)/shard_map/all_gather | solution.py:37
  9.0 130.6 %all-gather.8.cloned.1.call-start = ((), (), s32[]{:S(2)}) async-start(), calls=%async_computation.2 | async-start | bytes 1114112 | tf_op jit(solution)/shard_map/all_gather | solution.py:37
  9.7 7.4 %collective-permute-start = (bf16[144,128]{1,0:T(8,128)(2,1)S(1)}, bf16[144,128]{1,0:T(8,128)(2,1)S(1)}, u32[]{:S(2)}, u32[]{:S(2)}) collective-permute-start(bf16[144,128]{1,0:T(8,128)(2,1)S(1)} %get-tuple-element.30.own), channel_id=1, source_target_pairs={{0,8},{8,16},{16,24},{24,32},{32,40},{40,48},{48,56},{56,64},{64,7... | collective-permute-start | bytes 110600 | tf_op jit(solution)/shard_map/ppermute | solution.py:49
  12.8 5.3 %collective-permute-start.1 = (bf16[144,128]{1,0:T(8,128)(2,1)S(1)}, bf16[144,128]{1,0:T(8,128)(2,1)S(1)}, u32[]{:S(2)}, u32[]{:S(2)}) collective-permute-start(bf16[144,128]{1,0:T(8,128)(2,1)S(1)} %get-tuple-element.30.own), channel_id=1, source_target_pairs={{8,0},{16,8},{24,16},{32,24},{40,32},{48,40},{56,48},{64,56},{72,6... | collective-permute-start | bytes 110600 | tf_op jit(solution)/shard_map/ppermute | solution.py:53
  18.2 33.6 %copy-start.4 = (f32[3,1024]{1,0:T(4,128)S(1)}, f32[3,1024]{1,0:T(4,128)}, u32[]{:S(2)}) copy-start(f32[3,1024]{1,0:T(4,128)} %gain.5) | copy-start | bytes 36868
  18.2 6.4 %collective-permute-start.2 = (bf16[384,128]{1,0:T(8,128)(2,1)S(1)}, bf16[384,128]{1,0:T(8,128)(2,1)S(1)}, u32[]{:S(2)}, u32[]{:S(2)}) collective-permute-start(bf16[384,128]{1,0:T(8,128)(2,1)S(1)} %get-tuple-element.56), channel_id=1, source_target_pairs={{0,2},{2,4},{4,6},{6,0},{1,3},{3,5},{5,7},{7,1},{8,10},{10,12},{12... | collective-permute-start | bytes 294920 | tf_op jit(solution)/shard_map/ppermute | solution.py:29
  19.5 5.7 %collective-permute-start.3 = (bf16[384,128]{1,0:T(8,128)(2,1)S(1)}, bf16[384,128]{1,0:T(8,128)(2,1)S(1)}, u32[]{:S(2)}, u32[]{:S(2)}) collective-permute-start(bf16[384,128]{1,0:T(8,128)(2,1)S(1)} %get-tuple-element.56), channel_id=1, source_target_pairs={{0,4},{2,6},{4,0},{6,2},{1,5},{3,7},{5,1},{7,3},{8,12},{10,14},{12... | collective-permute-start | bytes 294920 | tf_op jit(solution)/shard_map/ppermute | solution.py:29
  22.2 4.4 %collective-permute-start.4 = (bf16[384,128]{1,0:T(8,128)(2,1)S(1)}, bf16[384,128]{1,0:T(8,128)(2,1)S(1)}, u32[]{:S(2)}, u32[]{:S(2)}) collective-permute-start(bf16[384,128]{1,0:T(8,128)(2,1)S(1)} %get-tuple-element.56), channel_id=1, source_target_pairs={{0,6},{2,0},{4,2},{6,4},{1,7},{3,1},{5,3},{7,5},{8,14},{10,8},{12,... | collective-permute-start | bytes 294920 | tf_op jit(solution)/shard_map/ppermute | solution.py:29
  26.6 4.0 %collective-permute-start.5 = (bf16[4,384,128]{2,1,0:T(8,128)(2,1)S(1)}, bf16[4,384,128]{2,1,0:T(8,128)(2,1)S(1)}, u32[]{:S(2)}, u32[]{:S(2)}) collective-permute-start(bf16[4,384,128]{2,1,0:T(8,128)(2,1)S(1)} %pad_maximum_fusion.own), channel_id=1, source_target_pairs={{0,1},{1,0},{2,3},{3,2},{4,5},{5,4},{6,7},{7,6},{8,9},{9,8},{10,11... | collective-permute-start | bytes 1179656 | tf_op jit(solution)/shard_map/ppermute | solution.py:45
  55.2 4.9 %collective-permute-start.6 = (bf16[128,256]{1,0:T(8,128)(2,1)S(1)}, bf16[128,256]{1,0:T(8,128)(2,1)S(1)}, u32[]{:S(2)}, u32[]{:S(2)}) collective-permute-start(bf16[128,256]{1,0:T(8,128)(2,1)S(1)} %get-tuple-element.36), channel_id=1, source_target_pairs={{0,2},{2,4},{4,6},{6,0},{1,3},{3,5},{5,7},{7,1},{8,10},{10,12},{12... | collective-permute-start | bytes 196616 | tf_op jit(solution)/shard_map/ppermute | solution.py:233
  56.5 4.8 %collective-permute-start.7 = (bf16[128,256]{1,0:T(8,128)(2,1)S(1)}, bf16[128,256]{1,0:T(8,128)(2,1)S(1)}, u32[]{:S(2)}, u32[]{:S(2)}) collective-permute-start(bf16[128,256]{1,0:T(8,128)(2,1)S(1)} %get-tuple-element.37), channel_id=1, source_target_pairs={{0,4},{2,6},{4,0},{6,2},{1,5},{3,7},{5,1},{7,3},{8,12},{10,14},{12... | collective-permute-start | bytes 196616 | tf_op jit(solution)/shard_map/ppermute | solution.py:235
  58.9 3.4 %collective-permute-start.8 = (bf16[128,256]{1,0:T(8,128)(2,1)S(1)}, bf16[128,256]{1,0:T(8,128)(2,1)S(1)}, u32[]{:S(2)}, u32[]{:S(2)}) collective-permute-start(bf16[128,256]{1,0:T(8,128)(2,1)S(1)} %get-tuple-element.38), channel_id=1, source_target_pairs={{0,6},{2,0},{4,2},{6,4},{1,7},{3,1},{5,3},{7,5},{8,14},{10,8},{12,... | collective-permute-start | bytes 196616 | tf_op jit(solution)/shard_map/ppermute | solution.py:234
  62.3 4.9 %collective-permute-start.9 = (f32[128,256]{1,0:T(8,128)S(1)}, f32[128,256]{1,0:T(8,128)S(1)}, u32[]{:S(2)}, u32[]{:S(2)}) collective-permute-start(f32[128,256]{1,0:T(8,128)S(1)} %sum.2.mine), channel_id=1, source_target_pairs={{0,1},{1,0},{2,3},{3,2},{4,5},{5,4},{6,7},{7,6},{8,9},{9,8},{10,11... | collective-permute-start | bytes 393224 | tf_op jit(solution)/shard_map/ppermute | solution.py:45
  67.3 28.4 %collective-permute-start.10 = (bf16[128,256]{1,0:T(8,128)(2,1)S(1)}, bf16[128,256]{1,0:T(8,128)(2,1)S(1)}, u32[]{:S(2)}, u32[]{:S(2)}) collective-permute-start(bf16[128,256]{1,0:T(8,128)(2,1)S(1)} %pair.2.x0), channel_id=1, source_target_pairs={{0,2},{2,4},{4,6},{6,0},{1,3},{3,5},{5,7},{7,1},{8,10},{10,12},{12... | collective-permute-start | bytes 196616 | tf_op jit(solution)/shard_map/ppermute | solution.py:29
  67.7 28.0 %collective-permute-start.11 = (bf16[128,256]{1,0:T(8,128)(2,1)S(1)}, bf16[128,256]{1,0:T(8,128)(2,1)S(1)}, u32[]{:S(2)}, u32[]{:S(2)}) collective-permute-start(bf16[128,256]{1,0:T(8,128)(2,1)S(1)} %pair.2.x0), channel_id=1, source_target_pairs={{0,4},{2,6},{4,0},{6,2},{1,5},{3,7},{5,1},{7,3},{8,12},{10,14},{12... | collective-permute-start | bytes 196616 | tf_op jit(solution)/shard_map/ppermute | solution.py:29
  70.9 24.7 %collective-permute-start.12 = (bf16[128,256]{1,0:T(8,128)(2,1)S(1)}, bf16[128,256]{1,0:T(8,128)(2,1)S(1)}, u32[]{:S(2)}, u32[]{:S(2)}) collective-permute-start(bf16[128,256]{1,0:T(8,128)(2,1)S(1)} %pair.2.x0), channel_id=1, source_target_pairs={{0,6},{2,0},{4,2},{6,4},{1,7},{3,1},{5,3},{7,5},{8,14},{10,8},{12,... | collective-permute-start | bytes 196616 | tf_op jit(solution)/shard_map/ppermute | solution.py:29
  97.4 7.4 %collective-permute-start.13 = (bf16[128,256]{1,0:T(8,128)(2,1)S(1)}, bf16[128,256]{1,0:T(8,128)(2,1)S(1)}, u32[]{:S(2)}, u32[]{:S(2)}) collective-permute-start(bf16[128,256]{1,0:T(8,128)(2,1)S(1)} %get-tuple-element.41.own), channel_id=1, source_target_pairs={{0,8},{8,16},{16,24},{24,32},{32,40},{40,48},{48,56},{56,64},{64,7... | collective-permute-start | bytes 196616 | tf_op jit(solution)/shard_map/ppermute | solution.py:49
  99.4 6.7 %collective-permute-start.14 = (bf16[128,256]{1,0:T(8,128)(2,1)S(1)}, bf16[128,256]{1,0:T(8,128)(2,1)S(1)}, u32[]{:S(2)}, u32[]{:S(2)}) collective-permute-start(bf16[128,256]{1,0:T(8,128)(2,1)S(1)} %get-tuple-element.41.own), channel_id=1, source_target_pairs={{8,0},{16,8},{24,16},{32,24},{40,32},{48,40},{56,48},{64,56},{72,6... | collective-permute-start | bytes 196616 | tf_op jit(solution)/shard_map/ppermute | solution.py:53
  107.1 4.9 %collective-permute-start.15 = (bf16[128,256]{1,0:T(8,128)(2,1)S(1)}, bf16[128,256]{1,0:T(8,128)(2,1)S(1)}, u32[]{:S(2)}, u32[]{:S(2)}) collective-permute-start(bf16[128,256]{1,0:T(8,128)(2,1)S(1)} %get-tuple-element.43), channel_id=1, source_target_pairs={{0,2},{2,4},{4,6},{6,0},{1,3},{3,5},{5,7},{7,1},{8,10},{10,12},{12... | collective-permute-start | bytes 196616 | tf_op jit(solution)/shard_map/ppermute | solution.py:233
  108.3 4.8 %collective-permute-start.16 = (bf16[128,256]{1,0:T(8,128)(2,1)S(1)}, bf16[128,256]{1,0:T(8,128)(2,1)S(1)}, u32[]{:S(2)}, u32[]{:S(2)}) collective-permute-start(bf16[128,256]{1,0:T(8,128)(2,1)S(1)} %get-tuple-element.44), channel_id=1, source_target_pairs={{0,4},{2,6},{4,0},{6,2},{1,5},{3,7},{5,1},{7,3},{8,12},{10,14},{12... | collective-permute-start | bytes 196616 | tf_op jit(solution)/shard_map/ppermute | solution.py:235
  110.8 3.4 %collective-permute-start.17 = (bf16[128,256]{1,0:T(8,128)(2,1)S(1)}, bf16[128,256]{1,0:T(8,128)(2,1)S(1)}, u32[]{:S(2)}, u32[]{:S(2)}) collective-permute-start(bf16[128,256]{1,0:T(8,128)(2,1)S(1)} %get-tuple-element.45), channel_id=1, source_target_pairs={{0,6},{2,0},{4,2},{6,4},{1,7},{3,1},{5,3},{7,5},{8,14},{10,8},{12,... | collective-permute-start | bytes 196616 | tf_op jit(solution)/shard_map/ppermute | solution.py:234
  114.2 6.1 %collective-permute-start.18 = (f32[128,256]{1,0:T(8,128)S(1)}, f32[128,256]{1,0:T(8,128)S(1)}, u32[]{:S(2)}, u32[]{:S(2)}) collective-permute-start(f32[128,256]{1,0:T(8,128)S(1)} %sum.3.mine), channel_id=1, source_target_pairs={{0,1},{1,0},{2,3},{3,2},{4,5},{5,4},{6,7},{7,6},{8,9},{9,8},{10,11... | collective-permute-start | bytes 393224 | tf_op jit(solution)/shard_map/ppermute | solution.py:45
  120.3 19.2 %collective-permute-start.19 = (bf16[128,256]{1,0:T(8,128)(2,1)S(1)}, bf16[128,256]{1,0:T(8,128)(2,1)S(1)}, u32[]{:S(2)}, u32[]{:S(2)}) collective-permute-start(bf16[128,256]{1,0:T(8,128)(2,1)S(1)} %pair.3.x0), channel_id=1, source_target_pairs={{0,2},{2,4},{4,6},{6,0},{1,3},{3,5},{5,7},{7,1},{8,10},{10,12},{12... | collective-permute-start | bytes 196616 | tf_op jit(solution)/shard_map/ppermute | solution.py:29
  120.7 18.8 %collective-permute-start.20 = (bf16[128,256]{1,0:T(8,128)(2,1)S(1)}, bf16[128,256]{1,0:T(8,128)(2,1)S(1)}, u32[]{:S(2)}, u32[]{:S(2)}) collective-permute-start(bf16[128,256]{1,0:T(8,128)(2,1)S(1)} %pair.3.x0), channel_id=1, source_target_pairs={{0,4},{2,6},{4,0},{6,2},{1,5},{3,7},{5,1},{7,3},{8,12},{10,14},{12... | collective-permute-start | bytes 196616 | tf_op jit(solution)/shard_map/ppermute | solution.py:29
  123.9 15.6 %collective-permute-start.21 = (bf16[128,256]{1,0:T(8,128)(2,1)S(1)}, bf16[128,256]{1,0:T(8,128)(2,1)S(1)}, u32[]{:S(2)}, u32[]{:S(2)}) collective-permute-start(bf16[128,256]{1,0:T(8,128)(2,1)S(1)} %pair.3.x0), channel_id=1, source_target_pairs={{0,6},{2,0},{4,2},{6,4},{1,7},{3,1},{5,3},{7,5},{8,14},{10,8},{12,... | collective-permute-start | bytes 196616 | tf_op jit(solution)/shard_map/ppermute | solution.py:29
  141.3 7.4 %collective-permute-start.22 = (bf16[128,256]{1,0:T(8,128)(2,1)S(1)}, bf16[128,256]{1,0:T(8,128)(2,1)S(1)}, u32[]{:S(2)}, u32[]{:S(2)}) collective-permute-start(bf16[128,256]{1,0:T(8,128)(2,1)S(1)} %get-tuple-element.48.own), channel_id=1, source_target_pairs={{0,8},{8,16},{16,24},{24,32},{32,40},{40,48},{48,56},{56,64},{64,7... | collective-permute-start | bytes 196616 | tf_op jit(solution)/shard_map/ppermute | solution.py:49
  143.3 6.7 %collective-permute-start.23 = (bf16[128,256]{1,0:T(8,128)(2,1)S(1)}, bf16[128,256]{1,0:T(8,128)(2,1)S(1)}, u32[]{:S(2)}, u32[]{:S(2)}) collective-permute-start(bf16[128,256]{1,0:T(8,128)(2,1)S(1)} %get-tuple-element.48.own), channel_id=1, source_target_pairs={{8,0},{16,8},{24,16},{32,24},{40,32},{48,40},{56,48},{64,56},{72,6... | collective-permute-start | bytes 196616 | tf_op jit(solution)/shard_map/ppermute | solution.py:53
  150.9 4.9 %collective-permute-start.24 = (bf16[128,256]{1,0:T(8,128)(2,1)S(1)}, bf16[128,256]{1,0:T(8,128)(2,1)S(1)}, u32[]{:S(2)}, u32[]{:S(2)}) collective-permute-start(bf16[128,256]{1,0:T(8,128)(2,1)S(1)} %get-tuple-element.50), channel_id=1, source_target_pairs={{0,2},{2,4},{4,6},{6,0},{1,3},{3,5},{5,7},{7,1},{8,10},{10,12},{12... | collective-permute-start | bytes 196616 | tf_op jit(solution)/shard_map/ppermute | solution.py:233
  152.2 4.8 %collective-permute-start.25 = (bf16[128,256]{1,0:T(8,128)(2,1)S(1)}, bf16[128,256]{1,0:T(8,128)(2,1)S(1)}, u32[]{:S(2)}, u32[]{:S(2)}) collective-permute-start(bf16[128,256]{1,0:T(8,128)(2,1)S(1)} %get-tuple-element.51), channel_id=1, source_target_pairs={{0,4},{2,6},{4,0},{6,2},{1,5},{3,7},{5,1},{7,3},{8,12},{10,14},{12... | collective-permute-start | bytes 196616 | tf_op jit(solution)/shard_map/ppermute | solution.py:235
  154.7 3.1 %collective-permute-start.26 = (bf16[128,256]{1,0:T(8,128)(2,1)S(1)}, bf16[128,256]{1,0:T(8,128)(2,1)S(1)}, u32[]{:S(2)}, u32[]{:S(2)}) collective-permute-start(bf16[128,256]{1,0:T(8,128)(2,1)S(1)} %get-tuple-element.52), channel_id=1, source_target_pairs={{0,6},{2,0},{4,2},{6,4},{1,7},{3,1},{5,3},{7,5},{8,14},{10,8},{12,... | collective-permute-start | bytes 196616 | tf_op jit(solution)/shard_map/ppermute | solution.py:234
  157.8 6.3 %collective-permute-start.27 = (f32[128,128]{1,0:T(8,128)S(1)}, f32[128,128]{1,0:T(8,128)S(1)}, u32[]{:S(2)}, u32[]{:S(2)}) collective-permute-start(f32[128,128]{1,0:T(8,128)S(1)} %get-tuple-element.54), channel_id=1, source_target_pairs={{0,1},{1,0},{2,3},{3,2},{4,5},{5,4},{6,7},{7,6},{8,9},{9,8},{10,11... | collective-permute-start | bytes 196616 | tf_op jit(solution)/shard_map/ppermute | solution.py:45
  (5 other events, 5.6 us)
Sparse Core Ops, SparseCore 0:
  9.5 42.2 all-gather.3
  53.9 41.6 all-gather.5
  97.8 41.6 all-gather.7

commit v5 on v3

--- a/solution.py
+++ b/solution.py
@@ -7,6 +7,7 @@
 from jax.experimental.pallas import tpu as pltpu
 from jax.sharding import Mesh
 from jax.sharding import PartitionSpec as P
+
 
 HEAD_DIM = 64
 WIN_ROWS = 8
@@ -61,13 +62,12 @@
     return (lax.axis_index(axis) + k) & 3
 
 
-def call(body, outs, *args, scratch=(), name=None, **specs):
+def call(body, outs, *args, scratch=(), **specs):
     return pl.pallas_call(
         body,
         out_shape=outs,
         **specs,
         scratch_shapes=list(scratch),
-        name=name,
         compiler_params=pltpu.CompilerParams(vmem_limit_bytes=24 * 1024 * 1024),
     )(*args)
 
@@ -77,10 +77,9 @@
 
 
 def pack_body(
-    wq, wk, wv, wo, tokens, docs, first, rest, payload, wq_in, wk_in, wv_in, wo_in, docs_in, sems
+    wq, wk, wv, wo, first, rest, wq_in, wk_in, wv_in, wo_in, sems
 ):
-    pairs = ((wq, wq_in), (wk, wk_in), (wv, wv_in), (wo, wo_in), (docs, docs_in))
-    pairs = pairs + ((tokens, payload.at[0:128]),)
+    pairs = ((wq, wq_in), (wk, wk_in), (wv, wv_in), (wo, wo_in))
     copies = [pltpu.make_async_copy(a, b, sems.at[n]) for n, (a, b) in enumerate(pairs)]
     for copy in copies:
         copy.start()
@@ -92,17 +91,19 @@
     for layer in (1, 2):
         for n, part in enumerate((wq_in, wk_in, wv_in, wo_in)):
             rest[layer - 1, :, n * 128 : n * 128 + 128] = part[layer]
-    payload[128:144, :] = jnp.broadcast_to((docs_in[...] + 1).astype(F32).astype(BF16), (16, 128))
-
-
-def table_body(bias, before, own, after, rest, table, many1, many2, wide):
+
+
+def many_body(rest, many1, many2):
     for n in range(16):
         many1[n] = rest[0]
         many2[n] = rest[1]
-    own_docs = own[128:144, :].astype(F32)[0:1]
+
+
+def table_body(bias, before, own, after, table, wide):
+    own_docs = own[128:144, 0:128].astype(F32)[0:1]
     query_docs = jnp.broadcast_to(own_docs, (128, 128)).T
     key_docs = jnp.concatenate(
-        [before[128:144, :].astype(F32)[0:1], own_docs, after[128:144, :].astype(F32)[0:1]], axis=1
+        [before[128:144, 0:128].astype(F32)[0:1], own_docs, after[128:144, 0:128].astype(F32)[0:1]], axis=1
     )
     same = jnp.concatenate([query_docs] * 3, axis=1) == key_docs
     r = lax.broadcasted_iota(jnp.int32, (128, 384), 0)
@@ -145,15 +146,15 @@
     kv[:, 128:256] = acc[:, 256:384].astype(BF16)
 
 
-def heads_first_body(own, partner, gain, weights, q, kv):
+def heads_first_body(own, partner, gain, docs, weights, q, kv):
     c = lax.axis_index("c")
-    total = jnp.zeros((384, 128), F32)
+    total = jnp.zeros((128, 128), F32)
     for k in range(4):
         for part in (own, partner):
             values = part[k].astype(F32)
             total = total + values * values
     scale = lax.rsqrt(jnp.sum(total, axis=1, keepdims=True) * (1.0 / 1024) + EPS)
-    acc = jnp.zeros((384, 384), F32)
+    acc = jnp.zeros((128, 384), F32)
     for k in range(4):
         for part, core in ((own, c), (partner, 1 - c)):
             block = behind("y", k) * 2 + core
@@ -161,9 +162,9 @@
             normed = (part[k].astype(F32) * scale * gains).astype(BF16)
             rows = weights[pl.ds(pl.multiple_of(block * 128, 128), 128), 0:384]
             acc = acc + jnp.dot(normed, rows, preferred_element_type=F32)
-    q[...] = normed_heads(acc[128:256, 0:128])
-    kv[:, 0:128] = normed_heads(acc[:, 128:256])
-    kv[:, 128:256] = acc[:, 256:384].astype(BF16)
+    finish_heads(acc, q, kv.at[0:128])
+    line = (docs[...] + 1).astype(F32).astype(BF16)
+    kv[128:144, :] = jnp.broadcast_to(jnp.concatenate([line, line], axis=1), (16, 256))
 
 
 def heads_pieces_body(x0, x1, x2, x3, gain, weights, q, kv, *, layer):
@@ -203,16 +204,12 @@
 
 
 def attend_scatter_body(q, before, own, after, table, weights, kept, s1, s2, s3, *, layer):
-    parts = [(p[:, 0:128], p[:, 128:256]) for p in (before, own, after)]
+    parts = [(p[0:128, 0:128], p[0:128, 128:256]) for p in (before, own, after)]
     attended = attend(q, parts, table.at[2 * layer : 2 * layer + 2])
     for k, into in enumerate((kept, s1, s2, s3)):
         rows = weights[pl.ds(pl.multiple_of(ahead("y", k) * 256, 256), 256), 384:512]
         share = lax.dot_general(attended, rows, NT, preferred_element_type=F32)
         into[...] = share.astype(into.dtype)
-
-
-def attend_first_body(q, kv, *rest):
-    attend_scatter_body(q, kv.at[0:128], kv.at[128:256], kv.at[256:384], *rest, layer=0)
 
 
 def sum_body(kept, r1, r2, r3, out):
@@ -234,7 +231,7 @@
 
 def scattered(body, *args):
     outs = [shaped(128, 256, dtype=F32)] + [shaped(128, 256)] * 3
-    kept, s1, s2, s3 = call(body, outs, *args, name="attend_scatter")
+    kept, s1, s2, s3 = call(body, outs, *args)
     r1 = lax.ppermute(s1, "y", turn(1))
     r3 = lax.ppermute(s3, "y", turn(3))
     r2 = lax.ppermute(s2, "y", turn(2))
@@ -243,61 +240,47 @@
 
 def local(tokens, norm_gain, w_query, w_key, w_value, w_out, offset_bias, documents):
     hbm = pl.BlockSpec(memory_space=pltpu.HBM)
-    first, rest, payload = call(
+    first, rest = call(
         pack_body,
-        [shaped(16, 64, 512), shaped(2, 64, 512), shaped(144, 128)],
+        [shaped(16, 64, 512), shaped(2, 64, 512)],
         *[
             pltpu.with_memory_space_constraint(a, pltpu.HBM)
-            for a in (
-                w_query,
-                w_key,
-                w_value,
-                jnp.swapaxes(w_out, 1, 2),
-                tokens,
-                documents.reshape(1, 128),
-            )
+            for a in (w_query, w_key, w_value, jnp.swapaxes(w_out, 1, 2))
         ],
-        name="pack",
-        in_specs=[hbm] * 6,
-        scratch=[pltpu.VMEM((3, 64, 128), BF16)] * 4
-        + [pltpu.VMEM((1, 128), jnp.int32), pltpu.SemaphoreType.DMA((6,))],
-    )
-    before = from_before(payload)
-    after = from_after(payload)
-    weights0 = gather_rows(after_this(first, (before, after)))
-    near = jnp.concatenate([before[0:128], payload[0:128], after[0:128]], axis=0)
-    near_y = jnp.stack(in_order(near, spread(near, "y")))
-    table, many1, many2 = call(
-        table_body, [shaped(6, 128, 384, dtype=F32)] + [shaped(16, 64, 512)] * 2,
-        offset_bias, before, payload, after, rest,
-        scratch=[pltpu.VMEM((8, 256), F32)], name="table",
-    )
-    near_partner = swap(after_this(near_y, table))
+        in_specs=[hbm] * 4,
+        scratch=[pltpu.VMEM((3, 64, 128), BF16)] * 4 + [pltpu.SemaphoreType.DMA((4,))],
+    )
+    weights = gather_rows(first)
+    near_y = jnp.stack(in_order(tokens, spread(tokens, "y")))
+    many1, many2 = call(many_body, [shaped(16, 64, 512)] * 2, rest)
+    near_partner = swap(after_this(near_y, many1))
 
     q, kv = call(
-        heads_first_body, [shaped(128, 128), shaped(384, 256)],
-        near_y, near_partner, norm_gain, weights0, name="heads0",
-    )
-    weights = weights0
-    body, args = attend_first_body, (q, kv)
+        heads_first_body, [shaped(128, 128), shaped(144, 256)],
+        near_y, near_partner, norm_gain, documents.reshape(1, 128), weights,
+    )
+    args = (q, from_before(kv), kv, from_after(kv))
+    table = call(
+        table_body, shaped(6, 128, 384, dtype=F32), offset_bias, *args[1:],
+        scratch=[pltpu.VMEM((8, 256), F32)],
+    )
+    body = functools.partial(attend_scatter_body, layer=0)
     for layer, many in ((1, many1), (2, many2)):
         kept, r1, r2, r3 = scattered(body, *args, table, weights)
         weights = gather_rows(after_this(many, kept))
-        half = call(sum_body, shaped(128, 256, dtype=F32), kept, r1, r2, r3, name="sum")
-        stream = call(pair_sum_body, shaped(128, 256), half, swap(half), name="pair")
+        half = call(sum_body, shaped(128, 256, dtype=F32), kept, r1, r2, r3)
+        stream = call(pair_sum_body, shaped(128, 256), half, swap(half))
         pieces = in_order(stream, spread(stream, "y"))
         q, kv = call(
             functools.partial(heads_pieces_body, layer=layer),
             [shaped(128, 128), shaped(128, 256)],
-            *pieces, norm_gain, weights, name="heads",
+            *pieces, norm_gain, weights,
         )
         body = functools.partial(attend_scatter_body, layer=layer)
         args = (q, from_before(kv), kv, from_after(kv))
     kept, r1, r2, r3 = scattered(body, *args, table, weights)
-    mine, theirs = call(
-        split_body, [shaped(128, 128, dtype=F32)] * 2, kept, r1, r2, r3, name="split"
-    )
-    return call(pair_sum_body, shaped(128, 128), mine, swap(theirs), name="pair_last")
+    mine, theirs = call(split_body, [shaped(128, 128, dtype=F32)] * 2, kept, r1, r2, r3)
+    return call(pair_sum_body, shaped(128, 128), mine, swap(theirs))
 
 
 def solution(mesh):

time: 123 us -> 125 us (1.016)
    all_to_all x3, waiting for transfers between devices: 1.14 us -> 2.88 us  [gather_rows(): return lax.all_to_all(a, SP, 0, 0, tiled=True).reshape(1024, 512)]
    pallas_call x14 -> x15, Pallas kernels: 9.49 us -> 9.19 us  [call(): pl.pallas_call(body, out_shape=outs, **specs, scratch_shapes=list(scratch...]
  transfers between devices with their start and end apart: 31 -> 31, of which waited for: 22 -> 21; matrix products, arithmetic and copies ran while one was open for 0% -> 0% of each run, Pallas kernels for 2% -> 1%
where the time goes in v5:
time: 125 us; the launch traced here: 124 us
  starting transfers between devices  70.9 us (57%)
  waiting for transfers between devices  43.9 us (35%)
  Pallas kernels  9.19 us (7%)
    ppermute x3, waiting for transfers between devices, from_before(): return lax.ppermute(a, SP, [(i, i + 1) for i in range(15)])  15.6 us
    ppermute x4, starting transfers between devices, swap(): return lax.ppermute(a, 'c', [(0, 1), (1, 0)])  15.6 us
    all_to_all x3, starting transfers between devices, gather_rows(): return lax.all_to_all(a, SP, 0, 0, tiled=True).reshape(1024, 512)  15.2 us
    ppermute x3, starting transfers between devices, from_after(): return lax.ppermute(a, SP, [(i + 1, i) for i in range(15)])  13.3 us
    ppermute x9, waiting for transfers between devices, spread(): return [lax.ppermute(a, axis, turn(k)) for k in (1, 3, 2)]  13.1 us
    ppermute x9, starting transfers between devices, spread(): return [lax.ppermute(a, axis, turn(k)) for k in (1, 3, 2)]  10.6 us
    pallas_call x15, Pallas kernels, call(): pl.pallas_call(body, out_shape=outs, **specs, scratch_shapes=list(scratch...  9.19 us
    ppermute x3, starting transfers between devices, from_before(): return lax.ppermute(a, SP, [(i, i + 1) for i in range(15)])  5.76 us
  transfers between devices with their start and end apart: 31, of which 21 were waited for; matrix products, arithmetic and copies ran while one was open for 0% of the time, Pallas kernels for 1%

profile of v5, /device:TPU:33, one launch (start us, length us, event | category | flops | bytes accessed | tf_op | source)
XLA Modules:
  0.0 124.3 jit_solution(1839874722529110789)
XLA Ops:
  0.0 2.0 %shard_map.82 = (bf16[16,64,512]{2,1,0:T(8,128)(2,1)}, bf16[2,64,512]{2,1,0:T(8,128)(2,1)S(1)}) custom-call(bf16[3,64,128]{2,1,0:T(8,128)(2,1)} %wq.1, bf16[3,64,128]{2,1,0:T(8,128)(2,1)} %wk.1, bf16[3,64,128]{2,1,0:T(8,128)(2,1)} %wv.1, bf16[3,64,128]{2,1,0:T(8,128)(2,1)} %bitcast.16), custom_call_target="tpu_custom_call" | custom-call | tf_op jit(solution)/shard_map/pallas_call | solution.py:66
  2.1 7.3 %all-to-all-start = ((bf16[16,64,512]{2,1,0:T(8,128)(2,1)}), bf16[16,64,512]{2,1,0:T(8,128)(2,1)S(1)}, u32[]{:S(2)}, u32[]{:S(2)}) async-start(bf16[16,64,512]{2,1,0:T(8,128)(2,1)} %get-tuple-element.35), calls=%async_computation | async-start | bytes 2097152 | tf_op jit(solution)/shard_map/all_to_all | solution.py:38
  12.3 1.6 %collective-permute-start.1 = (bf16[128,128]{1,0:T(8,128)(2,1)S(1)}, bf16[128,128]{1,0:T(8,128)(2,1)S(1)}, u32[]{:S(2)}, u32[]{:S(2)}) collective-permute-start(bf16[128,128]{1,0:T(8,128)(2,1)S(1)} %copy-done.3), channel_id=1, source_target_pairs={{0,4},{2,6},{4,0},{6,2},{1,5},{3,7},{5,1},{7,3},{8,12},{10,14},{12... | collective-permute-start | bytes 98312 | tf_op jit(solution)/shard_map/ppermute | solution.py:30
  15.4 1.7 %collective-permute-done.1 = bf16[128,128]{1,0:T(8,128)(2,1)S(1)} collective-permute-done((bf16[128,128]{1,0:T(8,128)(2,1)S(1)}, bf16[128,128]{1,0:T(8,128)(2,1)S(1)}, u32[]{:S(2)}, u32[]{:S(2)}) %collective-permute-start.1) | collective-permute-done | bytes 32800 | tf_op jit(solution)/shard_map/ppermute | solution.py:30
  17.1 2.4 %collective-permute-start.3 = (bf16[4,128,128]{2,1,0:T(8,128)(2,1)S(1)}, bf16[4,128,128]{2,1,0:T(8,128)(2,1)S(1)}, u32[]{:S(2)}, u32[]{:S(2)}) collective-permute-start(bf16[4,128,128]{2,1,0:T(8,128)(2,1)S(1)} %pad_maximum_fusion.own), channel_id=1, source_target_pairs={{0,1},{1,0},{2,3},{3,2},{4,5},{5,4},{6,7},{7,6},{8,9},{9,8},{10,11... | collective-permute-start | bytes 393224 | tf_op jit(solution)/shard_map/ppermute | solution.py:46
  20.5 2.9 %all-to-all-done = bf16[16,64,512]{2,1,0:T(8,128)(2,1)S(1)} async-done(((bf16[16,64,512]{2,1,0:T(8,128)(2,1)}), bf16[16,64,512]{2,1,0:T(8,128)(2,1)S(1)}, u32[]{:S(2)}, u32[]{:S(2)}) %all-to-all-start) | async-done | bytes 1048608 | tf_op jit(solution)/shard_map/all_to_all | solution.py:38
  23.9 4.6 %collective-permute-start.5 = (bf16[144,256]{1,0:T(8,128)(2,1)S(1)}, bf16[144,256]{1,0:T(8,128)(2,1)S(1)}, u32[]{:S(2)}, u32[]{:S(2)}) collective-permute-start(bf16[144,256]{1,0:T(8,128)(2,1)S(1)} %get-tuple-element.37.own), channel_id=1, source_target_pairs={{8,0},{16,8},{24,16},{32,24},{40,32},{48,40},{56,48},{64,56},{72,6... | collective-permute-start | bytes 221192 | tf_op jit(solution)/shard_map/ppermute | solution.py:54
  28.6 1.9 %collective-permute-start.4 = (bf16[144,256]{1,0:T(8,128)(2,1)S(1)}, bf16[144,256]{1,0:T(8,128)(2,1)S(1)}, u32[]{:S(2)}, u32[]{:S(2)}) collective-permute-start(bf16[144,256]{1,0:T(8,128)(2,1)S(1)} %get-tuple-element.37.own), channel_id=1, source_target_pairs={{0,8},{8,16},{16,24},{24,32},{32,40},{40,48},{48,56},{56,64},{64,7... | collective-permute-start | bytes 221192 | tf_op jit(solution)/shard_map/ppermute | solution.py:50
  30.5 5.3 %collective-permute-done.4.before = bf16[144,256]{1,0:T(8,128)(2,1)S(1)} collective-permute-done((bf16[144,256]{1,0:T(8,128)(2,1)S(1)}, bf16[144,256]{1,0:T(8,128)(2,1)S(1)}, u32[]{:S(2)}, u32[]{:S(2)}) %collective-permute-start.4) | collective-permute-done | bytes 73760 | tf_op jit(solution)/shard_map/ppermute | solution.py:50
  37.3 3.6 %all-to-all-start.1 = ((bf16[16,64,512]{2,1,0:T(8,128)(2,1)}), bf16[16,64,512]{2,1,0:T(8,128)(2,1)S(1)}, u32[]{:S(2)}, u32[]{:S(2)}) async-start(bf16[16,64,512]{2,1,0:T(8,128)(2,1)} %get-tuple-element.42), calls=%async_computation.1 | async-start | bytes 2097152 | tf_op jit(solution)/shard_map/all_to_all | solution.py:38
  42.3 2.6 %collective-permute-start.7 = (bf16[128,256]{1,0:T(8,128)(2,1)S(1)}, bf16[128,256]{1,0:T(8,128)(2,1)S(1)}, u32[]{:S(2)}, u32[]{:S(2)}) collective-permute-start(bf16[128,256]{1,0:T(8,128)(2,1)S(1)} %get-tuple-element.40), channel_id=1, source_target_pairs={{0,4},{2,6},{4,0},{6,2},{1,5},{3,7},{5,1},{7,3},{8,12},{10,14},{12... | collective-permute-start | bytes 196616 | tf_op jit(solution)/shard_map/ppermute | solution.py:237
  48.3 5.2 %collective-permute-start.9 = (f32[128,256]{1,0:T(8,128)S(1)}, f32[128,256]{1,0:T(8,128)S(1)}, u32[]{:S(2)}, u32[]{:S(2)}) collective-permute-start(f32[128,256]{1,0:T(8,128)S(1)} %shard_map.87.mine), channel_id=1, source_target_pairs={{0,1},{1,0},{2,3},{3,2},{4,5},{5,4},{6,7},{7,6},{8,9},{9,8},{10,11... | collective-permute-start | bytes 393224 | tf_op jit(solution)/shard_map/ppermute | solution.py:46
  54.6 2.3 %collective-permute-start.12 = (bf16[128,256]{1,0:T(8,128)(2,1)S(1)}, bf16[128,256]{1,0:T(8,128)(2,1)S(1)}, u32[]{:S(2)}, u32[]{:S(2)}) collective-permute-start(bf16[128,256]{1,0:T(8,128)(2,1)S(1)} %shard_map.88.x0), channel_id=1, source_target_pairs={{0,6},{2,0},{4,2},{6,4},{1,7},{3,1},{5,3},{7,5},{8,14},{10,8},{12,... | collective-permute-start | bytes 196616 | tf_op jit(solution)/shard_map/ppermute | solution.py:30
  58.2 3.4 %collective-permute-done.11.x2 = bf16[128,256]{1,0:T(8,128)(2,1)S(1)} collective-permute-done((bf16[128,256]{1,0:T(8,128)(2,1)S(1)}, bf16[128,256]{1,0:T(8,128)(2,1)S(1)}, u32[]{:S(2)}, u32[]{:S(2)}) %collective-permute-start.11) | collective-permute-done | bytes 65568 | tf_op jit(solution)/shard_map/ppermute | solution.py:30
  61.6 1.6 %collective-permute-done.10.x1 = bf16[128,256]{1,0:T(8,128)(2,1)S(1)} collective-permute-done((bf16[128,256]{1,0:T(8,128)(2,1)S(1)}, bf16[128,256]{1,0:T(8,128)(2,1)S(1)}, u32[]{:S(2)}, u32[]{:S(2)}) %collective-permute-start.10) | collective-permute-done | bytes 65568 | tf_op jit(solution)/shard_map/ppermute | solution.py:30
  63.8 4.3 %collective-permute-start.14 = (bf16[128,256]{1,0:T(8,128)(2,1)S(1)}, bf16[128,256]{1,0:T(8,128)(2,1)S(1)}, u32[]{:S(2)}, u32[]{:S(2)}) collective-permute-start(bf16[128,256]{1,0:T(8,128)(2,1)S(1)} %get-tuple-element.44.own), channel_id=1, source_target_pairs={{8,0},{16,8},{24,16},{32,24},{40,32},{48,40},{56,48},{64,56},{72,6... | collective-permute-start | bytes 196616 | tf_op jit(solution)/shard_map/ppermute | solution.py:54
  68.1 1.9 %collective-permute-start.13 = (bf16[128,256]{1,0:T(8,128)(2,1)S(1)}, bf16[128,256]{1,0:T(8,128)(2,1)S(1)}, u32[]{:S(2)}, u32[]{:S(2)}) collective-permute-start(bf16[128,256]{1,0:T(8,128)(2,1)S(1)} %get-tuple-element.44.own), channel_id=1, source_target_pairs={{0,8},{8,16},{16,24},{24,32},{32,40},{40,48},{48,56},{56,64},{64,7... | collective-permute-start | bytes 196616 | tf_op jit(solution)/shard_map/ppermute | solution.py:50
  70.0 5.2 %collective-permute-done.13.before = bf16[128,256]{1,0:T(8,128)(2,1)S(1)} collective-permute-done((bf16[128,256]{1,0:T(8,128)(2,1)S(1)}, bf16[128,256]{1,0:T(8,128)(2,1)S(1)}, u32[]{:S(2)}, u32[]{:S(2)}) %collective-permute-start.13) | collective-permute-done | bytes 65568 | tf_op jit(solution)/shard_map/ppermute | solution.py:50
  76.1 4.3 %all-to-all-start.2 = ((bf16[16,64,512]{2,1,0:T(8,128)(2,1)}), bf16[16,64,512]{2,1,0:T(8,128)(2,1)S(1)}, u32[]{:S(2)}, u32[]{:S(2)}) async-start(bf16[16,64,512]{2,1,0:T(8,128)(2,1)} %get-tuple-element.50), calls=%async_computation.2 | async-start | bytes 2097152 | tf_op jit(solution)/shard_map/all_to_all | solution.py:38
  81.5 1.6 %collective-permute-start.17 = (bf16[128,256]{1,0:T(8,128)(2,1)S(1)}, bf16[128,256]{1,0:T(8,128)(2,1)S(1)}, u32[]{:S(2)}, u32[]{:S(2)}) collective-permute-start(bf16[128,256]{1,0:T(8,128)(2,1)S(1)} %get-tuple-element.48), channel_id=1, source_target_pairs={{0,6},{2,0},{4,2},{6,4},{1,7},{3,1},{5,3},{7,5},{8,14},{10,8},{12,... | collective-permute-start | bytes 196616 | tf_op jit(solution)/shard_map/ppermute | solution.py:236
  83.1 2.3 %collective-permute-done.15.r1 = bf16[128,256]{1,0:T(8,128)(2,1)S(1)} collective-permute-done((bf16[128,256]{1,0:T(8,128)(2,1)S(1)}, bf16[128,256]{1,0:T(8,128)(2,1)S(1)}, u32[]{:S(2)}, u32[]{:S(2)}) %collective-permute-start.15) | collective-permute-done | bytes 65568 | tf_op jit(solution)/shard_map/ppermute | solution.py:235
  86.3 4.0 %collective-permute-start.18 = (f32[128,256]{1,0:T(8,128)S(1)}, f32[128,256]{1,0:T(8,128)S(1)}, u32[]{:S(2)}, u32[]{:S(2)}) collective-permute-start(f32[128,256]{1,0:T(8,128)S(1)} %shard_map.91.mine), channel_id=1, source_target_pairs={{0,1},{1,0},{2,3},{3,2},{4,5},{5,4},{6,7},{7,6},{8,9},{9,8},{10,11... | collective-permute-start | bytes 393224 | tf_op jit(solution)/shard_map/ppermute | solution.py:46
  91.3 2.5 %collective-permute-start.21 = (bf16[128,256]{1,0:T(8,128)(2,1)S(1)}, bf16[128,256]{1,0:T(8,128)(2,1)S(1)}, u32[]{:S(2)}, u32[]{:S(2)}) collective-permute-start(bf16[128,256]{1,0:T(8,128)(2,1)S(1)} %shard_map.92.x0), channel_id=1, source_target_pairs={{0,6},{2,0},{4,2},{6,4},{1,7},{3,1},{5,3},{7,5},{8,14},{10,8},{12,... | collective-permute-start | bytes 196616 | tf_op jit(solution)/shard_map/ppermute | solution.py:30
  94.5 2.0 %collective-permute-done.21.x3 = bf16[128,256]{1,0:T(8,128)(2,1)S(1)} collective-permute-done((bf16[128,256]{1,0:T(8,128)(2,1)S(1)}, bf16[128,256]{1,0:T(8,128)(2,1)S(1)}, u32[]{:S(2)}, u32[]{:S(2)}) %collective-permute-start.21) | collective-permute-done | bytes 65568 | tf_op jit(solution)/shard_map/ppermute | solution.py:30
  96.5 2.0 %collective-permute-done.20.x2 = bf16[128,256]{1,0:T(8,128)(2,1)S(1)} collective-permute-done((bf16[128,256]{1,0:T(8,128)(2,1)S(1)}, bf16[128,256]{1,0:T(8,128)(2,1)S(1)}, u32[]{:S(2)}, u32[]{:S(2)}) %collective-permute-start.20) | collective-permute-done | bytes 65568 | tf_op jit(solution)/shard_map/ppermute | solution.py:30
  98.5 1.7 %collective-permute-done.19.x1 = bf16[128,256]{1,0:T(8,128)(2,1)S(1)} collective-permute-done((bf16[128,256]{1,0:T(8,128)(2,1)S(1)}, bf16[128,256]{1,0:T(8,128)(2,1)S(1)}, u32[]{:S(2)}, u32[]{:S(2)}) %collective-permute-start.19) | collective-permute-done | bytes 65568 | tf_op jit(solution)/shard_map/ppermute | solution.py:30
  100.7 4.3 %collective-permute-start.23 = (bf16[128,256]{1,0:T(8,128)(2,1)S(1)}, bf16[128,256]{1,0:T(8,128)(2,1)S(1)}, u32[]{:S(2)}, u32[]{:S(2)}) collective-permute-start(bf16[128,256]{1,0:T(8,128)(2,1)S(1)} %get-tuple-element.52.own), channel_id=1, source_target_pairs={{8,0},{16,8},{24,16},{32,24},{40,32},{48,40},{56,48},{64,56},{72,6... | collective-permute-start | bytes 196616 | tf_op jit(solution)/shard_map/ppermute | solution.py:54
  105.0 1.9 %collective-permute-start.22 = (bf16[128,256]{1,0:T(8,128)(2,1)S(1)}, bf16[128,256]{1,0:T(8,128)(2,1)S(1)}, u32[]{:S(2)}, u32[]{:S(2)}) collective-permute-start(bf16[128,256]{1,0:T(8,128)(2,1)S(1)} %get-tuple-element.52.own), channel_id=1, source_target_pairs={{0,8},{8,16},{16,24},{24,32},{32,40},{40,48},{48,56},{56,64},{64,7... | collective-permute-start | bytes 196616 | tf_op jit(solution)/shard_map/ppermute | solution.py:50
  107.0 5.2 %collective-permute-done.22.before = bf16[128,256]{1,0:T(8,128)(2,1)S(1)} collective-permute-done((bf16[128,256]{1,0:T(8,128)(2,1)S(1)}, bf16[128,256]{1,0:T(8,128)(2,1)S(1)}, u32[]{:S(2)}, u32[]{:S(2)}) %collective-permute-start.22) | collective-permute-done | bytes 65568 | tf_op jit(solution)/shard_map/ppermute | solution.py:50
  114.2 1.7 %collective-permute-start.26 = (bf16[128,256]{1,0:T(8,128)(2,1)S(1)}, bf16[128,256]{1,0:T(8,128)(2,1)S(1)}, u32[]{:S(2)}, u32[]{:S(2)}) collective-permute-start(bf16[128,256]{1,0:T(8,128)(2,1)S(1)} %get-tuple-element.56), channel_id=1, source_target_pairs={{0,6},{2,0},{4,2},{6,4},{1,7},{3,1},{5,3},{7,5},{8,14},{10,8},{12,... | collective-permute-start | bytes 196616 | tf_op jit(solution)/shard_map/ppermute | solution.py:236
  115.9 2.3 %collective-permute-done.24.r1 = bf16[128,256]{1,0:T(8,128)(2,1)S(1)} collective-permute-done((bf16[128,256]{1,0:T(8,128)(2,1)S(1)}, bf16[128,256]{1,0:T(8,128)(2,1)S(1)}, u32[]{:S(2)}, u32[]{:S(2)}) %collective-permute-start.24) | collective-permute-done | bytes 65568 | tf_op jit(solution)/shard_map/ppermute | solution.py:235
  118.8 4.0 %collective-permute-start.27 = (f32[128,128]{1,0:T(8,128)S(1)}, f32[128,128]{1,0:T(8,128)S(1)}, u32[]{:S(2)}, u32[]{:S(2)}) collective-permute-start(f32[128,128]{1,0:T(8,128)S(1)} %get-tuple-element.58), channel_id=1, source_target_pairs={{0,1},{1,0},{2,3},{3,2},{4,5},{5,4},{6,7},{7,6},{8,9},{9,8},{10,11... | collective-permute-start | bytes 196616 | tf_op jit(solution)/shard_map/ppermute | solution.py:46
  (54 shorter events, 24.3 us)
Async XLA Ops:
  2.1 21.3 %all-to-all-start = ((bf16[16,64,512]{2,1,0:T(8,128)(2,1)}), bf16[16,64,512]{2,1,0:T(8,128)(2,1)S(1)}, u32[]{:S(2)}, u32[]{:S(2)}) async-start(bf16[16,64,512]{2,1,0:T(8,128)(2,1)} %get-tuple-element.35), calls=%async_computation | async-start | bytes 2097152 | tf_op jit(solution)/shard_map/all_to_all | solution.py:38
  9.4 26.4 %copy-start.1 = (f32[3,2,8,16]{3,2,1,0:T(8,128)S(1)}, f32[3,2,8,16]{3,2,1,0:T(8,128)}, u32[]{:S(2)}) copy-start(f32[3,2,8,16]{3,2,1,0:T(8,128)} %bias.1) | copy-start | bytes 9220
  9.4 5.9 %collective-permute-start = (bf16[128,128]{1,0:T(8,128)(2,1)S(1)}, bf16[128,128]{1,0:T(8,128)(2,1)S(1)}, u32[]{:S(2)}, u32[]{:S(2)}) collective-permute-start(bf16[128,128]{1,0:T(8,128)(2,1)S(1)} %copy-done.3), channel_id=1, source_target_pairs={{0,2},{2,4},{4,6},{6,0},{1,3},{3,5},{5,7},{7,1},{8,10},{10,12},{12... | collective-permute-start | bytes 98312 | tf_op jit(solution)/shard_map/ppermute | solution.py:30
  10.8 4.5 %collective-permute-start.2 = (bf16[128,128]{1,0:T(8,128)(2,1)S(1)}, bf16[128,128]{1,0:T(8,128)(2,1)S(1)}, u32[]{:S(2)}, u32[]{:S(2)}) collective-permute-start(bf16[128,128]{1,0:T(8,128)(2,1)S(1)} %copy-done.3), channel_id=1, source_target_pairs={{0,6},{2,0},{4,2},{6,4},{1,7},{3,1},{5,3},{7,5},{8,14},{10,8},{12,... | collective-permute-start | bytes 98312 | tf_op jit(solution)/shard_map/ppermute | solution.py:30
  12.3 4.7 %collective-permute-start.1 = (bf16[128,128]{1,0:T(8,128)(2,1)S(1)}, bf16[128,128]{1,0:T(8,128)(2,1)S(1)}, u32[]{:S(2)}, u32[]{:S(2)}) collective-permute-start(bf16[128,128]{1,0:T(8,128)(2,1)S(1)} %copy-done.3), channel_id=1, source_target_pairs={{0,4},{2,6},{4,0},{6,2},{1,5},{3,7},{5,1},{7,3},{8,12},{10,14},{12... | collective-permute-start | bytes 98312 | tf_op jit(solution)/shard_map/ppermute | solution.py:30
  17.1 3.4 %collective-permute-start.3 = (bf16[4,128,128]{2,1,0:T(8,128)(2,1)S(1)}, bf16[4,128,128]{2,1,0:T(8,128)(2,1)S(1)}, u32[]{:S(2)}, u32[]{:S(2)}) collective-permute-start(bf16[4,128,128]{2,1,0:T(8,128)(2,1)S(1)} %pad_maximum_fusion.own), channel_id=1, source_target_pairs={{0,1},{1,0},{2,3},{3,2},{4,5},{5,4},{6,7},{7,6},{8,9},{9,8},{10,11... | collective-permute-start | bytes 393224 | tf_op jit(solution)/shard_map/ppermute | solution.py:46
  23.9 6.6 %collective-permute-start.5 = (bf16[144,256]{1,0:T(8,128)(2,1)S(1)}, bf16[144,256]{1,0:T(8,128)(2,1)S(1)}, u32[]{:S(2)}, u32[]{:S(2)}) collective-permute-start(bf16[144,256]{1,0:T(8,128)(2,1)S(1)} %get-tuple-element.37.own), channel_id=1, source_target_pairs={{8,0},{16,8},{24,16},{32,24},{40,32},{48,40},{56,48},{64,56},{72,6... | collective-permute-start | bytes 221192 | tf_op jit(solution)/shard_map/ppermute | solution.py:54
  28.6 7.2 %collective-permute-start.4 = (bf16[144,256]{1,0:T(8,128)(2,1)S(1)}, bf16[144,256]{1,0:T(8,128)(2,1)S(1)}, u32[]{:S(2)}, u32[]{:S(2)}) collective-permute-start(bf16[144,256]{1,0:T(8,128)(2,1)S(1)} %get-tuple-element.37.own), channel_id=1, source_target_pairs={{0,8},{8,16},{16,24},{24,32},{32,40},{40,48},{48,56},{56,64},{64,7... | collective-permute-start | bytes 221192 | tf_op jit(solution)/shard_map/ppermute | solution.py:50
  37.3 25.9 %all-to-all-start.1 = ((bf16[16,64,512]{2,1,0:T(8,128)(2,1)}), bf16[16,64,512]{2,1,0:T(8,128)(2,1)S(1)}, u32[]{:S(2)}, u32[]{:S(2)}) async-start(bf16[16,64,512]{2,1,0:T(8,128)(2,1)} %get-tuple-element.42), calls=%async_computation.1 | async-start | bytes 2097152 | tf_op jit(solution)/shard_map/all_to_all | solution.py:38
  40.9 5.1 %collective-permute-start.6 = (bf16[128,256]{1,0:T(8,128)(2,1)S(1)}, bf16[128,256]{1,0:T(8,128)(2,1)S(1)}, u32[]{:S(2)}, u32[]{:S(2)}) collective-permute-start(bf16[128,256]{1,0:T(8,128)(2,1)S(1)} %get-tuple-element.39), channel_id=1, source_target_pairs={{0,2},{2,4},{4,6},{6,0},{1,3},{3,5},{5,7},{7,1},{8,10},{10,12},{12... | collective-permute-start | bytes 196616 | tf_op jit(solution)/shard_map/ppermute | solution.py:235
  42.3 5.0 %collective-permute-start.7 = (bf16[128,256]{1,0:T(8,128)(2,1)S(1)}, bf16[128,256]{1,0:T(8,128)(2,1)S(1)}, u32[]{:S(2)}, u32[]{:S(2)}) collective-permute-start(bf16[128,256]{1,0:T(8,128)(2,1)S(1)} %get-tuple-element.40), channel_id=1, source_target_pairs={{0,4},{2,6},{4,0},{6,2},{1,5},{3,7},{5,1},{7,3},{8,12},{10,14},{12... | collective-permute-start | bytes 196616 | tf_op jit(solution)/shard_map/ppermute | solution.py:237
  44.9 3.4 %collective-permute-start.8 = (bf16[128,256]{1,0:T(8,128)(2,1)S(1)}, bf16[128,256]{1,0:T(8,128)(2,1)S(1)}, u32[]{:S(2)}, u32[]{:S(2)}) collective-permute-start(bf16[128,256]{1,0:T(8,128)(2,1)S(1)} %get-tuple-element.41), channel_id=1, source_target_pairs={{0,6},{2,0},{4,2},{6,4},{1,7},{3,1},{5,3},{7,5},{8,14},{10,8},{12,... | collective-permute-start | bytes 196616 | tf_op jit(solution)/shard_map/ppermute | solution.py:236
  48.3 6.2 %collective-permute-start.9 = (f32[128,256]{1,0:T(8,128)S(1)}, f32[128,256]{1,0:T(8,128)S(1)}, u32[]{:S(2)}, u32[]{:S(2)}) collective-permute-start(f32[128,256]{1,0:T(8,128)S(1)} %shard_map.87.mine), channel_id=1, source_target_pairs={{0,1},{1,0},{2,3},{3,2},{4,5},{5,4},{6,7},{7,6},{8,9},{9,8},{10,11... | collective-permute-start | bytes 393224 | tf_op jit(solution)/shard_map/ppermute | solution.py:46
  54.6 3.7 %collective-permute-start.12 = (bf16[128,256]{1,0:T(8,128)(2,1)S(1)}, bf16[128,256]{1,0:T(8,128)(2,1)S(1)}, u32[]{:S(2)}, u32[]{:S(2)}) collective-permute-start(bf16[128,256]{1,0:T(8,128)(2,1)S(1)} %shard_map.88.x0), channel_id=1, source_target_pairs={{0,6},{2,0},{4,2},{6,4},{1,7},{3,1},{5,3},{7,5},{8,14},{10,8},{12,... | collective-permute-start | bytes 196616 | tf_op jit(solution)/shard_map/ppermute | solution.py:30
  56.9 4.7 %collective-permute-start.11 = (bf16[128,256]{1,0:T(8,128)(2,1)S(1)}, bf16[128,256]{1,0:T(8,128)(2,1)S(1)}, u32[]{:S(2)}, u32[]{:S(2)}) collective-permute-start(bf16[128,256]{1,0:T(8,128)(2,1)S(1)} %shard_map.88.x0), channel_id=1, source_target_pairs={{0,4},{2,6},{4,0},{6,2},{1,5},{3,7},{5,1},{7,3},{8,12},{10,14},{12... | collective-permute-start | bytes 196616 | tf_op jit(solution)/shard_map/ppermute | solution.py:30
  56.9 6.3 %collective-permute-start.10 = (bf16[128,256]{1,0:T(8,128)(2,1)S(1)}, bf16[128,256]{1,0:T(8,128)(2,1)S(1)}, u32[]{:S(2)}, u32[]{:S(2)}) collective-permute-start(bf16[128,256]{1,0:T(8,128)(2,1)S(1)} %shard_map.88.x0), channel_id=1, source_target_pairs={{0,2},{2,4},{4,6},{6,0},{1,3},{3,5},{5,7},{7,1},{8,10},{10,12},{12... | collective-permute-start | bytes 196616 | tf_op jit(solution)/shard_map/ppermute | solution.py:30
  63.8 6.2 %collective-permute-start.14 = (bf16[128,256]{1,0:T(8,128)(2,1)S(1)}, bf16[128,256]{1,0:T(8,128)(2,1)S(1)}, u32[]{:S(2)}, u32[]{:S(2)}) collective-permute-start(bf16[128,256]{1,0:T(8,128)(2,1)S(1)} %get-tuple-element.44.own), channel_id=1, source_target_pairs={{8,0},{16,8},{24,16},{32,24},{40,32},{48,40},{56,48},{64,56},{72,6... | collective-permute-start | bytes 196616 | tf_op jit(solution)/shard_map/ppermute | solution.py:54
  68.1 7.1 %collective-permute-start.13 = (bf16[128,256]{1,0:T(8,128)(2,1)S(1)}, bf16[128,256]{1,0:T(8,128)(2,1)S(1)}, u32[]{:S(2)}, u32[]{:S(2)}) collective-permute-start(bf16[128,256]{1,0:T(8,128)(2,1)S(1)} %get-tuple-element.44.own), channel_id=1, source_target_pairs={{0,8},{8,16},{16,24},{24,32},{32,40},{40,48},{48,56},{56,64},{64,7... | collective-permute-start | bytes 196616 | tf_op jit(solution)/shard_map/ppermute | solution.py:50
  76.1 24.1 %all-to-all-start.2 = ((bf16[16,64,512]{2,1,0:T(8,128)(2,1)}), bf16[16,64,512]{2,1,0:T(8,128)(2,1)S(1)}, u32[]{:S(2)}, u32[]{:S(2)}) async-start(bf16[16,64,512]{2,1,0:T(8,128)(2,1)} %get-tuple-element.50), calls=%async_computation.2 | async-start | bytes 2097152 | tf_op jit(solution)/shard_map/all_to_all | solution.py:38
  80.4 5.0 %collective-permute-start.15 = (bf16[128,256]{1,0:T(8,128)(2,1)S(1)}, bf16[128,256]{1,0:T(8,128)(2,1)S(1)}, u32[]{:S(2)}, u32[]{:S(2)}) collective-permute-start(bf16[128,256]{1,0:T(8,128)(2,1)S(1)} %get-tuple-element.46), channel_id=1, source_target_pairs={{0,2},{2,4},{4,6},{6,0},{1,3},{3,5},{5,7},{7,1},{8,10},{10,12},{12... | collective-permute-start | bytes 196616 | tf_op jit(solution)/shard_map/ppermute | solution.py:235
  80.4 5.0 %collective-permute-start.16 = (bf16[128,256]{1,0:T(8,128)(2,1)S(1)}, bf16[128,256]{1,0:T(8,128)(2,1)S(1)}, u32[]{:S(2)}, u32[]{:S(2)}) collective-permute-start(bf16[128,256]{1,0:T(8,128)(2,1)S(1)} %get-tuple-element.47), channel_id=1, source_target_pairs={{0,4},{2,6},{4,0},{6,2},{1,5},{3,7},{5,1},{7,3},{8,12},{10,14},{12... | collective-permute-start | bytes 196616 | tf_op jit(solution)/shard_map/ppermute | solution.py:237
  81.5 4.8 %collective-permute-start.17 = (bf16[128,256]{1,0:T(8,128)(2,1)S(1)}, bf16[128,256]{1,0:T(8,128)(2,1)S(1)}, u32[]{:S(2)}, u32[]{:S(2)}) collective-permute-start(bf16[128,256]{1,0:T(8,128)(2,1)S(1)} %get-tuple-element.48), channel_id=1, source_target_pairs={{0,6},{2,0},{4,2},{6,4},{1,7},{3,1},{5,3},{7,5},{8,14},{10,8},{12,... | collective-permute-start | bytes 196616 | tf_op jit(solution)/shard_map/ppermute | solution.py:236
  86.3 5.0 %collective-permute-start.18 = (f32[128,256]{1,0:T(8,128)S(1)}, f32[128,256]{1,0:T(8,128)S(1)}, u32[]{:S(2)}, u32[]{:S(2)}) collective-permute-start(f32[128,256]{1,0:T(8,128)S(1)} %shard_map.91.mine), channel_id=1, source_target_pairs={{0,1},{1,0},{2,3},{3,2},{4,5},{5,4},{6,7},{7,6},{8,9},{9,8},{10,11... | collective-permute-start | bytes 393224 | tf_op jit(solution)/shard_map/ppermute | solution.py:46
  91.3 5.1 %collective-permute-start.21 = (bf16[128,256]{1,0:T(8,128)(2,1)S(1)}, bf16[128,256]{1,0:T(8,128)(2,1)S(1)}, u32[]{:S(2)}, u32[]{:S(2)}) collective-permute-start(bf16[128,256]{1,0:T(8,128)(2,1)S(1)} %shard_map.92.x0), channel_id=1, source_target_pairs={{0,6},{2,0},{4,2},{6,4},{1,7},{3,1},{5,3},{7,5},{8,14},{10,8},{12,... | collective-permute-start | bytes 196616 | tf_op jit(solution)/shard_map/ppermute | solution.py:30
  93.8 4.7 %collective-permute-start.20 = (bf16[128,256]{1,0:T(8,128)(2,1)S(1)}, bf16[128,256]{1,0:T(8,128)(2,1)S(1)}, u32[]{:S(2)}, u32[]{:S(2)}) collective-permute-start(bf16[128,256]{1,0:T(8,128)(2,1)S(1)} %shard_map.92.x0), channel_id=1, source_target_pairs={{0,4},{2,6},{4,0},{6,2},{1,5},{3,7},{5,1},{7,3},{8,12},{10,14},{12... | collective-permute-start | bytes 196616 | tf_op jit(solution)/shard_map/ppermute | solution.py:30
  94.2 6.0 %collective-permute-start.19 = (bf16[128,256]{1,0:T(8,128)(2,1)S(1)}, bf16[128,256]{1,0:T(8,128)(2,1)S(1)}, u32[]{:S(2)}, u32[]{:S(2)}) collective-permute-start(bf16[128,256]{1,0:T(8,128)(2,1)S(1)} %shard_map.92.x0), channel_id=1, source_target_pairs={{0,2},{2,4},{4,6},{6,0},{1,3},{3,5},{5,7},{7,1},{8,10},{10,12},{12... | collective-permute-start | bytes 196616 | tf_op jit(solution)/shard_map/ppermute | solution.py:30
  100.7 6.2 %collective-permute-start.23 = (bf16[128,256]{1,0:T(8,128)(2,1)S(1)}, bf16[128,256]{1,0:T(8,128)(2,1)S(1)}, u32[]{:S(2)}, u32[]{:S(2)}) collective-permute-start(bf16[128,256]{1,0:T(8,128)(2,1)S(1)} %get-tuple-element.52.own), channel_id=1, source_target_pairs={{8,0},{16,8},{24,16},{32,24},{40,32},{48,40},{56,48},{64,56},{72,6... | collective-permute-start | bytes 196616 | tf_op jit(solution)/shard_map/ppermute | solution.py:54
  105.0 7.1 %collective-permute-start.22 = (bf16[128,256]{1,0:T(8,128)(2,1)S(1)}, bf16[128,256]{1,0:T(8,128)(2,1)S(1)}, u32[]{:S(2)}, u32[]{:S(2)}) collective-permute-start(bf16[128,256]{1,0:T(8,128)(2,1)S(1)} %get-tuple-element.52.own), channel_id=1, source_target_pairs={{0,8},{8,16},{16,24},{24,32},{32,40},{40,48},{48,56},{56,64},{64,7... | collective-permute-start | bytes 196616 | tf_op jit(solution)/shard_map/ppermute | solution.py:50
  113.1 5.1 %collective-permute-start.24 = (bf16[128,256]{1,0:T(8,128)(2,1)S(1)}, bf16[128,256]{1,0:T(8,128)(2,1)S(1)}, u32[]{:S(2)}, u32[]{:S(2)}) collective-permute-start(bf16[128,256]{1,0:T(8,128)(2,1)S(1)} %get-tuple-element.54), channel_id=1, source_target_pairs={{0,2},{2,4},{4,6},{6,0},{1,3},{3,5},{5,7},{7,1},{8,10},{10,12},{12... | collective-permute-start | bytes 196616 | tf_op jit(solution)/shard_map/ppermute | solution.py:235
  113.2 5.0 %collective-permute-start.25 = (bf16[128,256]{1,0:T(8,128)(2,1)S(1)}, bf16[128,256]{1,0:T(8,128)(2,1)S(1)}, u32[]{:S(2)}, u32[]{:S(2)}) collective-permute-start(bf16[128,256]{1,0:T(8,128)(2,1)S(1)} %get-tuple-element.55), channel_id=1, source_target_pairs={{0,4},{2,6},{4,0},{6,2},{1,5},{3,7},{5,1},{7,3},{8,12},{10,14},{12... | collective-permute-start | bytes 196616 | tf_op jit(solution)/shard_map/ppermute | solution.py:237
  114.2 4.6 %collective-permute-start.26 = (bf16[128,256]{1,0:T(8,128)(2,1)S(1)}, bf16[128,256]{1,0:T(8,128)(2,1)S(1)}, u32[]{:S(2)}, u32[]{:S(2)}) collective-permute-start(bf16[128,256]{1,0:T(8,128)(2,1)S(1)} %get-tuple-element.56), channel_id=1, source_target_pairs={{0,6},{2,0},{4,2},{6,4},{1,7},{3,1},{5,3},{7,5},{8,14},{10,8},{12,... | collective-permute-start | bytes 196616 | tf_op jit(solution)/shard_map/ppermute | solution.py:236
  118.8 4.9 %collective-permute-start.27 = (f32[128,128]{1,0:T(8,128)S(1)}, f32[128,128]{1,0:T(8,128)S(1)}, u32[]{:S(2)}, u32[]{:S(2)}) collective-permute-start(f32[128,128]{1,0:T(8,128)S(1)} %get-tuple-element.58), channel_id=1, source_target_pairs={{0,1},{1,0},{2,3},{3,2},{4,5},{5,4},{6,7},{7,6},{8,9},{9,8},{10,11... | collective-permute-start | bytes 196616 | tf_op jit(solution)/shard_map/ppermute | solution.py:46
  (3 other events, 52.0 us)

commit v6 on v5

--- a/solution.py
+++ b/solution.py
@@ -27,7 +27,10 @@
 
 
 def spread(a, axis):
-    return [lax.ppermute(a, axis, turn(k)) for k in (1, 3, 2)]
+    sent = []
+    for k in (1, 3, 2):
+        sent.append(lax.ppermute(a, axis, turn(k)))
+    return sent
 
 
 def in_order(a, three):
@@ -76,27 +79,28 @@
     return jax.ShapeDtypeStruct(shape, dtype)
 
 
-def pack_body(
-    wq, wk, wv, wo, first, rest, wq_in, wk_in, wv_in, wo_in, sems
-):
-    pairs = ((wq, wq_in), (wk, wk_in), (wv, wv_in), (wo, wo_in))
+def fetch(pairs, sems):
     copies = [pltpu.make_async_copy(a, b, sems.at[n]) for n, (a, b) in enumerate(pairs)]
     for copy in copies:
         copy.start()
     for copy in copies:
         copy.wait()
-    whole = jnp.concatenate([wq_in[0], wk_in[0], wv_in[0], wo_in[0]], axis=1)
+
+
+def pack_body(wq, wk, wv, wo, first, parts, sems):
+    fetch([(w.at[0], parts.at[n]) for n, w in enumerate((wq, wk, wv, wo))], sems)
+    whole = jnp.concatenate([parts[n] for n in range(4)], axis=1)
     for n in range(16):
         first[n] = whole
-    for layer in (1, 2):
-        for n, part in enumerate((wq_in, wk_in, wv_in, wo_in)):
-            rest[layer - 1, :, n * 128 : n * 128 + 128] = part[layer]
-
-
-def many_body(rest, many1, many2):
-    for n in range(16):
-        many1[n] = rest[0]
-        many2[n] = rest[1]
+
+
+def many_body(wq, wk, wv, wo, many1, many2, parts, sems):
+    pairs = [(w.at[1:3], parts.at[n]) for n, w in enumerate((wq, wk, wv, wo))]
+    fetch(pairs, sems)
+    for layer, many in enumerate((many1, many2)):
+        whole = jnp.concatenate([parts[n, layer] for n in range(4)], axis=1)
+        for n in range(16):
+            many[n] = whole
 
 
 def table_body(bias, before, own, after, table, wide):
@@ -240,19 +244,20 @@
 
 def local(tokens, norm_gain, w_query, w_key, w_value, w_out, offset_bias, documents):
     hbm = pl.BlockSpec(memory_space=pltpu.HBM)
-    first, rest = call(
-        pack_body,
-        [shaped(16, 64, 512), shaped(2, 64, 512)],
-        *[
-            pltpu.with_memory_space_constraint(a, pltpu.HBM)
-            for a in (w_query, w_key, w_value, jnp.swapaxes(w_out, 1, 2))
-        ],
-        in_specs=[hbm] * 4,
-        scratch=[pltpu.VMEM((3, 64, 128), BF16)] * 4 + [pltpu.SemaphoreType.DMA((4,))],
+    held = [
+        pltpu.with_memory_space_constraint(a, pltpu.HBM)
+        for a in (w_query, w_key, w_value, jnp.swapaxes(w_out, 1, 2))
+    ]
+    first = call(
+        pack_body, shaped(16, 64, 512), *held, in_specs=[hbm] * 4,
+        scratch=[pltpu.VMEM((4, 64, 128), BF16), pltpu.SemaphoreType.DMA((4,))],
     )
     weights = gather_rows(first)
     near_y = jnp.stack(in_order(tokens, spread(tokens, "y")))
-    many1, many2 = call(many_body, [shaped(16, 64, 512)] * 2, rest)
+    many1, many2 = call(
+        many_body, [shaped(16, 64, 512)] * 2, *held, in_specs=[hbm] * 4,
+        scratch=[pltpu.VMEM((4, 2, 64, 128), BF16), pltpu.SemaphoreType.DMA((4,))],
+    )
     near_partner = swap(after_this(near_y, many1))
 
     q, kv = call(

time: 125 us -> 125 us (level)
  transfers between devices with their start and end apart: 31 -> 31, of which waited for: 21 -> 21; matrix products, arithmetic and copies ran while one was open for 0% -> 0% of each run, Pallas kernels for 1% -> 2%
where the time goes in v6:
time: 125 us; the launch traced here: 124 us
  starting transfers between devices  71.1 us (57%)
  waiting for transfers between devices  43 us (34%)
  Pallas kernels  9.86 us (8%)
    ppermute x3, waiting for transfers between devices, from_before(): return lax.ppermute(a, SP, [(i, i + 1) for i in range(15)])  15.6 us
    ppermute x4, starting transfers between devices, swap(): return lax.ppermute(a, 'c', [(0, 1), (1, 0)])  15.6 us
    all_to_all x3, starting transfers between devices, gather_rows(): return lax.all_to_all(a, SP, 0, 0, tiled=True).reshape(1024, 512)  15.3 us
    ppermute x3, starting transfers between devices, from_after(): return lax.ppermute(a, SP, [(i + 1, i) for i in range(15)])  13.3 us
    ppermute x9, waiting for transfers between devices, spread(): sent.append(lax.ppermute(a, axis, turn(k)))  12.3 us
    ppermute x9, starting transfers between devices, spread(): sent.append(lax.ppermute(a, axis, turn(k)))  10.6 us
    pallas_call x15, Pallas kernels, call(): pl.pallas_call(body, out_shape=outs, **specs, scratch_shapes=list(scratch...  9.86 us
    ppermute x3, starting transfers between devices, from_before(): return lax.ppermute(a, SP, [(i, i + 1) for i in range(15)])  5.76 us
  transfers between devices with their start and end apart: 31, of which 21 were waited for; matrix products, arithmetic and copies ran while one was open for 0% of the time, Pallas kernels for 2%

profile of v6, /device:TPU:33, one launch (start us, length us, event | category | flops | bytes accessed | tf_op | source)
XLA Modules:
  0.0 124.3 jit_solution(5807461844010562955)
XLA Ops:
  0.0 1.9 %shard_map.83 = bf16[16,64,512]{2,1,0:T(8,128)(2,1)} custom-call(bf16[3,64,128]{2,1,0:T(8,128)(2,1)} %wq.3, bf16[3,64,128]{2,1,0:T(8,128)(2,1)} %wk.3, bf16[3,64,128]{2,1,0:T(8,128)(2,1)} %wv.3, bf16[3,64,128]{2,1,0:T(8,128)(2,1)} %bitcast.16), custom_call_target="tpu_custom_call" | custom-call | tf_op jit(solution)/shard_map/pallas_call | solution.py:69
  1.9 7.5 %all-to-all-start = ((bf16[16,64,512]{2,1,0:T(8,128)(2,1)}), bf16[16,64,512]{2,1,0:T(8,128)(2,1)S(1)}, u32[]{:S(2)}, u32[]{:S(2)}) async-start(bf16[16,64,512]{2,1,0:T(8,128)(2,1)} %shard_map.83), calls=%async_computation | async-start | bytes 2097152 | tf_op jit(solution)/shard_map/all_to_all | solution.py:41
  12.3 1.6 %collective-permute-start.1 = (bf16[128,128]{1,0:T(8,128)(2,1)S(1)}, bf16[128,128]{1,0:T(8,128)(2,1)S(1)}, u32[]{:S(2)}, u32[]{:S(2)}) collective-permute-start(bf16[128,128]{1,0:T(8,128)(2,1)S(1)} %copy-done.3), channel_id=1, source_target_pairs={{0,4},{2,6},{4,0},{6,2},{1,5},{3,7},{5,1},{7,3},{8,12},{10,14},{12... | collective-permute-start | bytes 98312 | tf_op jit(solution)/shard_map/ppermute | solution.py:32
  13.9 2.3 %shard_map.82 = (bf16[16,64,512]{2,1,0:T(8,128)(2,1)}, bf16[16,64,512]{2,1,0:T(8,128)(2,1)}) custom-call(bf16[3,64,128]{2,1,0:T(8,128)(2,1)} %wq.3, bf16[3,64,128]{2,1,0:T(8,128)(2,1)} %wk.3, bf16[3,64,128]{2,1,0:T(8,128)(2,1)} %wv.3, bf16[3,64,128]{2,1,0:T(8,128)(2,1)} %bitcast.17), custom_call_target="tpu_custom_call" | custom-call | tf_op jit(solution)/shard_map/pallas_call | solution.py:69
  17.1 2.4 %collective-permute-start.3 = (bf16[4,128,128]{2,1,0:T(8,128)(2,1)S(1)}, bf16[4,128,128]{2,1,0:T(8,128)(2,1)S(1)}, u32[]{:S(2)}, u32[]{:S(2)}) collective-permute-start(bf16[4,128,128]{2,1,0:T(8,128)(2,1)S(1)} %pad_maximum_fusion.own), channel_id=1, source_target_pairs={{0,1},{1,0},{2,3},{3,2},{4,5},{5,4},{6,7},{7,6},{8,9},{9,8},{10,11... | collective-permute-start | bytes 393224 | tf_op jit(solution)/shard_map/ppermute | solution.py:49
  20.5 2.9 %all-to-all-done = bf16[16,64,512]{2,1,0:T(8,128)(2,1)S(1)} async-done(((bf16[16,64,512]{2,1,0:T(8,128)(2,1)}), bf16[16,64,512]{2,1,0:T(8,128)(2,1)S(1)}, u32[]{:S(2)}, u32[]{:S(2)}) %all-to-all-start) | async-done | bytes 1048608 | tf_op jit(solution)/shard_map/all_to_all | solution.py:41
  23.9 4.6 %collective-permute-start.5 = (bf16[144,256]{1,0:T(8,128)(2,1)S(1)}, bf16[144,256]{1,0:T(8,128)(2,1)S(1)}, u32[]{:S(2)}, u32[]{:S(2)}) collective-permute-start(bf16[144,256]{1,0:T(8,128)(2,1)S(1)} %get-tuple-element.33.own), channel_id=1, source_target_pairs={{8,0},{16,8},{24,16},{32,24},{40,32},{48,40},{56,48},{64,56},{72,6... | collective-permute-start | bytes 221192 | tf_op jit(solution)/shard_map/ppermute | solution.py:57
  28.6 1.9 %collective-permute-start.4 = (bf16[144,256]{1,0:T(8,128)(2,1)S(1)}, bf16[144,256]{1,0:T(8,128)(2,1)S(1)}, u32[]{:S(2)}, u32[]{:S(2)}) collective-permute-start(bf16[144,256]{1,0:T(8,128)(2,1)S(1)} %get-tuple-element.33.own), channel_id=1, source_target_pairs={{0,8},{8,16},{16,24},{24,32},{32,40},{40,48},{48,56},{56,64},{64,7... | collective-permute-start | bytes 221192 | tf_op jit(solution)/shard_map/ppermute | solution.py:53
  30.5 5.3 %collective-permute-done.4.before = bf16[144,256]{1,0:T(8,128)(2,1)S(1)} collective-permute-done((bf16[144,256]{1,0:T(8,128)(2,1)S(1)}, bf16[144,256]{1,0:T(8,128)(2,1)S(1)}, u32[]{:S(2)}, u32[]{:S(2)}) %collective-permute-start.4) | collective-permute-done | bytes 73760 | tf_op jit(solution)/shard_map/ppermute | solution.py:53
  37.3 3.6 %all-to-all-start.1 = ((bf16[16,64,512]{2,1,0:T(8,128)(2,1)}), bf16[16,64,512]{2,1,0:T(8,128)(2,1)S(1)}, u32[]{:S(2)}, u32[]{:S(2)}) async-start(bf16[16,64,512]{2,1,0:T(8,128)(2,1)} %get-tuple-element.38), calls=%async_computation.1 | async-start | bytes 2097152 | tf_op jit(solution)/shard_map/all_to_all | solution.py:41
  42.3 2.6 %collective-permute-start.7 = (bf16[128,256]{1,0:T(8,128)(2,1)S(1)}, bf16[128,256]{1,0:T(8,128)(2,1)S(1)}, u32[]{:S(2)}, u32[]{:S(2)}) collective-permute-start(bf16[128,256]{1,0:T(8,128)(2,1)S(1)} %get-tuple-element.36), channel_id=1, source_target_pairs={{0,4},{2,6},{4,0},{6,2},{1,5},{3,7},{5,1},{7,3},{8,12},{10,14},{12... | collective-permute-start | bytes 196616 | tf_op jit(solution)/shard_map/ppermute | solution.py:241
  48.3 5.2 %collective-permute-start.9 = (f32[128,256]{1,0:T(8,128)S(1)}, f32[128,256]{1,0:T(8,128)S(1)}, u32[]{:S(2)}, u32[]{:S(2)}) collective-permute-start(f32[128,256]{1,0:T(8,128)S(1)} %shard_map.87.mine), channel_id=1, source_target_pairs={{0,1},{1,0},{2,3},{3,2},{4,5},{5,4},{6,7},{7,6},{8,9},{9,8},{10,11... | collective-permute-start | bytes 393224 | tf_op jit(solution)/shard_map/ppermute | solution.py:49
  54.6 2.3 %collective-permute-start.12 = (bf16[128,256]{1,0:T(8,128)(2,1)S(1)}, bf16[128,256]{1,0:T(8,128)(2,1)S(1)}, u32[]{:S(2)}, u32[]{:S(2)}) collective-permute-start(bf16[128,256]{1,0:T(8,128)(2,1)S(1)} %shard_map.88.x0), channel_id=1, source_target_pairs={{0,6},{2,0},{4,2},{6,4},{1,7},{3,1},{5,3},{7,5},{8,14},{10,8},{12,... | collective-permute-start | bytes 196616 | tf_op jit(solution)/shard_map/ppermute | solution.py:32
  58.2 3.4 %collective-permute-done.11.x2 = bf16[128,256]{1,0:T(8,128)(2,1)S(1)} collective-permute-done((bf16[128,256]{1,0:T(8,128)(2,1)S(1)}, bf16[128,256]{1,0:T(8,128)(2,1)S(1)}, u32[]{:S(2)}, u32[]{:S(2)}) %collective-permute-start.11) | collective-permute-done | bytes 65568 | tf_op jit(solution)/shard_map/ppermute | solution.py:32
  61.6 1.6 %collective-permute-done.10.x1 = bf16[128,256]{1,0:T(8,128)(2,1)S(1)} collective-permute-done((bf16[128,256]{1,0:T(8,128)(2,1)S(1)}, bf16[128,256]{1,0:T(8,128)(2,1)S(1)}, u32[]{:S(2)}, u32[]{:S(2)}) %collective-permute-start.10) | collective-permute-done | bytes 65568 | tf_op jit(solution)/shard_map/ppermute | solution.py:32
  63.8 4.3 %collective-permute-start.14 = (bf16[128,256]{1,0:T(8,128)(2,1)S(1)}, bf16[128,256]{1,0:T(8,128)(2,1)S(1)}, u32[]{:S(2)}, u32[]{:S(2)}) collective-permute-start(bf16[128,256]{1,0:T(8,128)(2,1)S(1)} %get-tuple-element.40.own), channel_id=1, source_target_pairs={{8,0},{16,8},{24,16},{32,24},{40,32},{48,40},{56,48},{64,56},{72,6... | collective-permute-start | bytes 196616 | tf_op jit(solution)/shard_map/ppermute | solution.py:57
  68.1 1.9 %collective-permute-start.13 = (bf16[128,256]{1,0:T(8,128)(2,1)S(1)}, bf16[128,256]{1,0:T(8,128)(2,1)S(1)}, u32[]{:S(2)}, u32[]{:S(2)}) collective-permute-start(bf16[128,256]{1,0:T(8,128)(2,1)S(1)} %get-tuple-element.40.own), channel_id=1, source_target_pairs={{0,8},{8,16},{16,24},{24,32},{32,40},{40,48},{48,56},{56,64},{64,7... | collective-permute-start | bytes 196616 | tf_op jit(solution)/shard_map/ppermute | solution.py:53
  70.0 5.2 %collective-permute-done.13.before = bf16[128,256]{1,0:T(8,128)(2,1)S(1)} collective-permute-done((bf16[128,256]{1,0:T(8,128)(2,1)S(1)}, bf16[128,256]{1,0:T(8,128)(2,1)S(1)}, u32[]{:S(2)}, u32[]{:S(2)}) %collective-permute-start.13) | collective-permute-done | bytes 65568 | tf_op jit(solution)/shard_map/ppermute | solution.py:53
  76.1 4.3 %all-to-all-start.2 = ((bf16[16,64,512]{2,1,0:T(8,128)(2,1)}), bf16[16,64,512]{2,1,0:T(8,128)(2,1)S(1)}, u32[]{:S(2)}, u32[]{:S(2)}) async-start(bf16[16,64,512]{2,1,0:T(8,128)(2,1)} %get-tuple-element.46), calls=%async_computation.2 | async-start | bytes 2097152 | tf_op jit(solution)/shard_map/all_to_all | solution.py:41
  81.5 1.6 %collective-permute-start.17 = (bf16[128,256]{1,0:T(8,128)(2,1)S(1)}, bf16[128,256]{1,0:T(8,128)(2,1)S(1)}, u32[]{:S(2)}, u32[]{:S(2)}) collective-permute-start(bf16[128,256]{1,0:T(8,128)(2,1)S(1)} %get-tuple-element.44), channel_id=1, source_target_pairs={{0,6},{2,0},{4,2},{6,4},{1,7},{3,1},{5,3},{7,5},{8,14},{10,8},{12,... | collective-permute-start | bytes 196616 | tf_op jit(solution)/shard_map/ppermute | solution.py:240
  83.1 2.3 %collective-permute-done.15.r1 = bf16[128,256]{1,0:T(8,128)(2,1)S(1)} collective-permute-done((bf16[128,256]{1,0:T(8,128)(2,1)S(1)}, bf16[128,256]{1,0:T(8,128)(2,1)S(1)}, u32[]{:S(2)}, u32[]{:S(2)}) %collective-permute-start.15) | collective-permute-done | bytes 65568 | tf_op jit(solution)/shard_map/ppermute | solution.py:239
  86.3 4.0 %collective-permute-start.18 = (f32[128,256]{1,0:T(8,128)S(1)}, f32[128,256]{1,0:T(8,128)S(1)}, u32[]{:S(2)}, u32[]{:S(2)}) collective-permute-start(f32[128,256]{1,0:T(8,128)S(1)} %shard_map.91.mine), channel_id=1, source_target_pairs={{0,1},{1,0},{2,3},{3,2},{4,5},{5,4},{6,7},{7,6},{8,9},{9,8},{10,11... | collective-permute-start | bytes 393224 | tf_op jit(solution)/shard_map/ppermute | solution.py:49
  91.3 2.5 %collective-permute-start.21 = (bf16[128,256]{1,0:T(8,128)(2,1)S(1)}, bf16[128,256]{1,0:T(8,128)(2,1)S(1)}, u32[]{:S(2)}, u32[]{:S(2)}) collective-permute-start(bf16[128,256]{1,0:T(8,128)(2,1)S(1)} %shard_map.92.x0), channel_id=1, source_target_pairs={{0,6},{2,0},{4,2},{6,4},{1,7},{3,1},{5,3},{7,5},{8,14},{10,8},{12,... | collective-permute-start | bytes 196616 | tf_op jit(solution)/shard_map/ppermute | solution.py:32
  94.5 2.0 %collective-permute-done.21.x3 = bf16[128,256]{1,0:T(8,128)(2,1)S(1)} collective-permute-done((bf16[128,256]{1,0:T(8,128)(2,1)S(1)}, bf16[128,256]{1,0:T(8,128)(2,1)S(1)}, u32[]{:S(2)}, u32[]{:S(2)}) %collective-permute-start.21) | collective-permute-done | bytes 65568 | tf_op jit(solution)/shard_map/ppermute | solution.py:32
  96.5 2.0 %collective-permute-done.20.x2 = bf16[128,256]{1,0:T(8,128)(2,1)S(1)} collective-permute-done((bf16[128,256]{1,0:T(8,128)(2,1)S(1)}, bf16[128,256]{1,0:T(8,128)(2,1)S(1)}, u32[]{:S(2)}, u32[]{:S(2)}) %collective-permute-start.20) | collective-permute-done | bytes 65568 | tf_op jit(solution)/shard_map/ppermute | solution.py:32
  98.5 1.7 %collective-permute-done.19.x1 = bf16[128,256]{1,0:T(8,128)(2,1)S(1)} collective-permute-done((bf16[128,256]{1,0:T(8,128)(2,1)S(1)}, bf16[128,256]{1,0:T(8,128)(2,1)S(1)}, u32[]{:S(2)}, u32[]{:S(2)}) %collective-permute-start.19) | collective-permute-done | bytes 65568 | tf_op jit(solution)/shard_map/ppermute | solution.py:32
  100.7 4.3 %collective-permute-start.23 = (bf16[128,256]{1,0:T(8,128)(2,1)S(1)}, bf16[128,256]{1,0:T(8,128)(2,1)S(1)}, u32[]{:S(2)}, u32[]{:S(2)}) collective-permute-start(bf16[128,256]{1,0:T(8,128)(2,1)S(1)} %get-tuple-element.48.own), channel_id=1, source_target_pairs={{8,0},{16,8},{24,16},{32,24},{40,32},{48,40},{56,48},{64,56},{72,6... | collective-permute-start | bytes 196616 | tf_op jit(solution)/shard_map/ppermute | solution.py:57
  105.0 1.9 %collective-permute-start.22 = (bf16[128,256]{1,0:T(8,128)(2,1)S(1)}, bf16[128,256]{1,0:T(8,128)(2,1)S(1)}, u32[]{:S(2)}, u32[]{:S(2)}) collective-permute-start(bf16[128,256]{1,0:T(8,128)(2,1)S(1)} %get-tuple-element.48.own), channel_id=1, source_target_pairs={{0,8},{8,16},{16,24},{24,32},{32,40},{40,48},{48,56},{56,64},{64,7... | collective-permute-start | bytes 196616 | tf_op jit(solution)/shard_map/ppermute | solution.py:53
  107.0 5.2 %collective-permute-done.22.before = bf16[128,256]{1,0:T(8,128)(2,1)S(1)} collective-permute-done((bf16[128,256]{1,0:T(8,128)(2,1)S(1)}, bf16[128,256]{1,0:T(8,128)(2,1)S(1)}, u32[]{:S(2)}, u32[]{:S(2)}) %collective-permute-start.22) | collective-permute-done | bytes 65568 | tf_op jit(solution)/shard_map/ppermute | solution.py:53
  114.2 1.7 %collective-permute-start.26 = (bf16[128,256]{1,0:T(8,128)(2,1)S(1)}, bf16[128,256]{1,0:T(8,128)(2,1)S(1)}, u32[]{:S(2)}, u32[]{:S(2)}) collective-permute-start(bf16[128,256]{1,0:T(8,128)(2,1)S(1)} %get-tuple-element.52), channel_id=1, source_target_pairs={{0,6},{2,0},{4,2},{6,4},{1,7},{3,1},{5,3},{7,5},{8,14},{10,8},{12,... | collective-permute-start | bytes 196616 | tf_op jit(solution)/shard_map/ppermute | solution.py:240
  115.9 2.3 %collective-permute-done.24.r1 = bf16[128,256]{1,0:T(8,128)(2,1)S(1)} collective-permute-done((bf16[128,256]{1,0:T(8,128)(2,1)S(1)}, bf16[128,256]{1,0:T(8,128)(2,1)S(1)}, u32[]{:S(2)}, u32[]{:S(2)}) %collective-permute-start.24) | collective-permute-done | bytes 65568 | tf_op jit(solution)/shard_map/ppermute | solution.py:239
  118.8 4.0 %collective-permute-start.27 = (f32[128,128]{1,0:T(8,128)S(1)}, f32[128,128]{1,0:T(8,128)S(1)}, u32[]{:S(2)}, u32[]{:S(2)}) collective-permute-start(f32[128,128]{1,0:T(8,128)S(1)} %get-tuple-element.54), channel_id=1, source_target_pairs={{0,1},{1,0},{2,3},{3,2},{4,5},{5,4},{6,7},{7,6},{8,9},{9,8},{10,11... | collective-permute-start | bytes 196616 | tf_op jit(solution)/shard_map/ppermute | solution.py:49
  (54 shorter events, 23.7 us)
Async XLA Ops:
  1.9 21.4 %all-to-all-start = ((bf16[16,64,512]{2,1,0:T(8,128)(2,1)}), bf16[16,64,512]{2,1,0:T(8,128)(2,1)S(1)}, u32[]{:S(2)}, u32[]{:S(2)}) async-start(bf16[16,64,512]{2,1,0:T(8,128)(2,1)} %shard_map.83), calls=%async_computation | async-start | bytes 2097152 | tf_op jit(solution)/shard_map/all_to_all | solution.py:41
  9.4 26.4 %copy-start.1 = (f32[3,2,8,16]{3,2,1,0:T(8,128)S(1)}, f32[3,2,8,16]{3,2,1,0:T(8,128)}, u32[]{:S(2)}) copy-start(f32[3,2,8,16]{3,2,1,0:T(8,128)} %bias.1) | copy-start | bytes 9220
  9.4 6.7 %collective-permute-start = (bf16[128,128]{1,0:T(8,128)(2,1)S(1)}, bf16[128,128]{1,0:T(8,128)(2,1)S(1)}, u32[]{:S(2)}, u32[]{:S(2)}) collective-permute-start(bf16[128,128]{1,0:T(8,128)(2,1)S(1)} %copy-done.3), channel_id=1, source_target_pairs={{0,2},{2,4},{4,6},{6,0},{1,3},{3,5},{5,7},{7,1},{8,10},{10,12},{12... | collective-permute-start | bytes 98312 | tf_op jit(solution)/shard_map/ppermute | solution.py:32
  10.8 5.4 %collective-permute-start.2 = (bf16[128,128]{1,0:T(8,128)(2,1)S(1)}, bf16[128,128]{1,0:T(8,128)(2,1)S(1)}, u32[]{:S(2)}, u32[]{:S(2)}) collective-permute-start(bf16[128,128]{1,0:T(8,128)(2,1)S(1)} %copy-done.3), channel_id=1, source_target_pairs={{0,6},{2,0},{4,2},{6,4},{1,7},{3,1},{5,3},{7,5},{8,14},{10,8},{12,... | collective-permute-start | bytes 98312 | tf_op jit(solution)/shard_map/ppermute | solution.py:32
  12.3 4.7 %collective-permute-start.1 = (bf16[128,128]{1,0:T(8,128)(2,1)S(1)}, bf16[128,128]{1,0:T(8,128)(2,1)S(1)}, u32[]{:S(2)}, u32[]{:S(2)}) collective-permute-start(bf16[128,128]{1,0:T(8,128)(2,1)S(1)} %copy-done.3), channel_id=1, source_target_pairs={{0,4},{2,6},{4,0},{6,2},{1,5},{3,7},{5,1},{7,3},{8,12},{10,14},{12... | collective-permute-start | bytes 98312 | tf_op jit(solution)/shard_map/ppermute | solution.py:32
  17.1 3.4 %collective-permute-start.3 = (bf16[4,128,128]{2,1,0:T(8,128)(2,1)S(1)}, bf16[4,128,128]{2,1,0:T(8,128)(2,1)S(1)}, u32[]{:S(2)}, u32[]{:S(2)}) collective-permute-start(bf16[4,128,128]{2,1,0:T(8,128)(2,1)S(1)} %pad_maximum_fusion.own), channel_id=1, source_target_pairs={{0,1},{1,0},{2,3},{3,2},{4,5},{5,4},{6,7},{7,6},{8,9},{9,8},{10,11... | collective-permute-start | bytes 393224 | tf_op jit(solution)/shard_map/ppermute | solution.py:49
  23.9 6.6 %collective-permute-start.5 = (bf16[144,256]{1,0:T(8,128)(2,1)S(1)}, bf16[144,256]{1,0:T(8,128)(2,1)S(1)}, u32[]{:S(2)}, u32[]{:S(2)}) collective-permute-start(bf16[144,256]{1,0:T(8,128)(2,1)S(1)} %get-tuple-element.33.own), channel_id=1, source_target_pairs={{8,0},{16,8},{24,16},{32,24},{40,32},{48,40},{56,48},{64,56},{72,6... | collective-permute-start | bytes 221192 | tf_op jit(solution)/shard_map/ppermute | solution.py:57
  28.6 7.2 %collective-permute-start.4 = (bf16[144,256]{1,0:T(8,128)(2,1)S(1)}, bf16[144,256]{1,0:T(8,128)(2,1)S(1)}, u32[]{:S(2)}, u32[]{:S(2)}) collective-permute-start(bf16[144,256]{1,0:T(8,128)(2,1)S(1)} %get-tuple-element.33.own), channel_id=1, source_target_pairs={{0,8},{8,16},{16,24},{24,32},{32,40},{40,48},{48,56},{56,64},{64,7... | collective-permute-start | bytes 221192 | tf_op jit(solution)/shard_map/ppermute | solution.py:53
  37.3 25.9 %all-to-all-start.1 = ((bf16[16,64,512]{2,1,0:T(8,128)(2,1)}), bf16[16,64,512]{2,1,0:T(8,128)(2,1)S(1)}, u32[]{:S(2)}, u32[]{:S(2)}) async-start(bf16[16,64,512]{2,1,0:T(8,128)(2,1)} %get-tuple-element.38), calls=%async_computation.1 | async-start | bytes 2097152 | tf_op jit(solution)/shard_map/all_to_all | solution.py:41
  40.9 5.1 %collective-permute-start.6 = (bf16[128,256]{1,0:T(8,128)(2,1)S(1)}, bf16[128,256]{1,0:T(8,128)(2,1)S(1)}, u32[]{:S(2)}, u32[]{:S(2)}) collective-permute-start(bf16[128,256]{1,0:T(8,128)(2,1)S(1)} %get-tuple-element.35), channel_id=1, source_target_pairs={{0,2},{2,4},{4,6},{6,0},{1,3},{3,5},{5,7},{7,1},{8,10},{10,12},{12... | collective-permute-start | bytes 196616 | tf_op jit(solution)/shard_map/ppermute | solution.py:239
  42.3 5.0 %collective-permute-start.7 = (bf16[128,256]{1,0:T(8,128)(2,1)S(1)}, bf16[128,256]{1,0:T(8,128)(2,1)S(1)}, u32[]{:S(2)}, u32[]{:S(2)}) collective-permute-start(bf16[128,256]{1,0:T(8,128)(2,1)S(1)} %get-tuple-element.36), channel_id=1, source_target_pairs={{0,4},{2,6},{4,0},{6,2},{1,5},{3,7},{5,1},{7,3},{8,12},{10,14},{12... | collective-permute-start | bytes 196616 | tf_op jit(solution)/shard_map/ppermute | solution.py:241
  44.9 3.4 %collective-permute-start.8 = (bf16[128,256]{1,0:T(8,128)(2,1)S(1)}, bf16[128,256]{1,0:T(8,128)(2,1)S(1)}, u32[]{:S(2)}, u32[]{:S(2)}) collective-permute-start(bf16[128,256]{1,0:T(8,128)(2,1)S(1)} %get-tuple-element.37), channel_id=1, source_target_pairs={{0,6},{2,0},{4,2},{6,4},{1,7},{3,1},{5,3},{7,5},{8,14},{10,8},{12,... | collective-permute-start | bytes 196616 | tf_op jit(solution)/shard_map/ppermute | solution.py:240
  48.3 6.2 %collective-permute-start.9 = (f32[128,256]{1,0:T(8,128)S(1)}, f32[128,256]{1,0:T(8,128)S(1)}, u32[]{:S(2)}, u32[]{:S(2)}) collective-permute-start(f32[128,256]{1,0:T(8,128)S(1)} %shard_map.87.mine), channel_id=1, source_target_pairs={{0,1},{1,0},{2,3},{3,2},{4,5},{5,4},{6,7},{7,6},{8,9},{9,8},{10,11... | collective-permute-start | bytes 393224 | tf_op jit(solution)/shard_map/ppermute | solution.py:49
  54.6 3.7 %collective-permute-start.12 = (bf16[128,256]{1,0:T(8,128)(2,1)S(1)}, bf16[128,256]{1,0:T(8,128)(2,1)S(1)}, u32[]{:S(2)}, u32[]{:S(2)}) collective-permute-start(bf16[128,256]{1,0:T(8,128)(2,1)S(1)} %shard_map.88.x0), channel_id=1, source_target_pairs={{0,6},{2,0},{4,2},{6,4},{1,7},{3,1},{5,3},{7,5},{8,14},{10,8},{12,... | collective-permute-start | bytes 196616 | tf_op jit(solution)/shard_map/ppermute | solution.py:32
  56.9 4.7 %collective-permute-start.11 = (bf16[128,256]{1,0:T(8,128)(2,1)S(1)}, bf16[128,256]{1,0:T(8,128)(2,1)S(1)}, u32[]{:S(2)}, u32[]{:S(2)}) collective-permute-start(bf16[128,256]{1,0:T(8,128)(2,1)S(1)} %shard_map.88.x0), channel_id=1, source_target_pairs={{0,4},{2,6},{4,0},{6,2},{1,5},{3,7},{5,1},{7,3},{8,12},{10,14},{12... | collective-permute-start | bytes 196616 | tf_op jit(solution)/shard_map/ppermute | solution.py:32
  56.9 6.3 %collective-permute-start.10 = (bf16[128,256]{1,0:T(8,128)(2,1)S(1)}, bf16[128,256]{1,0:T(8,128)(2,1)S(1)}, u32[]{:S(2)}, u32[]{:S(2)}) collective-permute-start(bf16[128,256]{1,0:T(8,128)(2,1)S(1)} %shard_map.88.x0), channel_id=1, source_target_pairs={{0,2},{2,4},{4,6},{6,0},{1,3},{3,5},{5,7},{7,1},{8,10},{10,12},{12... | collective-permute-start | bytes 196616 | tf_op jit(solution)/shard_map/ppermute | solution.py:32
  63.8 6.2 %collective-permute-start.14 = (bf16[128,256]{1,0:T(8,128)(2,1)S(1)}, bf16[128,256]{1,0:T(8,128)(2,1)S(1)}, u32[]{:S(2)}, u32[]{:S(2)}) collective-permute-start(bf16[128,256]{1,0:T(8,128)(2,1)S(1)} %get-tuple-element.40.own), channel_id=1, source_target_pairs={{8,0},{16,8},{24,16},{32,24},{40,32},{48,40},{56,48},{64,56},{72,6... | collective-permute-start | bytes 196616 | tf_op jit(solution)/shard_map/ppermute | solution.py:57
  68.1 7.1 %collective-permute-start.13 = (bf16[128,256]{1,0:T(8,128)(2,1)S(1)}, bf16[128,256]{1,0:T(8,128)(2,1)S(1)}, u32[]{:S(2)}, u32[]{:S(2)}) collective-permute-start(bf16[128,256]{1,0:T(8,128)(2,1)S(1)} %get-tuple-element.40.own), channel_id=1, source_target_pairs={{0,8},{8,16},{16,24},{24,32},{32,40},{40,48},{48,56},{56,64},{64,7... | collective-permute-start | bytes 196616 | tf_op jit(solution)/shard_map/ppermute | solution.py:53
  76.1 24.1 %all-to-all-start.2 = ((bf16[16,64,512]{2,1,0:T(8,128)(2,1)}), bf16[16,64,512]{2,1,0:T(8,128)(2,1)S(1)}, u32[]{:S(2)}, u32[]{:S(2)}) async-start(bf16[16,64,512]{2,1,0:T(8,128)(2,1)} %get-tuple-element.46), calls=%async_computation.2 | async-start | bytes 2097152 | tf_op jit(solution)/shard_map/all_to_all | solution.py:41
  80.4 5.0 %collective-permute-start.15 = (bf16[128,256]{1,0:T(8,128)(2,1)S(1)}, bf16[128,256]{1,0:T(8,128)(2,1)S(1)}, u32[]{:S(2)}, u32[]{:S(2)}) collective-permute-start(bf16[128,256]{1,0:T(8,128)(2,1)S(1)} %get-tuple-element.42), channel_id=1, source_target_pairs={{0,2},{2,4},{4,6},{6,0},{1,3},{3,5},{5,7},{7,1},{8,10},{10,12},{12... | collective-permute-start | bytes 196616 | tf_op jit(solution)/shard_map/ppermute | solution.py:239
  80.4 5.0 %collective-permute-start.16 = (bf16[128,256]{1,0:T(8,128)(2,1)S(1)}, bf16[128,256]{1,0:T(8,128)(2,1)S(1)}, u32[]{:S(2)}, u32[]{:S(2)}) collective-permute-start(bf16[128,256]{1,0:T(8,128)(2,1)S(1)} %get-tuple-element.43), channel_id=1, source_target_pairs={{0,4},{2,6},{4,0},{6,2},{1,5},{3,7},{5,1},{7,3},{8,12},{10,14},{12... | collective-permute-start | bytes 196616 | tf_op jit(solution)/shard_map/ppermute | solution.py:241
  81.5 4.8 %collective-permute-start.17 = (bf16[128,256]{1,0:T(8,128)(2,1)S(1)}, bf16[128,256]{1,0:T(8,128)(2,1)S(1)}, u32[]{:S(2)}, u32[]{:S(2)}) collective-permute-start(bf16[128,256]{1,0:T(8,128)(2,1)S(1)} %get-tuple-element.44), channel_id=1, source_target_pairs={{0,6},{2,0},{4,2},{6,4},{1,7},{3,1},{5,3},{7,5},{8,14},{10,8},{12,... | collective-permute-start | bytes 196616 | tf_op jit(solution)/shard_map/ppermute | solution.py:240
  86.3 5.0 %collective-permute-start.18 = (f32[128,256]{1,0:T(8,128)S(1)}, f32[128,256]{1,0:T(8,128)S(1)}, u32[]{:S(2)}, u32[]{:S(2)}) collective-permute-start(f32[128,256]{1,0:T(8,128)S(1)} %shard_map.91.mine), channel_id=1, source_target_pairs={{0,1},{1,0},{2,3},{3,2},{4,5},{5,4},{6,7},{7,6},{8,9},{9,8},{10,11... | collective-permute-start | bytes 393224 | tf_op jit(solution)/shard_map/ppermute | solution.py:49
  91.3 5.1 %collective-permute-start.21 = (bf16[128,256]{1,0:T(8,128)(2,1)S(1)}, bf16[128,256]{1,0:T(8,128)(2,1)S(1)}, u32[]{:S(2)}, u32[]{:S(2)}) collective-permute-start(bf16[128,256]{1,0:T(8,128)(2,1)S(1)} %shard_map.92.x0), channel_id=1, source_target_pairs={{0,6},{2,0},{4,2},{6,4},{1,7},{3,1},{5,3},{7,5},{8,14},{10,8},{12,... | collective-permute-start | bytes 196616 | tf_op jit(solution)/shard_map/ppermute | solution.py:32
  93.8 4.7 %collective-permute-start.20 = (bf16[128,256]{1,0:T(8,128)(2,1)S(1)}, bf16[128,256]{1,0:T(8,128)(2,1)S(1)}, u32[]{:S(2)}, u32[]{:S(2)}) collective-permute-start(bf16[128,256]{1,0:T(8,128)(2,1)S(1)} %shard_map.92.x0), channel_id=1, source_target_pairs={{0,4},{2,6},{4,0},{6,2},{1,5},{3,7},{5,1},{7,3},{8,12},{10,14},{12... | collective-permute-start | bytes 196616 | tf_op jit(solution)/shard_map/ppermute | solution.py:32
  94.2 6.0 %collective-permute-start.19 = (bf16[128,256]{1,0:T(8,128)(2,1)S(1)}, bf16[128,256]{1,0:T(8,128)(2,1)S(1)}, u32[]{:S(2)}, u32[]{:S(2)}) collective-permute-start(bf16[128,256]{1,0:T(8,128)(2,1)S(1)} %shard_map.92.x0), channel_id=1, source_target_pairs={{0,2},{2,4},{4,6},{6,0},{1,3},{3,5},{5,7},{7,1},{8,10},{10,12},{12... | collective-permute-start | bytes 196616 | tf_op jit(solution)/shard_map/ppermute | solution.py:32
  100.7 6.2 %collective-permute-start.23 = (bf16[128,256]{1,0:T(8,128)(2,1)S(1)}, bf16[128,256]{1,0:T(8,128)(2,1)S(1)}, u32[]{:S(2)}, u32[]{:S(2)}) collective-permute-start(bf16[128,256]{1,0:T(8,128)(2,1)S(1)} %get-tuple-element.48.own), channel_id=1, source_target_pairs={{8,0},{16,8},{24,16},{32,24},{40,32},{48,40},{56,48},{64,56},{72,6... | collective-permute-start | bytes 196616 | tf_op jit(solution)/shard_map/ppermute | solution.py:57
  105.0 7.1 %collective-permute-start.22 = (bf16[128,256]{1,0:T(8,128)(2,1)S(1)}, bf16[128,256]{1,0:T(8,128)(2,1)S(1)}, u32[]{:S(2)}, u32[]{:S(2)}) collective-permute-start(bf16[128,256]{1,0:T(8,128)(2,1)S(1)} %get-tuple-element.48.own), channel_id=1, source_target_pairs={{0,8},{8,16},{16,24},{24,32},{32,40},{40,48},{48,56},{56,64},{64,7... | collective-permute-start | bytes 196616 | tf_op jit(solution)/shard_map/ppermute | solution.py:53
  113.1 5.1 %collective-permute-start.24 = (bf16[128,256]{1,0:T(8,128)(2,1)S(1)}, bf16[128,256]{1,0:T(8,128)(2,1)S(1)}, u32[]{:S(2)}, u32[]{:S(2)}) collective-permute-start(bf16[128,256]{1,0:T(8,128)(2,1)S(1)} %get-tuple-element.50), channel_id=1, source_target_pairs={{0,2},{2,4},{4,6},{6,0},{1,3},{3,5},{5,7},{7,1},{8,10},{10,12},{12... | collective-permute-start | bytes 196616 | tf_op jit(solution)/shard_map/ppermute | solution.py:239
  113.2 5.0 %collective-permute-start.25 = (bf16[128,256]{1,0:T(8,128)(2,1)S(1)}, bf16[128,256]{1,0:T(8,128)(2,1)S(1)}, u32[]{:S(2)}, u32[]{:S(2)}) collective-permute-start(bf16[128,256]{1,0:T(8,128)(2,1)S(1)} %get-tuple-element.51), channel_id=1, source_target_pairs={{0,4},{2,6},{4,0},{6,2},{1,5},{3,7},{5,1},{7,3},{8,12},{10,14},{12... | collective-permute-start | bytes 196616 | tf_op jit(solution)/shard_map/ppermute | solution.py:241
  114.2 4.6 %collective-permute-start.26 = (bf16[128,256]{1,0:T(8,128)(2,1)S(1)}, bf16[128,256]{1,0:T(8,128)(2,1)S(1)}, u32[]{:S(2)}, u32[]{:S(2)}) collective-permute-start(bf16[128,256]{1,0:T(8,128)(2,1)S(1)} %get-tuple-element.52), channel_id=1, source_target_pairs={{0,6},{2,0},{4,2},{6,4},{1,7},{3,1},{5,3},{7,5},{8,14},{10,8},{12,... | collective-permute-start | bytes 196616 | tf_op jit(solution)/shard_map/ppermute | solution.py:240
  118.8 4.9 %collective-permute-start.27 = (f32[128,128]{1,0:T(8,128)S(1)}, f32[128,128]{1,0:T(8,128)S(1)}, u32[]{:S(2)}, u32[]{:S(2)}) collective-permute-start(f32[128,128]{1,0:T(8,128)S(1)} %get-tuple-element.54), channel_id=1, source_target_pairs={{0,1},{1,0},{2,3},{3,2},{4,5},{5,4},{6,7},{7,6},{8,9},{9,8},{10,11... | collective-permute-start | bytes 196616 | tf_op jit(solution)/shard_map/ppermute | solution.py:49
  (3 other events, 50.4 us)

commit v7 on v6

--- a/solution.py
+++ b/solution.py
@@ -27,10 +27,7 @@
 
 
 def spread(a, axis):
-    sent = []
-    for k in (1, 3, 2):
-        sent.append(lax.ppermute(a, axis, turn(k)))
-    return sent
+    return [lax.ppermute(a, axis, turn(k)) for k in (1, 3, 2)]
 
 
 def in_order(a, three):
@@ -94,16 +91,21 @@
         first[n] = whole
 
 
-def many_body(wq, wk, wv, wo, many1, many2, parts, sems):
+def many_body(wq, wk, wv, wo, bias, many1, many2, wide, parts, sems):
     pairs = [(w.at[1:3], parts.at[n]) for n, w in enumerate((wq, wk, wv, wo))]
     fetch(pairs, sems)
     for layer, many in enumerate((many1, many2)):
         whole = jnp.concatenate([parts[n, layer] for n in range(4)], axis=1)
         for n in range(16):
             many[n] = whole
-
-
-def table_body(bias, before, own, after, table, wide):
+    wide[...] = jnp.zeros((8, 256), F32)
+    for n in range(2 * LAYERS):
+        for lag_row in range(WIN_ROWS):
+            at = lag_row * GRID_W
+            wide[n : n + 1, at : at + WIN_COLS] = bias[n // 2, n % 2, lag_row : lag_row + 1, :]
+
+
+def table_body(wide, before, own, after, table):
     own_docs = own[128:144, 0:128].astype(F32)[0:1]
     query_docs = jnp.broadcast_to(own_docs, (128, 128)).T
     key_docs = jnp.concatenate(
@@ -115,11 +117,6 @@
     lag = (m >> 5) - (r >> 5)
     off = (m & 31) - (r & 31) + WIN_COLS // 2
     allowed = same & (lag >= 0) & (lag < WIN_ROWS) & (off >= 0) & (off < WIN_COLS)
-    wide[...] = jnp.zeros((8, 256), F32)
-    for n in range(2 * LAYERS):
-        for lag_row in range(WIN_ROWS):
-            at = lag_row * GRID_W
-            wide[n : n + 1, at : at + WIN_COLS] = bias[n // 2, n % 2, lag_row : lag_row + 1, :]
     for n in range(2 * LAYERS):
         line = jnp.broadcast_to(wide[n : n + 1, :], (GRID_W, 256))
         line = pltpu.roll(line, 256 - WIN_COLS // 2, 1, stride=1, stride_axis=0)
@@ -254,8 +251,9 @@
     )
     weights = gather_rows(first)
     near_y = jnp.stack(in_order(tokens, spread(tokens, "y")))
-    many1, many2 = call(
-        many_body, [shaped(16, 64, 512)] * 2, *held, in_specs=[hbm] * 4,
+    many1, many2, wide = call(
+        many_body, [shaped(16, 64, 512)] * 2 + [shaped(8, 256, dtype=F32)],
+        *held, offset_bias, in_specs=[hbm] * 4 + [pl.BlockSpec()],
         scratch=[pltpu.VMEM((4, 2, 64, 128), BF16), pltpu.SemaphoreType.DMA((4,))],
     )
     near_partner = swap(after_this(near_y, many1))
@@ -264,26 +262,27 @@
         heads_first_body, [shaped(128, 128), shaped(144, 256)],
         near_y, near_partner, norm_gain, documents.reshape(1, 128), weights,
     )
-    args = (q, from_before(kv), kv, from_after(kv))
-    table = call(
-        table_body, shaped(6, 128, 384, dtype=F32), offset_bias, *args[1:],
-        scratch=[pltpu.VMEM((8, 256), F32)],
-    )
-    body = functools.partial(attend_scatter_body, layer=0)
-    for layer, many in ((1, many1), (2, many2)):
-        kept, r1, r2, r3 = scattered(body, *args, table, weights)
-        weights = gather_rows(after_this(many, kept))
+    for layer in range(LAYERS):
+        after = from_after(kv)
+        before = from_before(kv)
+        if layer < 2:
+            next_weights = gather_rows(after_this((many1, many2)[layer], kv))
+        if layer == 0:
+            table = call(table_body, shaped(6, 128, 384, dtype=F32), wide, before, kv, after)
+        kept, r1, r2, r3 = scattered(
+            functools.partial(attend_scatter_body, layer=layer),
+            q, before, kv, after, table, weights,
+        )
+        if layer == 2:
+            break
         half = call(sum_body, shaped(128, 256, dtype=F32), kept, r1, r2, r3)
         stream = call(pair_sum_body, shaped(128, 256), half, swap(half))
-        pieces = in_order(stream, spread(stream, "y"))
+        weights = next_weights
         q, kv = call(
-            functools.partial(heads_pieces_body, layer=layer),
+            functools.partial(heads_pieces_body, layer=layer + 1),
             [shaped(128, 128), shaped(128, 256)],
-            *pieces, norm_gain, weights,
+            *in_order(stream, spread(stream, "y")), norm_gain, weights,
         )
-        body = functools.partial(attend_scatter_body, layer=layer)
-        args = (q, from_before(kv), kv, from_after(kv))
-    kept, r1, r2, r3 = scattered(body, *args, table, weights)
     mine, theirs = call(split_body, [shaped(128, 128, dtype=F32)] * 2, kept, r1, r2, r3)
     return call(pair_sum_body, shaped(128, 128), mine, swap(theirs))
 

time: 125 us -> 132 us (1.056)
  waiting for transfers between devices: 43 us -> 50.3 us
  local copies, waits for them, and re-layouts: 0.03 us -> 1.99 us
    ppermute x3, waiting for transfers between devices: 0.01 us -> 14.5 us  [from_after(): return lax.ppermute(a, SP, [(i + 1, i) for i in range(15)])]
    ppermute x3, waiting for transfers between devices: 15.6 us -> 9.19 us  [from_before(): return lax.ppermute(a, SP, [(i, i + 1) for i in range(15)])]
    all_to_all x3, starting transfers between devices: 15.3 us -> 19.4 us  [gather_rows(): return lax.all_to_all(a, SP, 0, 0, tiled=True).reshape(1024, 512)]
    ppermute x4, starting transfers between devices: 15.6 us -> 11.9 us  [swap(): return lax.ppermute(a, 'c', [(0, 1), (1, 0)])]
    unnamed x8 -> x12, local copies, waits for them, and re-layouts: 0.03 us -> 1.99 us
  transfers between devices with their start and end apart: 31 -> 31, of which waited for: 21 -> 24; matrix products, arithmetic and copies ran while one was open for 0% -> 0% of each run, Pallas kernels for 2% -> 3%
where the time goes in v7:
time: 132 us
  starting transfers between devices  70.3 us (53%)
  waiting for transfers between devices  50.3 us (38%)
  Pallas kernels  8.64 us (7%)
  local copies, waits for them, and re-layouts  1.99 us (2%)
    all_to_all x3, starting transfers between devices, gather_rows(): return lax.all_to_all(a, SP, 0, 0, tiled=True).reshape(1024, 512)  19.4 us
    ppermute x3, waiting for transfers between devices, from_after(): return lax.ppermute(a, SP, [(i + 1, i) for i in range(15)])  14.5 us
    ppermute x3, starting transfers between devices, from_after(): return lax.ppermute(a, SP, [(i + 1, i) for i in range(15)])  12.2 us
    ppermute x4, starting transfers between devices, swap(): return lax.ppermute(a, 'c', [(0, 1), (1, 0)])  11.9 us
    ppermute x9, waiting for transfers between devices, spread(): return [lax.ppermute(a, axis, turn(k)) for k in (1, 3, 2)]  11 us
    ppermute x9, starting transfers between devices, spread(): return [lax.ppermute(a, axis, turn(k)) for k in (1, 3, 2)]  10.4 us
    ppermute x3, waiting for transfers between devices, from_before(): return lax.ppermute(a, SP, [(i, i + 1) for i in range(15)])  9.19 us
    pallas_call x15, Pallas kernels, call(): pl.pallas_call(body, out_shape=outs, **specs, scratch_shapes=list(scratch...  8.64 us
  transfers between devices with their start and end apart: 31, of which 24 were waited for; matrix products, arithmetic and copies ran while one was open for 0% of the time, Pallas kernels for 3%

profile of v7, /device:TPU:33, one launch (start us, length us, event | category | flops | bytes accessed | tf_op | source)
XLA Modules:
  0.0 131.6 jit_solution(11587931039705365244)
XLA Ops:
  0.0 1.9 %shard_map.83 = bf16[16,64,512]{2,1,0:T(8,128)(2,1)} custom-call(bf16[3,64,128]{2,1,0:T(8,128)(2,1)} %wq.3, bf16[3,64,128]{2,1,0:T(8,128)(2,1)} %wk.3, bf16[3,64,128]{2,1,0:T(8,128)(2,1)} %wv.3, bf16[3,64,128]{2,1,0:T(8,128)(2,1)} %bitcast.16), custom_call_target="tpu_custom_call" | custom-call | tf_op jit(solution)/shard_map/pallas_call | solution.py:66
  1.9 7.5 %all-to-all-start = ((bf16[16,64,512]{2,1,0:T(8,128)(2,1)}), bf16[16,64,512]{2,1,0:T(8,128)(2,1)S(1)}, u32[]{:S(2)}, u32[]{:S(2)}) async-start(bf16[16,64,512]{2,1,0:T(8,128)(2,1)} %shard_map.83), calls=%async_computation | async-start | bytes 2097152 | tf_op jit(solution)/shard_map/all_to_all | solution.py:38
  10.8 1.5 %collective-permute-start.2 = (bf16[128,128]{1,0:T(8,128)(2,1)S(1)}, bf16[128,128]{1,0:T(8,128)(2,1)S(1)}, u32[]{:S(2)}, u32[]{:S(2)}) collective-permute-start(bf16[128,128]{1,0:T(8,128)(2,1)S(1)} %copy-done.5), channel_id=1, source_target_pairs={{0,6},{2,0},{4,2},{6,4},{1,7},{3,1},{5,3},{7,5},{8,14},{10,8},{12,... | collective-permute-start | bytes 98312 | tf_op jit(solution)/shard_map/ppermute | solution.py:30
  12.3 1.6 %collective-permute-start.1 = (bf16[128,128]{1,0:T(8,128)(2,1)S(1)}, bf16[128,128]{1,0:T(8,128)(2,1)S(1)}, u32[]{:S(2)}, u32[]{:S(2)}) collective-permute-start(bf16[128,128]{1,0:T(8,128)(2,1)S(1)} %copy-done.5), channel_id=1, source_target_pairs={{0,4},{2,6},{4,0},{6,2},{1,5},{3,7},{5,1},{7,3},{8,12},{10,14},{12... | collective-permute-start | bytes 98312 | tf_op jit(solution)/shard_map/ppermute | solution.py:30
  17.1 2.4 %collective-permute-start.3 = (bf16[4,128,128]{2,1,0:T(8,128)(2,1)S(1)}, bf16[4,128,128]{2,1,0:T(8,128)(2,1)S(1)}, u32[]{:S(2)}, u32[]{:S(2)}) collective-permute-start(bf16[4,128,128]{2,1,0:T(8,128)(2,1)S(1)} %pad_maximum_fusion.own), channel_id=1, source_target_pairs={{0,1},{1,0},{2,3},{3,2},{4,5},{5,4},{6,7},{7,6},{8,9},{9,8},{10,11... | collective-permute-start | bytes 393224 | tf_op jit(solution)/shard_map/ppermute | solution.py:46
  20.5 2.9 %all-to-all-done = bf16[16,64,512]{2,1,0:T(8,128)(2,1)S(1)} async-done(((bf16[16,64,512]{2,1,0:T(8,128)(2,1)}), bf16[16,64,512]{2,1,0:T(8,128)(2,1)S(1)}, u32[]{:S(2)}, u32[]{:S(2)}) %all-to-all-start) | async-done | bytes 1048608 | tf_op jit(solution)/shard_map/all_to_all | solution.py:38
  24.0 6.3 %all-to-all-start.1 = ((bf16[16,64,512]{2,1,0:T(8,128)(2,1)}), bf16[16,64,512]{2,1,0:T(8,128)(2,1)S(1)}, u32[]{:S(2)}, u32[]{:S(2)}) async-start(bf16[16,64,512]{2,1,0:T(8,128)(2,1)} %copy-done.1), calls=%async_computation.1 | async-start | bytes 2097152 | tf_op jit(solution)/shard_map/all_to_all | solution.py:38
  30.3 4.3 %collective-permute-start.5 = (bf16[144,256]{1,0:T(8,128)(2,1)S(1)}, bf16[144,256]{1,0:T(8,128)(2,1)S(1)}, u32[]{:S(2)}, u32[]{:S(2)}) collective-permute-start(bf16[144,256]{1,0:T(8,128)(2,1)S(1)} %get-tuple-element.34.own), channel_id=1, source_target_pairs={{8,0},{16,8},{24,16},{32,24},{40,32},{48,40},{56,48},{64,56},{72,6... | collective-permute-start | bytes 221192 | tf_op jit(solution)/shard_map/ppermute | solution.py:54
  34.6 1.9 %collective-permute-start.4 = (bf16[144,256]{1,0:T(8,128)(2,1)S(1)}, bf16[144,256]{1,0:T(8,128)(2,1)S(1)}, u32[]{:S(2)}, u32[]{:S(2)}) collective-permute-start(bf16[144,256]{1,0:T(8,128)(2,1)S(1)} %get-tuple-element.34.own), channel_id=1, source_target_pairs={{0,8},{8,16},{16,24},{24,32},{32,40},{40,48},{48,56},{56,64},{64,7... | collective-permute-start | bytes 221192 | tf_op jit(solution)/shard_map/ppermute | solution.py:50
  36.5 6.9 %collective-permute-done.5.after = bf16[144,256]{1,0:T(8,128)(2,1)S(1)} collective-permute-done((bf16[144,256]{1,0:T(8,128)(2,1)S(1)}, bf16[144,256]{1,0:T(8,128)(2,1)S(1)}, u32[]{:S(2)}, u32[]{:S(2)}) %collective-permute-start.5) | collective-permute-done | bytes 73760 | tf_op jit(solution)/shard_map/ppermute | solution.py:54
  43.4 2.4 %collective-permute-done.4.before = bf16[144,256]{1,0:T(8,128)(2,1)S(1)} collective-permute-done((bf16[144,256]{1,0:T(8,128)(2,1)S(1)}, bf16[144,256]{1,0:T(8,128)(2,1)S(1)}, u32[]{:S(2)}, u32[]{:S(2)}) %collective-permute-start.4) | collective-permute-done | bytes 73760 | tf_op jit(solution)/shard_map/ppermute | solution.py:50
  48.7 2.6 %collective-permute-start.7 = (bf16[128,256]{1,0:T(8,128)(2,1)S(1)}, bf16[128,256]{1,0:T(8,128)(2,1)S(1)}, u32[]{:S(2)}, u32[]{:S(2)}) collective-permute-start(bf16[128,256]{1,0:T(8,128)(2,1)S(1)} %get-tuple-element.38), channel_id=1, source_target_pairs={{0,4},{2,6},{4,0},{6,2},{1,5},{3,7},{5,1},{7,3},{8,12},{10,14},{12... | collective-permute-start | bytes 196616 | tf_op jit(solution)/shard_map/ppermute | solution.py:238
  53.8 1.6 %collective-permute-done.8.r3 = bf16[128,256]{1,0:T(8,128)(2,1)S(1)} collective-permute-done((bf16[128,256]{1,0:T(8,128)(2,1)S(1)}, bf16[128,256]{1,0:T(8,128)(2,1)S(1)}, u32[]{:S(2)}, u32[]{:S(2)}) %collective-permute-start.8) | collective-permute-done | bytes 65568 | tf_op jit(solution)/shard_map/ppermute | solution.py:237
  55.4 2.4 %collective-permute-start.9 = (f32[128,256]{1,0:T(8,128)S(1)}, f32[128,256]{1,0:T(8,128)S(1)}, u32[]{:S(2)}, u32[]{:S(2)}) collective-permute-start(f32[128,256]{1,0:T(8,128)S(1)} %shard_map.87.mine), channel_id=1, source_target_pairs={{0,1},{1,0},{2,3},{3,2},{4,5},{5,4},{6,7},{7,6},{8,9},{9,8},{10,11... | collective-permute-start | bytes 393224 | tf_op jit(solution)/shard_map/ppermute | solution.py:46
  58.8 2.3 %collective-permute-start.12 = (bf16[128,256]{1,0:T(8,128)(2,1)S(1)}, bf16[128,256]{1,0:T(8,128)(2,1)S(1)}, u32[]{:S(2)}, u32[]{:S(2)}) collective-permute-start(bf16[128,256]{1,0:T(8,128)(2,1)S(1)} %shard_map.88.x0), channel_id=1, source_target_pairs={{0,6},{2,0},{4,2},{6,4},{1,7},{3,1},{5,3},{7,5},{8,14},{10,8},{12,... | collective-permute-start | bytes 196616 | tf_op jit(solution)/shard_map/ppermute | solution.py:30
  62.5 3.4 %collective-permute-done.11.x2 = bf16[128,256]{1,0:T(8,128)(2,1)S(1)} collective-permute-done((bf16[128,256]{1,0:T(8,128)(2,1)S(1)}, bf16[128,256]{1,0:T(8,128)(2,1)S(1)}, u32[]{:S(2)}, u32[]{:S(2)}) %collective-permute-start.11) | collective-permute-done | bytes 65568 | tf_op jit(solution)/shard_map/ppermute | solution.py:30
  65.8 1.6 %collective-permute-done.10.x1 = bf16[128,256]{1,0:T(8,128)(2,1)S(1)} collective-permute-done((bf16[128,256]{1,0:T(8,128)(2,1)S(1)}, bf16[128,256]{1,0:T(8,128)(2,1)S(1)}, u32[]{:S(2)}, u32[]{:S(2)}) %collective-permute-start.10) | collective-permute-done | bytes 65568 | tf_op jit(solution)/shard_map/ppermute | solution.py:30
  68.0 5.6 %all-to-all-start.2 = ((bf16[16,64,512]{2,1,0:T(8,128)(2,1)}), bf16[16,64,512]{2,1,0:T(8,128)(2,1)S(1)}, u32[]{:S(2)}, u32[]{:S(2)}) async-start(bf16[16,64,512]{2,1,0:T(8,128)(2,1)} %copy-done), calls=%async_computation.2 | async-start | bytes 2097152 | tf_op jit(solution)/shard_map/all_to_all | solution.py:38
  73.6 4.3 %collective-permute-start.14 = (bf16[128,256]{1,0:T(8,128)(2,1)S(1)}, bf16[128,256]{1,0:T(8,128)(2,1)S(1)}, u32[]{:S(2)}, u32[]{:S(2)}) collective-permute-start(bf16[128,256]{1,0:T(8,128)(2,1)S(1)} %get-tuple-element.42.own), channel_id=1, source_target_pairs={{8,0},{16,8},{24,16},{32,24},{40,32},{48,40},{56,48},{64,56},{72,6... | collective-permute-start | bytes 196616 | tf_op jit(solution)/shard_map/ppermute | solution.py:54
  77.9 1.9 %collective-permute-start.13 = (bf16[128,256]{1,0:T(8,128)(2,1)S(1)}, bf16[128,256]{1,0:T(8,128)(2,1)S(1)}, u32[]{:S(2)}, u32[]{:S(2)}) collective-permute-start(bf16[128,256]{1,0:T(8,128)(2,1)S(1)} %get-tuple-element.42.own), channel_id=1, source_target_pairs={{0,8},{8,16},{16,24},{24,32},{32,40},{40,48},{48,56},{56,64},{64,7... | collective-permute-start | bytes 196616 | tf_op jit(solution)/shard_map/ppermute | solution.py:50
  79.8 7.6 %collective-permute-done.14.after = bf16[128,256]{1,0:T(8,128)(2,1)S(1)} collective-permute-done((bf16[128,256]{1,0:T(8,128)(2,1)S(1)}, bf16[128,256]{1,0:T(8,128)(2,1)S(1)}, u32[]{:S(2)}, u32[]{:S(2)}) %collective-permute-start.14) | collective-permute-done | bytes 65568 | tf_op jit(solution)/shard_map/ppermute | solution.py:54
  87.4 1.6 %collective-permute-done.13.before = bf16[128,256]{1,0:T(8,128)(2,1)S(1)} collective-permute-done((bf16[128,256]{1,0:T(8,128)(2,1)S(1)}, bf16[128,256]{1,0:T(8,128)(2,1)S(1)}, u32[]{:S(2)}, u32[]{:S(2)}) %collective-permute-start.13) | collective-permute-done | bytes 65568 | tf_op jit(solution)/shard_map/ppermute | solution.py:50
  91.0 1.6 %collective-permute-start.17 = (bf16[128,256]{1,0:T(8,128)(2,1)S(1)}, bf16[128,256]{1,0:T(8,128)(2,1)S(1)}, u32[]{:S(2)}, u32[]{:S(2)}) collective-permute-start(bf16[128,256]{1,0:T(8,128)(2,1)S(1)} %get-tuple-element.46), channel_id=1, source_target_pairs={{0,6},{2,0},{4,2},{6,4},{1,7},{3,1},{5,3},{7,5},{8,14},{10,8},{12,... | collective-permute-start | bytes 196616 | tf_op jit(solution)/shard_map/ppermute | solution.py:237
  92.6 2.0 %collective-permute-done.15.r1 = bf16[128,256]{1,0:T(8,128)(2,1)S(1)} collective-permute-done((bf16[128,256]{1,0:T(8,128)(2,1)S(1)}, bf16[128,256]{1,0:T(8,128)(2,1)S(1)}, u32[]{:S(2)}, u32[]{:S(2)}) %collective-permute-start.15) | collective-permute-done | bytes 65568 | tf_op jit(solution)/shard_map/ppermute | solution.py:236
  95.9 2.7 %collective-permute-start.18 = (f32[128,256]{1,0:T(8,128)S(1)}, f32[128,256]{1,0:T(8,128)S(1)}, u32[]{:S(2)}, u32[]{:S(2)}) collective-permute-start(f32[128,256]{1,0:T(8,128)S(1)} %shard_map.91.mine), channel_id=1, source_target_pairs={{0,1},{1,0},{2,3},{3,2},{4,5},{5,4},{6,7},{7,6},{8,9},{9,8},{10,11... | collective-permute-start | bytes 393224 | tf_op jit(solution)/shard_map/ppermute | solution.py:46
  99.6 2.2 %collective-permute-start.21 = (bf16[128,256]{1,0:T(8,128)(2,1)S(1)}, bf16[128,256]{1,0:T(8,128)(2,1)S(1)}, u32[]{:S(2)}, u32[]{:S(2)}) collective-permute-start(bf16[128,256]{1,0:T(8,128)(2,1)S(1)} %shard_map.92.x0), channel_id=1, source_target_pairs={{0,6},{2,0},{4,2},{6,4},{1,7},{3,1},{5,3},{7,5},{8,14},{10,8},{12,... | collective-permute-start | bytes 196616 | tf_op jit(solution)/shard_map/ppermute | solution.py:30
  103.1 3.3 %collective-permute-done.20.x2 = bf16[128,256]{1,0:T(8,128)(2,1)S(1)} collective-permute-done((bf16[128,256]{1,0:T(8,128)(2,1)S(1)}, bf16[128,256]{1,0:T(8,128)(2,1)S(1)}, u32[]{:S(2)}, u32[]{:S(2)}) %collective-permute-start.20) | collective-permute-done | bytes 65568 | tf_op jit(solution)/shard_map/ppermute | solution.py:30
  108.2 3.6 %collective-permute-start.23 = (bf16[128,256]{1,0:T(8,128)(2,1)S(1)}, bf16[128,256]{1,0:T(8,128)(2,1)S(1)}, u32[]{:S(2)}, u32[]{:S(2)}) collective-permute-start(bf16[128,256]{1,0:T(8,128)(2,1)S(1)} %get-tuple-element.50.own), channel_id=1, source_target_pairs={{8,0},{16,8},{24,16},{32,24},{40,32},{48,40},{56,48},{64,56},{72,6... | collective-permute-start | bytes 196616 | tf_op jit(solution)/shard_map/ppermute | solution.py:54
  111.8 1.9 %collective-permute-start.22 = (bf16[128,256]{1,0:T(8,128)(2,1)S(1)}, bf16[128,256]{1,0:T(8,128)(2,1)S(1)}, u32[]{:S(2)}, u32[]{:S(2)}) collective-permute-start(bf16[128,256]{1,0:T(8,128)(2,1)S(1)} %get-tuple-element.50.own), channel_id=1, source_target_pairs={{0,8},{8,16},{16,24},{24,32},{32,40},{40,48},{48,56},{56,64},{64,7... | collective-permute-start | bytes 196616 | tf_op jit(solution)/shard_map/ppermute | solution.py:50
  113.8 5.2 %collective-permute-done.22.before = bf16[128,256]{1,0:T(8,128)(2,1)S(1)} collective-permute-done((bf16[128,256]{1,0:T(8,128)(2,1)S(1)}, bf16[128,256]{1,0:T(8,128)(2,1)S(1)}, u32[]{:S(2)}, u32[]{:S(2)}) %collective-permute-start.22) | collective-permute-done | bytes 65568 | tf_op jit(solution)/shard_map/ppermute | solution.py:50
  122.8 2.2 %collective-permute-done.24.r1 = bf16[128,256]{1,0:T(8,128)(2,1)S(1)} collective-permute-done((bf16[128,256]{1,0:T(8,128)(2,1)S(1)}, bf16[128,256]{1,0:T(8,128)(2,1)S(1)}, u32[]{:S(2)}, u32[]{:S(2)}) %collective-permute-start.24) | collective-permute-done | bytes 65568 | tf_op jit(solution)/shard_map/ppermute | solution.py:236
  125.6 4.4 %collective-permute-start.27 = (f32[128,128]{1,0:T(8,128)S(1)}, f32[128,128]{1,0:T(8,128)S(1)}, u32[]{:S(2)}, u32[]{:S(2)}) collective-permute-start(f32[128,128]{1,0:T(8,128)S(1)} %get-tuple-element.56), channel_id=1, source_target_pairs={{0,1},{1,0},{2,3},{3,2},{4,5},{5,4},{6,7},{7,6},{8,9},{9,8},{10,11... | collective-permute-start | bytes 196616 | tf_op jit(solution)/shard_map/ppermute | solution.py:46
  (58 shorter events, 27.8 us)
Async XLA Ops:
  1.9 21.4 %copy-start.2 = (f32[3,1024]{1,0:T(4,128)S(1)}, f32[3,1024]{1,0:T(4,128)}, u32[]{:S(2)}) copy-start(f32[3,1024]{1,0:T(4,128)} %gain.5) | copy-start | bytes 36868
  1.9 21.4 %all-to-all-start = ((bf16[16,64,512]{2,1,0:T(8,128)(2,1)}), bf16[16,64,512]{2,1,0:T(8,128)(2,1)S(1)}, u32[]{:S(2)}, u32[]{:S(2)}) async-start(bf16[16,64,512]{2,1,0:T(8,128)(2,1)} %shard_map.83), calls=%async_computation | async-start | bytes 2097152 | tf_op jit(solution)/shard_map/all_to_all | solution.py:38
  9.4 7.5 %collective-permute-start = (bf16[128,128]{1,0:T(8,128)(2,1)S(1)}, bf16[128,128]{1,0:T(8,128)(2,1)S(1)}, u32[]{:S(2)}, u32[]{:S(2)}) collective-permute-start(bf16[128,128]{1,0:T(8,128)(2,1)S(1)} %copy-done.5), channel_id=1, source_target_pairs={{0,2},{2,4},{4,6},{6,0},{1,3},{3,5},{5,7},{7,1},{8,10},{10,12},{12... | collective-permute-start | bytes 98312 | tf_op jit(solution)/shard_map/ppermute | solution.py:30
  10.8 6.1 %collective-permute-start.2 = (bf16[128,128]{1,0:T(8,128)(2,1)S(1)}, bf16[128,128]{1,0:T(8,128)(2,1)S(1)}, u32[]{:S(2)}, u32[]{:S(2)}) collective-permute-start(bf16[128,128]{1,0:T(8,128)(2,1)S(1)} %copy-done.5), channel_id=1, source_target_pairs={{0,6},{2,0},{4,2},{6,4},{1,7},{3,1},{5,3},{7,5},{8,14},{10,8},{12,... | collective-permute-start | bytes 98312 | tf_op jit(solution)/shard_map/ppermute | solution.py:30
  12.3 4.7 %collective-permute-start.1 = (bf16[128,128]{1,0:T(8,128)(2,1)S(1)}, bf16[128,128]{1,0:T(8,128)(2,1)S(1)}, u32[]{:S(2)}, u32[]{:S(2)}) collective-permute-start(bf16[128,128]{1,0:T(8,128)(2,1)S(1)} %copy-done.5), channel_id=1, source_target_pairs={{0,4},{2,6},{4,0},{6,2},{1,5},{3,7},{5,1},{7,3},{8,12},{10,14},{12... | collective-permute-start | bytes 98312 | tf_op jit(solution)/shard_map/ppermute | solution.py:30
  17.1 3.4 %collective-permute-start.3 = (bf16[4,128,128]{2,1,0:T(8,128)(2,1)S(1)}, bf16[4,128,128]{2,1,0:T(8,128)(2,1)S(1)}, u32[]{:S(2)}, u32[]{:S(2)}) collective-permute-start(bf16[4,128,128]{2,1,0:T(8,128)(2,1)S(1)} %pad_maximum_fusion.own), channel_id=1, source_target_pairs={{0,1},{1,0},{2,3},{3,2},{4,5},{5,4},{6,7},{7,6},{8,9},{9,8},{10,11... | collective-permute-start | bytes 393224 | tf_op jit(solution)/shard_map/ppermute | solution.py:46
  24.0 43.5 %all-to-all-start.1 = ((bf16[16,64,512]{2,1,0:T(8,128)(2,1)}), bf16[16,64,512]{2,1,0:T(8,128)(2,1)S(1)}, u32[]{:S(2)}, u32[]{:S(2)}) async-start(bf16[16,64,512]{2,1,0:T(8,128)(2,1)} %copy-done.1), calls=%async_computation.1 | async-start | bytes 2097152 | tf_op jit(solution)/shard_map/all_to_all | solution.py:38
  30.3 13.1 %collective-permute-start.5 = (bf16[144,256]{1,0:T(8,128)(2,1)S(1)}, bf16[144,256]{1,0:T(8,128)(2,1)S(1)}, u32[]{:S(2)}, u32[]{:S(2)}) collective-permute-start(bf16[144,256]{1,0:T(8,128)(2,1)S(1)} %get-tuple-element.34.own), channel_id=1, source_target_pairs={{8,0},{16,8},{24,16},{32,24},{40,32},{48,40},{56,48},{64,56},{72,6... | collective-permute-start | bytes 221192 | tf_op jit(solution)/shard_map/ppermute | solution.py:54
  34.6 11.3 %collective-permute-start.4 = (bf16[144,256]{1,0:T(8,128)(2,1)S(1)}, bf16[144,256]{1,0:T(8,128)(2,1)S(1)}, u32[]{:S(2)}, u32[]{:S(2)}) collective-permute-start(bf16[144,256]{1,0:T(8,128)(2,1)S(1)} %get-tuple-element.34.own), channel_id=1, source_target_pairs={{0,8},{8,16},{16,24},{24,32},{32,40},{40,48},{48,56},{56,64},{64,7... | collective-permute-start | bytes 221192 | tf_op jit(solution)/shard_map/ppermute | solution.py:50
  47.4 5.1 %collective-permute-start.6 = (bf16[128,256]{1,0:T(8,128)(2,1)S(1)}, bf16[128,256]{1,0:T(8,128)(2,1)S(1)}, u32[]{:S(2)}, u32[]{:S(2)}) collective-permute-start(bf16[128,256]{1,0:T(8,128)(2,1)S(1)} %get-tuple-element.37), channel_id=1, source_target_pairs={{0,2},{2,4},{4,6},{6,0},{1,3},{3,5},{5,7},{7,1},{8,10},{10,12},{12... | collective-permute-start | bytes 196616 | tf_op jit(solution)/shard_map/ppermute | solution.py:236
  48.7 5.1 %collective-permute-start.7 = (bf16[128,256]{1,0:T(8,128)(2,1)S(1)}, bf16[128,256]{1,0:T(8,128)(2,1)S(1)}, u32[]{:S(2)}, u32[]{:S(2)}) collective-permute-start(bf16[128,256]{1,0:T(8,128)(2,1)S(1)} %get-tuple-element.38), channel_id=1, source_target_pairs={{0,4},{2,6},{4,0},{6,2},{1,5},{3,7},{5,1},{7,3},{8,12},{10,14},{12... | collective-permute-start | bytes 196616 | tf_op jit(solution)/shard_map/ppermute | solution.py:238
  51.4 4.0 %collective-permute-start.8 = (bf16[128,256]{1,0:T(8,128)(2,1)S(1)}, bf16[128,256]{1,0:T(8,128)(2,1)S(1)}, u32[]{:S(2)}, u32[]{:S(2)}) collective-permute-start(bf16[128,256]{1,0:T(8,128)(2,1)S(1)} %get-tuple-element.39), channel_id=1, source_target_pairs={{0,6},{2,0},{4,2},{6,4},{1,7},{3,1},{5,3},{7,5},{8,14},{10,8},{12,... | collective-permute-start | bytes 196616 | tf_op jit(solution)/shard_map/ppermute | solution.py:237
  55.4 3.3 %collective-permute-start.9 = (f32[128,256]{1,0:T(8,128)S(1)}, f32[128,256]{1,0:T(8,128)S(1)}, u32[]{:S(2)}, u32[]{:S(2)}) collective-permute-start(f32[128,256]{1,0:T(8,128)S(1)} %shard_map.87.mine), channel_id=1, source_target_pairs={{0,1},{1,0},{2,3},{3,2},{4,5},{5,4},{6,7},{7,6},{8,9},{9,8},{10,11... | collective-permute-start | bytes 393224 | tf_op jit(solution)/shard_map/ppermute | solution.py:46
  58.8 3.7 %collective-permute-start.12 = (bf16[128,256]{1,0:T(8,128)(2,1)S(1)}, bf16[128,256]{1,0:T(8,128)(2,1)S(1)}, u32[]{:S(2)}, u32[]{:S(2)}) collective-permute-start(bf16[128,256]{1,0:T(8,128)(2,1)S(1)} %shard_map.88.x0), channel_id=1, source_target_pairs={{0,6},{2,0},{4,2},{6,4},{1,7},{3,1},{5,3},{7,5},{8,14},{10,8},{12,... | collective-permute-start | bytes 196616 | tf_op jit(solution)/shard_map/ppermute | solution.py:30
  61.1 4.7 %collective-permute-start.11 = (bf16[128,256]{1,0:T(8,128)(2,1)S(1)}, bf16[128,256]{1,0:T(8,128)(2,1)S(1)}, u32[]{:S(2)}, u32[]{:S(2)}) collective-permute-start(bf16[128,256]{1,0:T(8,128)(2,1)S(1)} %shard_map.88.x0), channel_id=1, source_target_pairs={{0,4},{2,6},{4,0},{6,2},{1,5},{3,7},{5,1},{7,3},{8,12},{10,14},{12... | collective-permute-start | bytes 196616 | tf_op jit(solution)/shard_map/ppermute | solution.py:30
  61.1 6.3 %collective-permute-start.10 = (bf16[128,256]{1,0:T(8,128)(2,1)S(1)}, bf16[128,256]{1,0:T(8,128)(2,1)S(1)}, u32[]{:S(2)}, u32[]{:S(2)}) collective-permute-start(bf16[128,256]{1,0:T(8,128)(2,1)S(1)} %shard_map.88.x0), channel_id=1, source_target_pairs={{0,2},{2,4},{4,6},{6,0},{1,3},{3,5},{5,7},{7,1},{8,10},{10,12},{12... | collective-permute-start | bytes 196616 | tf_op jit(solution)/shard_map/ppermute | solution.py:30
  68.0 39.7 %all-to-all-start.2 = ((bf16[16,64,512]{2,1,0:T(8,128)(2,1)}), bf16[16,64,512]{2,1,0:T(8,128)(2,1)S(1)}, u32[]{:S(2)}, u32[]{:S(2)}) async-start(bf16[16,64,512]{2,1,0:T(8,128)(2,1)} %copy-done), calls=%async_computation.2 | async-start | bytes 2097152 | tf_op jit(solution)/shard_map/all_to_all | solution.py:38
  73.6 13.8 %collective-permute-start.14 = (bf16[128,256]{1,0:T(8,128)(2,1)S(1)}, bf16[128,256]{1,0:T(8,128)(2,1)S(1)}, u32[]{:S(2)}, u32[]{:S(2)}) collective-permute-start(bf16[128,256]{1,0:T(8,128)(2,1)S(1)} %get-tuple-element.42.own), channel_id=1, source_target_pairs={{8,0},{16,8},{24,16},{32,24},{40,32},{48,40},{56,48},{64,56},{72,6... | collective-permute-start | bytes 196616 | tf_op jit(solution)/shard_map/ppermute | solution.py:54
  77.9 11.1 %collective-permute-start.13 = (bf16[128,256]{1,0:T(8,128)(2,1)S(1)}, bf16[128,256]{1,0:T(8,128)(2,1)S(1)}, u32[]{:S(2)}, u32[]{:S(2)}) collective-permute-start(bf16[128,256]{1,0:T(8,128)(2,1)S(1)} %get-tuple-element.42.own), channel_id=1, source_target_pairs={{0,8},{8,16},{16,24},{24,32},{32,40},{40,48},{48,56},{56,64},{64,7... | collective-permute-start | bytes 196616 | tf_op jit(solution)/shard_map/ppermute | solution.py:50
  89.9 4.7 %collective-permute-start.15 = (bf16[128,256]{1,0:T(8,128)(2,1)S(1)}, bf16[128,256]{1,0:T(8,128)(2,1)S(1)}, u32[]{:S(2)}, u32[]{:S(2)}) collective-permute-start(bf16[128,256]{1,0:T(8,128)(2,1)S(1)} %get-tuple-element.44), channel_id=1, source_target_pairs={{0,2},{2,4},{4,6},{6,0},{1,3},{3,5},{5,7},{7,1},{8,10},{10,12},{12... | collective-permute-start | bytes 196616 | tf_op jit(solution)/shard_map/ppermute | solution.py:236
  90.0 5.3 %collective-permute-start.16 = (bf16[128,256]{1,0:T(8,128)(2,1)S(1)}, bf16[128,256]{1,0:T(8,128)(2,1)S(1)}, u32[]{:S(2)}, u32[]{:S(2)}) collective-permute-start(bf16[128,256]{1,0:T(8,128)(2,1)S(1)} %get-tuple-element.45), channel_id=1, source_target_pairs={{0,4},{2,6},{4,0},{6,2},{1,5},{3,7},{5,1},{7,3},{8,12},{10,14},{12... | collective-permute-start | bytes 196616 | tf_op jit(solution)/shard_map/ppermute | solution.py:238
  91.0 4.8 %collective-permute-start.17 = (bf16[128,256]{1,0:T(8,128)(2,1)S(1)}, bf16[128,256]{1,0:T(8,128)(2,1)S(1)}, u32[]{:S(2)}, u32[]{:S(2)}) collective-permute-start(bf16[128,256]{1,0:T(8,128)(2,1)S(1)} %get-tuple-element.46), channel_id=1, source_target_pairs={{0,6},{2,0},{4,2},{6,4},{1,7},{3,1},{5,3},{7,5},{8,14},{10,8},{12,... | collective-permute-start | bytes 196616 | tf_op jit(solution)/shard_map/ppermute | solution.py:237
  95.9 3.7 %collective-permute-start.18 = (f32[128,256]{1,0:T(8,128)S(1)}, f32[128,256]{1,0:T(8,128)S(1)}, u32[]{:S(2)}, u32[]{:S(2)}) collective-permute-start(f32[128,256]{1,0:T(8,128)S(1)} %shard_map.91.mine), channel_id=1, source_target_pairs={{0,1},{1,0},{2,3},{3,2},{4,5},{5,4},{6,7},{7,6},{8,9},{9,8},{10,11... | collective-permute-start | bytes 393224 | tf_op jit(solution)/shard_map/ppermute | solution.py:46
  99.6 3.5 %collective-permute-start.21 = (bf16[128,256]{1,0:T(8,128)(2,1)S(1)}, bf16[128,256]{1,0:T(8,128)(2,1)S(1)}, u32[]{:S(2)}, u32[]{:S(2)}) collective-permute-start(bf16[128,256]{1,0:T(8,128)(2,1)S(1)} %shard_map.92.x0), channel_id=1, source_target_pairs={{0,6},{2,0},{4,2},{6,4},{1,7},{3,1},{5,3},{7,5},{8,14},{10,8},{12,... | collective-permute-start | bytes 196616 | tf_op jit(solution)/shard_map/ppermute | solution.py:30
  101.8 4.6 %collective-permute-start.20 = (bf16[128,256]{1,0:T(8,128)(2,1)S(1)}, bf16[128,256]{1,0:T(8,128)(2,1)S(1)}, u32[]{:S(2)}, u32[]{:S(2)}) collective-permute-start(bf16[128,256]{1,0:T(8,128)(2,1)S(1)} %shard_map.92.x0), channel_id=1, source_target_pairs={{0,4},{2,6},{4,0},{6,2},{1,5},{3,7},{5,1},{7,3},{8,12},{10,14},{12... | collective-permute-start | bytes 196616 | tf_op jit(solution)/shard_map/ppermute | solution.py:30
  102.5 5.2 %collective-permute-start.19 = (bf16[128,256]{1,0:T(8,128)(2,1)S(1)}, bf16[128,256]{1,0:T(8,128)(2,1)S(1)}, u32[]{:S(2)}, u32[]{:S(2)}) collective-permute-start(bf16[128,256]{1,0:T(8,128)(2,1)S(1)} %shard_map.92.x0), channel_id=1, source_target_pairs={{0,2},{2,4},{4,6},{6,0},{1,3},{3,5},{5,7},{7,1},{8,10},{10,12},{12... | collective-permute-start | bytes 196616 | tf_op jit(solution)/shard_map/ppermute | solution.py:30
  108.2 5.6 %collective-permute-start.23 = (bf16[128,256]{1,0:T(8,128)(2,1)S(1)}, bf16[128,256]{1,0:T(8,128)(2,1)S(1)}, u32[]{:S(2)}, u32[]{:S(2)}) collective-permute-start(bf16[128,256]{1,0:T(8,128)(2,1)S(1)} %get-tuple-element.50.own), channel_id=1, source_target_pairs={{8,0},{16,8},{24,16},{32,24},{40,32},{48,40},{56,48},{64,56},{72,6... | collective-permute-start | bytes 196616 | tf_op jit(solution)/shard_map/ppermute | solution.py:54
  111.8 7.1 %collective-permute-start.22 = (bf16[128,256]{1,0:T(8,128)(2,1)S(1)}, bf16[128,256]{1,0:T(8,128)(2,1)S(1)}, u32[]{:S(2)}, u32[]{:S(2)}) collective-permute-start(bf16[128,256]{1,0:T(8,128)(2,1)S(1)} %get-tuple-element.50.own), channel_id=1, source_target_pairs={{0,8},{8,16},{16,24},{24,32},{32,40},{40,48},{48,56},{56,64},{64,7... | collective-permute-start | bytes 196616 | tf_op jit(solution)/shard_map/ppermute | solution.py:50
  119.9 5.1 %collective-permute-start.24 = (bf16[128,256]{1,0:T(8,128)(2,1)S(1)}, bf16[128,256]{1,0:T(8,128)(2,1)S(1)}, u32[]{:S(2)}, u32[]{:S(2)}) collective-permute-start(bf16[128,256]{1,0:T(8,128)(2,1)S(1)} %get-tuple-element.52), channel_id=1, source_target_pairs={{0,2},{2,4},{4,6},{6,0},{1,3},{3,5},{5,7},{7,1},{8,10},{10,12},{12... | collective-permute-start | bytes 196616 | tf_op jit(solution)/shard_map/ppermute | solution.py:236
  120.0 5.0 %collective-permute-start.25 = (bf16[128,256]{1,0:T(8,128)(2,1)S(1)}, bf16[128,256]{1,0:T(8,128)(2,1)S(1)}, u32[]{:S(2)}, u32[]{:S(2)}) collective-permute-start(bf16[128,256]{1,0:T(8,128)(2,1)S(1)} %get-tuple-element.53), channel_id=1, source_target_pairs={{0,4},{2,6},{4,0},{6,2},{1,5},{3,7},{5,1},{7,3},{8,12},{10,14},{12... | collective-permute-start | bytes 196616 | tf_op jit(solution)/shard_map/ppermute | solution.py:238
  121.4 4.1 %collective-permute-start.26 = (bf16[128,256]{1,0:T(8,128)(2,1)S(1)}, bf16[128,256]{1,0:T(8,128)(2,1)S(1)}, u32[]{:S(2)}, u32[]{:S(2)}) collective-permute-start(bf16[128,256]{1,0:T(8,128)(2,1)S(1)} %get-tuple-element.54), channel_id=1, source_target_pairs={{0,6},{2,0},{4,2},{6,4},{1,7},{3,1},{5,3},{7,5},{8,14},{10,8},{12,... | collective-permute-start | bytes 196616 | tf_op jit(solution)/shard_map/ppermute | solution.py:237
  125.6 5.3 %collective-permute-start.27 = (f32[128,128]{1,0:T(8,128)S(1)}, f32[128,128]{1,0:T(8,128)S(1)}, u32[]{:S(2)}, u32[]{:S(2)}) collective-permute-start(f32[128,128]{1,0:T(8,128)S(1)} %get-tuple-element.56), channel_id=1, source_target_pairs={{0,1},{1,0},{2,3},{3,2},{4,5},{5,4},{6,7},{7,6},{8,9},{9,8},{10,11... | collective-permute-start | bytes 196616 | tf_op jit(solution)/shard_map/ppermute | solution.py:46
  (5 other events, 42.9 us)

commit v8 on v7

--- a/solution.py
+++ b/solution.py
@@ -34,8 +34,8 @@
     return [a, three[0], three[2], three[1]]
 
 
-def gather_rows(a):
-    return lax.all_to_all(a, SP, 0, 0, tiled=True).reshape(1024, 512)
+def gather_rows(a, axes):
+    return lax.all_to_all(a, axes, 0, 0, tiled=True).reshape(1024, 512)
 
 
 def after_this(a, done):
@@ -91,18 +91,25 @@
         first[n] = whole
 
 
-def many_body(wq, wk, wv, wo, bias, many1, many2, wide, parts, sems):
+def many_body(wq, wk, wv, wo, bias, many, third, wide, parts, sems):
     pairs = [(w.at[1:3], parts.at[n]) for n, w in enumerate((wq, wk, wv, wo))]
     fetch(pairs, sems)
-    for layer, many in enumerate((many1, many2)):
-        whole = jnp.concatenate([parts[n, layer] for n in range(4)], axis=1)
-        for n in range(16):
-            many[n] = whole
+    third[...] = jnp.concatenate([parts[n, 1] for n in range(4)], axis=1)
+    whole = jnp.concatenate([parts[n, 0] for n in range(4)], axis=1)
+    for n in range(16):
+        many[n] = whole
     wide[...] = jnp.zeros((8, 256), F32)
     for n in range(2 * LAYERS):
         for lag_row in range(WIN_ROWS):
             at = lag_row * GRID_W
             wide[n : n + 1, at : at + WIN_COLS] = bias[n // 2, n % 2, lag_row : lag_row + 1, :]
+
+
+def line_body(p0, p1, p2, p3, many):
+    for k, part in enumerate((p0, p1, p2, p3)):
+        at = behind("x", k)
+        for n in range(4):
+            many[n, at] = part[...]
 
 
 def table_body(wide, before, own, after, table):
@@ -249,24 +256,28 @@
         pack_body, shaped(16, 64, 512), *held, in_specs=[hbm] * 4,
         scratch=[pltpu.VMEM((4, 64, 128), BF16), pltpu.SemaphoreType.DMA((4,))],
     )
-    weights = gather_rows(first)
-    near_y = jnp.stack(in_order(tokens, spread(tokens, "y")))
-    many1, many2, wide = call(
-        many_body, [shaped(16, 64, 512)] * 2 + [shaped(8, 256, dtype=F32)],
+    weights = gather_rows(first, SP)
+    tokens_y = spread(tokens, "y")
+    near_y = jnp.stack(in_order(tokens, tokens_y))
+    many1, third, wide = call(
+        many_body, [shaped(16, 64, 512), shaped(64, 512), shaped(8, 256, dtype=F32)],
         *held, offset_bias, in_specs=[hbm] * 4 + [pl.BlockSpec()],
         scratch=[pltpu.VMEM((4, 2, 64, 128), BF16), pltpu.SemaphoreType.DMA((4,))],
     )
+    third_x = in_order(third, spread(third, "x"))
     near_partner = swap(after_this(near_y, many1))
 
     q, kv = call(
         heads_first_body, [shaped(128, 128), shaped(144, 256)],
         near_y, near_partner, norm_gain, documents.reshape(1, 128), weights,
     )
+    many2 = call(line_body, shaped(4, 4, 64, 512), *third_x)
     for layer in range(LAYERS):
         after = from_after(kv)
         before = from_before(kv)
         if layer < 2:
-            next_weights = gather_rows(after_this((many1, many2)[layer], kv))
+            many, axes = ((many1, SP), (many2, "z"))[layer]
+            next_weights = gather_rows(after_this(many, kv), axes)
         if layer == 0:
             table = call(table_body, shaped(6, 128, 384, dtype=F32), wide, before, kv, after)
         kept, r1, r2, r3 = scattered(
@@ -275,6 +286,8 @@
         )
         if layer == 2:
             break
+        if layer == 0:
+            kept = after_this(kept, many2)
         half = call(sum_body, shaped(128, 256, dtype=F32), kept, r1, r2, r3)
         stream = call(pair_sum_body, shaped(128, 256), half, swap(half))
         weights = next_weights

time: 132 us -> 127 us (0.962)
  the two profiles are of different devices: /device:TPU:33 before, /device:TPU:39 now
where the time goes in v8:
time: 127 us; the launch traced here: 126 us
  starting transfers between devices  78.1 us (61%)
  waiting for transfers between devices  36.9 us (29%)
  Pallas kernels  8.66 us (7%)
  local copies, waits for them, and re-layouts  2 us (2%)
    all_to_all x3, starting transfers between devices, gather_rows(): return lax.all_to_all(a, axes, 0, 0, tiled=True).reshape(1024, 512)  19.1 us
    ppermute x4, starting transfers between devices, swap(): return lax.ppermute(a, 'c', [(0, 1), (1, 0)])  15.6 us
    ppermute x12, starting transfers between devices, spread(): return [lax.ppermute(a, axis, turn(k)) for k in (1, 3, 2)]  14.3 us
    ppermute x3, waiting for transfers between devices, from_after(): return lax.ppermute(a, SP, [(i + 1, i) for i in range(15)])  11.3 us
    ppermute x3, starting transfers between devices, from_before(): return lax.ppermute(a, SP, [(i, i + 1) for i in range(15)])  9.49 us
    ppermute x3, starting transfers between devices, scattered(): r2 = lax.ppermute(s2, 'y', turn(2))  8.84 us
    pallas_call x16, Pallas kernels, call(): pl.pallas_call(body, out_shape=outs, **specs, scratch_shapes=list(scratch...  8.66 us
    ppermute x3, starting transfers between devices, from_after(): return lax.ppermute(a, SP, [(i + 1, i) for i in range(15)])  7.47 us
  transfers between devices with their start and end apart: 34, of which 22 were waited for; matrix products, arithmetic and copies ran while one was open for 0% of the time, Pallas kernels for 3%

profile of v8, /device:TPU:39, one launch (start us, length us, event | category | flops | bytes accessed | tf_op | source)
XLA Modules:
  0.0 126.0 jit_solution(5989742581512480099)
XLA Ops:
  0.0 1.9 %shard_map.83 = bf16[16,64,512]{2,1,0:T(8,128)(2,1)} custom-call(bf16[3,64,128]{2,1,0:T(8,128)(2,1)} %wq.3, bf16[3,64,128]{2,1,0:T(8,128)(2,1)} %wk.3, bf16[3,64,128]{2,1,0:T(8,128)(2,1)} %wv.3, bf16[3,64,128]{2,1,0:T(8,128)(2,1)} %bitcast.16), custom_call_target="tpu_custom_call" | custom-call | tf_op jit(solution)/shard_map/pallas_call | solution.py:66
  2.0 7.4 %all-to-all-start = ((bf16[16,64,512]{2,1,0:T(8,128)(2,1)}), bf16[16,64,512]{2,1,0:T(8,128)(2,1)S(1)}, u32[]{:S(2)}, u32[]{:S(2)}) async-start(bf16[16,64,512]{2,1,0:T(8,128)(2,1)} %shard_map.83), calls=%async_computation | async-start | bytes 2097152 | tf_op jit(solution)/shard_map/all_to_all | solution.py:38
  9.4 1.4 %collective-permute-start = (bf16[128,128]{1,0:T(8,128)(2,1)S(1)}, bf16[128,128]{1,0:T(8,128)(2,1)S(1)}, u32[]{:S(2)}, u32[]{:S(2)}) collective-permute-start(bf16[128,128]{1,0:T(8,128)(2,1)S(1)} %copy-done.5), channel_id=1, source_target_pairs={{0,2},{2,4},{4,6},{6,0},{1,3},{3,5},{5,7},{7,1},{8,10},{10,12},{12... | collective-permute-start | bytes 98312 | tf_op jit(solution)/shard_map/ppermute | solution.py:30
  10.7 2.6 %collective-permute-start.1 = (bf16[128,128]{1,0:T(8,128)(2,1)S(1)}, bf16[128,128]{1,0:T(8,128)(2,1)S(1)}, u32[]{:S(2)}, u32[]{:S(2)}) collective-permute-start(bf16[128,128]{1,0:T(8,128)(2,1)S(1)} %copy-done.5), channel_id=1, source_target_pairs={{0,4},{2,6},{4,0},{6,2},{1,5},{3,7},{5,1},{7,3},{8,12},{10,14},{12... | collective-permute-start | bytes 98312 | tf_op jit(solution)/shard_map/ppermute | solution.py:30
  16.6 2.5 %collective-permute-start.3 = (bf16[4,128,128]{2,1,0:T(8,128)(2,1)S(1)}, bf16[4,128,128]{2,1,0:T(8,128)(2,1)S(1)}, u32[]{:S(2)}, u32[]{:S(2)}) collective-permute-start(bf16[4,128,128]{2,1,0:T(8,128)(2,1)S(1)} %pad_maximum_fusion.own), channel_id=1, source_target_pairs={{0,1},{1,0},{2,3},{3,2},{4,5},{5,4},{6,7},{7,6},{8,9},{9,8},{10,11... | collective-permute-start | bytes 393224 | tf_op jit(solution)/shard_map/ppermute | solution.py:46
  20.1 1.7 %all-to-all-done = bf16[16,64,512]{2,1,0:T(8,128)(2,1)S(1)} async-done(((bf16[16,64,512]{2,1,0:T(8,128)(2,1)}), bf16[16,64,512]{2,1,0:T(8,128)(2,1)S(1)}, u32[]{:S(2)}, u32[]{:S(2)}) %all-to-all-start) | async-done | bytes 1048608 | tf_op jit(solution)/shard_map/all_to_all | solution.py:38
  22.5 7.7 %all-to-all-start.1 = ((bf16[16,64,512]{2,1,0:T(8,128)(2,1)}), bf16[16,64,512]{2,1,0:T(8,128)(2,1)S(1)}, u32[]{:S(2)}, u32[]{:S(2)}) async-start(bf16[16,64,512]{2,1,0:T(8,128)(2,1)} %copy-done.1), calls=%async_computation.1 | async-start | bytes 2097152 | tf_op jit(solution)/shard_map/all_to_all | solution.py:38
  30.2 3.1 %collective-permute-start.4 = (bf16[144,256]{1,0:T(8,128)(2,1)S(1)}, bf16[144,256]{1,0:T(8,128)(2,1)S(1)}, u32[]{:S(2)}, u32[]{:S(2)}) collective-permute-start(bf16[144,256]{1,0:T(8,128)(2,1)S(1)} %get-tuple-element.35.own), channel_id=1, source_target_pairs={{0,8},{8,16},{16,24},{24,32},{32,40},{40,48},{48,56},{56,64},{64,7... | collective-permute-start | bytes 221192 | tf_op jit(solution)/shard_map/ppermute | solution.py:50
  33.3 2.2 %collective-permute-start.5 = (bf16[144,256]{1,0:T(8,128)(2,1)S(1)}, bf16[144,256]{1,0:T(8,128)(2,1)S(1)}, u32[]{:S(2)}, u32[]{:S(2)}) collective-permute-start(bf16[144,256]{1,0:T(8,128)(2,1)S(1)} %get-tuple-element.35.own), channel_id=1, source_target_pairs={{8,0},{16,8},{24,16},{32,24},{40,32},{48,40},{56,48},{64,56},{72,6... | collective-permute-start | bytes 221192 | tf_op jit(solution)/shard_map/ppermute | solution.py:54
  35.5 2.5 %collective-permute-start.6 = (bf16[64,512]{1,0:T(8,128)(2,1)S(1)}, bf16[64,512]{1,0:T(8,128)(2,1)S(1)}, u32[]{:S(2)}, u32[]{:S(2)}) collective-permute-start(bf16[64,512]{1,0:T(8,128)(2,1)S(1)} %get-tuple-element.38.p0), channel_id=1, source_target_pairs={{0,8},{8,16},{16,24},{24,0},{1,9},{9,17},{17,25},{25,1},{2,10},{10... | collective-permute-start | bytes 196616 | tf_op jit(solution)/shard_map/ppermute | solution.py:30
  38.6 4.1 %collective-permute-done.4.before = bf16[144,256]{1,0:T(8,128)(2,1)S(1)} collective-permute-done((bf16[144,256]{1,0:T(8,128)(2,1)S(1)}, bf16[144,256]{1,0:T(8,128)(2,1)S(1)}, u32[]{:S(2)}, u32[]{:S(2)}) %collective-permute-start.4) | collective-permute-done | bytes 73760 | tf_op jit(solution)/shard_map/ppermute | solution.py:50
  42.7 1.7 %collective-permute-done.5.after = bf16[144,256]{1,0:T(8,128)(2,1)S(1)} collective-permute-done((bf16[144,256]{1,0:T(8,128)(2,1)S(1)}, bf16[144,256]{1,0:T(8,128)(2,1)S(1)}, u32[]{:S(2)}, u32[]{:S(2)}) %collective-permute-start.5) | collective-permute-done | bytes 73760 | tf_op jit(solution)/shard_map/ppermute | solution.py:54
  45.9 3.0 %collective-permute-start.10 = (bf16[128,256]{1,0:T(8,128)(2,1)S(1)}, bf16[128,256]{1,0:T(8,128)(2,1)S(1)}, u32[]{:S(2)}, u32[]{:S(2)}) collective-permute-start(bf16[128,256]{1,0:T(8,128)(2,1)S(1)} %get-tuple-element.41), channel_id=1, source_target_pairs={{0,4},{2,6},{4,0},{6,2},{1,5},{3,7},{5,1},{7,3},{8,12},{10,14},{12... | collective-permute-start | bytes 196616 | tf_op jit(solution)/shard_map/ppermute | solution.py:245
  52.0 2.6 %collective-permute-done.9.r1 = bf16[128,256]{1,0:T(8,128)(2,1)S(1)} collective-permute-done((bf16[128,256]{1,0:T(8,128)(2,1)S(1)}, bf16[128,256]{1,0:T(8,128)(2,1)S(1)}, u32[]{:S(2)}, u32[]{:S(2)}) %collective-permute-start.9) | collective-permute-done | bytes 65568 | tf_op jit(solution)/shard_map/ppermute | solution.py:243
  54.6 4.0 %collective-permute-start.12 = (f32[128,256]{1,0:T(8,128)S(1)}, f32[128,256]{1,0:T(8,128)S(1)}, u32[]{:S(2)}, u32[]{:S(2)}) collective-permute-start(f32[128,256]{1,0:T(8,128)S(1)} %shard_map.88.mine), channel_id=1, source_target_pairs={{0,1},{1,0},{2,3},{3,2},{4,5},{5,4},{6,7},{7,6},{8,9},{9,8},{10,11... | collective-permute-start | bytes 393224 | tf_op jit(solution)/shard_map/ppermute | solution.py:46
  60.6 1.8 %collective-permute-start.15 = (bf16[128,256]{1,0:T(8,128)(2,1)S(1)}, bf16[128,256]{1,0:T(8,128)(2,1)S(1)}, u32[]{:S(2)}, u32[]{:S(2)}) collective-permute-start(bf16[128,256]{1,0:T(8,128)(2,1)S(1)} %shard_map.89.x0), channel_id=1, source_target_pairs={{0,6},{2,0},{4,2},{6,4},{1,7},{3,1},{5,3},{7,5},{8,14},{10,8},{12,... | collective-permute-start | bytes 196616 | tf_op jit(solution)/shard_map/ppermute | solution.py:30
  62.4 3.6 %collective-permute-done.13.x1 = bf16[128,256]{1,0:T(8,128)(2,1)S(1)} collective-permute-done((bf16[128,256]{1,0:T(8,128)(2,1)S(1)}, bf16[128,256]{1,0:T(8,128)(2,1)S(1)}, u32[]{:S(2)}, u32[]{:S(2)}) %collective-permute-start.13) | collective-permute-done | bytes 65568 | tf_op jit(solution)/shard_map/ppermute | solution.py:30
  66.4 4.0 %all-to-all-start.2 = ((bf16[4,4,64,512]{3,2,1,0:T(8,128)(2,1)}), bf16[4,4,64,512]{3,2,1,0:T(8,128)(2,1)S(1)}, u32[]{:S(2)}, u32[]{:S(2)}) async-start(bf16[4,4,64,512]{3,2,1,0:T(8,128)(2,1)} %copy-done), calls=%async_computation.2 | async-start | bytes 2097152 | tf_op jit(solution)/shard_map/all_to_all | solution.py:38
  70.4 4.5 %collective-permute-start.16 = (bf16[128,256]{1,0:T(8,128)(2,1)S(1)}, bf16[128,256]{1,0:T(8,128)(2,1)S(1)}, u32[]{:S(2)}, u32[]{:S(2)}) collective-permute-start(bf16[128,256]{1,0:T(8,128)(2,1)S(1)} %get-tuple-element.45.own), channel_id=1, source_target_pairs={{0,8},{8,16},{16,24},{24,32},{32,40},{40,48},{48,56},{56,64},{64,7... | collective-permute-start | bytes 196616 | tf_op jit(solution)/shard_map/ppermute | solution.py:50
  74.9 1.9 %collective-permute-start.17 = (bf16[128,256]{1,0:T(8,128)(2,1)S(1)}, bf16[128,256]{1,0:T(8,128)(2,1)S(1)}, u32[]{:S(2)}, u32[]{:S(2)}) collective-permute-start(bf16[128,256]{1,0:T(8,128)(2,1)S(1)} %get-tuple-element.45.own), channel_id=1, source_target_pairs={{8,0},{16,8},{24,16},{32,24},{40,32},{48,40},{56,48},{64,56},{72,6... | collective-permute-start | bytes 196616 | tf_op jit(solution)/shard_map/ppermute | solution.py:54
  76.9 5.9 %collective-permute-done.17.after = bf16[128,256]{1,0:T(8,128)(2,1)S(1)} collective-permute-done((bf16[128,256]{1,0:T(8,128)(2,1)S(1)}, bf16[128,256]{1,0:T(8,128)(2,1)S(1)}, u32[]{:S(2)}, u32[]{:S(2)}) %collective-permute-start.17) | collective-permute-done | bytes 65568 | tf_op jit(solution)/shard_map/ppermute | solution.py:54
  84.2 3.5 %collective-permute-start.19 = (bf16[128,256]{1,0:T(8,128)(2,1)S(1)}, bf16[128,256]{1,0:T(8,128)(2,1)S(1)}, u32[]{:S(2)}, u32[]{:S(2)}) collective-permute-start(bf16[128,256]{1,0:T(8,128)(2,1)S(1)} %get-tuple-element.48), channel_id=1, source_target_pairs={{0,4},{2,6},{4,0},{6,2},{1,5},{3,7},{5,1},{7,3},{8,12},{10,14},{12... | collective-permute-start | bytes 196616 | tf_op jit(solution)/shard_map/ppermute | solution.py:245
  88.2 1.9 %collective-permute-done.19.r2 = bf16[128,256]{1,0:T(8,128)(2,1)S(1)} collective-permute-done((bf16[128,256]{1,0:T(8,128)(2,1)S(1)}, bf16[128,256]{1,0:T(8,128)(2,1)S(1)}, u32[]{:S(2)}, u32[]{:S(2)}) %collective-permute-start.19) | collective-permute-done | bytes 65568 | tf_op jit(solution)/shard_map/ppermute | solution.py:245
  90.9 4.6 %collective-permute-start.21 = (f32[128,256]{1,0:T(8,128)S(1)}, f32[128,256]{1,0:T(8,128)S(1)}, u32[]{:S(2)}, u32[]{:S(2)}) collective-permute-start(f32[128,256]{1,0:T(8,128)S(1)} %shard_map.92.mine), channel_id=1, source_target_pairs={{0,1},{1,0},{2,3},{3,2},{4,5},{5,4},{6,7},{7,6},{8,9},{9,8},{10,11... | collective-permute-start | bytes 393224 | tf_op jit(solution)/shard_map/ppermute | solution.py:46
  96.5 2.5 %collective-permute-start.23 = (bf16[128,256]{1,0:T(8,128)(2,1)S(1)}, bf16[128,256]{1,0:T(8,128)(2,1)S(1)}, u32[]{:S(2)}, u32[]{:S(2)}) collective-permute-start(bf16[128,256]{1,0:T(8,128)(2,1)S(1)} %shard_map.93.x0), channel_id=1, source_target_pairs={{0,4},{2,6},{4,0},{6,2},{1,5},{3,7},{5,1},{7,3},{8,12},{10,14},{12... | collective-permute-start | bytes 196616 | tf_op jit(solution)/shard_map/ppermute | solution.py:30
  99.8 1.8 %collective-permute-done.22.x1 = bf16[128,256]{1,0:T(8,128)(2,1)S(1)} collective-permute-done((bf16[128,256]{1,0:T(8,128)(2,1)S(1)}, bf16[128,256]{1,0:T(8,128)(2,1)S(1)}, u32[]{:S(2)}, u32[]{:S(2)}) %collective-permute-start.22) | collective-permute-done | bytes 65568 | tf_op jit(solution)/shard_map/ppermute | solution.py:30
  103.2 1.9 %collective-permute-start.25 = (bf16[128,256]{1,0:T(8,128)(2,1)S(1)}, bf16[128,256]{1,0:T(8,128)(2,1)S(1)}, u32[]{:S(2)}, u32[]{:S(2)}) collective-permute-start(bf16[128,256]{1,0:T(8,128)(2,1)S(1)} %get-tuple-element.52.own), channel_id=1, source_target_pairs={{0,8},{8,16},{16,24},{24,32},{32,40},{40,48},{48,56},{56,64},{64,7... | collective-permute-start | bytes 196616 | tf_op jit(solution)/shard_map/ppermute | solution.py:50
  105.2 3.4 %collective-permute-start.26 = (bf16[128,256]{1,0:T(8,128)(2,1)S(1)}, bf16[128,256]{1,0:T(8,128)(2,1)S(1)}, u32[]{:S(2)}, u32[]{:S(2)}) collective-permute-start(bf16[128,256]{1,0:T(8,128)(2,1)S(1)} %get-tuple-element.52.own), channel_id=1, source_target_pairs={{8,0},{16,8},{24,16},{32,24},{40,32},{48,40},{56,48},{64,56},{72,6... | collective-permute-start | bytes 196616 | tf_op jit(solution)/shard_map/ppermute | solution.py:54
  108.6 3.7 %collective-permute-done.26.after = bf16[128,256]{1,0:T(8,128)(2,1)S(1)} collective-permute-done((bf16[128,256]{1,0:T(8,128)(2,1)S(1)}, bf16[128,256]{1,0:T(8,128)(2,1)S(1)}, u32[]{:S(2)}, u32[]{:S(2)}) %collective-permute-start.26) | collective-permute-done | bytes 65568 | tf_op jit(solution)/shard_map/ppermute | solution.py:54
  114.5 2.4 %collective-permute-start.28 = (bf16[128,256]{1,0:T(8,128)(2,1)S(1)}, bf16[128,256]{1,0:T(8,128)(2,1)S(1)}, u32[]{:S(2)}, u32[]{:S(2)}) collective-permute-start(bf16[128,256]{1,0:T(8,128)(2,1)S(1)} %get-tuple-element.55), channel_id=1, source_target_pairs={{0,4},{2,6},{4,0},{6,2},{1,5},{3,7},{5,1},{7,3},{8,12},{10,14},{12... | collective-permute-start | bytes 196616 | tf_op jit(solution)/shard_map/ppermute | solution.py:245
  117.6 1.6 %collective-permute-done.28.r2 = bf16[128,256]{1,0:T(8,128)(2,1)S(1)} collective-permute-done((bf16[128,256]{1,0:T(8,128)(2,1)S(1)}, bf16[128,256]{1,0:T(8,128)(2,1)S(1)}, u32[]{:S(2)}, u32[]{:S(2)}) %collective-permute-start.28) | collective-permute-done | bytes 65568 | tf_op jit(solution)/shard_map/ppermute | solution.py:245
  120.0 4.4 %collective-permute-start.30 = (f32[128,128]{1,0:T(8,128)S(1)}, f32[128,128]{1,0:T(8,128)S(1)}, u32[]{:S(2)}, u32[]{:S(2)}) collective-permute-start(f32[128,128]{1,0:T(8,128)S(1)} %get-tuple-element.58), channel_id=1, source_target_pairs={{0,1},{1,0},{2,3},{3,2},{4,5},{5,4},{6,7},{7,6},{8,9},{9,8},{10,11... | collective-permute-start | bytes 196616 | tf_op jit(solution)/shard_map/ppermute | solution.py:46
  (65 shorter events, 24.2 us)
Async XLA Ops:
  2.0 19.9 %all-to-all-start = ((bf16[16,64,512]{2,1,0:T(8,128)(2,1)}), bf16[16,64,512]{2,1,0:T(8,128)(2,1)S(1)}, u32[]{:S(2)}, u32[]{:S(2)}) async-start(bf16[16,64,512]{2,1,0:T(8,128)(2,1)} %shard_map.83), calls=%async_computation | async-start | bytes 2097152 | tf_op jit(solution)/shard_map/all_to_all | solution.py:38
  9.4 7.0 %collective-permute-start = (bf16[128,128]{1,0:T(8,128)(2,1)S(1)}, bf16[128,128]{1,0:T(8,128)(2,1)S(1)}, u32[]{:S(2)}, u32[]{:S(2)}) collective-permute-start(bf16[128,128]{1,0:T(8,128)(2,1)S(1)} %copy-done.5), channel_id=1, source_target_pairs={{0,2},{2,4},{4,6},{6,0},{1,3},{3,5},{5,7},{7,1},{8,10},{10,12},{12... | collective-permute-start | bytes 98312 | tf_op jit(solution)/shard_map/ppermute | solution.py:30
  10.7 5.7 %collective-permute-start.1 = (bf16[128,128]{1,0:T(8,128)(2,1)S(1)}, bf16[128,128]{1,0:T(8,128)(2,1)S(1)}, u32[]{:S(2)}, u32[]{:S(2)}) collective-permute-start(bf16[128,128]{1,0:T(8,128)(2,1)S(1)} %copy-done.5), channel_id=1, source_target_pairs={{0,4},{2,6},{4,0},{6,2},{1,5},{3,7},{5,1},{7,3},{8,12},{10,14},{12... | collective-permute-start | bytes 98312 | tf_op jit(solution)/shard_map/ppermute | solution.py:30
  13.3 3.3 %collective-permute-start.2 = (bf16[128,128]{1,0:T(8,128)(2,1)S(1)}, bf16[128,128]{1,0:T(8,128)(2,1)S(1)}, u32[]{:S(2)}, u32[]{:S(2)}) collective-permute-start(bf16[128,128]{1,0:T(8,128)(2,1)S(1)} %copy-done.5), channel_id=1, source_target_pairs={{0,6},{2,0},{4,2},{6,4},{1,7},{3,1},{5,3},{7,5},{8,14},{10,8},{12,... | collective-permute-start | bytes 98312 | tf_op jit(solution)/shard_map/ppermute | solution.py:30
  16.6 3.5 %collective-permute-start.3 = (bf16[4,128,128]{2,1,0:T(8,128)(2,1)S(1)}, bf16[4,128,128]{2,1,0:T(8,128)(2,1)S(1)}, u32[]{:S(2)}, u32[]{:S(2)}) collective-permute-start(bf16[4,128,128]{2,1,0:T(8,128)(2,1)S(1)} %pad_maximum_fusion.own), channel_id=1, source_target_pairs={{0,1},{1,0},{2,3},{3,2},{4,5},{5,4},{6,7},{7,6},{8,9},{9,8},{10,11... | collective-permute-start | bytes 393224 | tf_op jit(solution)/shard_map/ppermute | solution.py:46
  22.5 43.4 %all-to-all-start.1 = ((bf16[16,64,512]{2,1,0:T(8,128)(2,1)}), bf16[16,64,512]{2,1,0:T(8,128)(2,1)S(1)}, u32[]{:S(2)}, u32[]{:S(2)}) async-start(bf16[16,64,512]{2,1,0:T(8,128)(2,1)} %copy-done.1), calls=%async_computation.1 | async-start | bytes 2097152 | tf_op jit(solution)/shard_map/all_to_all | solution.py:38
  30.2 12.5 %collective-permute-start.4 = (bf16[144,256]{1,0:T(8,128)(2,1)S(1)}, bf16[144,256]{1,0:T(8,128)(2,1)S(1)}, u32[]{:S(2)}, u32[]{:S(2)}) collective-permute-start(bf16[144,256]{1,0:T(8,128)(2,1)S(1)} %get-tuple-element.35.own), channel_id=1, source_target_pairs={{0,8},{8,16},{16,24},{24,32},{32,40},{40,48},{48,56},{56,64},{64,7... | collective-permute-start | bytes 221192 | tf_op jit(solution)/shard_map/ppermute | solution.py:50
  33.3 11.1 %collective-permute-start.5 = (bf16[144,256]{1,0:T(8,128)(2,1)S(1)}, bf16[144,256]{1,0:T(8,128)(2,1)S(1)}, u32[]{:S(2)}, u32[]{:S(2)}) collective-permute-start(bf16[144,256]{1,0:T(8,128)(2,1)S(1)} %get-tuple-element.35.own), channel_id=1, source_target_pairs={{8,0},{16,8},{24,16},{32,24},{40,32},{48,40},{56,48},{64,56},{72,6... | collective-permute-start | bytes 221192 | tf_op jit(solution)/shard_map/ppermute | solution.py:54
  35.5 14.2 %collective-permute-start.6 = (bf16[64,512]{1,0:T(8,128)(2,1)S(1)}, bf16[64,512]{1,0:T(8,128)(2,1)S(1)}, u32[]{:S(2)}, u32[]{:S(2)}) collective-permute-start(bf16[64,512]{1,0:T(8,128)(2,1)S(1)} %get-tuple-element.38.p0), channel_id=1, source_target_pairs={{0,8},{8,16},{16,24},{24,0},{1,9},{9,17},{17,25},{25,1},{2,10},{10... | collective-permute-start | bytes 196616 | tf_op jit(solution)/shard_map/ppermute | solution.py:30
  38.0 12.4 %collective-permute-start.7 = (bf16[64,512]{1,0:T(8,128)(2,1)S(1)}, bf16[64,512]{1,0:T(8,128)(2,1)S(1)}, u32[]{:S(2)}, u32[]{:S(2)}) collective-permute-start(bf16[64,512]{1,0:T(8,128)(2,1)S(1)} %get-tuple-element.38.p0), channel_id=1, source_target_pairs={{0,16},{8,24},{16,0},{24,8},{1,17},{9,25},{17,1},{25,9},{2,18},{10... | collective-permute-start | bytes 196616 | tf_op jit(solution)/shard_map/ppermute | solution.py:30
  38.0 12.4 %collective-permute-start.8 = (bf16[64,512]{1,0:T(8,128)(2,1)S(1)}, bf16[64,512]{1,0:T(8,128)(2,1)S(1)}, u32[]{:S(2)}, u32[]{:S(2)}) collective-permute-start(bf16[64,512]{1,0:T(8,128)(2,1)S(1)} %get-tuple-element.38.p0), channel_id=1, source_target_pairs={{0,24},{8,0},{16,8},{24,16},{1,25},{9,1},{17,9},{25,17},{2,26},{10... | collective-permute-start | bytes 196616 | tf_op jit(solution)/shard_map/ppermute | solution.py:30
  45.9 5.5 %collective-permute-start.10 = (bf16[128,256]{1,0:T(8,128)(2,1)S(1)}, bf16[128,256]{1,0:T(8,128)(2,1)S(1)}, u32[]{:S(2)}, u32[]{:S(2)}) collective-permute-start(bf16[128,256]{1,0:T(8,128)(2,1)S(1)} %get-tuple-element.41), channel_id=1, source_target_pairs={{0,4},{2,6},{4,0},{6,2},{1,5},{3,7},{5,1},{7,3},{8,12},{10,14},{12... | collective-permute-start | bytes 196616 | tf_op jit(solution)/shard_map/ppermute | solution.py:245
  49.6 4.9 %collective-permute-start.9 = (bf16[128,256]{1,0:T(8,128)(2,1)S(1)}, bf16[128,256]{1,0:T(8,128)(2,1)S(1)}, u32[]{:S(2)}, u32[]{:S(2)}) collective-permute-start(bf16[128,256]{1,0:T(8,128)(2,1)S(1)} %get-tuple-element.40), channel_id=1, source_target_pairs={{0,2},{2,4},{4,6},{6,0},{1,3},{3,5},{5,7},{7,1},{8,10},{10,12},{12... | collective-permute-start | bytes 196616 | tf_op jit(solution)/shard_map/ppermute | solution.py:243
  54.6 5.0 %collective-permute-start.12 = (f32[128,256]{1,0:T(8,128)S(1)}, f32[128,256]{1,0:T(8,128)S(1)}, u32[]{:S(2)}, u32[]{:S(2)}) collective-permute-start(f32[128,256]{1,0:T(8,128)S(1)} %shard_map.88.mine), channel_id=1, source_target_pairs={{0,1},{1,0},{2,3},{3,2},{4,5},{5,4},{6,7},{7,6},{8,9},{9,8},{10,11... | collective-permute-start | bytes 393224 | tf_op jit(solution)/shard_map/ppermute | solution.py:46
  59.6 6.3 %collective-permute-start.13 = (bf16[128,256]{1,0:T(8,128)(2,1)S(1)}, bf16[128,256]{1,0:T(8,128)(2,1)S(1)}, u32[]{:S(2)}, u32[]{:S(2)}) collective-permute-start(bf16[128,256]{1,0:T(8,128)(2,1)S(1)} %shard_map.89.x0), channel_id=1, source_target_pairs={{0,2},{2,4},{4,6},{6,0},{1,3},{3,5},{5,7},{7,1},{8,10},{10,12},{12... | collective-permute-start | bytes 196616 | tf_op jit(solution)/shard_map/ppermute | solution.py:30
  59.7 6.2 %collective-permute-start.14 = (bf16[128,256]{1,0:T(8,128)(2,1)S(1)}, bf16[128,256]{1,0:T(8,128)(2,1)S(1)}, u32[]{:S(2)}, u32[]{:S(2)}) collective-permute-start(bf16[128,256]{1,0:T(8,128)(2,1)S(1)} %shard_map.89.x0), channel_id=1, source_target_pairs={{0,4},{2,6},{4,0},{6,2},{1,5},{3,7},{5,1},{7,3},{8,12},{10,14},{12... | collective-permute-start | bytes 196616 | tf_op jit(solution)/shard_map/ppermute | solution.py:30
  60.6 5.3 %collective-permute-start.15 = (bf16[128,256]{1,0:T(8,128)(2,1)S(1)}, bf16[128,256]{1,0:T(8,128)(2,1)S(1)}, u32[]{:S(2)}, u32[]{:S(2)}) collective-permute-start(bf16[128,256]{1,0:T(8,128)(2,1)S(1)} %shard_map.89.x0), channel_id=1, source_target_pairs={{0,6},{2,0},{4,2},{6,4},{1,7},{3,1},{5,3},{7,5},{8,14},{10,8},{12,... | collective-permute-start | bytes 196616 | tf_op jit(solution)/shard_map/ppermute | solution.py:30
  66.4 36.3 %all-to-all-start.2 = ((bf16[4,4,64,512]{3,2,1,0:T(8,128)(2,1)}), bf16[4,4,64,512]{3,2,1,0:T(8,128)(2,1)S(1)}, u32[]{:S(2)}, u32[]{:S(2)}) async-start(bf16[4,4,64,512]{3,2,1,0:T(8,128)(2,1)} %copy-done), calls=%async_computation.2 | async-start | bytes 2097152 | tf_op jit(solution)/shard_map/all_to_all | solution.py:38
  70.4 6.4 %collective-permute-start.16 = (bf16[128,256]{1,0:T(8,128)(2,1)S(1)}, bf16[128,256]{1,0:T(8,128)(2,1)S(1)}, u32[]{:S(2)}, u32[]{:S(2)}) collective-permute-start(bf16[128,256]{1,0:T(8,128)(2,1)S(1)} %get-tuple-element.45.own), channel_id=1, source_target_pairs={{0,8},{8,16},{16,24},{24,32},{32,40},{40,48},{48,56},{56,64},{64,7... | collective-permute-start | bytes 196616 | tf_op jit(solution)/shard_map/ppermute | solution.py:50
  74.9 7.8 %collective-permute-start.17 = (bf16[128,256]{1,0:T(8,128)(2,1)S(1)}, bf16[128,256]{1,0:T(8,128)(2,1)S(1)}, u32[]{:S(2)}, u32[]{:S(2)}) collective-permute-start(bf16[128,256]{1,0:T(8,128)(2,1)S(1)} %get-tuple-element.45.own), channel_id=1, source_target_pairs={{8,0},{16,8},{24,16},{32,24},{40,32},{48,40},{56,48},{64,56},{72,6... | collective-permute-start | bytes 196616 | tf_op jit(solution)/shard_map/ppermute | solution.py:54
  83.7 4.5 %collective-permute-start.18 = (bf16[128,256]{1,0:T(8,128)(2,1)S(1)}, bf16[128,256]{1,0:T(8,128)(2,1)S(1)}, u32[]{:S(2)}, u32[]{:S(2)}) collective-permute-start(bf16[128,256]{1,0:T(8,128)(2,1)S(1)} %get-tuple-element.47), channel_id=1, source_target_pairs={{0,2},{2,4},{4,6},{6,0},{1,3},{3,5},{5,7},{7,1},{8,10},{10,12},{12... | collective-permute-start | bytes 196616 | tf_op jit(solution)/shard_map/ppermute | solution.py:243
  84.2 5.8 %collective-permute-start.19 = (bf16[128,256]{1,0:T(8,128)(2,1)S(1)}, bf16[128,256]{1,0:T(8,128)(2,1)S(1)}, u32[]{:S(2)}, u32[]{:S(2)}) collective-permute-start(bf16[128,256]{1,0:T(8,128)(2,1)S(1)} %get-tuple-element.48), channel_id=1, source_target_pairs={{0,4},{2,6},{4,0},{6,2},{1,5},{3,7},{5,1},{7,3},{8,12},{10,14},{12... | collective-permute-start | bytes 196616 | tf_op jit(solution)/shard_map/ppermute | solution.py:245
  87.7 3.1 %collective-permute-start.20 = (bf16[128,256]{1,0:T(8,128)(2,1)S(1)}, bf16[128,256]{1,0:T(8,128)(2,1)S(1)}, u32[]{:S(2)}, u32[]{:S(2)}) collective-permute-start(bf16[128,256]{1,0:T(8,128)(2,1)S(1)} %get-tuple-element.49), channel_id=1, source_target_pairs={{0,6},{2,0},{4,2},{6,4},{1,7},{3,1},{5,3},{7,5},{8,14},{10,8},{12,... | collective-permute-start | bytes 196616 | tf_op jit(solution)/shard_map/ppermute | solution.py:244
  90.9 5.6 %collective-permute-start.21 = (f32[128,256]{1,0:T(8,128)S(1)}, f32[128,256]{1,0:T(8,128)S(1)}, u32[]{:S(2)}, u32[]{:S(2)}) collective-permute-start(f32[128,256]{1,0:T(8,128)S(1)} %shard_map.92.mine), channel_id=1, source_target_pairs={{0,1},{1,0},{2,3},{3,2},{4,5},{5,4},{6,7},{7,6},{8,9},{9,8},{10,11... | collective-permute-start | bytes 393224 | tf_op jit(solution)/shard_map/ppermute | solution.py:46
  96.4 5.1 %collective-permute-start.22 = (bf16[128,256]{1,0:T(8,128)(2,1)S(1)}, bf16[128,256]{1,0:T(8,128)(2,1)S(1)}, u32[]{:S(2)}, u32[]{:S(2)}) collective-permute-start(bf16[128,256]{1,0:T(8,128)(2,1)S(1)} %shard_map.93.x0), channel_id=1, source_target_pairs={{0,2},{2,4},{4,6},{6,0},{1,3},{3,5},{5,7},{7,1},{8,10},{10,12},{12... | collective-permute-start | bytes 196616 | tf_op jit(solution)/shard_map/ppermute | solution.py:30
  96.5 5.4 %collective-permute-start.23 = (bf16[128,256]{1,0:T(8,128)(2,1)S(1)}, bf16[128,256]{1,0:T(8,128)(2,1)S(1)}, u32[]{:S(2)}, u32[]{:S(2)}) collective-permute-start(bf16[128,256]{1,0:T(8,128)(2,1)S(1)} %shard_map.93.x0), channel_id=1, source_target_pairs={{0,4},{2,6},{4,0},{6,2},{1,5},{3,7},{5,1},{7,3},{8,12},{10,14},{12... | collective-permute-start | bytes 196616 | tf_op jit(solution)/shard_map/ppermute | solution.py:30
  99.0 3.7 %collective-permute-start.24 = (bf16[128,256]{1,0:T(8,128)(2,1)S(1)}, bf16[128,256]{1,0:T(8,128)(2,1)S(1)}, u32[]{:S(2)}, u32[]{:S(2)}) collective-permute-start(bf16[128,256]{1,0:T(8,128)(2,1)S(1)} %shard_map.93.x0), channel_id=1, source_target_pairs={{0,6},{2,0},{4,2},{6,4},{1,7},{3,1},{5,3},{7,5},{8,14},{10,8},{12,... | collective-permute-start | bytes 196616 | tf_op jit(solution)/shard_map/ppermute | solution.py:30
  103.2 5.3 %collective-permute-start.25 = (bf16[128,256]{1,0:T(8,128)(2,1)S(1)}, bf16[128,256]{1,0:T(8,128)(2,1)S(1)}, u32[]{:S(2)}, u32[]{:S(2)}) collective-permute-start(bf16[128,256]{1,0:T(8,128)(2,1)S(1)} %get-tuple-element.52.own), channel_id=1, source_target_pairs={{0,8},{8,16},{16,24},{24,32},{32,40},{40,48},{48,56},{56,64},{64,7... | collective-permute-start | bytes 196616 | tf_op jit(solution)/shard_map/ppermute | solution.py:50
  105.2 7.1 %collective-permute-start.26 = (bf16[128,256]{1,0:T(8,128)(2,1)S(1)}, bf16[128,256]{1,0:T(8,128)(2,1)S(1)}, u32[]{:S(2)}, u32[]{:S(2)}) collective-permute-start(bf16[128,256]{1,0:T(8,128)(2,1)S(1)} %get-tuple-element.52.own), channel_id=1, source_target_pairs={{8,0},{16,8},{24,16},{32,24},{40,32},{48,40},{56,48},{64,56},{72,6... | collective-permute-start | bytes 196616 | tf_op jit(solution)/shard_map/ppermute | solution.py:54
  113.2 4.4 %collective-permute-start.27 = (bf16[128,256]{1,0:T(8,128)(2,1)S(1)}, bf16[128,256]{1,0:T(8,128)(2,1)S(1)}, u32[]{:S(2)}, u32[]{:S(2)}) collective-permute-start(bf16[128,256]{1,0:T(8,128)(2,1)S(1)} %get-tuple-element.54), channel_id=1, source_target_pairs={{0,2},{2,4},{4,6},{6,0},{1,3},{3,5},{5,7},{7,1},{8,10},{10,12},{12... | collective-permute-start | bytes 196616 | tf_op jit(solution)/shard_map/ppermute | solution.py:243
  114.5 4.7 %collective-permute-start.28 = (bf16[128,256]{1,0:T(8,128)(2,1)S(1)}, bf16[128,256]{1,0:T(8,128)(2,1)S(1)}, u32[]{:S(2)}, u32[]{:S(2)}) collective-permute-start(bf16[128,256]{1,0:T(8,128)(2,1)S(1)} %get-tuple-element.55), channel_id=1, source_target_pairs={{0,4},{2,6},{4,0},{6,2},{1,5},{3,7},{5,1},{7,3},{8,12},{10,14},{12... | collective-permute-start | bytes 196616 | tf_op jit(solution)/shard_map/ppermute | solution.py:245
  120.0 5.3 %collective-permute-start.30 = (f32[128,128]{1,0:T(8,128)S(1)}, f32[128,128]{1,0:T(8,128)S(1)}, u32[]{:S(2)}, u32[]{:S(2)}) collective-permute-start(f32[128,128]{1,0:T(8,128)S(1)} %get-tuple-element.58), channel_id=1, source_target_pairs={{0,1},{1,0},{2,3},{3,2},{4,5},{5,4},{6,7},{7,6},{8,9},{9,8},{10,11... | collective-permute-start | bytes 196616 | tf_op jit(solution)/shard_map/ppermute | solution.py:46
  (8 other events, 68.1 us)

commit v9 on v8

--- a/solution.py
+++ b/solution.py
@@ -105,25 +105,19 @@
             wide[n : n + 1, at : at + WIN_COLS] = bias[n // 2, n % 2, lag_row : lag_row + 1, :]
 
 
-def line_body(p0, p1, p2, p3, many):
+def line_body(p0, p1, p2, p3, many, sems):
+    pairs = []
     for k, part in enumerate((p0, p1, p2, p3)):
-        at = behind("x", k)
-        for n in range(4):
-            many[n, at] = part[...]
-
-
-def table_body(wide, before, own, after, table):
-    own_docs = own[128:144, 0:128].astype(F32)[0:1]
-    query_docs = jnp.broadcast_to(own_docs, (128, 128)).T
-    key_docs = jnp.concatenate(
-        [before[128:144, 0:128].astype(F32)[0:1], own_docs, after[128:144, 0:128].astype(F32)[0:1]], axis=1
-    )
-    same = jnp.concatenate([query_docs] * 3, axis=1) == key_docs
+        pairs += [(part, many.at[n, behind("x", k)]) for n in range(4)]
+    fetch(pairs, sems)
+
+
+def table_body(wide, table):
     r = lax.broadcasted_iota(jnp.int32, (128, 384), 0)
     m = lax.broadcasted_iota(jnp.int32, (128, 384), 1)
     lag = (m >> 5) - (r >> 5)
     off = (m & 31) - (r & 31) + WIN_COLS // 2
-    allowed = same & (lag >= 0) & (lag < WIN_ROWS) & (off >= 0) & (off < WIN_COLS)
+    allowed = (lag >= 0) & (lag < WIN_ROWS) & (off >= 0) & (off < WIN_COLS)
     for n in range(2 * LAYERS):
         line = jnp.broadcast_to(wide[n : n + 1, :], (GRID_W, 256))
         line = pltpu.roll(line, 256 - WIN_COLS // 2, 1, stride=1, stride_axis=0)
@@ -189,8 +183,14 @@
     finish_heads(acc, q, kv)
 
 
-def attend(q, keys_values, table):
+def line_of(documents):
+    return documents[128:144, 0:128].astype(F32)[0:1]
+
+
+def attend(q, keys_values, table, documents):
     queries = q[...]
+    query_docs = jnp.broadcast_to(line_of(documents[1]), (128, 128)).T
+    same = [query_docs == line_of(d) for d in documents]
     low = lax.broadcasted_iota(jnp.int32, (128, 128), 1) < HEAD_DIM
     results = []
     for h in range(2):
@@ -199,7 +199,7 @@
         for b, (keys, _) in enumerate(keys_values):
             scores = lax.dot_general(mine, keys, NT, preferred_element_type=F32)
             scores = scores * HEAD_DIM**-0.5 + table[h, :, b * 128 : (b + 1) * 128]
-            grown = jnp.exp(scores)
+            grown = jnp.where(same[b], jnp.exp(scores), 0.0)
             weights.append(grown)
             total = total + jnp.sum(grown, axis=1, keepdims=True)
         share = 1.0 / total
@@ -211,9 +211,13 @@
     return jnp.where(low, results[0], results[1]).astype(BF16)
 
 
-def attend_scatter_body(q, before, own, after, table, weights, kept, s1, s2, s3, *, layer):
+def attend_scatter_body(
+    q, before, own, after, doc_before, doc_own, doc_after, table, weights,
+    kept, s1, s2, s3, *, layer,
+):
     parts = [(p[0:128, 0:128], p[0:128, 128:256]) for p in (before, own, after)]
-    attended = attend(q, parts, table.at[2 * layer : 2 * layer + 2])
+    table = table.at[2 * layer : 2 * layer + 2]
+    attended = attend(q, parts, table, (doc_before, doc_own, doc_after))
     for k, into in enumerate((kept, s1, s2, s3)):
         rows = weights[pl.ds(pl.multiple_of(ahead("y", k) * 256, 256), 256), 384:512]
         share = lax.dot_general(attended, rows, NT, preferred_element_type=F32)
@@ -265,13 +269,17 @@
         scratch=[pltpu.VMEM((4, 2, 64, 128), BF16), pltpu.SemaphoreType.DMA((4,))],
     )
     third_x = in_order(third, spread(third, "x"))
-    near_partner = swap(after_this(near_y, many1))
+    table = call(table_body, shaped(6, 128, 384, dtype=F32), wide)
+    near_partner = swap(after_this(near_y, (many1, table)))
 
     q, kv = call(
         heads_first_body, [shaped(128, 128), shaped(144, 256)],
         near_y, near_partner, norm_gain, documents.reshape(1, 128), weights,
     )
-    many2 = call(line_body, shaped(4, 4, 64, 512), *third_x)
+    many2 = call(
+        line_body, pltpu.HBM((4, 4, 64, 512), BF16), *third_x, out_specs=hbm,
+        scratch=[pltpu.SemaphoreType.DMA((16,))],
+    )
     for layer in range(LAYERS):
         after = from_after(kv)
         before = from_before(kv)
@@ -279,10 +287,10 @@
             many, axes = ((many1, SP), (many2, "z"))[layer]
             next_weights = gather_rows(after_this(many, kv), axes)
         if layer == 0:
-            table = call(table_body, shaped(6, 128, 384, dtype=F32), wide, before, kv, after)
+            docs = (before, kv, after)
         kept, r1, r2, r3 = scattered(
             functools.partial(attend_scatter_body, layer=layer),
-            q, before, kv, after, table, weights,
+            q, before, kv, after, *docs, table, weights,
         )
         if layer == 2:
             break

time: 127 us -> 128 us (level)
    unnamed x12 -> x18, local copies, waits for them, and re-layouts: 2 us -> 3.09 us
  transfers between devices with their start and end apart: 34 -> 34, of which waited for: 22 -> 21; matrix products, arithmetic and copies ran while one was open for 0% -> 0% of each run, Pallas kernels for 3% -> 4%
where the time goes in v9:
time: 128 us; the launch traced here: 127 us
  starting transfers between devices  77.6 us (61%)
  waiting for transfers between devices  36.2 us (28%)
  Pallas kernels  9.77 us (8%)
  local copies, waits for them, and re-layouts  3.09 us (2%)
    all_to_all x3, starting transfers between devices, gather_rows(): return lax.all_to_all(a, axes, 0, 0, tiled=True).reshape(1024, 512)  19 us
    ppermute x4, starting transfers between devices, swap(): return lax.ppermute(a, 'c', [(0, 1), (1, 0)])  15.2 us
    ppermute x12, starting transfers between devices, spread(): return [lax.ppermute(a, axis, turn(k)) for k in (1, 3, 2)]  14.3 us
    ppermute x3, waiting for transfers between devices, from_after(): return lax.ppermute(a, SP, [(i + 1, i) for i in range(15)])  11.5 us
    pallas_call x16, Pallas kernels, call(): pl.pallas_call(body, out_shape=outs, **specs, scratch_shapes=list(scratch...  9.77 us
    ppermute x3, starting transfers between devices, from_before(): return lax.ppermute(a, SP, [(i, i + 1) for i in range(15)])  9.5 us
    ppermute x3, starting transfers between devices, scattered(): r2 = lax.ppermute(s2, 'y', turn(2))  8.84 us
    ppermute x3, starting transfers between devices, from_after(): return lax.ppermute(a, SP, [(i + 1, i) for i in range(15)])  7.47 us
  transfers between devices with their start and end apart: 34, of which 21 were waited for; matrix products, arithmetic and copies ran while one was open for 0% of the time, Pallas kernels for 4%

profile of v9, /device:TPU:39, one launch (start us, length us, event | category | flops | bytes accessed | tf_op | source)
XLA Modules:
  0.0 127.0 jit_solution(12924539579855472489)
XLA Ops:
  0.0 1.9 %shard_map.84 = bf16[16,64,512]{2,1,0:T(8,128)(2,1)} custom-call(bf16[3,64,128]{2,1,0:T(8,128)(2,1)} %wq.3, bf16[3,64,128]{2,1,0:T(8,128)(2,1)} %wk.3, bf16[3,64,128]{2,1,0:T(8,128)(2,1)} %wv.3, bf16[3,64,128]{2,1,0:T(8,128)(2,1)} %bitcast.16), custom_call_target="tpu_custom_call" | custom-call | tf_op jit(solution)/shard_map/pallas_call | solution.py:66
  1.9 7.3 %all-to-all-start = ((bf16[16,64,512]{2,1,0:T(8,128)(2,1)}), bf16[16,64,512]{2,1,0:T(8,128)(2,1)S(1)}, u32[]{:S(2)}, u32[]{:S(2)}) async-start(bf16[16,64,512]{2,1,0:T(8,128)(2,1)} %shard_map.84), calls=%async_computation | async-start | bytes 2097152 | tf_op jit(solution)/shard_map/all_to_all | solution.py:38
  9.2 1.4 %collective-permute-start = (bf16[128,128]{1,0:T(8,128)(2,1)S(1)}, bf16[128,128]{1,0:T(8,128)(2,1)S(1)}, u32[]{:S(2)}, u32[]{:S(2)}) collective-permute-start(bf16[128,128]{1,0:T(8,128)(2,1)S(1)} %copy-done.8), channel_id=1, source_target_pairs={{0,2},{2,4},{4,6},{6,0},{1,3},{3,5},{5,7},{7,1},{8,10},{10,12},{12... | collective-permute-start | bytes 98312 | tf_op jit(solution)/shard_map/ppermute | solution.py:30
  10.6 2.6 %collective-permute-start.1 = (bf16[128,128]{1,0:T(8,128)(2,1)S(1)}, bf16[128,128]{1,0:T(8,128)(2,1)S(1)}, u32[]{:S(2)}, u32[]{:S(2)}) collective-permute-start(bf16[128,128]{1,0:T(8,128)(2,1)S(1)} %copy-done.8), channel_id=1, source_target_pairs={{0,4},{2,6},{4,0},{6,2},{1,5},{3,7},{5,1},{7,3},{8,12},{10,14},{12... | collective-permute-start | bytes 98312 | tf_op jit(solution)/shard_map/ppermute | solution.py:30
  17.5 2.2 %collective-permute-start.3 = (bf16[4,128,128]{2,1,0:T(8,128)(2,1)S(1)}, bf16[4,128,128]{2,1,0:T(8,128)(2,1)S(1)}, u32[]{:S(2)}, u32[]{:S(2)}) collective-permute-start(bf16[4,128,128]{2,1,0:T(8,128)(2,1)S(1)} %pad_maximum_fusion.own), channel_id=1, source_target_pairs={{0,1},{1,0},{2,3},{3,2},{4,5},{5,4},{6,7},{7,6},{8,9},{9,8},{10,11... | collective-permute-start | bytes 393224 | tf_op jit(solution)/shard_map/ppermute | solution.py:46
  22.3 7.7 %all-to-all-start.1 = ((bf16[16,64,512]{2,1,0:T(8,128)(2,1)}), bf16[16,64,512]{2,1,0:T(8,128)(2,1)S(1)}, u32[]{:S(2)}, u32[]{:S(2)}) async-start(bf16[16,64,512]{2,1,0:T(8,128)(2,1)} %copy-done), calls=%async_computation.1 | async-start | bytes 2097152 | tf_op jit(solution)/shard_map/all_to_all | solution.py:38
  30.0 3.1 %collective-permute-start.4 = (bf16[144,256]{1,0:T(8,128)(2,1)S(1)}, bf16[144,256]{1,0:T(8,128)(2,1)S(1)}, u32[]{:S(2)}, u32[]{:S(2)}) collective-permute-start(bf16[144,256]{1,0:T(8,128)(2,1)S(1)} %get-tuple-element.36.own.doc_own), channel_id=1, source_target_pairs={{0,8},{8,16},{16,24},{24,32},{32,40},{40,48},{48,56},{56,64},{64,7... | collective-permute-start | bytes 221192 | tf_op jit(solution)/shard_map/ppermute | solution.py:50
  33.1 2.2 %collective-permute-start.5 = (bf16[144,256]{1,0:T(8,128)(2,1)S(1)}, bf16[144,256]{1,0:T(8,128)(2,1)S(1)}, u32[]{:S(2)}, u32[]{:S(2)}) collective-permute-start(bf16[144,256]{1,0:T(8,128)(2,1)S(1)} %get-tuple-element.36.own.doc_own), channel_id=1, source_target_pairs={{8,0},{16,8},{24,16},{32,24},{40,32},{48,40},{56,48},{64,56},{72,6... | collective-permute-start | bytes 221192 | tf_op jit(solution)/shard_map/ppermute | solution.py:54
  35.3 2.5 %collective-permute-start.6 = (bf16[64,512]{1,0:T(8,128)(2,1)}, bf16[64,512]{1,0:T(8,128)(2,1)S(1)}, u32[]{:S(2)}, u32[]{:S(2)}) collective-permute-start(bf16[64,512]{1,0:T(8,128)(2,1)} %copy-done.2), channel_id=1, source_target_pairs={{0,8},{8,16},{16,24},{24,0},{1,9},{9,17},{17,25},{25,1},{2,10},{10... | collective-permute-start | bytes 196616 | tf_op jit(solution)/shard_map/ppermute | solution.py:30
  38.4 4.1 %collective-permute-done.4.before.doc_before = bf16[144,256]{1,0:T(8,128)(2,1)S(1)} collective-permute-done((bf16[144,256]{1,0:T(8,128)(2,1)S(1)}, bf16[144,256]{1,0:T(8,128)(2,1)S(1)}, u32[]{:S(2)}, u32[]{:S(2)}) %collective-permute-start.4) | collective-permute-done | bytes 73760 | tf_op jit(solution)/shard_map/ppermute | solution.py:50
  42.5 1.7 %collective-permute-done.5.after.doc_after = bf16[144,256]{1,0:T(8,128)(2,1)S(1)} collective-permute-done((bf16[144,256]{1,0:T(8,128)(2,1)S(1)}, bf16[144,256]{1,0:T(8,128)(2,1)S(1)}, u32[]{:S(2)}, u32[]{:S(2)}) %collective-permute-start.5) | collective-permute-done | bytes 73760 | tf_op jit(solution)/shard_map/ppermute | solution.py:54
  45.2 3.0 %collective-permute-start.10 = (bf16[128,256]{1,0:T(8,128)(2,1)S(1)}, bf16[128,256]{1,0:T(8,128)(2,1)S(1)}, u32[]{:S(2)}, u32[]{:S(2)}) collective-permute-start(bf16[128,256]{1,0:T(8,128)(2,1)S(1)} %get-tuple-element.41), channel_id=1, source_target_pairs={{0,4},{2,6},{4,0},{6,2},{1,5},{3,7},{5,1},{7,3},{8,12},{10,14},{12... | collective-permute-start | bytes 196616 | tf_op jit(solution)/shard_map/ppermute | solution.py:249
  51.3 2.5 %collective-permute-done.9.r1 = bf16[128,256]{1,0:T(8,128)(2,1)S(1)} collective-permute-done((bf16[128,256]{1,0:T(8,128)(2,1)S(1)}, bf16[128,256]{1,0:T(8,128)(2,1)S(1)}, u32[]{:S(2)}, u32[]{:S(2)}) %collective-permute-start.9) | collective-permute-done | bytes 65568 | tf_op jit(solution)/shard_map/ppermute | solution.py:247
  53.9 4.0 %collective-permute-start.12 = (f32[128,256]{1,0:T(8,128)S(1)}, f32[128,256]{1,0:T(8,128)S(1)}, u32[]{:S(2)}, u32[]{:S(2)}) collective-permute-start(f32[128,256]{1,0:T(8,128)S(1)} %shard_map.88.mine), channel_id=1, source_target_pairs={{0,1},{1,0},{2,3},{3,2},{4,5},{5,4},{6,7},{7,6},{8,9},{9,8},{10,11... | collective-permute-start | bytes 393224 | tf_op jit(solution)/shard_map/ppermute | solution.py:46
  59.9 1.8 %collective-permute-start.15 = (bf16[128,256]{1,0:T(8,128)(2,1)S(1)}, bf16[128,256]{1,0:T(8,128)(2,1)S(1)}, u32[]{:S(2)}, u32[]{:S(2)}) collective-permute-start(bf16[128,256]{1,0:T(8,128)(2,1)S(1)} %shard_map.89.x0), channel_id=1, source_target_pairs={{0,6},{2,0},{4,2},{6,4},{1,7},{3,1},{5,3},{7,5},{8,14},{10,8},{12,... | collective-permute-start | bytes 196616 | tf_op jit(solution)/shard_map/ppermute | solution.py:30
  61.7 3.6 %collective-permute-done.13.x1 = bf16[128,256]{1,0:T(8,128)(2,1)S(1)} collective-permute-done((bf16[128,256]{1,0:T(8,128)(2,1)S(1)}, bf16[128,256]{1,0:T(8,128)(2,1)S(1)}, u32[]{:S(2)}, u32[]{:S(2)}) %collective-permute-start.13) | collective-permute-done | bytes 65568 | tf_op jit(solution)/shard_map/ppermute | solution.py:30
  66.4 4.0 %all-to-all-start.2 = ((bf16[4,4,64,512]{3,2,1,0:T(8,128)(2,1)}), bf16[4,4,64,512]{3,2,1,0:T(8,128)(2,1)S(1)}, u32[]{:S(2)}, u32[]{:S(2)}) async-start(bf16[4,4,64,512]{3,2,1,0:T(8,128)(2,1)} %shard_map.87), calls=%async_computation.2 | async-start | bytes 2097152 | tf_op jit(solution)/shard_map/all_to_all | solution.py:38
  70.4 4.5 %collective-permute-start.16 = (bf16[128,256]{1,0:T(8,128)(2,1)}, bf16[128,256]{1,0:T(8,128)(2,1)S(1)}, u32[]{:S(2)}, u32[]{:S(2)}) collective-permute-start(bf16[128,256]{1,0:T(8,128)(2,1)} %copy-done.4), channel_id=1, source_target_pairs={{0,8},{8,16},{16,24},{24,32},{32,40},{40,48},{48,56},{56,64},{64,7... | collective-permute-start | bytes 196616 | tf_op jit(solution)/shard_map/ppermute | solution.py:50
  74.9 1.9 %collective-permute-start.17 = (bf16[128,256]{1,0:T(8,128)(2,1)}, bf16[128,256]{1,0:T(8,128)(2,1)S(1)}, u32[]{:S(2)}, u32[]{:S(2)}) collective-permute-start(bf16[128,256]{1,0:T(8,128)(2,1)} %copy-done.4), channel_id=1, source_target_pairs={{8,0},{16,8},{24,16},{32,24},{40,32},{48,40},{56,48},{64,56},{72,6... | collective-permute-start | bytes 196616 | tf_op jit(solution)/shard_map/ppermute | solution.py:54
  76.8 6.1 %collective-permute-done.17.after = bf16[128,256]{1,0:T(8,128)(2,1)S(1)} collective-permute-done((bf16[128,256]{1,0:T(8,128)(2,1)}, bf16[128,256]{1,0:T(8,128)(2,1)S(1)}, u32[]{:S(2)}, u32[]{:S(2)}) %collective-permute-start.17) | collective-permute-done | bytes 65568 | tf_op jit(solution)/shard_map/ppermute | solution.py:54
  85.3 3.4 %collective-permute-start.19 = (bf16[128,256]{1,0:T(8,128)(2,1)S(1)}, bf16[128,256]{1,0:T(8,128)(2,1)S(1)}, u32[]{:S(2)}, u32[]{:S(2)}) collective-permute-start(bf16[128,256]{1,0:T(8,128)(2,1)S(1)} %get-tuple-element.48), channel_id=1, source_target_pairs={{0,4},{2,6},{4,0},{6,2},{1,5},{3,7},{5,1},{7,3},{8,12},{10,14},{12... | collective-permute-start | bytes 196616 | tf_op jit(solution)/shard_map/ppermute | solution.py:249
  89.2 1.9 %collective-permute-done.19.r2 = bf16[128,256]{1,0:T(8,128)(2,1)S(1)} collective-permute-done((bf16[128,256]{1,0:T(8,128)(2,1)S(1)}, bf16[128,256]{1,0:T(8,128)(2,1)S(1)}, u32[]{:S(2)}, u32[]{:S(2)}) %collective-permute-start.19) | collective-permute-done | bytes 65568 | tf_op jit(solution)/shard_map/ppermute | solution.py:249
  91.9 4.6 %collective-permute-start.21 = (f32[128,256]{1,0:T(8,128)S(1)}, f32[128,256]{1,0:T(8,128)S(1)}, u32[]{:S(2)}, u32[]{:S(2)}) collective-permute-start(f32[128,256]{1,0:T(8,128)S(1)} %shard_map.92.mine), channel_id=1, source_target_pairs={{0,1},{1,0},{2,3},{3,2},{4,5},{5,4},{6,7},{7,6},{8,9},{9,8},{10,11... | collective-permute-start | bytes 393224 | tf_op jit(solution)/shard_map/ppermute | solution.py:46
  97.5 2.5 %collective-permute-start.23 = (bf16[128,256]{1,0:T(8,128)(2,1)S(1)}, bf16[128,256]{1,0:T(8,128)(2,1)S(1)}, u32[]{:S(2)}, u32[]{:S(2)}) collective-permute-start(bf16[128,256]{1,0:T(8,128)(2,1)S(1)} %shard_map.93.x0), channel_id=1, source_target_pairs={{0,4},{2,6},{4,0},{6,2},{1,5},{3,7},{5,1},{7,3},{8,12},{10,14},{12... | collective-permute-start | bytes 196616 | tf_op jit(solution)/shard_map/ppermute | solution.py:30
  100.8 1.8 %collective-permute-done.22.x1 = bf16[128,256]{1,0:T(8,128)(2,1)S(1)} collective-permute-done((bf16[128,256]{1,0:T(8,128)(2,1)S(1)}, bf16[128,256]{1,0:T(8,128)(2,1)S(1)}, u32[]{:S(2)}, u32[]{:S(2)}) %collective-permute-start.22) | collective-permute-done | bytes 65568 | tf_op jit(solution)/shard_map/ppermute | solution.py:30
  104.3 1.9 %collective-permute-start.25 = (bf16[128,256]{1,0:T(8,128)(2,1)S(1)}, bf16[128,256]{1,0:T(8,128)(2,1)S(1)}, u32[]{:S(2)}, u32[]{:S(2)}) collective-permute-start(bf16[128,256]{1,0:T(8,128)(2,1)S(1)} %get-tuple-element.52.own), channel_id=1, source_target_pairs={{0,8},{8,16},{16,24},{24,32},{32,40},{40,48},{48,56},{56,64},{64,7... | collective-permute-start | bytes 196616 | tf_op jit(solution)/shard_map/ppermute | solution.py:50
  106.2 3.4 %collective-permute-start.26 = (bf16[128,256]{1,0:T(8,128)(2,1)S(1)}, bf16[128,256]{1,0:T(8,128)(2,1)S(1)}, u32[]{:S(2)}, u32[]{:S(2)}) collective-permute-start(bf16[128,256]{1,0:T(8,128)(2,1)S(1)} %get-tuple-element.52.own), channel_id=1, source_target_pairs={{8,0},{16,8},{24,16},{32,24},{40,32},{48,40},{56,48},{64,56},{72,6... | collective-permute-start | bytes 196616 | tf_op jit(solution)/shard_map/ppermute | solution.py:54
  109.6 3.7 %collective-permute-done.26.after = bf16[128,256]{1,0:T(8,128)(2,1)S(1)} collective-permute-done((bf16[128,256]{1,0:T(8,128)(2,1)S(1)}, bf16[128,256]{1,0:T(8,128)(2,1)S(1)}, u32[]{:S(2)}, u32[]{:S(2)}) %collective-permute-start.26) | collective-permute-done | bytes 65568 | tf_op jit(solution)/shard_map/ppermute | solution.py:54
  114.3 1.2 collective-permute-start.27
  115.5 2.4 %collective-permute-start.28 = (bf16[128,256]{1,0:T(8,128)(2,1)S(1)}, bf16[128,256]{1,0:T(8,128)(2,1)S(1)}, u32[]{:S(2)}, u32[]{:S(2)}) collective-permute-start(bf16[128,256]{1,0:T(8,128)(2,1)S(1)} %get-tuple-element.55), channel_id=1, source_target_pairs={{0,4},{2,6},{4,0},{6,2},{1,5},{3,7},{5,1},{7,3},{8,12},{10,14},{12... | collective-permute-start | bytes 196616 | tf_op jit(solution)/shard_map/ppermute | solution.py:249
  118.7 1.6 %collective-permute-done.28.r2 = bf16[128,256]{1,0:T(8,128)(2,1)S(1)} collective-permute-done((bf16[128,256]{1,0:T(8,128)(2,1)S(1)}, bf16[128,256]{1,0:T(8,128)(2,1)S(1)}, u32[]{:S(2)}, u32[]{:S(2)}) %collective-permute-start.28) | collective-permute-done | bytes 65568 | tf_op jit(solution)/shard_map/ppermute | solution.py:249
  121.1 4.4 %collective-permute-start.30 = (f32[128,128]{1,0:T(8,128)S(1)}, f32[128,128]{1,0:T(8,128)S(1)}, u32[]{:S(2)}, u32[]{:S(2)}) collective-permute-start(f32[128,128]{1,0:T(8,128)S(1)} %get-tuple-element.58), channel_id=1, source_target_pairs={{0,1},{1,0},{2,3},{3,2},{4,5},{5,4},{6,7},{7,6},{8,9},{9,8},{10,11... | collective-permute-start | bytes 196616 | tf_op jit(solution)/shard_map/ppermute | solution.py:46
  (71 shorter events, 26.0 us)
Async XLA Ops:
  1.9 19.8 %all-to-all-start = ((bf16[16,64,512]{2,1,0:T(8,128)(2,1)}), bf16[16,64,512]{2,1,0:T(8,128)(2,1)S(1)}, u32[]{:S(2)}, u32[]{:S(2)}) async-start(bf16[16,64,512]{2,1,0:T(8,128)(2,1)} %shard_map.84), calls=%async_computation | async-start | bytes 2097152 | tf_op jit(solution)/shard_map/all_to_all | solution.py:38
  9.2 8.2 %collective-permute-start = (bf16[128,128]{1,0:T(8,128)(2,1)S(1)}, bf16[128,128]{1,0:T(8,128)(2,1)S(1)}, u32[]{:S(2)}, u32[]{:S(2)}) collective-permute-start(bf16[128,128]{1,0:T(8,128)(2,1)S(1)} %copy-done.8), channel_id=1, source_target_pairs={{0,2},{2,4},{4,6},{6,0},{1,3},{3,5},{5,7},{7,1},{8,10},{10,12},{12... | collective-permute-start | bytes 98312 | tf_op jit(solution)/shard_map/ppermute | solution.py:30
  10.6 6.8 %collective-permute-start.1 = (bf16[128,128]{1,0:T(8,128)(2,1)S(1)}, bf16[128,128]{1,0:T(8,128)(2,1)S(1)}, u32[]{:S(2)}, u32[]{:S(2)}) collective-permute-start(bf16[128,128]{1,0:T(8,128)(2,1)S(1)} %copy-done.8), channel_id=1, source_target_pairs={{0,4},{2,6},{4,0},{6,2},{1,5},{3,7},{5,1},{7,3},{8,12},{10,14},{12... | collective-permute-start | bytes 98312 | tf_op jit(solution)/shard_map/ppermute | solution.py:30
  13.2 4.2 %collective-permute-start.2 = (bf16[128,128]{1,0:T(8,128)(2,1)S(1)}, bf16[128,128]{1,0:T(8,128)(2,1)S(1)}, u32[]{:S(2)}, u32[]{:S(2)}) collective-permute-start(bf16[128,128]{1,0:T(8,128)(2,1)S(1)} %copy-done.8), channel_id=1, source_target_pairs={{0,6},{2,0},{4,2},{6,4},{1,7},{3,1},{5,3},{7,5},{8,14},{10,8},{12,... | collective-permute-start | bytes 98312 | tf_op jit(solution)/shard_map/ppermute | solution.py:30
  17.5 3.1 %collective-permute-start.3 = (bf16[4,128,128]{2,1,0:T(8,128)(2,1)S(1)}, bf16[4,128,128]{2,1,0:T(8,128)(2,1)S(1)}, u32[]{:S(2)}, u32[]{:S(2)}) collective-permute-start(bf16[4,128,128]{2,1,0:T(8,128)(2,1)S(1)} %pad_maximum_fusion.own), channel_id=1, source_target_pairs={{0,1},{1,0},{2,3},{3,2},{4,5},{5,4},{6,7},{7,6},{8,9},{9,8},{10,11... | collective-permute-start | bytes 393224 | tf_op jit(solution)/shard_map/ppermute | solution.py:46
  22.3 42.9 %all-to-all-start.1 = ((bf16[16,64,512]{2,1,0:T(8,128)(2,1)}), bf16[16,64,512]{2,1,0:T(8,128)(2,1)S(1)}, u32[]{:S(2)}, u32[]{:S(2)}) async-start(bf16[16,64,512]{2,1,0:T(8,128)(2,1)} %copy-done), calls=%async_computation.1 | async-start | bytes 2097152 | tf_op jit(solution)/shard_map/all_to_all | solution.py:38
  30.0 12.5 %collective-permute-start.4 = (bf16[144,256]{1,0:T(8,128)(2,1)S(1)}, bf16[144,256]{1,0:T(8,128)(2,1)S(1)}, u32[]{:S(2)}, u32[]{:S(2)}) collective-permute-start(bf16[144,256]{1,0:T(8,128)(2,1)S(1)} %get-tuple-element.36.own.doc_own), channel_id=1, source_target_pairs={{0,8},{8,16},{16,24},{24,32},{32,40},{40,48},{48,56},{56,64},{64,7... | collective-permute-start | bytes 221192 | tf_op jit(solution)/shard_map/ppermute | solution.py:50
  33.1 11.1 %collective-permute-start.5 = (bf16[144,256]{1,0:T(8,128)(2,1)S(1)}, bf16[144,256]{1,0:T(8,128)(2,1)S(1)}, u32[]{:S(2)}, u32[]{:S(2)}) collective-permute-start(bf16[144,256]{1,0:T(8,128)(2,1)S(1)} %get-tuple-element.36.own.doc_own), channel_id=1, source_target_pairs={{8,0},{16,8},{24,16},{32,24},{40,32},{48,40},{56,48},{64,56},{72,6... | collective-permute-start | bytes 221192 | tf_op jit(solution)/shard_map/ppermute | solution.py:54
  35.3 13.6 %collective-permute-start.6 = (bf16[64,512]{1,0:T(8,128)(2,1)}, bf16[64,512]{1,0:T(8,128)(2,1)S(1)}, u32[]{:S(2)}, u32[]{:S(2)}) collective-permute-start(bf16[64,512]{1,0:T(8,128)(2,1)} %copy-done.2), channel_id=1, source_target_pairs={{0,8},{8,16},{16,24},{24,0},{1,9},{9,17},{17,25},{25,1},{2,10},{10... | collective-permute-start | bytes 196616 | tf_op jit(solution)/shard_map/ppermute | solution.py:30
  37.8 11.9 %collective-permute-start.7 = (bf16[64,512]{1,0:T(8,128)(2,1)}, bf16[64,512]{1,0:T(8,128)(2,1)S(1)}, u32[]{:S(2)}, u32[]{:S(2)}) collective-permute-start(bf16[64,512]{1,0:T(8,128)(2,1)} %copy-done.2), channel_id=1, source_target_pairs={{0,16},{8,24},{16,0},{24,8},{1,17},{9,25},{17,1},{25,9},{2,18},{10... | collective-permute-start | bytes 196616 | tf_op jit(solution)/shard_map/ppermute | solution.py:30
  37.8 11.9 %collective-permute-start.8 = (bf16[64,512]{1,0:T(8,128)(2,1)}, bf16[64,512]{1,0:T(8,128)(2,1)S(1)}, u32[]{:S(2)}, u32[]{:S(2)}) collective-permute-start(bf16[64,512]{1,0:T(8,128)(2,1)} %copy-done.2), channel_id=1, source_target_pairs={{0,24},{8,0},{16,8},{24,16},{1,25},{9,1},{17,9},{25,17},{2,26},{10... | collective-permute-start | bytes 196616 | tf_op jit(solution)/shard_map/ppermute | solution.py:30
  45.2 5.6 %collective-permute-start.10 = (bf16[128,256]{1,0:T(8,128)(2,1)S(1)}, bf16[128,256]{1,0:T(8,128)(2,1)S(1)}, u32[]{:S(2)}, u32[]{:S(2)}) collective-permute-start(bf16[128,256]{1,0:T(8,128)(2,1)S(1)} %get-tuple-element.41), channel_id=1, source_target_pairs={{0,4},{2,6},{4,0},{6,2},{1,5},{3,7},{5,1},{7,3},{8,12},{10,14},{12... | collective-permute-start | bytes 196616 | tf_op jit(solution)/shard_map/ppermute | solution.py:249
  49.0 4.9 %collective-permute-start.9 = (bf16[128,256]{1,0:T(8,128)(2,1)S(1)}, bf16[128,256]{1,0:T(8,128)(2,1)S(1)}, u32[]{:S(2)}, u32[]{:S(2)}) collective-permute-start(bf16[128,256]{1,0:T(8,128)(2,1)S(1)} %get-tuple-element.40), channel_id=1, source_target_pairs={{0,2},{2,4},{4,6},{6,0},{1,3},{3,5},{5,7},{7,1},{8,10},{10,12},{12... | collective-permute-start | bytes 196616 | tf_op jit(solution)/shard_map/ppermute | solution.py:247
  53.9 5.0 %collective-permute-start.12 = (f32[128,256]{1,0:T(8,128)S(1)}, f32[128,256]{1,0:T(8,128)S(1)}, u32[]{:S(2)}, u32[]{:S(2)}) collective-permute-start(f32[128,256]{1,0:T(8,128)S(1)} %shard_map.88.mine), channel_id=1, source_target_pairs={{0,1},{1,0},{2,3},{3,2},{4,5},{5,4},{6,7},{7,6},{8,9},{9,8},{10,11... | collective-permute-start | bytes 393224 | tf_op jit(solution)/shard_map/ppermute | solution.py:46
  58.9 6.3 %collective-permute-start.13 = (bf16[128,256]{1,0:T(8,128)(2,1)S(1)}, bf16[128,256]{1,0:T(8,128)(2,1)S(1)}, u32[]{:S(2)}, u32[]{:S(2)}) collective-permute-start(bf16[128,256]{1,0:T(8,128)(2,1)S(1)} %shard_map.89.x0), channel_id=1, source_target_pairs={{0,2},{2,4},{4,6},{6,0},{1,3},{3,5},{5,7},{7,1},{8,10},{10,12},{12... | collective-permute-start | bytes 196616 | tf_op jit(solution)/shard_map/ppermute | solution.py:30
  59.0 6.2 %collective-permute-start.14 = (bf16[128,256]{1,0:T(8,128)(2,1)S(1)}, bf16[128,256]{1,0:T(8,128)(2,1)S(1)}, u32[]{:S(2)}, u32[]{:S(2)}) collective-permute-start(bf16[128,256]{1,0:T(8,128)(2,1)S(1)} %shard_map.89.x0), channel_id=1, source_target_pairs={{0,4},{2,6},{4,0},{6,2},{1,5},{3,7},{5,1},{7,3},{8,12},{10,14},{12... | collective-permute-start | bytes 196616 | tf_op jit(solution)/shard_map/ppermute | solution.py:30
  59.9 5.3 %collective-permute-start.15 = (bf16[128,256]{1,0:T(8,128)(2,1)S(1)}, bf16[128,256]{1,0:T(8,128)(2,1)S(1)}, u32[]{:S(2)}, u32[]{:S(2)}) collective-permute-start(bf16[128,256]{1,0:T(8,128)(2,1)S(1)} %shard_map.89.x0), channel_id=1, source_target_pairs={{0,6},{2,0},{4,2},{6,4},{1,7},{3,1},{5,3},{7,5},{8,14},{10,8},{12,... | collective-permute-start | bytes 196616 | tf_op jit(solution)/shard_map/ppermute | solution.py:30
  66.4 37.4 %all-to-all-start.2 = ((bf16[4,4,64,512]{3,2,1,0:T(8,128)(2,1)}), bf16[4,4,64,512]{3,2,1,0:T(8,128)(2,1)S(1)}, u32[]{:S(2)}, u32[]{:S(2)}) async-start(bf16[4,4,64,512]{3,2,1,0:T(8,128)(2,1)} %shard_map.87), calls=%async_computation.2 | async-start | bytes 2097152 | tf_op jit(solution)/shard_map/all_to_all | solution.py:38
  70.4 6.4 %collective-permute-start.16 = (bf16[128,256]{1,0:T(8,128)(2,1)}, bf16[128,256]{1,0:T(8,128)(2,1)S(1)}, u32[]{:S(2)}, u32[]{:S(2)}) collective-permute-start(bf16[128,256]{1,0:T(8,128)(2,1)} %copy-done.4), channel_id=1, source_target_pairs={{0,8},{8,16},{16,24},{24,32},{32,40},{40,48},{48,56},{56,64},{64,7... | collective-permute-start | bytes 196616 | tf_op jit(solution)/shard_map/ppermute | solution.py:50
  74.9 8.0 %collective-permute-start.17 = (bf16[128,256]{1,0:T(8,128)(2,1)}, bf16[128,256]{1,0:T(8,128)(2,1)S(1)}, u32[]{:S(2)}, u32[]{:S(2)}) collective-permute-start(bf16[128,256]{1,0:T(8,128)(2,1)} %copy-done.4), channel_id=1, source_target_pairs={{8,0},{16,8},{24,16},{32,24},{40,32},{48,40},{56,48},{64,56},{72,6... | collective-permute-start | bytes 196616 | tf_op jit(solution)/shard_map/ppermute | solution.py:54
  84.7 4.5 %collective-permute-start.18 = (bf16[128,256]{1,0:T(8,128)(2,1)S(1)}, bf16[128,256]{1,0:T(8,128)(2,1)S(1)}, u32[]{:S(2)}, u32[]{:S(2)}) collective-permute-start(bf16[128,256]{1,0:T(8,128)(2,1)S(1)} %get-tuple-element.47), channel_id=1, source_target_pairs={{0,2},{2,4},{4,6},{6,0},{1,3},{3,5},{5,7},{7,1},{8,10},{10,12},{12... | collective-permute-start | bytes 196616 | tf_op jit(solution)/shard_map/ppermute | solution.py:247
  85.3 5.8 %collective-permute-start.19 = (bf16[128,256]{1,0:T(8,128)(2,1)S(1)}, bf16[128,256]{1,0:T(8,128)(2,1)S(1)}, u32[]{:S(2)}, u32[]{:S(2)}) collective-permute-start(bf16[128,256]{1,0:T(8,128)(2,1)S(1)} %get-tuple-element.48), channel_id=1, source_target_pairs={{0,4},{2,6},{4,0},{6,2},{1,5},{3,7},{5,1},{7,3},{8,12},{10,14},{12... | collective-permute-start | bytes 196616 | tf_op jit(solution)/shard_map/ppermute | solution.py:249
  88.7 3.1 %collective-permute-start.20 = (bf16[128,256]{1,0:T(8,128)(2,1)S(1)}, bf16[128,256]{1,0:T(8,128)(2,1)S(1)}, u32[]{:S(2)}, u32[]{:S(2)}) collective-permute-start(bf16[128,256]{1,0:T(8,128)(2,1)S(1)} %get-tuple-element.49), channel_id=1, source_target_pairs={{0,6},{2,0},{4,2},{6,4},{1,7},{3,1},{5,3},{7,5},{8,14},{10,8},{12,... | collective-permute-start | bytes 196616 | tf_op jit(solution)/shard_map/ppermute | solution.py:248
  91.9 5.6 %collective-permute-start.21 = (f32[128,256]{1,0:T(8,128)S(1)}, f32[128,256]{1,0:T(8,128)S(1)}, u32[]{:S(2)}, u32[]{:S(2)}) collective-permute-start(f32[128,256]{1,0:T(8,128)S(1)} %shard_map.92.mine), channel_id=1, source_target_pairs={{0,1},{1,0},{2,3},{3,2},{4,5},{5,4},{6,7},{7,6},{8,9},{9,8},{10,11... | collective-permute-start | bytes 393224 | tf_op jit(solution)/shard_map/ppermute | solution.py:46
  97.4 5.1 %collective-permute-start.22 = (bf16[128,256]{1,0:T(8,128)(2,1)S(1)}, bf16[128,256]{1,0:T(8,128)(2,1)S(1)}, u32[]{:S(2)}, u32[]{:S(2)}) collective-permute-start(bf16[128,256]{1,0:T(8,128)(2,1)S(1)} %shard_map.93.x0), channel_id=1, source_target_pairs={{0,2},{2,4},{4,6},{6,0},{1,3},{3,5},{5,7},{7,1},{8,10},{10,12},{12... | collective-permute-start | bytes 196616 | tf_op jit(solution)/shard_map/ppermute | solution.py:30
  97.5 5.4 %collective-permute-start.23 = (bf16[128,256]{1,0:T(8,128)(2,1)S(1)}, bf16[128,256]{1,0:T(8,128)(2,1)S(1)}, u32[]{:S(2)}, u32[]{:S(2)}) collective-permute-start(bf16[128,256]{1,0:T(8,128)(2,1)S(1)} %shard_map.93.x0), channel_id=1, source_target_pairs={{0,4},{2,6},{4,0},{6,2},{1,5},{3,7},{5,1},{7,3},{8,12},{10,14},{12... | collective-permute-start | bytes 196616 | tf_op jit(solution)/shard_map/ppermute | solution.py:30
  100.0 3.7 %collective-permute-start.24 = (bf16[128,256]{1,0:T(8,128)(2,1)S(1)}, bf16[128,256]{1,0:T(8,128)(2,1)S(1)}, u32[]{:S(2)}, u32[]{:S(2)}) collective-permute-start(bf16[128,256]{1,0:T(8,128)(2,1)S(1)} %shard_map.93.x0), channel_id=1, source_target_pairs={{0,6},{2,0},{4,2},{6,4},{1,7},{3,1},{5,3},{7,5},{8,14},{10,8},{12,... | collective-permute-start | bytes 196616 | tf_op jit(solution)/shard_map/ppermute | solution.py:30
  104.3 5.3 %collective-permute-start.25 = (bf16[128,256]{1,0:T(8,128)(2,1)S(1)}, bf16[128,256]{1,0:T(8,128)(2,1)S(1)}, u32[]{:S(2)}, u32[]{:S(2)}) collective-permute-start(bf16[128,256]{1,0:T(8,128)(2,1)S(1)} %get-tuple-element.52.own), channel_id=1, source_target_pairs={{0,8},{8,16},{16,24},{24,32},{32,40},{40,48},{48,56},{56,64},{64,7... | collective-permute-start | bytes 196616 | tf_op jit(solution)/shard_map/ppermute | solution.py:50
  106.2 7.1 %collective-permute-start.26 = (bf16[128,256]{1,0:T(8,128)(2,1)S(1)}, bf16[128,256]{1,0:T(8,128)(2,1)S(1)}, u32[]{:S(2)}, u32[]{:S(2)}) collective-permute-start(bf16[128,256]{1,0:T(8,128)(2,1)S(1)} %get-tuple-element.52.own), channel_id=1, source_target_pairs={{8,0},{16,8},{24,16},{32,24},{40,32},{48,40},{56,48},{64,56},{72,6... | collective-permute-start | bytes 196616 | tf_op jit(solution)/shard_map/ppermute | solution.py:54
  114.3 4.4 %collective-permute-start.27 = (bf16[128,256]{1,0:T(8,128)(2,1)S(1)}, bf16[128,256]{1,0:T(8,128)(2,1)S(1)}, u32[]{:S(2)}, u32[]{:S(2)}) collective-permute-start(bf16[128,256]{1,0:T(8,128)(2,1)S(1)} %get-tuple-element.54), channel_id=1, source_target_pairs={{0,2},{2,4},{4,6},{6,0},{1,3},{3,5},{5,7},{7,1},{8,10},{10,12},{12... | collective-permute-start | bytes 196616 | tf_op jit(solution)/shard_map/ppermute | solution.py:247
  115.5 4.7 %collective-permute-start.28 = (bf16[128,256]{1,0:T(8,128)(2,1)S(1)}, bf16[128,256]{1,0:T(8,128)(2,1)S(1)}, u32[]{:S(2)}, u32[]{:S(2)}) collective-permute-start(bf16[128,256]{1,0:T(8,128)(2,1)S(1)} %get-tuple-element.55), channel_id=1, source_target_pairs={{0,4},{2,6},{4,0},{6,2},{1,5},{3,7},{5,1},{7,3},{8,12},{10,14},{12... | collective-permute-start | bytes 196616 | tf_op jit(solution)/shard_map/ppermute | solution.py:249
  121.1 5.3 %collective-permute-start.30 = (f32[128,128]{1,0:T(8,128)S(1)}, f32[128,128]{1,0:T(8,128)S(1)}, u32[]{:S(2)}, u32[]{:S(2)}) collective-permute-start(f32[128,128]{1,0:T(8,128)S(1)} %get-tuple-element.58), channel_id=1, source_target_pairs={{0,1},{1,0},{2,3},{3,2},{4,5},{5,4},{6,7},{7,6},{8,9},{9,8},{10,11... | collective-permute-start | bytes 196616 | tf_op jit(solution)/shard_map/ppermute | solution.py:46
  (11 other events, 59.5 us)

commit v10 on v9

--- a/solution.py
+++ b/solution.py
@@ -105,11 +105,11 @@
             wide[n : n + 1, at : at + WIN_COLS] = bias[n // 2, n % 2, lag_row : lag_row + 1, :]
 
 
-def line_body(p0, p1, p2, p3, many, sems):
-    pairs = []
+def line_body(p0, p1, p2, p3, many):
     for k, part in enumerate((p0, p1, p2, p3)):
-        pairs += [(part, many.at[n, behind("x", k)]) for n in range(4)]
-    fetch(pairs, sems)
+        at = behind("x", k)
+        for n in range(4):
+            many[n, at] = part[...]
 
 
 def table_body(wide, table):
@@ -276,10 +276,7 @@
         heads_first_body, [shaped(128, 128), shaped(144, 256)],
         near_y, near_partner, norm_gain, documents.reshape(1, 128), weights,
     )
-    many2 = call(
-        line_body, pltpu.HBM((4, 4, 64, 512), BF16), *third_x, out_specs=hbm,
-        scratch=[pltpu.SemaphoreType.DMA((16,))],
-    )
+    many2 = call(line_body, shaped(4, 4, 64, 512), *third_x)
     for layer in range(LAYERS):
         after = from_after(kv)
         before = from_before(kv)

time: 128 us -> 128 us (level)
    unnamed x18 -> x20, local copies, waits for them, and re-layouts: 3.09 us -> 4.06 us
  transfers between devices with their start and end apart: 34 -> 34, of which waited for: 21 -> 21; matrix products, arithmetic and copies ran while one was open for 0% -> 0% of each run, Pallas kernels for 4% -> 3%
where the time goes in v10:
time: 128 us; the launch traced here: 127 us
  starting transfers between devices  77.6 us (61%)
  waiting for transfers between devices  36.3 us (28%)
  Pallas kernels  8.71 us (7%)
  local copies, waits for them, and re-layouts  4.06 us (3%)
    all_to_all x3, starting transfers between devices, gather_rows(): return lax.all_to_all(a, axes, 0, 0, tiled=True).reshape(1024, 512)  19 us
    ppermute x4, starting transfers between devices, swap(): return lax.ppermute(a, 'c', [(0, 1), (1, 0)])  15.2 us
    ppermute x12, starting transfers between devices, spread(): return [lax.ppermute(a, axis, turn(k)) for k in (1, 3, 2)]  14.3 us
    ppermute x3, waiting for transfers between devices, from_after(): return lax.ppermute(a, SP, [(i + 1, i) for i in range(15)])  11.5 us
    ppermute x3, starting transfers between devices, from_before(): return lax.ppermute(a, SP, [(i, i + 1) for i in range(15)])  9.49 us
    ppermute x3, starting transfers between devices, scattered(): r2 = lax.ppermute(s2, 'y', turn(2))  8.81 us
    pallas_call x16, Pallas kernels, call(): pl.pallas_call(body, out_shape=outs, **specs, scratch_shapes=list(scratch...  8.71 us
    ppermute x3, starting transfers between devices, from_after(): return lax.ppermute(a, SP, [(i + 1, i) for i in range(15)])  7.47 us
  transfers between devices with their start and end apart: 34, of which 21 were waited for; matrix products, arithmetic and copies ran while one was open for 0% of the time, Pallas kernels for 3%

profile of v10, /device:TPU:39, one launch (start us, length us, event | category | flops | bytes accessed | tf_op | source)
XLA Modules:
  0.0 127.0 jit_solution(10543470205366565848)
XLA Ops:
  0.0 1.9 %shard_map.84 = bf16[16,64,512]{2,1,0:T(8,128)(2,1)} custom-call(bf16[3,64,128]{2,1,0:T(8,128)(2,1)} %wq.3, bf16[3,64,128]{2,1,0:T(8,128)(2,1)} %wk.3, bf16[3,64,128]{2,1,0:T(8,128)(2,1)} %wv.3, bf16[3,64,128]{2,1,0:T(8,128)(2,1)} %bitcast.16), custom_call_target="tpu_custom_call" | custom-call | tf_op jit(solution)/shard_map/pallas_call | solution.py:66
  1.9 7.3 %all-to-all-start = ((bf16[16,64,512]{2,1,0:T(8,128)(2,1)}), bf16[16,64,512]{2,1,0:T(8,128)(2,1)S(1)}, u32[]{:S(2)}, u32[]{:S(2)}) async-start(bf16[16,64,512]{2,1,0:T(8,128)(2,1)} %shard_map.84), calls=%async_computation | async-start | bytes 2097152 | tf_op jit(solution)/shard_map/all_to_all | solution.py:38
  9.2 1.4 %collective-permute-start = (bf16[128,128]{1,0:T(8,128)(2,1)S(1)}, bf16[128,128]{1,0:T(8,128)(2,1)S(1)}, u32[]{:S(2)}, u32[]{:S(2)}) collective-permute-start(bf16[128,128]{1,0:T(8,128)(2,1)S(1)} %copy-done.9), channel_id=1, source_target_pairs={{0,2},{2,4},{4,6},{6,0},{1,3},{3,5},{5,7},{7,1},{8,10},{10,12},{12... | collective-permute-start | bytes 98312 | tf_op jit(solution)/shard_map/ppermute | solution.py:30
  10.6 2.6 %collective-permute-start.1 = (bf16[128,128]{1,0:T(8,128)(2,1)S(1)}, bf16[128,128]{1,0:T(8,128)(2,1)S(1)}, u32[]{:S(2)}, u32[]{:S(2)}) collective-permute-start(bf16[128,128]{1,0:T(8,128)(2,1)S(1)} %copy-done.9), channel_id=1, source_target_pairs={{0,4},{2,6},{4,0},{6,2},{1,5},{3,7},{5,1},{7,3},{8,12},{10,14},{12... | collective-permute-start | bytes 98312 | tf_op jit(solution)/shard_map/ppermute | solution.py:30
  17.5 2.2 %collective-permute-start.3 = (bf16[4,128,128]{2,1,0:T(8,128)(2,1)S(1)}, bf16[4,128,128]{2,1,0:T(8,128)(2,1)S(1)}, u32[]{:S(2)}, u32[]{:S(2)}) collective-permute-start(bf16[4,128,128]{2,1,0:T(8,128)(2,1)S(1)} %pad_maximum_fusion.own), channel_id=1, source_target_pairs={{0,1},{1,0},{2,3},{3,2},{4,5},{5,4},{6,7},{7,6},{8,9},{9,8},{10,11... | collective-permute-start | bytes 393224 | tf_op jit(solution)/shard_map/ppermute | solution.py:46
  22.3 7.7 %all-to-all-start.1 = ((bf16[16,64,512]{2,1,0:T(8,128)(2,1)}), bf16[16,64,512]{2,1,0:T(8,128)(2,1)S(1)}, u32[]{:S(2)}, u32[]{:S(2)}) async-start(bf16[16,64,512]{2,1,0:T(8,128)(2,1)} %copy-done.1), calls=%async_computation.1 | async-start | bytes 2097152 | tf_op jit(solution)/shard_map/all_to_all | solution.py:38
  30.0 3.1 %collective-permute-start.4 = (bf16[144,256]{1,0:T(8,128)(2,1)S(1)}, bf16[144,256]{1,0:T(8,128)(2,1)S(1)}, u32[]{:S(2)}, u32[]{:S(2)}) collective-permute-start(bf16[144,256]{1,0:T(8,128)(2,1)S(1)} %get-tuple-element.36.own.doc_own), channel_id=1, source_target_pairs={{0,8},{8,16},{16,24},{24,32},{32,40},{40,48},{48,56},{56,64},{64,7... | collective-permute-start | bytes 221192 | tf_op jit(solution)/shard_map/ppermute | solution.py:50
  33.1 2.2 %collective-permute-start.5 = (bf16[144,256]{1,0:T(8,128)(2,1)S(1)}, bf16[144,256]{1,0:T(8,128)(2,1)S(1)}, u32[]{:S(2)}, u32[]{:S(2)}) collective-permute-start(bf16[144,256]{1,0:T(8,128)(2,1)S(1)} %get-tuple-element.36.own.doc_own), channel_id=1, source_target_pairs={{8,0},{16,8},{24,16},{32,24},{40,32},{48,40},{56,48},{64,56},{72,6... | collective-permute-start | bytes 221192 | tf_op jit(solution)/shard_map/ppermute | solution.py:54
  35.3 2.5 %collective-permute-start.6 = (bf16[64,512]{1,0:T(8,128)(2,1)}, bf16[64,512]{1,0:T(8,128)(2,1)S(1)}, u32[]{:S(2)}, u32[]{:S(2)}) collective-permute-start(bf16[64,512]{1,0:T(8,128)(2,1)} %copy-done.3), channel_id=1, source_target_pairs={{0,8},{8,16},{16,24},{24,0},{1,9},{9,17},{17,25},{25,1},{2,10},{10... | collective-permute-start | bytes 196616 | tf_op jit(solution)/shard_map/ppermute | solution.py:30
  38.4 4.1 %collective-permute-done.4.before.doc_before = bf16[144,256]{1,0:T(8,128)(2,1)S(1)} collective-permute-done((bf16[144,256]{1,0:T(8,128)(2,1)S(1)}, bf16[144,256]{1,0:T(8,128)(2,1)S(1)}, u32[]{:S(2)}, u32[]{:S(2)}) %collective-permute-start.4) | collective-permute-done | bytes 73760 | tf_op jit(solution)/shard_map/ppermute | solution.py:50
  42.5 1.7 %collective-permute-done.5.after.doc_after = bf16[144,256]{1,0:T(8,128)(2,1)S(1)} collective-permute-done((bf16[144,256]{1,0:T(8,128)(2,1)S(1)}, bf16[144,256]{1,0:T(8,128)(2,1)S(1)}, u32[]{:S(2)}, u32[]{:S(2)}) %collective-permute-start.5) | collective-permute-done | bytes 73760 | tf_op jit(solution)/shard_map/ppermute | solution.py:54
  45.2 3.0 %collective-permute-start.10 = (bf16[128,256]{1,0:T(8,128)(2,1)S(1)}, bf16[128,256]{1,0:T(8,128)(2,1)S(1)}, u32[]{:S(2)}, u32[]{:S(2)}) collective-permute-start(bf16[128,256]{1,0:T(8,128)(2,1)S(1)} %get-tuple-element.41), channel_id=1, source_target_pairs={{0,4},{2,6},{4,0},{6,2},{1,5},{3,7},{5,1},{7,3},{8,12},{10,14},{12... | collective-permute-start | bytes 196616 | tf_op jit(solution)/shard_map/ppermute | solution.py:249
  51.3 2.6 %collective-permute-done.9.r1 = bf16[128,256]{1,0:T(8,128)(2,1)S(1)} collective-permute-done((bf16[128,256]{1,0:T(8,128)(2,1)S(1)}, bf16[128,256]{1,0:T(8,128)(2,1)S(1)}, u32[]{:S(2)}, u32[]{:S(2)}) %collective-permute-start.9) | collective-permute-done | bytes 65568 | tf_op jit(solution)/shard_map/ppermute | solution.py:247
  53.9 4.0 %collective-permute-start.12 = (f32[128,256]{1,0:T(8,128)S(1)}, f32[128,256]{1,0:T(8,128)S(1)}, u32[]{:S(2)}, u32[]{:S(2)}) collective-permute-start(f32[128,256]{1,0:T(8,128)S(1)} %shard_map.88.mine), channel_id=1, source_target_pairs={{0,1},{1,0},{2,3},{3,2},{4,5},{5,4},{6,7},{7,6},{8,9},{9,8},{10,11... | collective-permute-start | bytes 393224 | tf_op jit(solution)/shard_map/ppermute | solution.py:46
  59.9 1.8 %collective-permute-start.15 = (bf16[128,256]{1,0:T(8,128)(2,1)S(1)}, bf16[128,256]{1,0:T(8,128)(2,1)S(1)}, u32[]{:S(2)}, u32[]{:S(2)}) collective-permute-start(bf16[128,256]{1,0:T(8,128)(2,1)S(1)} %shard_map.89.x0), channel_id=1, source_target_pairs={{0,6},{2,0},{4,2},{6,4},{1,7},{3,1},{5,3},{7,5},{8,14},{10,8},{12,... | collective-permute-start | bytes 196616 | tf_op jit(solution)/shard_map/ppermute | solution.py:30
  61.6 3.6 %collective-permute-done.13.x1 = bf16[128,256]{1,0:T(8,128)(2,1)S(1)} collective-permute-done((bf16[128,256]{1,0:T(8,128)(2,1)S(1)}, bf16[128,256]{1,0:T(8,128)(2,1)S(1)}, u32[]{:S(2)}, u32[]{:S(2)}) %collective-permute-start.13) | collective-permute-done | bytes 65568 | tf_op jit(solution)/shard_map/ppermute | solution.py:30
  66.4 4.0 %all-to-all-start.2 = ((bf16[4,4,64,512]{3,2,1,0:T(8,128)(2,1)}), bf16[4,4,64,512]{3,2,1,0:T(8,128)(2,1)S(1)}, u32[]{:S(2)}, u32[]{:S(2)}) async-start(bf16[4,4,64,512]{3,2,1,0:T(8,128)(2,1)} %copy-done), calls=%async_computation.2 | async-start | bytes 2097152 | tf_op jit(solution)/shard_map/all_to_all | solution.py:38
  70.4 4.5 %collective-permute-start.16 = (bf16[128,256]{1,0:T(8,128)(2,1)}, bf16[128,256]{1,0:T(8,128)(2,1)S(1)}, u32[]{:S(2)}, u32[]{:S(2)}) collective-permute-start(bf16[128,256]{1,0:T(8,128)(2,1)} %copy-done.5), channel_id=1, source_target_pairs={{0,8},{8,16},{16,24},{24,32},{32,40},{40,48},{48,56},{56,64},{64,7... | collective-permute-start | bytes 196616 | tf_op jit(solution)/shard_map/ppermute | solution.py:50
  74.9 1.9 %collective-permute-start.17 = (bf16[128,256]{1,0:T(8,128)(2,1)}, bf16[128,256]{1,0:T(8,128)(2,1)S(1)}, u32[]{:S(2)}, u32[]{:S(2)}) collective-permute-start(bf16[128,256]{1,0:T(8,128)(2,1)} %copy-done.5), channel_id=1, source_target_pairs={{8,0},{16,8},{24,16},{32,24},{40,32},{48,40},{56,48},{64,56},{72,6... | collective-permute-start | bytes 196616 | tf_op jit(solution)/shard_map/ppermute | solution.py:54
  76.8 6.1 %collective-permute-done.17.after = bf16[128,256]{1,0:T(8,128)(2,1)S(1)} collective-permute-done((bf16[128,256]{1,0:T(8,128)(2,1)}, bf16[128,256]{1,0:T(8,128)(2,1)S(1)}, u32[]{:S(2)}, u32[]{:S(2)}) %collective-permute-start.17) | collective-permute-done | bytes 65568 | tf_op jit(solution)/shard_map/ppermute | solution.py:54
  85.3 3.4 %collective-permute-start.19 = (bf16[128,256]{1,0:T(8,128)(2,1)S(1)}, bf16[128,256]{1,0:T(8,128)(2,1)S(1)}, u32[]{:S(2)}, u32[]{:S(2)}) collective-permute-start(bf16[128,256]{1,0:T(8,128)(2,1)S(1)} %get-tuple-element.48), channel_id=1, source_target_pairs={{0,4},{2,6},{4,0},{6,2},{1,5},{3,7},{5,1},{7,3},{8,12},{10,14},{12... | collective-permute-start | bytes 196616 | tf_op jit(solution)/shard_map/ppermute | solution.py:249
  89.2 1.9 %collective-permute-done.19.r2 = bf16[128,256]{1,0:T(8,128)(2,1)S(1)} collective-permute-done((bf16[128,256]{1,0:T(8,128)(2,1)S(1)}, bf16[128,256]{1,0:T(8,128)(2,1)S(1)}, u32[]{:S(2)}, u32[]{:S(2)}) %collective-permute-start.19) | collective-permute-done | bytes 65568 | tf_op jit(solution)/shard_map/ppermute | solution.py:249
  91.8 4.6 %collective-permute-start.21 = (f32[128,256]{1,0:T(8,128)S(1)}, f32[128,256]{1,0:T(8,128)S(1)}, u32[]{:S(2)}, u32[]{:S(2)}) collective-permute-start(f32[128,256]{1,0:T(8,128)S(1)} %shard_map.92.mine), channel_id=1, source_target_pairs={{0,1},{1,0},{2,3},{3,2},{4,5},{5,4},{6,7},{7,6},{8,9},{9,8},{10,11... | collective-permute-start | bytes 393224 | tf_op jit(solution)/shard_map/ppermute | solution.py:46
  97.5 2.5 %collective-permute-start.23 = (bf16[128,256]{1,0:T(8,128)(2,1)S(1)}, bf16[128,256]{1,0:T(8,128)(2,1)S(1)}, u32[]{:S(2)}, u32[]{:S(2)}) collective-permute-start(bf16[128,256]{1,0:T(8,128)(2,1)S(1)} %shard_map.93.x0), channel_id=1, source_target_pairs={{0,4},{2,6},{4,0},{6,2},{1,5},{3,7},{5,1},{7,3},{8,12},{10,14},{12... | collective-permute-start | bytes 196616 | tf_op jit(solution)/shard_map/ppermute | solution.py:30
  100.8 1.8 %collective-permute-done.22.x1 = bf16[128,256]{1,0:T(8,128)(2,1)S(1)} collective-permute-done((bf16[128,256]{1,0:T(8,128)(2,1)S(1)}, bf16[128,256]{1,0:T(8,128)(2,1)S(1)}, u32[]{:S(2)}, u32[]{:S(2)}) %collective-permute-start.22) | collective-permute-done | bytes 65568 | tf_op jit(solution)/shard_map/ppermute | solution.py:30
  104.2 1.9 %collective-permute-start.25 = (bf16[128,256]{1,0:T(8,128)(2,1)S(1)}, bf16[128,256]{1,0:T(8,128)(2,1)S(1)}, u32[]{:S(2)}, u32[]{:S(2)}) collective-permute-start(bf16[128,256]{1,0:T(8,128)(2,1)S(1)} %get-tuple-element.52.own), channel_id=1, source_target_pairs={{0,8},{8,16},{16,24},{24,32},{32,40},{40,48},{48,56},{56,64},{64,7... | collective-permute-start | bytes 196616 | tf_op jit(solution)/shard_map/ppermute | solution.py:50
  106.1 3.4 %collective-permute-start.26 = (bf16[128,256]{1,0:T(8,128)(2,1)S(1)}, bf16[128,256]{1,0:T(8,128)(2,1)S(1)}, u32[]{:S(2)}, u32[]{:S(2)}) collective-permute-start(bf16[128,256]{1,0:T(8,128)(2,1)S(1)} %get-tuple-element.52.own), channel_id=1, source_target_pairs={{8,0},{16,8},{24,16},{32,24},{40,32},{48,40},{56,48},{64,56},{72,6... | collective-permute-start | bytes 196616 | tf_op jit(solution)/shard_map/ppermute | solution.py:54
  109.5 3.7 %collective-permute-done.26.after = bf16[128,256]{1,0:T(8,128)(2,1)S(1)} collective-permute-done((bf16[128,256]{1,0:T(8,128)(2,1)S(1)}, bf16[128,256]{1,0:T(8,128)(2,1)S(1)}, u32[]{:S(2)}, u32[]{:S(2)}) %collective-permute-start.26) | collective-permute-done | bytes 65568 | tf_op jit(solution)/shard_map/ppermute | solution.py:54
  114.2 1.3 collective-permute-start.27
  115.5 2.4 %collective-permute-start.28 = (bf16[128,256]{1,0:T(8,128)(2,1)S(1)}, bf16[128,256]{1,0:T(8,128)(2,1)S(1)}, u32[]{:S(2)}, u32[]{:S(2)}) collective-permute-start(bf16[128,256]{1,0:T(8,128)(2,1)S(1)} %get-tuple-element.55), channel_id=1, source_target_pairs={{0,4},{2,6},{4,0},{6,2},{1,5},{3,7},{5,1},{7,3},{8,12},{10,14},{12... | collective-permute-start | bytes 196616 | tf_op jit(solution)/shard_map/ppermute | solution.py:249
  118.6 1.6 %collective-permute-done.28.r2 = bf16[128,256]{1,0:T(8,128)(2,1)S(1)} collective-permute-done((bf16[128,256]{1,0:T(8,128)(2,1)S(1)}, bf16[128,256]{1,0:T(8,128)(2,1)S(1)}, u32[]{:S(2)}, u32[]{:S(2)}) %collective-permute-start.28) | collective-permute-done | bytes 65568 | tf_op jit(solution)/shard_map/ppermute | solution.py:249
  121.0 4.4 %collective-permute-start.30 = (f32[128,128]{1,0:T(8,128)S(1)}, f32[128,128]{1,0:T(8,128)S(1)}, u32[]{:S(2)}, u32[]{:S(2)}) collective-permute-start(f32[128,128]{1,0:T(8,128)S(1)} %get-tuple-element.58), channel_id=1, source_target_pairs={{0,1},{1,0},{2,3},{3,2},{4,5},{5,4},{6,7},{7,6},{8,9},{9,8},{10,11... | collective-permute-start | bytes 196616 | tf_op jit(solution)/shard_map/ppermute | solution.py:46
  (73 shorter events, 26.0 us)
Async XLA Ops:
  1.9 19.8 %all-to-all-start = ((bf16[16,64,512]{2,1,0:T(8,128)(2,1)}), bf16[16,64,512]{2,1,0:T(8,128)(2,1)S(1)}, u32[]{:S(2)}, u32[]{:S(2)}) async-start(bf16[16,64,512]{2,1,0:T(8,128)(2,1)} %shard_map.84), calls=%async_computation | async-start | bytes 2097152 | tf_op jit(solution)/shard_map/all_to_all | solution.py:38
  9.2 8.2 %collective-permute-start = (bf16[128,128]{1,0:T(8,128)(2,1)S(1)}, bf16[128,128]{1,0:T(8,128)(2,1)S(1)}, u32[]{:S(2)}, u32[]{:S(2)}) collective-permute-start(bf16[128,128]{1,0:T(8,128)(2,1)S(1)} %copy-done.9), channel_id=1, source_target_pairs={{0,2},{2,4},{4,6},{6,0},{1,3},{3,5},{5,7},{7,1},{8,10},{10,12},{12... | collective-permute-start | bytes 98312 | tf_op jit(solution)/shard_map/ppermute | solution.py:30
  10.6 6.9 %collective-permute-start.1 = (bf16[128,128]{1,0:T(8,128)(2,1)S(1)}, bf16[128,128]{1,0:T(8,128)(2,1)S(1)}, u32[]{:S(2)}, u32[]{:S(2)}) collective-permute-start(bf16[128,128]{1,0:T(8,128)(2,1)S(1)} %copy-done.9), channel_id=1, source_target_pairs={{0,4},{2,6},{4,0},{6,2},{1,5},{3,7},{5,1},{7,3},{8,12},{10,14},{12... | collective-permute-start | bytes 98312 | tf_op jit(solution)/shard_map/ppermute | solution.py:30
  13.2 4.2 %collective-permute-start.2 = (bf16[128,128]{1,0:T(8,128)(2,1)S(1)}, bf16[128,128]{1,0:T(8,128)(2,1)S(1)}, u32[]{:S(2)}, u32[]{:S(2)}) collective-permute-start(bf16[128,128]{1,0:T(8,128)(2,1)S(1)} %copy-done.9), channel_id=1, source_target_pairs={{0,6},{2,0},{4,2},{6,4},{1,7},{3,1},{5,3},{7,5},{8,14},{10,8},{12,... | collective-permute-start | bytes 98312 | tf_op jit(solution)/shard_map/ppermute | solution.py:30
  17.5 3.1 %collective-permute-start.3 = (bf16[4,128,128]{2,1,0:T(8,128)(2,1)S(1)}, bf16[4,128,128]{2,1,0:T(8,128)(2,1)S(1)}, u32[]{:S(2)}, u32[]{:S(2)}) collective-permute-start(bf16[4,128,128]{2,1,0:T(8,128)(2,1)S(1)} %pad_maximum_fusion.own), channel_id=1, source_target_pairs={{0,1},{1,0},{2,3},{3,2},{4,5},{5,4},{6,7},{7,6},{8,9},{9,8},{10,11... | collective-permute-start | bytes 393224 | tf_op jit(solution)/shard_map/ppermute | solution.py:46
  22.3 42.9 %all-to-all-start.1 = ((bf16[16,64,512]{2,1,0:T(8,128)(2,1)}), bf16[16,64,512]{2,1,0:T(8,128)(2,1)S(1)}, u32[]{:S(2)}, u32[]{:S(2)}) async-start(bf16[16,64,512]{2,1,0:T(8,128)(2,1)} %copy-done.1), calls=%async_computation.1 | async-start | bytes 2097152 | tf_op jit(solution)/shard_map/all_to_all | solution.py:38
  30.0 12.5 %collective-permute-start.4 = (bf16[144,256]{1,0:T(8,128)(2,1)S(1)}, bf16[144,256]{1,0:T(8,128)(2,1)S(1)}, u32[]{:S(2)}, u32[]{:S(2)}) collective-permute-start(bf16[144,256]{1,0:T(8,128)(2,1)S(1)} %get-tuple-element.36.own.doc_own), channel_id=1, source_target_pairs={{0,8},{8,16},{16,24},{24,32},{32,40},{40,48},{48,56},{56,64},{64,7... | collective-permute-start | bytes 221192 | tf_op jit(solution)/shard_map/ppermute | solution.py:50
  33.1 11.1 %collective-permute-start.5 = (bf16[144,256]{1,0:T(8,128)(2,1)S(1)}, bf16[144,256]{1,0:T(8,128)(2,1)S(1)}, u32[]{:S(2)}, u32[]{:S(2)}) collective-permute-start(bf16[144,256]{1,0:T(8,128)(2,1)S(1)} %get-tuple-element.36.own.doc_own), channel_id=1, source_target_pairs={{8,0},{16,8},{24,16},{32,24},{40,32},{48,40},{56,48},{64,56},{72,6... | collective-permute-start | bytes 221192 | tf_op jit(solution)/shard_map/ppermute | solution.py:54
  35.3 13.6 %collective-permute-start.6 = (bf16[64,512]{1,0:T(8,128)(2,1)}, bf16[64,512]{1,0:T(8,128)(2,1)S(1)}, u32[]{:S(2)}, u32[]{:S(2)}) collective-permute-start(bf16[64,512]{1,0:T(8,128)(2,1)} %copy-done.3), channel_id=1, source_target_pairs={{0,8},{8,16},{16,24},{24,0},{1,9},{9,17},{17,25},{25,1},{2,10},{10... | collective-permute-start | bytes 196616 | tf_op jit(solution)/shard_map/ppermute | solution.py:30
  37.8 11.9 %collective-permute-start.7 = (bf16[64,512]{1,0:T(8,128)(2,1)}, bf16[64,512]{1,0:T(8,128)(2,1)S(1)}, u32[]{:S(2)}, u32[]{:S(2)}) collective-permute-start(bf16[64,512]{1,0:T(8,128)(2,1)} %copy-done.3), channel_id=1, source_target_pairs={{0,16},{8,24},{16,0},{24,8},{1,17},{9,25},{17,1},{25,9},{2,18},{10... | collective-permute-start | bytes 196616 | tf_op jit(solution)/shard_map/ppermute | solution.py:30
  37.8 11.9 %collective-permute-start.8 = (bf16[64,512]{1,0:T(8,128)(2,1)}, bf16[64,512]{1,0:T(8,128)(2,1)S(1)}, u32[]{:S(2)}, u32[]{:S(2)}) collective-permute-start(bf16[64,512]{1,0:T(8,128)(2,1)} %copy-done.3), channel_id=1, source_target_pairs={{0,24},{8,0},{16,8},{24,16},{1,25},{9,1},{17,9},{25,17},{2,26},{10... | collective-permute-start | bytes 196616 | tf_op jit(solution)/shard_map/ppermute | solution.py:30
  45.2 5.5 %collective-permute-start.10 = (bf16[128,256]{1,0:T(8,128)(2,1)S(1)}, bf16[128,256]{1,0:T(8,128)(2,1)S(1)}, u32[]{:S(2)}, u32[]{:S(2)}) collective-permute-start(bf16[128,256]{1,0:T(8,128)(2,1)S(1)} %get-tuple-element.41), channel_id=1, source_target_pairs={{0,4},{2,6},{4,0},{6,2},{1,5},{3,7},{5,1},{7,3},{8,12},{10,14},{12... | collective-permute-start | bytes 196616 | tf_op jit(solution)/shard_map/ppermute | solution.py:249
  48.2 3.1 %collective-permute-start.11 = (bf16[128,256]{1,0:T(8,128)(2,1)S(1)}, bf16[128,256]{1,0:T(8,128)(2,1)S(1)}, u32[]{:S(2)}, u32[]{:S(2)}) collective-permute-start(bf16[128,256]{1,0:T(8,128)(2,1)S(1)} %get-tuple-element.42), channel_id=1, source_target_pairs={{0,6},{2,0},{4,2},{6,4},{1,7},{3,1},{5,3},{7,5},{8,14},{10,8},{12,... | collective-permute-start | bytes 196616 | tf_op jit(solution)/shard_map/ppermute | solution.py:248
  48.9 4.9 %collective-permute-start.9 = (bf16[128,256]{1,0:T(8,128)(2,1)S(1)}, bf16[128,256]{1,0:T(8,128)(2,1)S(1)}, u32[]{:S(2)}, u32[]{:S(2)}) collective-permute-start(bf16[128,256]{1,0:T(8,128)(2,1)S(1)} %get-tuple-element.40), channel_id=1, source_target_pairs={{0,2},{2,4},{4,6},{6,0},{1,3},{3,5},{5,7},{7,1},{8,10},{10,12},{12... | collective-permute-start | bytes 196616 | tf_op jit(solution)/shard_map/ppermute | solution.py:247
  53.9 5.0 %collective-permute-start.12 = (f32[128,256]{1,0:T(8,128)S(1)}, f32[128,256]{1,0:T(8,128)S(1)}, u32[]{:S(2)}, u32[]{:S(2)}) collective-permute-start(f32[128,256]{1,0:T(8,128)S(1)} %shard_map.88.mine), channel_id=1, source_target_pairs={{0,1},{1,0},{2,3},{3,2},{4,5},{5,4},{6,7},{7,6},{8,9},{9,8},{10,11... | collective-permute-start | bytes 393224 | tf_op jit(solution)/shard_map/ppermute | solution.py:46
  58.9 6.3 %collective-permute-start.13 = (bf16[128,256]{1,0:T(8,128)(2,1)S(1)}, bf16[128,256]{1,0:T(8,128)(2,1)S(1)}, u32[]{:S(2)}, u32[]{:S(2)}) collective-permute-start(bf16[128,256]{1,0:T(8,128)(2,1)S(1)} %shard_map.89.x0), channel_id=1, source_target_pairs={{0,2},{2,4},{4,6},{6,0},{1,3},{3,5},{5,7},{7,1},{8,10},{10,12},{12... | collective-permute-start | bytes 196616 | tf_op jit(solution)/shard_map/ppermute | solution.py:30
  59.0 6.2 %collective-permute-start.14 = (bf16[128,256]{1,0:T(8,128)(2,1)S(1)}, bf16[128,256]{1,0:T(8,128)(2,1)S(1)}, u32[]{:S(2)}, u32[]{:S(2)}) collective-permute-start(bf16[128,256]{1,0:T(8,128)(2,1)S(1)} %shard_map.89.x0), channel_id=1, source_target_pairs={{0,4},{2,6},{4,0},{6,2},{1,5},{3,7},{5,1},{7,3},{8,12},{10,14},{12... | collective-permute-start | bytes 196616 | tf_op jit(solution)/shard_map/ppermute | solution.py:30
  59.9 5.3 %collective-permute-start.15 = (bf16[128,256]{1,0:T(8,128)(2,1)S(1)}, bf16[128,256]{1,0:T(8,128)(2,1)S(1)}, u32[]{:S(2)}, u32[]{:S(2)}) collective-permute-start(bf16[128,256]{1,0:T(8,128)(2,1)S(1)} %shard_map.89.x0), channel_id=1, source_target_pairs={{0,6},{2,0},{4,2},{6,4},{1,7},{3,1},{5,3},{7,5},{8,14},{10,8},{12,... | collective-permute-start | bytes 196616 | tf_op jit(solution)/shard_map/ppermute | solution.py:30
  66.4 37.4 %all-to-all-start.2 = ((bf16[4,4,64,512]{3,2,1,0:T(8,128)(2,1)}), bf16[4,4,64,512]{3,2,1,0:T(8,128)(2,1)S(1)}, u32[]{:S(2)}, u32[]{:S(2)}) async-start(bf16[4,4,64,512]{3,2,1,0:T(8,128)(2,1)} %copy-done), calls=%async_computation.2 | async-start | bytes 2097152 | tf_op jit(solution)/shard_map/all_to_all | solution.py:38
  70.4 6.4 %collective-permute-start.16 = (bf16[128,256]{1,0:T(8,128)(2,1)}, bf16[128,256]{1,0:T(8,128)(2,1)S(1)}, u32[]{:S(2)}, u32[]{:S(2)}) collective-permute-start(bf16[128,256]{1,0:T(8,128)(2,1)} %copy-done.5), channel_id=1, source_target_pairs={{0,8},{8,16},{16,24},{24,32},{32,40},{40,48},{48,56},{56,64},{64,7... | collective-permute-start | bytes 196616 | tf_op jit(solution)/shard_map/ppermute | solution.py:50
  74.9 8.0 %collective-permute-start.17 = (bf16[128,256]{1,0:T(8,128)(2,1)}, bf16[128,256]{1,0:T(8,128)(2,1)S(1)}, u32[]{:S(2)}, u32[]{:S(2)}) collective-permute-start(bf16[128,256]{1,0:T(8,128)(2,1)} %copy-done.5), channel_id=1, source_target_pairs={{8,0},{16,8},{24,16},{32,24},{40,32},{48,40},{56,48},{64,56},{72,6... | collective-permute-start | bytes 196616 | tf_op jit(solution)/shard_map/ppermute | solution.py:54
  84.7 4.5 %collective-permute-start.18 = (bf16[128,256]{1,0:T(8,128)(2,1)S(1)}, bf16[128,256]{1,0:T(8,128)(2,1)S(1)}, u32[]{:S(2)}, u32[]{:S(2)}) collective-permute-start(bf16[128,256]{1,0:T(8,128)(2,1)S(1)} %get-tuple-element.47), channel_id=1, source_target_pairs={{0,2},{2,4},{4,6},{6,0},{1,3},{3,5},{5,7},{7,1},{8,10},{10,12},{12... | collective-permute-start | bytes 196616 | tf_op jit(solution)/shard_map/ppermute | solution.py:247
  85.3 5.8 %collective-permute-start.19 = (bf16[128,256]{1,0:T(8,128)(2,1)S(1)}, bf16[128,256]{1,0:T(8,128)(2,1)S(1)}, u32[]{:S(2)}, u32[]{:S(2)}) collective-permute-start(bf16[128,256]{1,0:T(8,128)(2,1)S(1)} %get-tuple-element.48), channel_id=1, source_target_pairs={{0,4},{2,6},{4,0},{6,2},{1,5},{3,7},{5,1},{7,3},{8,12},{10,14},{12... | collective-permute-start | bytes 196616 | tf_op jit(solution)/shard_map/ppermute | solution.py:249
  91.8 5.6 %collective-permute-start.21 = (f32[128,256]{1,0:T(8,128)S(1)}, f32[128,256]{1,0:T(8,128)S(1)}, u32[]{:S(2)}, u32[]{:S(2)}) collective-permute-start(f32[128,256]{1,0:T(8,128)S(1)} %shard_map.92.mine), channel_id=1, source_target_pairs={{0,1},{1,0},{2,3},{3,2},{4,5},{5,4},{6,7},{7,6},{8,9},{9,8},{10,11... | collective-permute-start | bytes 393224 | tf_op jit(solution)/shard_map/ppermute | solution.py:46
  97.4 5.2 %collective-permute-start.22 = (bf16[128,256]{1,0:T(8,128)(2,1)S(1)}, bf16[128,256]{1,0:T(8,128)(2,1)S(1)}, u32[]{:S(2)}, u32[]{:S(2)}) collective-permute-start(bf16[128,256]{1,0:T(8,128)(2,1)S(1)} %shard_map.93.x0), channel_id=1, source_target_pairs={{0,2},{2,4},{4,6},{6,0},{1,3},{3,5},{5,7},{7,1},{8,10},{10,12},{12... | collective-permute-start | bytes 196616 | tf_op jit(solution)/shard_map/ppermute | solution.py:30
  97.5 5.4 %collective-permute-start.23 = (bf16[128,256]{1,0:T(8,128)(2,1)S(1)}, bf16[128,256]{1,0:T(8,128)(2,1)S(1)}, u32[]{:S(2)}, u32[]{:S(2)}) collective-permute-start(bf16[128,256]{1,0:T(8,128)(2,1)S(1)} %shard_map.93.x0), channel_id=1, source_target_pairs={{0,4},{2,6},{4,0},{6,2},{1,5},{3,7},{5,1},{7,3},{8,12},{10,14},{12... | collective-permute-start | bytes 196616 | tf_op jit(solution)/shard_map/ppermute | solution.py:30
  100.0 3.7 %collective-permute-start.24 = (bf16[128,256]{1,0:T(8,128)(2,1)S(1)}, bf16[128,256]{1,0:T(8,128)(2,1)S(1)}, u32[]{:S(2)}, u32[]{:S(2)}) collective-permute-start(bf16[128,256]{1,0:T(8,128)(2,1)S(1)} %shard_map.93.x0), channel_id=1, source_target_pairs={{0,6},{2,0},{4,2},{6,4},{1,7},{3,1},{5,3},{7,5},{8,14},{10,8},{12,... | collective-permute-start | bytes 196616 | tf_op jit(solution)/shard_map/ppermute | solution.py:30
  104.2 5.3 %collective-permute-start.25 = (bf16[128,256]{1,0:T(8,128)(2,1)S(1)}, bf16[128,256]{1,0:T(8,128)(2,1)S(1)}, u32[]{:S(2)}, u32[]{:S(2)}) collective-permute-start(bf16[128,256]{1,0:T(8,128)(2,1)S(1)} %get-tuple-element.52.own), channel_id=1, source_target_pairs={{0,8},{8,16},{16,24},{24,32},{32,40},{40,48},{48,56},{56,64},{64,7... | collective-permute-start | bytes 196616 | tf_op jit(solution)/shard_map/ppermute | solution.py:50
  106.1 7.1 %collective-permute-start.26 = (bf16[128,256]{1,0:T(8,128)(2,1)S(1)}, bf16[128,256]{1,0:T(8,128)(2,1)S(1)}, u32[]{:S(2)}, u32[]{:S(2)}) collective-permute-start(bf16[128,256]{1,0:T(8,128)(2,1)S(1)} %get-tuple-element.52.own), channel_id=1, source_target_pairs={{8,0},{16,8},{24,16},{32,24},{40,32},{48,40},{56,48},{64,56},{72,6... | collective-permute-start | bytes 196616 | tf_op jit(solution)/shard_map/ppermute | solution.py:54
  114.2 4.4 %collective-permute-start.27 = (bf16[128,256]{1,0:T(8,128)(2,1)S(1)}, bf16[128,256]{1,0:T(8,128)(2,1)S(1)}, u32[]{:S(2)}, u32[]{:S(2)}) collective-permute-start(bf16[128,256]{1,0:T(8,128)(2,1)S(1)} %get-tuple-element.54), channel_id=1, source_target_pairs={{0,2},{2,4},{4,6},{6,0},{1,3},{3,5},{5,7},{7,1},{8,10},{10,12},{12... | collective-permute-start | bytes 196616 | tf_op jit(solution)/shard_map/ppermute | solution.py:247
  115.5 4.7 %collective-permute-start.28 = (bf16[128,256]{1,0:T(8,128)(2,1)S(1)}, bf16[128,256]{1,0:T(8,128)(2,1)S(1)}, u32[]{:S(2)}, u32[]{:S(2)}) collective-permute-start(bf16[128,256]{1,0:T(8,128)(2,1)S(1)} %get-tuple-element.55), channel_id=1, source_target_pairs={{0,4},{2,6},{4,0},{6,2},{1,5},{3,7},{5,1},{7,3},{8,12},{10,14},{12... | collective-permute-start | bytes 196616 | tf_op jit(solution)/shard_map/ppermute | solution.py:249
  121.0 5.3 %collective-permute-start.30 = (f32[128,128]{1,0:T(8,128)S(1)}, f32[128,128]{1,0:T(8,128)S(1)}, u32[]{:S(2)}, u32[]{:S(2)}) collective-permute-start(f32[128,128]{1,0:T(8,128)S(1)} %get-tuple-element.58), channel_id=1, source_target_pairs={{0,1},{1,0},{2,3},{3,2},{4,5},{5,4},{6,7},{7,6},{8,9},{9,8},{10,11... | collective-permute-start | bytes 196616 | tf_op jit(solution)/shard_map/ppermute | solution.py:46
  (12 other events, 60.4 us)

commit v11 on v8

--- a/solution.py
+++ b/solution.py
@@ -91,13 +91,11 @@
         first[n] = whole
 
 
-def many_body(wq, wk, wv, wo, bias, many, third, wide, parts, sems):
+def many_body(wq, wk, wv, wo, bias, rest, wide, parts, sems):
     pairs = [(w.at[1:3], parts.at[n]) for n, w in enumerate((wq, wk, wv, wo))]
     fetch(pairs, sems)
-    third[...] = jnp.concatenate([parts[n, 1] for n in range(4)], axis=1)
-    whole = jnp.concatenate([parts[n, 0] for n in range(4)], axis=1)
-    for n in range(16):
-        many[n] = whole
+    for layer in range(2):
+        rest[layer] = jnp.concatenate([parts[n, layer] for n in range(4)], axis=1)
     wide[...] = jnp.zeros((8, 256), F32)
     for n in range(2 * LAYERS):
         for lag_row in range(WIN_ROWS):
@@ -105,11 +103,11 @@
             wide[n : n + 1, at : at + WIN_COLS] = bias[n // 2, n % 2, lag_row : lag_row + 1, :]
 
 
-def line_body(p0, p1, p2, p3, many):
+def line_body(p0, p1, p2, p3, many, *, layer):
     for k, part in enumerate((p0, p1, p2, p3)):
         at = behind("x", k)
         for n in range(4):
-            many[n, at] = part[...]
+            many[n, at] = part[layer]
 
 
 def table_body(wide, before, own, after, table):
@@ -259,25 +257,27 @@
     weights = gather_rows(first, SP)
     tokens_y = spread(tokens, "y")
     near_y = jnp.stack(in_order(tokens, tokens_y))
-    many1, third, wide = call(
-        many_body, [shaped(16, 64, 512), shaped(64, 512), shaped(8, 256, dtype=F32)],
+    rest, wide = call(
+        many_body, [shaped(2, 64, 512), shaped(8, 256, dtype=F32)],
         *held, offset_bias, in_specs=[hbm] * 4 + [pl.BlockSpec()],
         scratch=[pltpu.VMEM((4, 2, 64, 128), BF16), pltpu.SemaphoreType.DMA((4,))],
     )
-    third_x = in_order(third, spread(third, "x"))
-    near_partner = swap(after_this(near_y, many1))
+    third_x = in_order(rest, spread(rest, "x"))
+    near_partner = swap(after_this(near_y, wide))
 
     q, kv = call(
         heads_first_body, [shaped(128, 128), shaped(144, 256)],
         near_y, near_partner, norm_gain, documents.reshape(1, 128), weights,
     )
-    many2 = call(line_body, shaped(4, 4, 64, 512), *third_x)
+    many1, many2 = [
+        call(functools.partial(line_body, layer=n), shaped(4, 4, 64, 512), *third_x)
+        for n in range(2)
+    ]
     for layer in range(LAYERS):
         after = from_after(kv)
         before = from_before(kv)
         if layer < 2:
-            many, axes = ((many1, SP), (many2, "z"))[layer]
-            next_weights = gather_rows(after_this(many, kv), axes)
+            next_weights = gather_rows(after_this((many1, many2)[layer], kv), "z")
         if layer == 0:
             table = call(table_body, shaped(6, 128, 384, dtype=F32), wide, before, kv, after)
         kept, r1, r2, r3 = scattered(

time: 127 us -> 129 us (1.016)
  the two profiles are of different devices: /device:TPU:39 before, /device:TPU:7 now
where the time goes in v11:
time: 129 us; the launch traced here: 128 us
  starting transfers between devices  75.1 us (58%)
  waiting for transfers between devices  38 us (29%)
  Pallas kernels  8.7 us (7%)
  local copies, waits for them, and re-layouts  5.73 us (4%)
    ppermute x4, starting transfers between devices, swap(): return lax.ppermute(a, 'c', [(0, 1), (1, 0)])  16.6 us
    all_to_all x3, starting transfers between devices, gather_rows(): return lax.all_to_all(a, axes, 0, 0, tiled=True).reshape(1024, 512)  15.5 us
    ppermute x12, starting transfers between devices, spread(): return [lax.ppermute(a, axis, turn(k)) for k in (1, 3, 2)]  13.5 us
    ppermute x3, waiting for transfers between devices, from_after(): return lax.ppermute(a, SP, [(i + 1, i) for i in range(15)])  13.1 us
    ppermute x12, waiting for transfers between devices, spread(): return [lax.ppermute(a, axis, turn(k)) for k in (1, 3, 2)]  12.9 us
    ppermute x3, starting transfers between devices, scattered(): r2 = lax.ppermute(s2, 'y', turn(2))  8.82 us
    pallas_call x17, Pallas kernels, call(): pl.pallas_call(body, out_shape=outs, **specs, scratch_shapes=list(scratch...  8.7 us
    ppermute x3, starting transfers between devices, from_before(): return lax.ppermute(a, SP, [(i, i + 1) for i in range(15)])  8.66 us
  transfers between devices with their start and end apart: 34, of which 21 were waited for; matrix products, arithmetic and copies ran while one was open for 0% of the time, Pallas kernels for 3%

profile of v11, /device:TPU:7, one launch (start us, length us, event | category | flops | bytes accessed | tf_op | source)
XLA Modules:
  0.0 127.9 jit_solution(12812036432940999572)
XLA Ops:
  0.0 1.9 %shard_map.83 = bf16[16,64,512]{2,1,0:T(8,128)(2,1)} custom-call(bf16[3,64,128]{2,1,0:T(8,128)(2,1)} %wq.3, bf16[3,64,128]{2,1,0:T(8,128)(2,1)} %wk.3, bf16[3,64,128]{2,1,0:T(8,128)(2,1)} %wv.3, bf16[3,64,128]{2,1,0:T(8,128)(2,1)} %bitcast.16), custom_call_target="tpu_custom_call" | custom-call | tf_op jit(solution)/shard_map/pallas_call | solution.py:66
  1.9 7.7 %all-to-all-start = ((bf16[16,64,512]{2,1,0:T(8,128)(2,1)}), bf16[16,64,512]{2,1,0:T(8,128)(2,1)S(1)}, u32[]{:S(2)}, u32[]{:S(2)}) async-start(bf16[16,64,512]{2,1,0:T(8,128)(2,1)} %shard_map.83), calls=%async_computation | async-start | bytes 2097152 | tf_op jit(solution)/shard_map/all_to_all | solution.py:38
  9.7 1.4 %collective-permute-start = (bf16[128,128]{1,0:T(8,128)(2,1)S(1)}, bf16[128,128]{1,0:T(8,128)(2,1)S(1)}, u32[]{:S(2)}, u32[]{:S(2)}) collective-permute-start(bf16[128,128]{1,0:T(8,128)(2,1)S(1)} %copy-done.18), channel_id=1, source_target_pairs={{0,2},{2,4},{4,6},{6,0},{1,3},{3,5},{5,7},{7,1},{8,10},{10,12},{12... | collective-permute-start | bytes 98312 | tf_op jit(solution)/shard_map/ppermute | solution.py:30
  11.0 2.6 %collective-permute-start.1 = (bf16[128,128]{1,0:T(8,128)(2,1)S(1)}, bf16[128,128]{1,0:T(8,128)(2,1)S(1)}, u32[]{:S(2)}, u32[]{:S(2)}) collective-permute-start(bf16[128,128]{1,0:T(8,128)(2,1)S(1)} %copy-done.18), channel_id=1, source_target_pairs={{0,4},{2,6},{4,0},{6,2},{1,5},{3,7},{5,1},{7,3},{8,12},{10,14},{12... | collective-permute-start | bytes 98312 | tf_op jit(solution)/shard_map/ppermute | solution.py:30
  16.4 2.3 %collective-permute-start.7 = (bf16[2,64,512]{2,1,0:T(8,128)(2,1)S(1)}, bf16[2,64,512]{2,1,0:T(8,128)(2,1)S(1)}, u32[]{:S(2)}, u32[]{:S(2)}) collective-permute-start(bf16[2,64,512]{2,1,0:T(8,128)(2,1)S(1)} %get-tuple-element.36.p0), channel_id=1, source_target_pairs={{0,16},{8,24},{16,0},{24,8},{1,17},{9,25},{17,1},{25,9},{2,18},{10... | collective-permute-start | bytes 393224 | tf_op jit(solution)/shard_map/ppermute | solution.py:30
  18.7 2.7 %collective-permute-start.3 = (bf16[4,128,128]{2,1,0:T(8,128)(2,1)S(1)}, bf16[4,128,128]{2,1,0:T(8,128)(2,1)S(1)}, u32[]{:S(2)}, u32[]{:S(2)}) collective-permute-start(bf16[4,128,128]{2,1,0:T(8,128)(2,1)S(1)} %pad_maximum_fusion.own), channel_id=1, source_target_pairs={{0,1},{1,0},{2,3},{3,2},{4,5},{5,4},{6,7},{7,6},{8,9},{9,8},{10,11... | collective-permute-start | bytes 393224 | tf_op jit(solution)/shard_map/ppermute | solution.py:46
  21.4 3.0 %collective-permute-done.6.p1 = bf16[2,64,512]{2,1,0:T(8,128)(2,1)S(1)} collective-permute-done((bf16[2,64,512]{2,1,0:T(8,128)(2,1)S(1)}, bf16[2,64,512]{2,1,0:T(8,128)(2,1)S(1)}, u32[]{:S(2)}, u32[]{:S(2)}) %collective-permute-start.6) | collective-permute-done | bytes 131104 | tf_op jit(solution)/shard_map/ppermute | solution.py:30
  25.0 2.8 %collective-permute-done.8.p3 = bf16[2,64,512]{2,1,0:T(8,128)(2,1)S(1)} collective-permute-done((bf16[2,64,512]{2,1,0:T(8,128)(2,1)S(1)}, bf16[2,64,512]{2,1,0:T(8,128)(2,1)S(1)}, u32[]{:S(2)}, u32[]{:S(2)}) %collective-permute-start.8) | collective-permute-done | bytes 131104 | tf_op jit(solution)/shard_map/ppermute | solution.py:30
  30.2 4.0 %all-to-all-start.1 = ((bf16[4,4,64,512]{3,2,1,0:T(8,128)(2,1)}), bf16[4,4,64,512]{3,2,1,0:T(8,128)(2,1)S(1)}, u32[]{:S(2)}, u32[]{:S(2)}) async-start(bf16[4,4,64,512]{3,2,1,0:T(8,128)(2,1)} %copy-done.1), calls=%async_computation.1 | async-start | bytes 2097152 | tf_op jit(solution)/shard_map/all_to_all | solution.py:38
  34.2 4.8 %collective-permute-start.4 = (bf16[144,256]{1,0:T(8,128)(2,1)S(1)}, bf16[144,256]{1,0:T(8,128)(2,1)S(1)}, u32[]{:S(2)}, u32[]{:S(2)}) collective-permute-start(bf16[144,256]{1,0:T(8,128)(2,1)S(1)} %get-tuple-element.34.own), channel_id=1, source_target_pairs={{0,8},{8,16},{16,24},{24,32},{32,40},{40,48},{48,56},{56,64},{64,7... | collective-permute-start | bytes 221192 | tf_op jit(solution)/shard_map/ppermute | solution.py:50
  39.0 1.9 %collective-permute-start.5 = (bf16[144,256]{1,0:T(8,128)(2,1)S(1)}, bf16[144,256]{1,0:T(8,128)(2,1)S(1)}, u32[]{:S(2)}, u32[]{:S(2)}) collective-permute-start(bf16[144,256]{1,0:T(8,128)(2,1)S(1)} %get-tuple-element.34.own), channel_id=1, source_target_pairs={{8,0},{16,8},{24,16},{32,24},{40,32},{48,40},{56,48},{64,56},{72,6... | collective-permute-start | bytes 221192 | tf_op jit(solution)/shard_map/ppermute | solution.py:54
  41.0 5.5 %collective-permute-done.5.after = bf16[144,256]{1,0:T(8,128)(2,1)S(1)} collective-permute-done((bf16[144,256]{1,0:T(8,128)(2,1)S(1)}, bf16[144,256]{1,0:T(8,128)(2,1)S(1)}, u32[]{:S(2)}, u32[]{:S(2)}) %collective-permute-start.5) | collective-permute-done | bytes 73760 | tf_op jit(solution)/shard_map/ppermute | solution.py:54
  49.9 3.0 %collective-permute-start.10 = (bf16[128,256]{1,0:T(8,128)(2,1)S(1)}, bf16[128,256]{1,0:T(8,128)(2,1)S(1)}, u32[]{:S(2)}, u32[]{:S(2)}) collective-permute-start(bf16[128,256]{1,0:T(8,128)(2,1)S(1)} %get-tuple-element.39), channel_id=1, source_target_pairs={{0,4},{2,6},{4,0},{6,2},{1,5},{3,7},{5,1},{7,3},{8,12},{10,14},{12... | collective-permute-start | bytes 196616 | tf_op jit(solution)/shard_map/ppermute | solution.py:243
  56.0 2.3 %collective-permute-done.9.r1 = bf16[128,256]{1,0:T(8,128)(2,1)S(1)} collective-permute-done((bf16[128,256]{1,0:T(8,128)(2,1)S(1)}, bf16[128,256]{1,0:T(8,128)(2,1)S(1)}, u32[]{:S(2)}, u32[]{:S(2)}) %collective-permute-start.9) | collective-permute-done | bytes 65568 | tf_op jit(solution)/shard_map/ppermute | solution.py:241
  58.4 5.0 %collective-permute-start.12 = (f32[128,256]{1,0:T(8,128)S(1)}, f32[128,256]{1,0:T(8,128)S(1)}, u32[]{:S(2)}, u32[]{:S(2)}) collective-permute-start(f32[128,256]{1,0:T(8,128)S(1)} %shard_map.88.mine), channel_id=1, source_target_pairs={{0,1},{1,0},{2,3},{3,2},{4,5},{5,4},{6,7},{7,6},{8,9},{9,8},{10,11... | collective-permute-start | bytes 393224 | tf_op jit(solution)/shard_map/ppermute | solution.py:46
  65.3 1.8 %collective-permute-start.15 = (bf16[128,256]{1,0:T(8,128)(2,1)S(1)}, bf16[128,256]{1,0:T(8,128)(2,1)S(1)}, u32[]{:S(2)}, u32[]{:S(2)}) collective-permute-start(bf16[128,256]{1,0:T(8,128)(2,1)S(1)} %shard_map.89.x0), channel_id=1, source_target_pairs={{0,6},{2,0},{4,2},{6,4},{1,7},{3,1},{5,3},{7,5},{8,14},{10,8},{12,... | collective-permute-start | bytes 196616 | tf_op jit(solution)/shard_map/ppermute | solution.py:30
  67.1 3.6 %collective-permute-done.13.x1 = bf16[128,256]{1,0:T(8,128)(2,1)S(1)} collective-permute-done((bf16[128,256]{1,0:T(8,128)(2,1)S(1)}, bf16[128,256]{1,0:T(8,128)(2,1)S(1)}, u32[]{:S(2)}, u32[]{:S(2)}) %collective-permute-start.13) | collective-permute-done | bytes 65568 | tf_op jit(solution)/shard_map/ppermute | solution.py:30
  71.8 3.8 %all-to-all-start.2 = ((bf16[4,4,64,512]{3,2,1,0:T(8,128)(2,1)}), bf16[4,4,64,512]{3,2,1,0:T(8,128)(2,1)S(1)}, u32[]{:S(2)}, u32[]{:S(2)}) async-start(bf16[4,4,64,512]{3,2,1,0:T(8,128)(2,1)} %copy-done), calls=%async_computation.2 | async-start | bytes 2097152 | tf_op jit(solution)/shard_map/all_to_all | solution.py:38
  75.6 1.9 %collective-permute-start.16 = (bf16[128,256]{1,0:T(8,128)(2,1)S(1)}, bf16[128,256]{1,0:T(8,128)(2,1)S(1)}, u32[]{:S(2)}, u32[]{:S(2)}) collective-permute-start(bf16[128,256]{1,0:T(8,128)(2,1)S(1)} %get-tuple-element.43.own), channel_id=1, source_target_pairs={{0,8},{8,16},{16,24},{24,32},{32,40},{40,48},{48,56},{56,64},{64,7... | collective-permute-start | bytes 196616 | tf_op jit(solution)/shard_map/ppermute | solution.py:50
  77.5 3.4 %collective-permute-start.17 = (bf16[128,256]{1,0:T(8,128)(2,1)S(1)}, bf16[128,256]{1,0:T(8,128)(2,1)S(1)}, u32[]{:S(2)}, u32[]{:S(2)}) collective-permute-start(bf16[128,256]{1,0:T(8,128)(2,1)S(1)} %get-tuple-element.43.own), channel_id=1, source_target_pairs={{8,0},{16,8},{24,16},{32,24},{40,32},{48,40},{56,48},{64,56},{72,6... | collective-permute-start | bytes 196616 | tf_op jit(solution)/shard_map/ppermute | solution.py:54
  80.9 3.8 %collective-permute-done.17.after = bf16[128,256]{1,0:T(8,128)(2,1)S(1)} collective-permute-done((bf16[128,256]{1,0:T(8,128)(2,1)S(1)}, bf16[128,256]{1,0:T(8,128)(2,1)S(1)}, u32[]{:S(2)}, u32[]{:S(2)}) %collective-permute-start.17) | collective-permute-done | bytes 65568 | tf_op jit(solution)/shard_map/ppermute | solution.py:54
  86.2 3.4 %collective-permute-start.19 = (bf16[128,256]{1,0:T(8,128)(2,1)S(1)}, bf16[128,256]{1,0:T(8,128)(2,1)S(1)}, u32[]{:S(2)}, u32[]{:S(2)}) collective-permute-start(bf16[128,256]{1,0:T(8,128)(2,1)S(1)} %get-tuple-element.46), channel_id=1, source_target_pairs={{0,4},{2,6},{4,0},{6,2},{1,5},{3,7},{5,1},{7,3},{8,12},{10,14},{12... | collective-permute-start | bytes 196616 | tf_op jit(solution)/shard_map/ppermute | solution.py:243
  90.4 1.6 %collective-permute-done.19.r2 = bf16[128,256]{1,0:T(8,128)(2,1)S(1)} collective-permute-done((bf16[128,256]{1,0:T(8,128)(2,1)S(1)}, bf16[128,256]{1,0:T(8,128)(2,1)S(1)}, u32[]{:S(2)}, u32[]{:S(2)}) %collective-permute-start.19) | collective-permute-done | bytes 65568 | tf_op jit(solution)/shard_map/ppermute | solution.py:243
  92.8 4.5 %collective-permute-start.21 = (f32[128,256]{1,0:T(8,128)S(1)}, f32[128,256]{1,0:T(8,128)S(1)}, u32[]{:S(2)}, u32[]{:S(2)}) collective-permute-start(f32[128,256]{1,0:T(8,128)S(1)} %shard_map.93.mine), channel_id=1, source_target_pairs={{0,1},{1,0},{2,3},{3,2},{4,5},{5,4},{6,7},{7,6},{8,9},{9,8},{10,11... | collective-permute-start | bytes 393224 | tf_op jit(solution)/shard_map/ppermute | solution.py:46
  98.4 2.5 %collective-permute-start.23 = (bf16[128,256]{1,0:T(8,128)(2,1)S(1)}, bf16[128,256]{1,0:T(8,128)(2,1)S(1)}, u32[]{:S(2)}, u32[]{:S(2)}) collective-permute-start(bf16[128,256]{1,0:T(8,128)(2,1)S(1)} %shard_map.94.x0), channel_id=1, source_target_pairs={{0,4},{2,6},{4,0},{6,2},{1,5},{3,7},{5,1},{7,3},{8,12},{10,14},{12... | collective-permute-start | bytes 196616 | tf_op jit(solution)/shard_map/ppermute | solution.py:30
  101.7 1.8 %collective-permute-done.22.x1 = bf16[128,256]{1,0:T(8,128)(2,1)S(1)} collective-permute-done((bf16[128,256]{1,0:T(8,128)(2,1)S(1)}, bf16[128,256]{1,0:T(8,128)(2,1)S(1)}, u32[]{:S(2)}, u32[]{:S(2)}) %collective-permute-start.22) | collective-permute-done | bytes 65568 | tf_op jit(solution)/shard_map/ppermute | solution.py:30
  105.1 1.9 %collective-permute-start.25 = (bf16[128,256]{1,0:T(8,128)(2,1)S(1)}, bf16[128,256]{1,0:T(8,128)(2,1)S(1)}, u32[]{:S(2)}, u32[]{:S(2)}) collective-permute-start(bf16[128,256]{1,0:T(8,128)(2,1)S(1)} %get-tuple-element.50.own), channel_id=1, source_target_pairs={{0,8},{8,16},{16,24},{24,32},{32,40},{40,48},{48,56},{56,64},{64,7... | collective-permute-start | bytes 196616 | tf_op jit(solution)/shard_map/ppermute | solution.py:50
  107.1 3.4 %collective-permute-start.26 = (bf16[128,256]{1,0:T(8,128)(2,1)S(1)}, bf16[128,256]{1,0:T(8,128)(2,1)S(1)}, u32[]{:S(2)}, u32[]{:S(2)}) collective-permute-start(bf16[128,256]{1,0:T(8,128)(2,1)S(1)} %get-tuple-element.50.own), channel_id=1, source_target_pairs={{8,0},{16,8},{24,16},{32,24},{40,32},{48,40},{56,48},{64,56},{72,6... | collective-permute-start | bytes 196616 | tf_op jit(solution)/shard_map/ppermute | solution.py:54
  110.4 3.7 %collective-permute-done.26.after = bf16[128,256]{1,0:T(8,128)(2,1)S(1)} collective-permute-done((bf16[128,256]{1,0:T(8,128)(2,1)S(1)}, bf16[128,256]{1,0:T(8,128)(2,1)S(1)}, u32[]{:S(2)}, u32[]{:S(2)}) %collective-permute-start.26) | collective-permute-done | bytes 65568 | tf_op jit(solution)/shard_map/ppermute | solution.py:54
  116.4 2.4 %collective-permute-start.28 = (bf16[128,256]{1,0:T(8,128)(2,1)S(1)}, bf16[128,256]{1,0:T(8,128)(2,1)S(1)}, u32[]{:S(2)}, u32[]{:S(2)}) collective-permute-start(bf16[128,256]{1,0:T(8,128)(2,1)S(1)} %get-tuple-element.53), channel_id=1, source_target_pairs={{0,4},{2,6},{4,0},{6,2},{1,5},{3,7},{5,1},{7,3},{8,12},{10,14},{12... | collective-permute-start | bytes 196616 | tf_op jit(solution)/shard_map/ppermute | solution.py:243
  119.5 1.6 %collective-permute-done.28.r2 = bf16[128,256]{1,0:T(8,128)(2,1)S(1)} collective-permute-done((bf16[128,256]{1,0:T(8,128)(2,1)S(1)}, bf16[128,256]{1,0:T(8,128)(2,1)S(1)}, u32[]{:S(2)}, u32[]{:S(2)}) %collective-permute-start.28) | collective-permute-done | bytes 65568 | tf_op jit(solution)/shard_map/ppermute | solution.py:243
  121.9 4.4 %collective-permute-start.30 = (f32[128,128]{1,0:T(8,128)S(1)}, f32[128,128]{1,0:T(8,128)S(1)}, u32[]{:S(2)}, u32[]{:S(2)}) collective-permute-start(f32[128,128]{1,0:T(8,128)S(1)} %get-tuple-element.56), channel_id=1, source_target_pairs={{0,1},{1,0},{2,3},{3,2},{4,5},{5,4},{6,7},{7,6},{8,9},{9,8},{10,11... | collective-permute-start | bytes 196616 | tf_op jit(solution)/shard_map/ppermute | solution.py:46
  (92 shorter events, 27.2 us)
Async XLA Ops:
  1.9 27.6 %all-to-all-start = ((bf16[16,64,512]{2,1,0:T(8,128)(2,1)}), bf16[16,64,512]{2,1,0:T(8,128)(2,1)S(1)}, u32[]{:S(2)}, u32[]{:S(2)}) async-start(bf16[16,64,512]{2,1,0:T(8,128)(2,1)} %shard_map.83), calls=%async_computation | async-start | bytes 2097152 | tf_op jit(solution)/shard_map/all_to_all | solution.py:38
  9.7 9.0 %collective-permute-start = (bf16[128,128]{1,0:T(8,128)(2,1)S(1)}, bf16[128,128]{1,0:T(8,128)(2,1)S(1)}, u32[]{:S(2)}, u32[]{:S(2)}) collective-permute-start(bf16[128,128]{1,0:T(8,128)(2,1)S(1)} %copy-done.18), channel_id=1, source_target_pairs={{0,2},{2,4},{4,6},{6,0},{1,3},{3,5},{5,7},{7,1},{8,10},{10,12},{12... | collective-permute-start | bytes 98312 | tf_op jit(solution)/shard_map/ppermute | solution.py:30
  11.0 7.6 %collective-permute-start.1 = (bf16[128,128]{1,0:T(8,128)(2,1)S(1)}, bf16[128,128]{1,0:T(8,128)(2,1)S(1)}, u32[]{:S(2)}, u32[]{:S(2)}) collective-permute-start(bf16[128,128]{1,0:T(8,128)(2,1)S(1)} %copy-done.18), channel_id=1, source_target_pairs={{0,4},{2,6},{4,0},{6,2},{1,5},{3,7},{5,1},{7,3},{8,12},{10,14},{12... | collective-permute-start | bytes 98312 | tf_op jit(solution)/shard_map/ppermute | solution.py:30
  13.7 5.0 %collective-permute-start.2 = (bf16[128,128]{1,0:T(8,128)(2,1)S(1)}, bf16[128,128]{1,0:T(8,128)(2,1)S(1)}, u32[]{:S(2)}, u32[]{:S(2)}) collective-permute-start(bf16[128,128]{1,0:T(8,128)(2,1)S(1)} %copy-done.18), channel_id=1, source_target_pairs={{0,6},{2,0},{4,2},{6,4},{1,7},{3,1},{5,3},{7,5},{8,14},{10,8},{12,... | collective-permute-start | bytes 98312 | tf_op jit(solution)/shard_map/ppermute | solution.py:30
  16.3 8.1 %collective-permute-start.6 = (bf16[2,64,512]{2,1,0:T(8,128)(2,1)S(1)}, bf16[2,64,512]{2,1,0:T(8,128)(2,1)S(1)}, u32[]{:S(2)}, u32[]{:S(2)}) collective-permute-start(bf16[2,64,512]{2,1,0:T(8,128)(2,1)S(1)} %get-tuple-element.36.p0), channel_id=1, source_target_pairs={{0,8},{8,16},{16,24},{24,0},{1,9},{9,17},{17,25},{25,1},{2,10},{10... | collective-permute-start | bytes 393224 | tf_op jit(solution)/shard_map/ppermute | solution.py:30
  16.4 8.6 %collective-permute-start.7 = (bf16[2,64,512]{2,1,0:T(8,128)(2,1)S(1)}, bf16[2,64,512]{2,1,0:T(8,128)(2,1)S(1)}, u32[]{:S(2)}, u32[]{:S(2)}) collective-permute-start(bf16[2,64,512]{2,1,0:T(8,128)(2,1)S(1)} %get-tuple-element.36.p0), channel_id=1, source_target_pairs={{0,16},{8,24},{16,0},{24,8},{1,17},{9,25},{17,1},{25,9},{2,18},{10... | collective-permute-start | bytes 393224 | tf_op jit(solution)/shard_map/ppermute | solution.py:30
  18.7 9.2 %collective-permute-start.8 = (bf16[2,64,512]{2,1,0:T(8,128)(2,1)S(1)}, bf16[2,64,512]{2,1,0:T(8,128)(2,1)S(1)}, u32[]{:S(2)}, u32[]{:S(2)}) collective-permute-start(bf16[2,64,512]{2,1,0:T(8,128)(2,1)S(1)} %get-tuple-element.36.p0), channel_id=1, source_target_pairs={{0,24},{8,0},{16,8},{24,16},{1,25},{9,1},{17,9},{25,17},{2,26},{10... | collective-permute-start | bytes 393224 | tf_op jit(solution)/shard_map/ppermute | solution.py:30
  18.7 10.8 %collective-permute-start.3 = (bf16[4,128,128]{2,1,0:T(8,128)(2,1)S(1)}, bf16[4,128,128]{2,1,0:T(8,128)(2,1)S(1)}, u32[]{:S(2)}, u32[]{:S(2)}) collective-permute-start(bf16[4,128,128]{2,1,0:T(8,128)(2,1)S(1)} %pad_maximum_fusion.own), channel_id=1, source_target_pairs={{0,1},{1,0},{2,3},{3,2},{4,5},{5,4},{6,7},{7,6},{8,9},{9,8},{10,11... | collective-permute-start | bytes 393224 | tf_op jit(solution)/shard_map/ppermute | solution.py:46
  30.2 40.5 %all-to-all-start.1 = ((bf16[4,4,64,512]{3,2,1,0:T(8,128)(2,1)}), bf16[4,4,64,512]{3,2,1,0:T(8,128)(2,1)S(1)}, u32[]{:S(2)}, u32[]{:S(2)}) async-start(bf16[4,4,64,512]{3,2,1,0:T(8,128)(2,1)} %copy-done.1), calls=%async_computation.1 | async-start | bytes 2097152 | tf_op jit(solution)/shard_map/all_to_all | solution.py:38
  34.2 6.8 %collective-permute-start.4 = (bf16[144,256]{1,0:T(8,128)(2,1)S(1)}, bf16[144,256]{1,0:T(8,128)(2,1)S(1)}, u32[]{:S(2)}, u32[]{:S(2)}) collective-permute-start(bf16[144,256]{1,0:T(8,128)(2,1)S(1)} %get-tuple-element.34.own), channel_id=1, source_target_pairs={{0,8},{8,16},{16,24},{24,32},{32,40},{40,48},{48,56},{56,64},{64,7... | collective-permute-start | bytes 221192 | tf_op jit(solution)/shard_map/ppermute | solution.py:50
  39.0 7.5 %collective-permute-start.5 = (bf16[144,256]{1,0:T(8,128)(2,1)S(1)}, bf16[144,256]{1,0:T(8,128)(2,1)S(1)}, u32[]{:S(2)}, u32[]{:S(2)}) collective-permute-start(bf16[144,256]{1,0:T(8,128)(2,1)S(1)} %get-tuple-element.34.own), channel_id=1, source_target_pairs={{8,0},{16,8},{24,16},{32,24},{40,32},{48,40},{56,48},{64,56},{72,6... | collective-permute-start | bytes 221192 | tf_op jit(solution)/shard_map/ppermute | solution.py:54
  49.9 5.5 %collective-permute-start.10 = (bf16[128,256]{1,0:T(8,128)(2,1)S(1)}, bf16[128,256]{1,0:T(8,128)(2,1)S(1)}, u32[]{:S(2)}, u32[]{:S(2)}) collective-permute-start(bf16[128,256]{1,0:T(8,128)(2,1)S(1)} %get-tuple-element.39), channel_id=1, source_target_pairs={{0,4},{2,6},{4,0},{6,2},{1,5},{3,7},{5,1},{7,3},{8,12},{10,14},{12... | collective-permute-start | bytes 196616 | tf_op jit(solution)/shard_map/ppermute | solution.py:243
  52.9 3.1 %collective-permute-start.11 = (bf16[128,256]{1,0:T(8,128)(2,1)S(1)}, bf16[128,256]{1,0:T(8,128)(2,1)S(1)}, u32[]{:S(2)}, u32[]{:S(2)}) collective-permute-start(bf16[128,256]{1,0:T(8,128)(2,1)S(1)} %get-tuple-element.40), channel_id=1, source_target_pairs={{0,6},{2,0},{4,2},{6,4},{1,7},{3,1},{5,3},{7,5},{8,14},{10,8},{12,... | collective-permute-start | bytes 196616 | tf_op jit(solution)/shard_map/ppermute | solution.py:242
  53.7 4.6 %collective-permute-start.9 = (bf16[128,256]{1,0:T(8,128)(2,1)S(1)}, bf16[128,256]{1,0:T(8,128)(2,1)S(1)}, u32[]{:S(2)}, u32[]{:S(2)}) collective-permute-start(bf16[128,256]{1,0:T(8,128)(2,1)S(1)} %get-tuple-element.38), channel_id=1, source_target_pairs={{0,2},{2,4},{4,6},{6,0},{1,3},{3,5},{5,7},{7,1},{8,10},{10,12},{12... | collective-permute-start | bytes 196616 | tf_op jit(solution)/shard_map/ppermute | solution.py:241
  58.4 5.9 %collective-permute-start.12 = (f32[128,256]{1,0:T(8,128)S(1)}, f32[128,256]{1,0:T(8,128)S(1)}, u32[]{:S(2)}, u32[]{:S(2)}) collective-permute-start(f32[128,256]{1,0:T(8,128)S(1)} %shard_map.88.mine), channel_id=1, source_target_pairs={{0,1},{1,0},{2,3},{3,2},{4,5},{5,4},{6,7},{7,6},{8,9},{9,8},{10,11... | collective-permute-start | bytes 393224 | tf_op jit(solution)/shard_map/ppermute | solution.py:46
  64.3 6.3 %collective-permute-start.13 = (bf16[128,256]{1,0:T(8,128)(2,1)S(1)}, bf16[128,256]{1,0:T(8,128)(2,1)S(1)}, u32[]{:S(2)}, u32[]{:S(2)}) collective-permute-start(bf16[128,256]{1,0:T(8,128)(2,1)S(1)} %shard_map.89.x0), channel_id=1, source_target_pairs={{0,2},{2,4},{4,6},{6,0},{1,3},{3,5},{5,7},{7,1},{8,10},{10,12},{12... | collective-permute-start | bytes 196616 | tf_op jit(solution)/shard_map/ppermute | solution.py:30
  64.4 6.2 %collective-permute-start.14 = (bf16[128,256]{1,0:T(8,128)(2,1)S(1)}, bf16[128,256]{1,0:T(8,128)(2,1)S(1)}, u32[]{:S(2)}, u32[]{:S(2)}) collective-permute-start(bf16[128,256]{1,0:T(8,128)(2,1)S(1)} %shard_map.89.x0), channel_id=1, source_target_pairs={{0,4},{2,6},{4,0},{6,2},{1,5},{3,7},{5,1},{7,3},{8,12},{10,14},{12... | collective-permute-start | bytes 196616 | tf_op jit(solution)/shard_map/ppermute | solution.py:30
  65.3 5.3 %collective-permute-start.15 = (bf16[128,256]{1,0:T(8,128)(2,1)S(1)}, bf16[128,256]{1,0:T(8,128)(2,1)S(1)}, u32[]{:S(2)}, u32[]{:S(2)}) collective-permute-start(bf16[128,256]{1,0:T(8,128)(2,1)S(1)} %shard_map.89.x0), channel_id=1, source_target_pairs={{0,6},{2,0},{4,2},{6,4},{1,7},{3,1},{5,3},{7,5},{8,14},{10,8},{12,... | collective-permute-start | bytes 196616 | tf_op jit(solution)/shard_map/ppermute | solution.py:30
  71.8 32.9 %all-to-all-start.2 = ((bf16[4,4,64,512]{3,2,1,0:T(8,128)(2,1)}), bf16[4,4,64,512]{3,2,1,0:T(8,128)(2,1)S(1)}, u32[]{:S(2)}, u32[]{:S(2)}) async-start(bf16[4,4,64,512]{3,2,1,0:T(8,128)(2,1)} %copy-done), calls=%async_computation.2 | async-start | bytes 2097152 | tf_op jit(solution)/shard_map/all_to_all | solution.py:38
  75.6 5.3 %collective-permute-start.16 = (bf16[128,256]{1,0:T(8,128)(2,1)S(1)}, bf16[128,256]{1,0:T(8,128)(2,1)S(1)}, u32[]{:S(2)}, u32[]{:S(2)}) collective-permute-start(bf16[128,256]{1,0:T(8,128)(2,1)S(1)} %get-tuple-element.43.own), channel_id=1, source_target_pairs={{0,8},{8,16},{16,24},{24,32},{32,40},{40,48},{48,56},{56,64},{64,7... | collective-permute-start | bytes 196616 | tf_op jit(solution)/shard_map/ppermute | solution.py:50
  77.5 7.2 %collective-permute-start.17 = (bf16[128,256]{1,0:T(8,128)(2,1)S(1)}, bf16[128,256]{1,0:T(8,128)(2,1)S(1)}, u32[]{:S(2)}, u32[]{:S(2)}) collective-permute-start(bf16[128,256]{1,0:T(8,128)(2,1)S(1)} %get-tuple-element.43.own), channel_id=1, source_target_pairs={{8,0},{16,8},{24,16},{32,24},{40,32},{48,40},{56,48},{64,56},{72,6... | collective-permute-start | bytes 196616 | tf_op jit(solution)/shard_map/ppermute | solution.py:54
  85.7 4.8 %collective-permute-start.18 = (bf16[128,256]{1,0:T(8,128)(2,1)S(1)}, bf16[128,256]{1,0:T(8,128)(2,1)S(1)}, u32[]{:S(2)}, u32[]{:S(2)}) collective-permute-start(bf16[128,256]{1,0:T(8,128)(2,1)S(1)} %get-tuple-element.45), channel_id=1, source_target_pairs={{0,2},{2,4},{4,6},{6,0},{1,3},{3,5},{5,7},{7,1},{8,10},{10,12},{12... | collective-permute-start | bytes 196616 | tf_op jit(solution)/shard_map/ppermute | solution.py:241
  86.2 5.8 %collective-permute-start.19 = (bf16[128,256]{1,0:T(8,128)(2,1)S(1)}, bf16[128,256]{1,0:T(8,128)(2,1)S(1)}, u32[]{:S(2)}, u32[]{:S(2)}) collective-permute-start(bf16[128,256]{1,0:T(8,128)(2,1)S(1)} %get-tuple-element.46), channel_id=1, source_target_pairs={{0,4},{2,6},{4,0},{6,2},{1,5},{3,7},{5,1},{7,3},{8,12},{10,14},{12... | collective-permute-start | bytes 196616 | tf_op jit(solution)/shard_map/ppermute | solution.py:243
  92.8 5.5 %collective-permute-start.21 = (f32[128,256]{1,0:T(8,128)S(1)}, f32[128,256]{1,0:T(8,128)S(1)}, u32[]{:S(2)}, u32[]{:S(2)}) collective-permute-start(f32[128,256]{1,0:T(8,128)S(1)} %shard_map.93.mine), channel_id=1, source_target_pairs={{0,1},{1,0},{2,3},{3,2},{4,5},{5,4},{6,7},{7,6},{8,9},{9,8},{10,11... | collective-permute-start | bytes 393224 | tf_op jit(solution)/shard_map/ppermute | solution.py:46
  98.3 5.1 %collective-permute-start.22 = (bf16[128,256]{1,0:T(8,128)(2,1)S(1)}, bf16[128,256]{1,0:T(8,128)(2,1)S(1)}, u32[]{:S(2)}, u32[]{:S(2)}) collective-permute-start(bf16[128,256]{1,0:T(8,128)(2,1)S(1)} %shard_map.94.x0), channel_id=1, source_target_pairs={{0,2},{2,4},{4,6},{6,0},{1,3},{3,5},{5,7},{7,1},{8,10},{10,12},{12... | collective-permute-start | bytes 196616 | tf_op jit(solution)/shard_map/ppermute | solution.py:30
  98.4 5.4 %collective-permute-start.23 = (bf16[128,256]{1,0:T(8,128)(2,1)S(1)}, bf16[128,256]{1,0:T(8,128)(2,1)S(1)}, u32[]{:S(2)}, u32[]{:S(2)}) collective-permute-start(bf16[128,256]{1,0:T(8,128)(2,1)S(1)} %shard_map.94.x0), channel_id=1, source_target_pairs={{0,4},{2,6},{4,0},{6,2},{1,5},{3,7},{5,1},{7,3},{8,12},{10,14},{12... | collective-permute-start | bytes 196616 | tf_op jit(solution)/shard_map/ppermute | solution.py:30
  100.9 3.7 %collective-permute-start.24 = (bf16[128,256]{1,0:T(8,128)(2,1)S(1)}, bf16[128,256]{1,0:T(8,128)(2,1)S(1)}, u32[]{:S(2)}, u32[]{:S(2)}) collective-permute-start(bf16[128,256]{1,0:T(8,128)(2,1)S(1)} %shard_map.94.x0), channel_id=1, source_target_pairs={{0,6},{2,0},{4,2},{6,4},{1,7},{3,1},{5,3},{7,5},{8,14},{10,8},{12,... | collective-permute-start | bytes 196616 | tf_op jit(solution)/shard_map/ppermute | solution.py:30
  105.1 5.3 %collective-permute-start.25 = (bf16[128,256]{1,0:T(8,128)(2,1)S(1)}, bf16[128,256]{1,0:T(8,128)(2,1)S(1)}, u32[]{:S(2)}, u32[]{:S(2)}) collective-permute-start(bf16[128,256]{1,0:T(8,128)(2,1)S(1)} %get-tuple-element.50.own), channel_id=1, source_target_pairs={{0,8},{8,16},{16,24},{24,32},{32,40},{40,48},{48,56},{56,64},{64,7... | collective-permute-start | bytes 196616 | tf_op jit(solution)/shard_map/ppermute | solution.py:50
  107.1 7.1 %collective-permute-start.26 = (bf16[128,256]{1,0:T(8,128)(2,1)S(1)}, bf16[128,256]{1,0:T(8,128)(2,1)S(1)}, u32[]{:S(2)}, u32[]{:S(2)}) collective-permute-start(bf16[128,256]{1,0:T(8,128)(2,1)S(1)} %get-tuple-element.50.own), channel_id=1, source_target_pairs={{8,0},{16,8},{24,16},{32,24},{40,32},{48,40},{56,48},{64,56},{72,6... | collective-permute-start | bytes 196616 | tf_op jit(solution)/shard_map/ppermute | solution.py:54
  115.1 4.4 %collective-permute-start.27 = (bf16[128,256]{1,0:T(8,128)(2,1)S(1)}, bf16[128,256]{1,0:T(8,128)(2,1)S(1)}, u32[]{:S(2)}, u32[]{:S(2)}) collective-permute-start(bf16[128,256]{1,0:T(8,128)(2,1)S(1)} %get-tuple-element.52), channel_id=1, source_target_pairs={{0,2},{2,4},{4,6},{6,0},{1,3},{3,5},{5,7},{7,1},{8,10},{10,12},{12... | collective-permute-start | bytes 196616 | tf_op jit(solution)/shard_map/ppermute | solution.py:241
  116.4 4.7 %collective-permute-start.28 = (bf16[128,256]{1,0:T(8,128)(2,1)S(1)}, bf16[128,256]{1,0:T(8,128)(2,1)S(1)}, u32[]{:S(2)}, u32[]{:S(2)}) collective-permute-start(bf16[128,256]{1,0:T(8,128)(2,1)S(1)} %get-tuple-element.53), channel_id=1, source_target_pairs={{0,4},{2,6},{4,0},{6,2},{1,5},{3,7},{5,1},{7,3},{8,12},{10,14},{12... | collective-permute-start | bytes 196616 | tf_op jit(solution)/shard_map/ppermute | solution.py:243
  121.9 5.3 %collective-permute-start.30 = (f32[128,128]{1,0:T(8,128)S(1)}, f32[128,128]{1,0:T(8,128)S(1)}, u32[]{:S(2)}, u32[]{:S(2)}) collective-permute-start(f32[128,128]{1,0:T(8,128)S(1)} %get-tuple-element.56), channel_id=1, source_target_pairs={{0,1},{1,0},{2,3},{3,2},{4,5},{5,4},{6,7},{7,6},{8,9},{9,8},{10,11... | collective-permute-start | bytes 196616 | tf_op jit(solution)/shard_map/ppermute | solution.py:46
  (21 other events, 124.3 us)

commit v12 on v8

--- a/solution.py
+++ b/solution.py
@@ -286,15 +286,16 @@
         )
         if layer == 2:
             break
-        if layer == 0:
-            kept = after_this(kept, many2)
         half = call(sum_body, shaped(128, 256, dtype=F32), kept, r1, r2, r3)
         stream = call(pair_sum_body, shaped(128, 256), half, swap(half))
         weights = next_weights
+        pieces = in_order(stream, spread(stream, "y"))
+        if layer == 0:
+            pieces = after_this(pieces, many2)
         q, kv = call(
             functools.partial(heads_pieces_body, layer=layer + 1),
             [shaped(128, 128), shaped(128, 256)],
-            *in_order(stream, spread(stream, "y")), norm_gain, weights,
+            *pieces, norm_gain, weights,
         )
     mine, theirs = call(split_body, [shaped(128, 128, dtype=F32)] * 2, kept, r1, r2, r3)
     return call(pair_sum_body, shaped(128, 128), mine, swap(theirs))

time: 127 us -> 128 us (level)
  the two profiles are of different devices: /device:TPU:39 before, /device:TPU:7 now
where the time goes in v12:
time: 128 us
  starting transfers between devices  78.5 us (61%)
  waiting for transfers between devices  38.2 us (30%)
  Pallas kernels  8.65 us (7%)
  local copies, waits for them, and re-layouts  2 us (2%)
    all_to_all x3, starting transfers between devices, gather_rows(): return lax.all_to_all(a, axes, 0, 0, tiled=True).reshape(1024, 512)  17.8 us
    ppermute x4, starting transfers between devices, swap(): return lax.ppermute(a, 'c', [(0, 1), (1, 0)])  15.9 us
    ppermute x12, starting transfers between devices, spread(): return [lax.ppermute(a, axis, turn(k)) for k in (1, 3, 2)]  14.2 us
    ppermute x3, waiting for transfers between devices, from_after(): return lax.ppermute(a, SP, [(i + 1, i) for i in range(15)])  10.9 us
    ppermute x3, starting transfers between devices, from_before(): return lax.ppermute(a, SP, [(i, i + 1) for i in range(15)])  10.8 us
    pallas_call x16, Pallas kernels, call(): pl.pallas_call(body, out_shape=outs, **specs, scratch_shapes=list(scratch...  8.65 us
    ppermute x3, starting transfers between devices, scattered(): r2 = lax.ppermute(s2, 'y', turn(2))  8.45 us
    ppermute x3, starting transfers between devices, from_after(): return lax.ppermute(a, SP, [(i + 1, i) for i in range(15)])  7.47 us
  transfers between devices with their start and end apart: 34, of which 22 were waited for; matrix products, arithmetic and copies ran while one was open for 0% of the time, Pallas kernels for 3%

profile of v12, /device:TPU:7, one launch (start us, length us, event | category | flops | bytes accessed | tf_op | source)
XLA Modules:
  0.0 127.7 jit_solution(2819551167931398706)
XLA Ops:
  0.0 1.9 %shard_map.83 = bf16[16,64,512]{2,1,0:T(8,128)(2,1)} custom-call(bf16[3,64,128]{2,1,0:T(8,128)(2,1)} %wq.3, bf16[3,64,128]{2,1,0:T(8,128)(2,1)} %wk.3, bf16[3,64,128]{2,1,0:T(8,128)(2,1)} %wv.3, bf16[3,64,128]{2,1,0:T(8,128)(2,1)} %bitcast.16), custom_call_target="tpu_custom_call" | custom-call | tf_op jit(solution)/shard_map/pallas_call | solution.py:66
  2.0 7.8 %all-to-all-start = ((bf16[16,64,512]{2,1,0:T(8,128)(2,1)}), bf16[16,64,512]{2,1,0:T(8,128)(2,1)S(1)}, u32[]{:S(2)}, u32[]{:S(2)}) async-start(bf16[16,64,512]{2,1,0:T(8,128)(2,1)} %shard_map.83), calls=%async_computation | async-start | bytes 2097152 | tf_op jit(solution)/shard_map/all_to_all | solution.py:38
  9.8 1.4 %collective-permute-start = (bf16[128,128]{1,0:T(8,128)(2,1)S(1)}, bf16[128,128]{1,0:T(8,128)(2,1)S(1)}, u32[]{:S(2)}, u32[]{:S(2)}) collective-permute-start(bf16[128,128]{1,0:T(8,128)(2,1)S(1)} %copy-done.5), channel_id=1, source_target_pairs={{0,2},{2,4},{4,6},{6,0},{1,3},{3,5},{5,7},{7,1},{8,10},{10,12},{12... | collective-permute-start | bytes 98312 | tf_op jit(solution)/shard_map/ppermute | solution.py:30
  11.2 2.6 %collective-permute-start.1 = (bf16[128,128]{1,0:T(8,128)(2,1)S(1)}, bf16[128,128]{1,0:T(8,128)(2,1)S(1)}, u32[]{:S(2)}, u32[]{:S(2)}) collective-permute-start(bf16[128,128]{1,0:T(8,128)(2,1)S(1)} %copy-done.5), channel_id=1, source_target_pairs={{0,4},{2,6},{4,0},{6,2},{1,5},{3,7},{5,1},{7,3},{8,12},{10,14},{12... | collective-permute-start | bytes 98312 | tf_op jit(solution)/shard_map/ppermute | solution.py:30
  17.1 2.5 %collective-permute-start.3 = (bf16[4,128,128]{2,1,0:T(8,128)(2,1)S(1)}, bf16[4,128,128]{2,1,0:T(8,128)(2,1)S(1)}, u32[]{:S(2)}, u32[]{:S(2)}) collective-permute-start(bf16[4,128,128]{2,1,0:T(8,128)(2,1)S(1)} %pad_maximum_fusion.own), channel_id=1, source_target_pairs={{0,1},{1,0},{2,3},{3,2},{4,5},{5,4},{6,7},{7,6},{8,9},{9,8},{10,11... | collective-permute-start | bytes 393224 | tf_op jit(solution)/shard_map/ppermute | solution.py:46
  20.6 3.5 %all-to-all-done = bf16[16,64,512]{2,1,0:T(8,128)(2,1)S(1)} async-done(((bf16[16,64,512]{2,1,0:T(8,128)(2,1)}), bf16[16,64,512]{2,1,0:T(8,128)(2,1)S(1)}, u32[]{:S(2)}, u32[]{:S(2)}) %all-to-all-start) | async-done | bytes 1048608 | tf_op jit(solution)/shard_map/all_to_all | solution.py:38
  24.7 6.0 %all-to-all-start.1 = ((bf16[16,64,512]{2,1,0:T(8,128)(2,1)}), bf16[16,64,512]{2,1,0:T(8,128)(2,1)S(1)}, u32[]{:S(2)}, u32[]{:S(2)}) async-start(bf16[16,64,512]{2,1,0:T(8,128)(2,1)} %copy-done.1), calls=%async_computation.1 | async-start | bytes 2097152 | tf_op jit(solution)/shard_map/all_to_all | solution.py:38
  30.7 3.1 %collective-permute-start.4 = (bf16[144,256]{1,0:T(8,128)(2,1)S(1)}, bf16[144,256]{1,0:T(8,128)(2,1)S(1)}, u32[]{:S(2)}, u32[]{:S(2)}) collective-permute-start(bf16[144,256]{1,0:T(8,128)(2,1)S(1)} %get-tuple-element.38.own), channel_id=1, source_target_pairs={{0,8},{8,16},{16,24},{24,32},{32,40},{40,48},{48,56},{56,64},{64,7... | collective-permute-start | bytes 221192 | tf_op jit(solution)/shard_map/ppermute | solution.py:50
  33.7 2.2 %collective-permute-start.5 = (bf16[144,256]{1,0:T(8,128)(2,1)S(1)}, bf16[144,256]{1,0:T(8,128)(2,1)S(1)}, u32[]{:S(2)}, u32[]{:S(2)}) collective-permute-start(bf16[144,256]{1,0:T(8,128)(2,1)S(1)} %get-tuple-element.38.own), channel_id=1, source_target_pairs={{8,0},{16,8},{24,16},{32,24},{40,32},{48,40},{56,48},{64,56},{72,6... | collective-permute-start | bytes 221192 | tf_op jit(solution)/shard_map/ppermute | solution.py:54
  35.9 7.3 %collective-permute-done.4.before = bf16[144,256]{1,0:T(8,128)(2,1)S(1)} collective-permute-done((bf16[144,256]{1,0:T(8,128)(2,1)S(1)}, bf16[144,256]{1,0:T(8,128)(2,1)S(1)}, u32[]{:S(2)}, u32[]{:S(2)}) %collective-permute-start.4) | collective-permute-done | bytes 73760 | tf_op jit(solution)/shard_map/ppermute | solution.py:50
  43.2 1.7 %collective-permute-done.5.after = bf16[144,256]{1,0:T(8,128)(2,1)S(1)} collective-permute-done((bf16[144,256]{1,0:T(8,128)(2,1)S(1)}, bf16[144,256]{1,0:T(8,128)(2,1)S(1)}, u32[]{:S(2)}, u32[]{:S(2)}) %collective-permute-start.5) | collective-permute-done | bytes 73760 | tf_op jit(solution)/shard_map/ppermute | solution.py:54
  46.4 1.4 %collective-permute-start.6 = (bf16[128,256]{1,0:T(8,128)(2,1)S(1)}, bf16[128,256]{1,0:T(8,128)(2,1)S(1)}, u32[]{:S(2)}, u32[]{:S(2)}) collective-permute-start(bf16[128,256]{1,0:T(8,128)(2,1)S(1)} %get-tuple-element.41), channel_id=1, source_target_pairs={{0,2},{2,4},{4,6},{6,0},{1,3},{3,5},{5,7},{7,1},{8,10},{10,12},{12... | collective-permute-start | bytes 196616 | tf_op jit(solution)/shard_map/ppermute | solution.py:243
  47.8 2.6 %collective-permute-start.7 = (bf16[128,256]{1,0:T(8,128)(2,1)S(1)}, bf16[128,256]{1,0:T(8,128)(2,1)S(1)}, u32[]{:S(2)}, u32[]{:S(2)}) collective-permute-start(bf16[128,256]{1,0:T(8,128)(2,1)S(1)} %get-tuple-element.42), channel_id=1, source_target_pairs={{0,4},{2,6},{4,0},{6,2},{1,5},{3,7},{5,1},{7,3},{8,12},{10,14},{12... | collective-permute-start | bytes 196616 | tf_op jit(solution)/shard_map/ppermute | solution.py:245
  53.9 3.7 %collective-permute-start.9 = (f32[128,256]{1,0:T(8,128)S(1)}, f32[128,256]{1,0:T(8,128)S(1)}, u32[]{:S(2)}, u32[]{:S(2)}) collective-permute-start(f32[128,256]{1,0:T(8,128)S(1)} %shard_map.87.mine), channel_id=1, source_target_pairs={{0,1},{1,0},{2,3},{3,2},{4,5},{5,4},{6,7},{7,6},{8,9},{9,8},{10,11... | collective-permute-start | bytes 393224 | tf_op jit(solution)/shard_map/ppermute | solution.py:46
  57.6 1.4 %collective-permute-start.14 = (bf16[64,512]{1,0:T(8,128)(2,1)S(1)}, bf16[64,512]{1,0:T(8,128)(2,1)S(1)}, u32[]{:S(2)}, u32[]{:S(2)}) collective-permute-start(bf16[64,512]{1,0:T(8,128)(2,1)S(1)} %get-tuple-element.44.p0), channel_id=1, source_target_pairs={{0,16},{8,24},{16,0},{24,8},{1,17},{9,25},{17,1},{25,9},{2,18},{10... | collective-permute-start | bytes 196616 | tf_op jit(solution)/shard_map/ppermute | solution.py:30
  59.2 3.4 %collective-permute-start.11 = (bf16[128,256]{1,0:T(8,128)(2,1)S(1)}, bf16[128,256]{1,0:T(8,128)(2,1)S(1)}, u32[]{:S(2)}, u32[]{:S(2)}) collective-permute-start(bf16[128,256]{1,0:T(8,128)(2,1)S(1)} %shard_map.88.x0), channel_id=1, source_target_pairs={{0,4},{2,6},{4,0},{6,2},{1,5},{3,7},{5,1},{7,3},{8,12},{10,14},{12... | collective-permute-start | bytes 196616 | tf_op jit(solution)/shard_map/ppermute | solution.py:30
  65.1 1.6 %collective-permute-done.12.x3 = bf16[128,256]{1,0:T(8,128)(2,1)S(1)} collective-permute-done((bf16[128,256]{1,0:T(8,128)(2,1)S(1)}, bf16[128,256]{1,0:T(8,128)(2,1)S(1)}, u32[]{:S(2)}, u32[]{:S(2)}) %collective-permute-start.12) | collective-permute-done | bytes 65568 | tf_op jit(solution)/shard_map/ppermute | solution.py:30
  67.1 4.0 %all-to-all-start.2 = ((bf16[4,4,64,512]{3,2,1,0:T(8,128)(2,1)}), bf16[4,4,64,512]{3,2,1,0:T(8,128)(2,1)S(1)}, u32[]{:S(2)}, u32[]{:S(2)}) async-start(bf16[4,4,64,512]{3,2,1,0:T(8,128)(2,1)} %copy-done), calls=%async_computation.2 | async-start | bytes 2097152 | tf_op jit(solution)/shard_map/all_to_all | solution.py:38
  71.1 5.8 %collective-permute-start.16 = (bf16[128,256]{1,0:T(8,128)(2,1)S(1)}, bf16[128,256]{1,0:T(8,128)(2,1)S(1)}, u32[]{:S(2)}, u32[]{:S(2)}) collective-permute-start(bf16[128,256]{1,0:T(8,128)(2,1)S(1)} %get-tuple-element.51.own), channel_id=1, source_target_pairs={{0,8},{8,16},{16,24},{24,32},{32,40},{40,48},{48,56},{56,64},{64,7... | collective-permute-start | bytes 196616 | tf_op jit(solution)/shard_map/ppermute | solution.py:50
  76.9 1.9 %collective-permute-start.17 = (bf16[128,256]{1,0:T(8,128)(2,1)S(1)}, bf16[128,256]{1,0:T(8,128)(2,1)S(1)}, u32[]{:S(2)}, u32[]{:S(2)}) collective-permute-start(bf16[128,256]{1,0:T(8,128)(2,1)S(1)} %get-tuple-element.51.own), channel_id=1, source_target_pairs={{8,0},{16,8},{24,16},{32,24},{40,32},{48,40},{56,48},{64,56},{72,6... | collective-permute-start | bytes 196616 | tf_op jit(solution)/shard_map/ppermute | solution.py:54
  78.8 5.5 %collective-permute-done.17.after = bf16[128,256]{1,0:T(8,128)(2,1)S(1)} collective-permute-done((bf16[128,256]{1,0:T(8,128)(2,1)S(1)}, bf16[128,256]{1,0:T(8,128)(2,1)S(1)}, u32[]{:S(2)}, u32[]{:S(2)}) %collective-permute-start.17) | collective-permute-done | bytes 65568 | tf_op jit(solution)/shard_map/ppermute | solution.py:54
  85.3 3.4 %collective-permute-start.19 = (bf16[128,256]{1,0:T(8,128)(2,1)S(1)}, bf16[128,256]{1,0:T(8,128)(2,1)S(1)}, u32[]{:S(2)}, u32[]{:S(2)}) collective-permute-start(bf16[128,256]{1,0:T(8,128)(2,1)S(1)} %get-tuple-element.54), channel_id=1, source_target_pairs={{0,4},{2,6},{4,0},{6,2},{1,5},{3,7},{5,1},{7,3},{8,12},{10,14},{12... | collective-permute-start | bytes 196616 | tf_op jit(solution)/shard_map/ppermute | solution.py:245
  89.6 1.5 %collective-permute-done.19.r2 = bf16[128,256]{1,0:T(8,128)(2,1)S(1)} collective-permute-done((bf16[128,256]{1,0:T(8,128)(2,1)S(1)}, bf16[128,256]{1,0:T(8,128)(2,1)S(1)}, u32[]{:S(2)}, u32[]{:S(2)}) %collective-permute-start.19) | collective-permute-done | bytes 65568 | tf_op jit(solution)/shard_map/ppermute | solution.py:245
  91.9 5.2 %collective-permute-start.21 = (f32[128,256]{1,0:T(8,128)S(1)}, f32[128,256]{1,0:T(8,128)S(1)}, u32[]{:S(2)}, u32[]{:S(2)}) collective-permute-start(f32[128,256]{1,0:T(8,128)S(1)} %shard_map.92.mine), channel_id=1, source_target_pairs={{0,1},{1,0},{2,3},{3,2},{4,5},{5,4},{6,7},{7,6},{8,9},{9,8},{10,11... | collective-permute-start | bytes 393224 | tf_op jit(solution)/shard_map/ppermute | solution.py:46
  98.2 2.3 %collective-permute-start.23 = (bf16[128,256]{1,0:T(8,128)(2,1)S(1)}, bf16[128,256]{1,0:T(8,128)(2,1)S(1)}, u32[]{:S(2)}, u32[]{:S(2)}) collective-permute-start(bf16[128,256]{1,0:T(8,128)(2,1)S(1)} %shard_map.93.x0), channel_id=1, source_target_pairs={{0,4},{2,6},{4,0},{6,2},{1,5},{3,7},{5,1},{7,3},{8,12},{10,14},{12... | collective-permute-start | bytes 196616 | tf_op jit(solution)/shard_map/ppermute | solution.py:30
  101.5 2.0 %collective-permute-done.22.x1 = bf16[128,256]{1,0:T(8,128)(2,1)S(1)} collective-permute-done((bf16[128,256]{1,0:T(8,128)(2,1)S(1)}, bf16[128,256]{1,0:T(8,128)(2,1)S(1)}, u32[]{:S(2)}, u32[]{:S(2)}) %collective-permute-start.22) | collective-permute-done | bytes 65568 | tf_op jit(solution)/shard_map/ppermute | solution.py:30
  104.9 1.9 %collective-permute-start.25 = (bf16[128,256]{1,0:T(8,128)(2,1)S(1)}, bf16[128,256]{1,0:T(8,128)(2,1)S(1)}, u32[]{:S(2)}, u32[]{:S(2)}) collective-permute-start(bf16[128,256]{1,0:T(8,128)(2,1)S(1)} %get-tuple-element.58.own), channel_id=1, source_target_pairs={{0,8},{8,16},{16,24},{24,32},{32,40},{40,48},{48,56},{56,64},{64,7... | collective-permute-start | bytes 196616 | tf_op jit(solution)/shard_map/ppermute | solution.py:50
  106.8 3.4 %collective-permute-start.26 = (bf16[128,256]{1,0:T(8,128)(2,1)S(1)}, bf16[128,256]{1,0:T(8,128)(2,1)S(1)}, u32[]{:S(2)}, u32[]{:S(2)}) collective-permute-start(bf16[128,256]{1,0:T(8,128)(2,1)S(1)} %get-tuple-element.58.own), channel_id=1, source_target_pairs={{8,0},{16,8},{24,16},{32,24},{40,32},{48,40},{56,48},{64,56},{72,6... | collective-permute-start | bytes 196616 | tf_op jit(solution)/shard_map/ppermute | solution.py:54
  110.2 3.7 %collective-permute-done.26.after = bf16[128,256]{1,0:T(8,128)(2,1)S(1)} collective-permute-done((bf16[128,256]{1,0:T(8,128)(2,1)S(1)}, bf16[128,256]{1,0:T(8,128)(2,1)S(1)}, u32[]{:S(2)}, u32[]{:S(2)}) %collective-permute-start.26) | collective-permute-done | bytes 65568 | tf_op jit(solution)/shard_map/ppermute | solution.py:54
  116.2 2.4 %collective-permute-start.28 = (bf16[128,256]{1,0:T(8,128)(2,1)S(1)}, bf16[128,256]{1,0:T(8,128)(2,1)S(1)}, u32[]{:S(2)}, u32[]{:S(2)}) collective-permute-start(bf16[128,256]{1,0:T(8,128)(2,1)S(1)} %get-tuple-element.61), channel_id=1, source_target_pairs={{0,4},{2,6},{4,0},{6,2},{1,5},{3,7},{5,1},{7,3},{8,12},{10,14},{12... | collective-permute-start | bytes 196616 | tf_op jit(solution)/shard_map/ppermute | solution.py:245
  119.3 1.6 %collective-permute-done.28.r2 = bf16[128,256]{1,0:T(8,128)(2,1)S(1)} collective-permute-done((bf16[128,256]{1,0:T(8,128)(2,1)S(1)}, bf16[128,256]{1,0:T(8,128)(2,1)S(1)}, u32[]{:S(2)}, u32[]{:S(2)}) %collective-permute-start.28) | collective-permute-done | bytes 65568 | tf_op jit(solution)/shard_map/ppermute | solution.py:245
  121.7 4.4 %collective-permute-start.30 = (f32[128,128]{1,0:T(8,128)S(1)}, f32[128,128]{1,0:T(8,128)S(1)}, u32[]{:S(2)}, u32[]{:S(2)}) collective-permute-start(f32[128,128]{1,0:T(8,128)S(1)} %get-tuple-element.64), channel_id=1, source_target_pairs={{0,1},{1,0},{2,3},{3,2},{4,5},{5,4},{6,7},{7,6},{8,9},{9,8},{10,11... | collective-permute-start | bytes 196616 | tf_op jit(solution)/shard_map/ppermute | solution.py:46
  (65 shorter events, 24.3 us)
Async XLA Ops:
  2.0 22.1 %all-to-all-start = ((bf16[16,64,512]{2,1,0:T(8,128)(2,1)}), bf16[16,64,512]{2,1,0:T(8,128)(2,1)S(1)}, u32[]{:S(2)}, u32[]{:S(2)}) async-start(bf16[16,64,512]{2,1,0:T(8,128)(2,1)} %shard_map.83), calls=%async_computation | async-start | bytes 2097152 | tf_op jit(solution)/shard_map/all_to_all | solution.py:38
  9.8 7.0 %collective-permute-start = (bf16[128,128]{1,0:T(8,128)(2,1)S(1)}, bf16[128,128]{1,0:T(8,128)(2,1)S(1)}, u32[]{:S(2)}, u32[]{:S(2)}) collective-permute-start(bf16[128,128]{1,0:T(8,128)(2,1)S(1)} %copy-done.5), channel_id=1, source_target_pairs={{0,2},{2,4},{4,6},{6,0},{1,3},{3,5},{5,7},{7,1},{8,10},{10,12},{12... | collective-permute-start | bytes 98312 | tf_op jit(solution)/shard_map/ppermute | solution.py:30
  11.2 5.7 %collective-permute-start.1 = (bf16[128,128]{1,0:T(8,128)(2,1)S(1)}, bf16[128,128]{1,0:T(8,128)(2,1)S(1)}, u32[]{:S(2)}, u32[]{:S(2)}) collective-permute-start(bf16[128,128]{1,0:T(8,128)(2,1)S(1)} %copy-done.5), channel_id=1, source_target_pairs={{0,4},{2,6},{4,0},{6,2},{1,5},{3,7},{5,1},{7,3},{8,12},{10,14},{12... | collective-permute-start | bytes 98312 | tf_op jit(solution)/shard_map/ppermute | solution.py:30
  13.8 3.3 %collective-permute-start.2 = (bf16[128,128]{1,0:T(8,128)(2,1)S(1)}, bf16[128,128]{1,0:T(8,128)(2,1)S(1)}, u32[]{:S(2)}, u32[]{:S(2)}) collective-permute-start(bf16[128,128]{1,0:T(8,128)(2,1)S(1)} %copy-done.5), channel_id=1, source_target_pairs={{0,6},{2,0},{4,2},{6,4},{1,7},{3,1},{5,3},{7,5},{8,14},{10,8},{12,... | collective-permute-start | bytes 98312 | tf_op jit(solution)/shard_map/ppermute | solution.py:30
  17.1 3.5 %collective-permute-start.3 = (bf16[4,128,128]{2,1,0:T(8,128)(2,1)S(1)}, bf16[4,128,128]{2,1,0:T(8,128)(2,1)S(1)}, u32[]{:S(2)}, u32[]{:S(2)}) collective-permute-start(bf16[4,128,128]{2,1,0:T(8,128)(2,1)S(1)} %pad_maximum_fusion.own), channel_id=1, source_target_pairs={{0,1},{1,0},{2,3},{3,2},{4,5},{5,4},{6,7},{7,6},{8,9},{9,8},{10,11... | collective-permute-start | bytes 393224 | tf_op jit(solution)/shard_map/ppermute | solution.py:46
  24.7 42.0 %all-to-all-start.1 = ((bf16[16,64,512]{2,1,0:T(8,128)(2,1)}), bf16[16,64,512]{2,1,0:T(8,128)(2,1)S(1)}, u32[]{:S(2)}, u32[]{:S(2)}) async-start(bf16[16,64,512]{2,1,0:T(8,128)(2,1)} %copy-done.1), calls=%async_computation.1 | async-start | bytes 2097152 | tf_op jit(solution)/shard_map/all_to_all | solution.py:38
  30.7 12.5 %collective-permute-start.4 = (bf16[144,256]{1,0:T(8,128)(2,1)S(1)}, bf16[144,256]{1,0:T(8,128)(2,1)S(1)}, u32[]{:S(2)}, u32[]{:S(2)}) collective-permute-start(bf16[144,256]{1,0:T(8,128)(2,1)S(1)} %get-tuple-element.38.own), channel_id=1, source_target_pairs={{0,8},{8,16},{16,24},{24,32},{32,40},{40,48},{48,56},{56,64},{64,7... | collective-permute-start | bytes 221192 | tf_op jit(solution)/shard_map/ppermute | solution.py:50
  33.7 11.2 %collective-permute-start.5 = (bf16[144,256]{1,0:T(8,128)(2,1)S(1)}, bf16[144,256]{1,0:T(8,128)(2,1)S(1)}, u32[]{:S(2)}, u32[]{:S(2)}) collective-permute-start(bf16[144,256]{1,0:T(8,128)(2,1)S(1)} %get-tuple-element.38.own), channel_id=1, source_target_pairs={{8,0},{16,8},{24,16},{32,24},{40,32},{48,40},{56,48},{64,56},{72,6... | collective-permute-start | bytes 221192 | tf_op jit(solution)/shard_map/ppermute | solution.py:54
  46.4 5.1 %collective-permute-start.6 = (bf16[128,256]{1,0:T(8,128)(2,1)S(1)}, bf16[128,256]{1,0:T(8,128)(2,1)S(1)}, u32[]{:S(2)}, u32[]{:S(2)}) collective-permute-start(bf16[128,256]{1,0:T(8,128)(2,1)S(1)} %get-tuple-element.41), channel_id=1, source_target_pairs={{0,2},{2,4},{4,6},{6,0},{1,3},{3,5},{5,7},{7,1},{8,10},{10,12},{12... | collective-permute-start | bytes 196616 | tf_op jit(solution)/shard_map/ppermute | solution.py:243
  47.8 5.0 %collective-permute-start.7 = (bf16[128,256]{1,0:T(8,128)(2,1)S(1)}, bf16[128,256]{1,0:T(8,128)(2,1)S(1)}, u32[]{:S(2)}, u32[]{:S(2)}) collective-permute-start(bf16[128,256]{1,0:T(8,128)(2,1)S(1)} %get-tuple-element.42), channel_id=1, source_target_pairs={{0,4},{2,6},{4,0},{6,2},{1,5},{3,7},{5,1},{7,3},{8,12},{10,14},{12... | collective-permute-start | bytes 196616 | tf_op jit(solution)/shard_map/ppermute | solution.py:245
  50.4 3.4 %collective-permute-start.8 = (bf16[128,256]{1,0:T(8,128)(2,1)S(1)}, bf16[128,256]{1,0:T(8,128)(2,1)S(1)}, u32[]{:S(2)}, u32[]{:S(2)}) collective-permute-start(bf16[128,256]{1,0:T(8,128)(2,1)S(1)} %get-tuple-element.43), channel_id=1, source_target_pairs={{0,6},{2,0},{4,2},{6,4},{1,7},{3,1},{5,3},{7,5},{8,14},{10,8},{12,... | collective-permute-start | bytes 196616 | tf_op jit(solution)/shard_map/ppermute | solution.py:244
  53.9 5.2 %collective-permute-start.9 = (f32[128,256]{1,0:T(8,128)S(1)}, f32[128,256]{1,0:T(8,128)S(1)}, u32[]{:S(2)}, u32[]{:S(2)}) collective-permute-start(f32[128,256]{1,0:T(8,128)S(1)} %shard_map.87.mine), channel_id=1, source_target_pairs={{0,1},{1,0},{2,3},{3,2},{4,5},{5,4},{6,7},{7,6},{8,9},{9,8},{10,11... | collective-permute-start | bytes 393224 | tf_op jit(solution)/shard_map/ppermute | solution.py:46
  57.6 5.0 %collective-permute-start.13 = (bf16[64,512]{1,0:T(8,128)(2,1)S(1)}, bf16[64,512]{1,0:T(8,128)(2,1)S(1)}, u32[]{:S(2)}, u32[]{:S(2)}) collective-permute-start(bf16[64,512]{1,0:T(8,128)(2,1)S(1)} %get-tuple-element.44.p0), channel_id=1, source_target_pairs={{0,8},{8,16},{16,24},{24,0},{1,9},{9,17},{17,25},{25,1},{2,10},{10... | collective-permute-start | bytes 196616 | tf_op jit(solution)/shard_map/ppermute | solution.py:30
  57.6 5.8 %collective-permute-start.14 = (bf16[64,512]{1,0:T(8,128)(2,1)S(1)}, bf16[64,512]{1,0:T(8,128)(2,1)S(1)}, u32[]{:S(2)}, u32[]{:S(2)}) collective-permute-start(bf16[64,512]{1,0:T(8,128)(2,1)S(1)} %get-tuple-element.44.p0), channel_id=1, source_target_pairs={{0,16},{8,24},{16,0},{24,8},{1,17},{9,25},{17,1},{25,9},{2,18},{10... | collective-permute-start | bytes 196616 | tf_op jit(solution)/shard_map/ppermute | solution.py:30
  59.0 4.6 %collective-permute-start.15 = (bf16[64,512]{1,0:T(8,128)(2,1)S(1)}, bf16[64,512]{1,0:T(8,128)(2,1)S(1)}, u32[]{:S(2)}, u32[]{:S(2)}) collective-permute-start(bf16[64,512]{1,0:T(8,128)(2,1)S(1)} %get-tuple-element.44.p0), channel_id=1, source_target_pairs={{0,24},{8,0},{16,8},{24,16},{1,25},{9,1},{17,9},{25,17},{2,26},{10... | collective-permute-start | bytes 196616 | tf_op jit(solution)/shard_map/ppermute | solution.py:30
  59.1 5.6 %collective-permute-start.10 = (bf16[128,256]{1,0:T(8,128)(2,1)S(1)}, bf16[128,256]{1,0:T(8,128)(2,1)S(1)}, u32[]{:S(2)}, u32[]{:S(2)}) collective-permute-start(bf16[128,256]{1,0:T(8,128)(2,1)S(1)} %shard_map.88.x0), channel_id=1, source_target_pairs={{0,2},{2,4},{4,6},{6,0},{1,3},{3,5},{5,7},{7,1},{8,10},{10,12},{12... | collective-permute-start | bytes 196616 | tf_op jit(solution)/shard_map/ppermute | solution.py:30
  59.2 5.9 %collective-permute-start.11 = (bf16[128,256]{1,0:T(8,128)(2,1)S(1)}, bf16[128,256]{1,0:T(8,128)(2,1)S(1)}, u32[]{:S(2)}, u32[]{:S(2)}) collective-permute-start(bf16[128,256]{1,0:T(8,128)(2,1)S(1)} %shard_map.88.x0), channel_id=1, source_target_pairs={{0,4},{2,6},{4,0},{6,2},{1,5},{3,7},{5,1},{7,3},{8,12},{10,14},{12... | collective-permute-start | bytes 196616 | tf_op jit(solution)/shard_map/ppermute | solution.py:30
  62.6 4.0 %collective-permute-start.12 = (bf16[128,256]{1,0:T(8,128)(2,1)S(1)}, bf16[128,256]{1,0:T(8,128)(2,1)S(1)}, u32[]{:S(2)}, u32[]{:S(2)}) collective-permute-start(bf16[128,256]{1,0:T(8,128)(2,1)S(1)} %shard_map.88.x0), channel_id=1, source_target_pairs={{0,6},{2,0},{4,2},{6,4},{1,7},{3,1},{5,3},{7,5},{8,14},{10,8},{12,... | collective-permute-start | bytes 196616 | tf_op jit(solution)/shard_map/ppermute | solution.py:30
  67.1 37.3 %all-to-all-start.2 = ((bf16[4,4,64,512]{3,2,1,0:T(8,128)(2,1)}), bf16[4,4,64,512]{3,2,1,0:T(8,128)(2,1)S(1)}, u32[]{:S(2)}, u32[]{:S(2)}) async-start(bf16[4,4,64,512]{3,2,1,0:T(8,128)(2,1)} %copy-done), calls=%async_computation.2 | async-start | bytes 2097152 | tf_op jit(solution)/shard_map/all_to_all | solution.py:38
  71.1 7.7 %collective-permute-start.16 = (bf16[128,256]{1,0:T(8,128)(2,1)S(1)}, bf16[128,256]{1,0:T(8,128)(2,1)S(1)}, u32[]{:S(2)}, u32[]{:S(2)}) collective-permute-start(bf16[128,256]{1,0:T(8,128)(2,1)S(1)} %get-tuple-element.51.own), channel_id=1, source_target_pairs={{0,8},{8,16},{16,24},{24,32},{32,40},{40,48},{48,56},{56,64},{64,7... | collective-permute-start | bytes 196616 | tf_op jit(solution)/shard_map/ppermute | solution.py:50
  76.9 7.4 %collective-permute-start.17 = (bf16[128,256]{1,0:T(8,128)(2,1)S(1)}, bf16[128,256]{1,0:T(8,128)(2,1)S(1)}, u32[]{:S(2)}, u32[]{:S(2)}) collective-permute-start(bf16[128,256]{1,0:T(8,128)(2,1)S(1)} %get-tuple-element.51.own), channel_id=1, source_target_pairs={{8,0},{16,8},{24,16},{32,24},{40,32},{48,40},{56,48},{64,56},{72,6... | collective-permute-start | bytes 196616 | tf_op jit(solution)/shard_map/ppermute | solution.py:54
  85.3 4.4 %collective-permute-start.18 = (bf16[128,256]{1,0:T(8,128)(2,1)S(1)}, bf16[128,256]{1,0:T(8,128)(2,1)S(1)}, u32[]{:S(2)}, u32[]{:S(2)}) collective-permute-start(bf16[128,256]{1,0:T(8,128)(2,1)S(1)} %get-tuple-element.53), channel_id=1, source_target_pairs={{0,2},{2,4},{4,6},{6,0},{1,3},{3,5},{5,7},{7,1},{8,10},{10,12},{12... | collective-permute-start | bytes 196616 | tf_op jit(solution)/shard_map/ppermute | solution.py:243
  85.3 5.8 %collective-permute-start.19 = (bf16[128,256]{1,0:T(8,128)(2,1)S(1)}, bf16[128,256]{1,0:T(8,128)(2,1)S(1)}, u32[]{:S(2)}, u32[]{:S(2)}) collective-permute-start(bf16[128,256]{1,0:T(8,128)(2,1)S(1)} %get-tuple-element.54), channel_id=1, source_target_pairs={{0,4},{2,6},{4,0},{6,2},{1,5},{3,7},{5,1},{7,3},{8,12},{10,14},{12... | collective-permute-start | bytes 196616 | tf_op jit(solution)/shard_map/ppermute | solution.py:245
  91.9 6.2 %collective-permute-start.21 = (f32[128,256]{1,0:T(8,128)S(1)}, f32[128,256]{1,0:T(8,128)S(1)}, u32[]{:S(2)}, u32[]{:S(2)}) collective-permute-start(f32[128,256]{1,0:T(8,128)S(1)} %shard_map.92.mine), channel_id=1, source_target_pairs={{0,1},{1,0},{2,3},{3,2},{4,5},{5,4},{6,7},{7,6},{8,9},{9,8},{10,11... | collective-permute-start | bytes 393224 | tf_op jit(solution)/shard_map/ppermute | solution.py:46
  98.1 5.4 %collective-permute-start.22 = (bf16[128,256]{1,0:T(8,128)(2,1)S(1)}, bf16[128,256]{1,0:T(8,128)(2,1)S(1)}, u32[]{:S(2)}, u32[]{:S(2)}) collective-permute-start(bf16[128,256]{1,0:T(8,128)(2,1)S(1)} %shard_map.93.x0), channel_id=1, source_target_pairs={{0,2},{2,4},{4,6},{6,0},{1,3},{3,5},{5,7},{7,1},{8,10},{10,12},{12... | collective-permute-start | bytes 196616 | tf_op jit(solution)/shard_map/ppermute | solution.py:30
  98.2 5.3 %collective-permute-start.23 = (bf16[128,256]{1,0:T(8,128)(2,1)S(1)}, bf16[128,256]{1,0:T(8,128)(2,1)S(1)}, u32[]{:S(2)}, u32[]{:S(2)}) collective-permute-start(bf16[128,256]{1,0:T(8,128)(2,1)S(1)} %shard_map.93.x0), channel_id=1, source_target_pairs={{0,4},{2,6},{4,0},{6,2},{1,5},{3,7},{5,1},{7,3},{8,12},{10,14},{12... | collective-permute-start | bytes 196616 | tf_op jit(solution)/shard_map/ppermute | solution.py:30
  100.5 3.9 %collective-permute-start.24 = (bf16[128,256]{1,0:T(8,128)(2,1)S(1)}, bf16[128,256]{1,0:T(8,128)(2,1)S(1)}, u32[]{:S(2)}, u32[]{:S(2)}) collective-permute-start(bf16[128,256]{1,0:T(8,128)(2,1)S(1)} %shard_map.93.x0), channel_id=1, source_target_pairs={{0,6},{2,0},{4,2},{6,4},{1,7},{3,1},{5,3},{7,5},{8,14},{10,8},{12,... | collective-permute-start | bytes 196616 | tf_op jit(solution)/shard_map/ppermute | solution.py:30
  104.9 5.3 %collective-permute-start.25 = (bf16[128,256]{1,0:T(8,128)(2,1)S(1)}, bf16[128,256]{1,0:T(8,128)(2,1)S(1)}, u32[]{:S(2)}, u32[]{:S(2)}) collective-permute-start(bf16[128,256]{1,0:T(8,128)(2,1)S(1)} %get-tuple-element.58.own), channel_id=1, source_target_pairs={{0,8},{8,16},{16,24},{24,32},{32,40},{40,48},{48,56},{56,64},{64,7... | collective-permute-start | bytes 196616 | tf_op jit(solution)/shard_map/ppermute | solution.py:50
  106.8 7.1 %collective-permute-start.26 = (bf16[128,256]{1,0:T(8,128)(2,1)S(1)}, bf16[128,256]{1,0:T(8,128)(2,1)S(1)}, u32[]{:S(2)}, u32[]{:S(2)}) collective-permute-start(bf16[128,256]{1,0:T(8,128)(2,1)S(1)} %get-tuple-element.58.own), channel_id=1, source_target_pairs={{8,0},{16,8},{24,16},{32,24},{40,32},{48,40},{56,48},{64,56},{72,6... | collective-permute-start | bytes 196616 | tf_op jit(solution)/shard_map/ppermute | solution.py:54
  114.9 4.4 %collective-permute-start.27 = (bf16[128,256]{1,0:T(8,128)(2,1)S(1)}, bf16[128,256]{1,0:T(8,128)(2,1)S(1)}, u32[]{:S(2)}, u32[]{:S(2)}) collective-permute-start(bf16[128,256]{1,0:T(8,128)(2,1)S(1)} %get-tuple-element.60), channel_id=1, source_target_pairs={{0,2},{2,4},{4,6},{6,0},{1,3},{3,5},{5,7},{7,1},{8,10},{10,12},{12... | collective-permute-start | bytes 196616 | tf_op jit(solution)/shard_map/ppermute | solution.py:243
  116.2 4.7 %collective-permute-start.28 = (bf16[128,256]{1,0:T(8,128)(2,1)S(1)}, bf16[128,256]{1,0:T(8,128)(2,1)S(1)}, u32[]{:S(2)}, u32[]{:S(2)}) collective-permute-start(bf16[128,256]{1,0:T(8,128)(2,1)S(1)} %get-tuple-element.61), channel_id=1, source_target_pairs={{0,4},{2,6},{4,0},{6,2},{1,5},{3,7},{5,1},{7,3},{8,12},{10,14},{12... | collective-permute-start | bytes 196616 | tf_op jit(solution)/shard_map/ppermute | solution.py:245
  121.7 5.3 %collective-permute-start.30 = (f32[128,128]{1,0:T(8,128)S(1)}, f32[128,128]{1,0:T(8,128)S(1)}, u32[]{:S(2)}, u32[]{:S(2)}) collective-permute-start(f32[128,128]{1,0:T(8,128)S(1)} %get-tuple-element.64), channel_id=1, source_target_pairs={{0,1},{1,0},{2,3},{3,2},{4,5},{5,4},{6,7},{7,6},{8,9},{9,8},{10,11... | collective-permute-start | bytes 196616 | tf_op jit(solution)/shard_map/ppermute | solution.py:46
  (8 other events, 73.4 us)

commit v13 on v8

--- a/solution.py
+++ b/solution.py
@@ -154,7 +154,7 @@
     kv[:, 128:256] = acc[:, 256:384].astype(BF16)
 
 
-def heads_first_body(own, partner, gain, docs, weights, q, kv):
+def heads_of(own, partner, gain, weights, layer):
     c = lax.axis_index("c")
     total = jnp.zeros((128, 128), F32)
     for k in range(4):
@@ -166,27 +166,21 @@
     for k in range(4):
         for part, core in ((own, c), (partner, 1 - c)):
             block = behind("y", k) * 2 + core
-            gains = gain[0:1, pl.ds(pl.multiple_of(block * 128, 128), 128)]
+            gains = gain[layer : layer + 1, pl.ds(pl.multiple_of(block * 128, 128), 128)]
             normed = (part[k].astype(F32) * scale * gains).astype(BF16)
             rows = weights[pl.ds(pl.multiple_of(block * 128, 128), 128), 0:384]
             acc = acc + jnp.dot(normed, rows, preferred_element_type=F32)
-    finish_heads(acc, q, kv.at[0:128])
+    return acc
+
+
+def heads_next_body(own, partner, gain, weights, q, kv, *, layer):
+    finish_heads(heads_of(own, partner, gain, weights, layer), q, kv)
+
+
+def heads_first_body(own, partner, gain, docs, weights, q, kv):
+    finish_heads(heads_of(own, partner, gain, weights, 0), q, kv.at[0:128])
     line = (docs[...] + 1).astype(F32).astype(BF16)
     kv[128:144, :] = jnp.broadcast_to(jnp.concatenate([line, line], axis=1), (16, 256))
-
-
-def heads_pieces_body(x0, x1, x2, x3, gain, weights, q, kv, *, layer):
-    pieces = [x[...].astype(F32) for x in (x0, x1, x2, x3)]
-    total = sum(p * p for p in pieces)
-    scale = lax.rsqrt(jnp.sum(total, axis=1, keepdims=True) * (1.0 / 1024) + EPS)
-    acc = jnp.zeros((128, 384), F32)
-    for k in range(4):
-        block = behind("y", k)
-        at = pl.ds(pl.multiple_of(block * 256, 256), 256)
-        normed = (pieces[k] * scale * gain[layer : layer + 1, at]).astype(BF16)
-        rows = weights[at, 0:384]
-        acc = acc + jnp.dot(normed, rows, preferred_element_type=F32)
-    finish_heads(acc, q, kv)
 
 
 def attend(q, keys_values, table):
@@ -211,39 +205,43 @@
     return jnp.where(low, results[0], results[1]).astype(BF16)
 
 
-def attend_scatter_body(q, before, own, after, table, weights, kept, s1, s2, s3, *, layer):
+def attend_halves_body(q, before, own, after, table, weights, mine, theirs, *, layer):
     parts = [(p[0:128, 0:128], p[0:128, 128:256]) for p in (before, own, after)]
     attended = attend(q, parts, table.at[2 * layer : 2 * layer + 2])
+    c = lax.axis_index("c")
+    for k in range(4):
+        for into, core in ((mine, c), (theirs, 1 - c)):
+            at = ahead("y", k) * 256 + core * 128
+            rows = weights[pl.ds(pl.multiple_of(at, 128), 128), 384:512]
+            share = lax.dot_general(attended, rows, NT, preferred_element_type=F32)
+            into[k] = share.astype(into.dtype)
+
+
+def join_body(mine, theirs, kept, s1, s2, s3):
     for k, into in enumerate((kept, s1, s2, s3)):
-        rows = weights[pl.ds(pl.multiple_of(ahead("y", k) * 256, 256), 256), 384:512]
-        share = lax.dot_general(attended, rows, NT, preferred_element_type=F32)
-        into[...] = share.astype(into.dtype)
-
-
-def sum_body(kept, r1, r2, r3, out):
-    out[...] = kept[...] + r1[...].astype(F32) + r2[...].astype(F32) + r3[...].astype(F32)
-
-
-def pair_sum_body(mine, theirs, out):
-    out[...] = (mine[...] + theirs[...]).astype(BF16)
-
-
-def split_body(kept, r1, r2, r3, mine, theirs):
-    c = lax.axis_index("c")
-    for into, core in ((mine, c), (theirs, 1 - c)):
-        at = pl.ds(pl.multiple_of(core * 128, 128), 128)
-        into[...] = (
-            kept[:, at] + r1[:, at].astype(F32) + r2[:, at].astype(F32) + r3[:, at].astype(F32)
-        )
-
-
-def scattered(body, *args):
-    outs = [shaped(128, 256, dtype=F32)] + [shaped(128, 256)] * 3
-    kept, s1, s2, s3 = call(body, outs, *args)
+        into[...] = (mine[k] + theirs[k].astype(F32)).astype(into.dtype)
+
+
+def total_body(kept, r1, r2, r3, out):
+    total = kept[...] + r1[...].astype(F32) + r2[...].astype(F32) + r3[...].astype(F32)
+    out[...] = total.astype(BF16)
+
+
+def turned(s1, s2, s3):
     r1 = lax.ppermute(s1, "y", turn(1))
     r3 = lax.ppermute(s3, "y", turn(3))
     r2 = lax.ppermute(s2, "y", turn(2))
-    return kept, r1, r2, r3
+    return r1, r2, r3
+
+
+def scattered_halves(body, needed, *args):
+    outs = [shaped(4, 128, 128, dtype=F32), shaped(4, 128, 128)]
+    mine, theirs = call(body, outs, *args)
+    if needed is not None:
+        mine = after_this(mine, needed)
+    outs = [shaped(128, 128, dtype=F32)] + [shaped(128, 128)] * 3
+    kept, *sent = call(join_body, outs, mine, swap(theirs))
+    return call(total_body, shaped(128, 128), kept, *turned(*sent))
 
 
 def local(tokens, norm_gain, w_query, w_key, w_value, w_out, offset_bias, documents):
@@ -279,25 +277,23 @@
             many, axes = ((many1, SP), (many2, "z"))[layer]
             next_weights = gather_rows(after_this(many, kv), axes)
         if layer == 0:
-            table = call(table_body, shaped(6, 128, 384, dtype=F32), wide, before, kv, after)
-        kept, r1, r2, r3 = scattered(
-            functools.partial(attend_scatter_body, layer=layer),
+            table = call(
+                table_body, shaped(6, 128, 384, dtype=F32), wide, before, kv, after,
+            )
+        stream = scattered_halves(
+            functools.partial(attend_halves_body, layer=layer),
+            many2 if layer == 0 else None,
             q, before, kv, after, table, weights,
         )
         if layer == 2:
-            break
-        if layer == 0:
-            kept = after_this(kept, many2)
-        half = call(sum_body, shaped(128, 256, dtype=F32), kept, r1, r2, r3)
-        stream = call(pair_sum_body, shaped(128, 256), half, swap(half))
+            return stream
         weights = next_weights
+        near_y = jnp.stack(in_order(stream, spread(stream, "y")))
         q, kv = call(
-            functools.partial(heads_pieces_body, layer=layer + 1),
+            functools.partial(heads_next_body, layer=layer + 1),
             [shaped(128, 128), shaped(128, 256)],
-            *in_order(stream, spread(stream, "y")), norm_gain, weights,
+            near_y, swap(near_y), norm_gain, weights,
         )
-    mine, theirs = call(split_body, [shaped(128, 128, dtype=F32)] * 2, kept, r1, r2, r3)
-    return call(pair_sum_body, shaped(128, 128), mine, swap(theirs))
 
 
 def solution(mesh):

time: 127 us -> 135 us (1.063)
  the two profiles are of different devices: /device:TPU:39 before, /device:TPU:38 now
where the time goes in v13:
time: 135 us; the launch traced here: 134 us
  starting transfers between devices  69.1 us (51%)
  waiting for transfers between devices  53.7 us (40%)
  Pallas kernels  10 us (7%)
    all_to_all x3, starting transfers between devices, gather_rows(): return lax.all_to_all(a, axes, 0, 0, tiled=True).reshape(1024, 512)  19.9 us
    ppermute x12, starting transfers between devices, spread(): return [lax.ppermute(a, axis, turn(k)) for k in (1, 3, 2)]  16.4 us
    ppermute x12, waiting for transfers between devices, spread(): return [lax.ppermute(a, axis, turn(k)) for k in (1, 3, 2)]  12.6 us
    ppermute x3, waiting for transfers between devices, from_after(): return lax.ppermute(a, SP, [(i + 1, i) for i in range(15)])  11.8 us
    pallas_call x16, Pallas kernels, call(): pl.pallas_call(body, out_shape=outs, **specs, scratch_shapes=list(scratch...  10 us
    ppermute x3, starting transfers between devices, turned(): r2 = lax.ppermute(s2, 'y', turn(2))  9.73 us
    ppermute x3, starting transfers between devices, from_before(): return lax.ppermute(a, SP, [(i, i + 1) for i in range(15)])  8.76 us
    ppermute x3, starting transfers between devices, from_after(): return lax.ppermute(a, SP, [(i + 1, i) for i in range(15)])  8.75 us
  transfers between devices with their start and end apart: 36, of which 30 were waited for; matrix products, arithmetic and copies ran while one was open for 0% of the time, Pallas kernels for 4%

profile of v13, /device:TPU:38, one launch (start us, length us, event | category | flops | bytes accessed | tf_op | source)
XLA Modules:
  0.0 134.1 jit_solution(10097007750178246363)
XLA Ops:
  0.0 1.9 %shard_map.83 = bf16[16,64,512]{2,1,0:T(8,128)(2,1)} custom-call(bf16[3,64,128]{2,1,0:T(8,128)(2,1)} %wq.3, bf16[3,64,128]{2,1,0:T(8,128)(2,1)} %wk.3, bf16[3,64,128]{2,1,0:T(8,128)(2,1)} %wv.3, bf16[3,64,128]{2,1,0:T(8,128)(2,1)} %bitcast.26), custom_call_target="tpu_custom_call" | custom-call | tf_op jit(solution)/shard_map/pallas_call | solution.py:66
  1.9 8.0 %all-to-all-start = ((bf16[16,64,512]{2,1,0:T(8,128)(2,1)}), bf16[16,64,512]{2,1,0:T(8,128)(2,1)S(1)}, u32[]{:S(2)}, u32[]{:S(2)}) async-start(bf16[16,64,512]{2,1,0:T(8,128)(2,1)} %shard_map.83), calls=%async_computation | async-start | bytes 2097152 | tf_op jit(solution)/shard_map/all_to_all | solution.py:38
  9.9 1.6 %collective-permute-start = (bf16[128,128]{1,0:T(8,128)(2,1)S(1)}, bf16[128,128]{1,0:T(8,128)(2,1)S(1)}, u32[]{:S(2)}, u32[]{:S(2)}) collective-permute-start(bf16[128,128]{1,0:T(8,128)(2,1)S(1)} %copy-done.4), channel_id=1, source_target_pairs={{0,2},{2,4},{4,6},{6,0},{1,3},{3,5},{5,7},{7,1},{8,10},{10,12},{12... | collective-permute-start | bytes 98312 | tf_op jit(solution)/shard_map/ppermute | solution.py:30
  11.5 2.9 %collective-permute-start.1 = (bf16[128,128]{1,0:T(8,128)(2,1)S(1)}, bf16[128,128]{1,0:T(8,128)(2,1)S(1)}, u32[]{:S(2)}, u32[]{:S(2)}) collective-permute-start(bf16[128,128]{1,0:T(8,128)(2,1)S(1)} %copy-done.4), channel_id=1, source_target_pairs={{0,4},{2,6},{4,0},{6,2},{1,5},{3,7},{5,1},{7,3},{8,12},{10,14},{12... | collective-permute-start | bytes 98312 | tf_op jit(solution)/shard_map/ppermute | solution.py:30
  15.8 2.0 %shard_map.82 = (bf16[16,64,512]{2,1,0:T(8,128)(2,1)}, bf16[64,512]{1,0:T(8,128)(2,1)S(1)}, f32[8,256]{1,0:T(8,128)S(1)}) custom-call(bf16[3,64,128]{2,1,0:T(8,128)(2,1)} %wq.3, bf16[3,64,128]{2,1,0:T(8,128)(2,1)} %wk.3, bf16[3,64,128]{2,1,0:T(8,128)(2,1)} %wv.3, bf16[3,64,128]{2,1,0:T(8,128)(2,1)} %bitcast.27, f32[3,2,8,16]{3,2,1,0:T(8,128)S(1)} %copy-done.2), custom_call_target="tpu_custom_call" | custom-call | tf_op jit(solution)/shard_map/pallas_call | solution.py:66
  19.8 4.2 %all-to-all-done = bf16[16,64,512]{2,1,0:T(8,128)(2,1)S(1)} async-done(((bf16[16,64,512]{2,1,0:T(8,128)(2,1)}), bf16[16,64,512]{2,1,0:T(8,128)(2,1)S(1)}, u32[]{:S(2)}, u32[]{:S(2)}) %all-to-all-start) | async-done | bytes 1048608 | tf_op jit(solution)/shard_map/all_to_all | solution.py:38
  24.6 7.1 %all-to-all-start.1 = ((bf16[16,64,512]{2,1,0:T(8,128)(2,1)}), bf16[16,64,512]{2,1,0:T(8,128)(2,1)S(1)}, u32[]{:S(2)}, u32[]{:S(2)}) async-start(bf16[16,64,512]{2,1,0:T(8,128)(2,1)} %get-tuple-element.49), calls=%async_computation.1 | async-start | bytes 2097152 | tf_op jit(solution)/shard_map/all_to_all | solution.py:38
  31.7 3.4 %collective-permute-start.4 = (bf16[144,256]{1,0:T(8,128)(2,1)S(1)}, bf16[144,256]{1,0:T(8,128)(2,1)S(1)}, u32[]{:S(2)}, u32[]{:S(2)}) collective-permute-start(bf16[144,256]{1,0:T(8,128)(2,1)S(1)} %get-tuple-element.39.own), channel_id=1, source_target_pairs={{0,8},{8,16},{16,24},{24,32},{32,40},{40,48},{48,56},{56,64},{64,7... | collective-permute-start | bytes 221192 | tf_op jit(solution)/shard_map/ppermute | solution.py:50
  35.1 2.5 %collective-permute-start.5 = (bf16[144,256]{1,0:T(8,128)(2,1)S(1)}, bf16[144,256]{1,0:T(8,128)(2,1)S(1)}, u32[]{:S(2)}, u32[]{:S(2)}) collective-permute-start(bf16[144,256]{1,0:T(8,128)(2,1)S(1)} %get-tuple-element.39.own), channel_id=1, source_target_pairs={{8,0},{16,8},{24,16},{32,24},{40,32},{48,40},{56,48},{64,56},{72,6... | collective-permute-start | bytes 221192 | tf_op jit(solution)/shard_map/ppermute | solution.py:54
  37.6 7.5 %collective-permute-done.4.before = bf16[144,256]{1,0:T(8,128)(2,1)S(1)} collective-permute-done((bf16[144,256]{1,0:T(8,128)(2,1)S(1)}, bf16[144,256]{1,0:T(8,128)(2,1)S(1)}, u32[]{:S(2)}, u32[]{:S(2)}) %collective-permute-start.4) | collective-permute-done | bytes 73760 | tf_op jit(solution)/shard_map/ppermute | solution.py:50
  50.2 2.9 %collective-permute-done.6.p1 = bf16[64,512]{1,0:T(8,128)(2,1)S(1)} collective-permute-done((bf16[64,512]{1,0:T(8,128)(2,1)S(1)}, bf16[64,512]{1,0:T(8,128)(2,1)S(1)}, u32[]{:S(2)}, u32[]{:S(2)}) %collective-permute-start.6) | collective-permute-done | bytes 65568 | tf_op jit(solution)/shard_map/ppermute | solution.py:30
  53.2 1.5 %collective-permute-done.7.p2 = bf16[64,512]{1,0:T(8,128)(2,1)S(1)} collective-permute-done((bf16[64,512]{1,0:T(8,128)(2,1)S(1)}, bf16[64,512]{1,0:T(8,128)(2,1)S(1)}, u32[]{:S(2)}, u32[]{:S(2)}) %collective-permute-start.7) | collective-permute-done | bytes 65568 | tf_op jit(solution)/shard_map/ppermute | solution.py:30
  57.0 1.7 %collective-permute-start.10 = (bf16[128,128]{1,0:T(8,128)(2,1)S(1)}, bf16[128,128]{1,0:T(8,128)(2,1)S(1)}, u32[]{:S(2)}, u32[]{:S(2)}) collective-permute-start(bf16[128,128]{1,0:T(8,128)(2,1)S(1)} %get-tuple-element.46), channel_id=1, source_target_pairs={{0,2},{2,4},{4,6},{6,0},{1,3},{3,5},{5,7},{7,1},{8,10},{10,12},{12... | collective-permute-start | bytes 98312 | tf_op jit(solution)/shard_map/ppermute | solution.py:231
  58.7 2.9 %collective-permute-start.11 = (bf16[128,128]{1,0:T(8,128)(2,1)S(1)}, bf16[128,128]{1,0:T(8,128)(2,1)S(1)}, u32[]{:S(2)}, u32[]{:S(2)}) collective-permute-start(bf16[128,128]{1,0:T(8,128)(2,1)S(1)} %get-tuple-element.47), channel_id=1, source_target_pairs={{0,4},{2,6},{4,0},{6,2},{1,5},{3,7},{5,1},{7,3},{8,12},{10,14},{12... | collective-permute-start | bytes 98312 | tf_op jit(solution)/shard_map/ppermute | solution.py:233
  65.5 2.6 %collective-permute-start.15 = (bf16[128,128]{1,0:T(8,128)(2,1)S(1)}, bf16[128,128]{1,0:T(8,128)(2,1)S(1)}, u32[]{:S(2)}, u32[]{:S(2)}) collective-permute-start(bf16[128,128]{1,0:T(8,128)(2,1)S(1)} %shard_map.89), channel_id=1, source_target_pairs={{0,6},{2,0},{4,2},{6,4},{1,7},{3,1},{5,3},{7,5},{8,14},{10,8},{12,... | collective-permute-start | bytes 98312 | tf_op jit(solution)/shard_map/ppermute | solution.py:30
  68.1 1.5 %collective-permute-start.14 = (bf16[128,128]{1,0:T(8,128)(2,1)S(1)}, bf16[128,128]{1,0:T(8,128)(2,1)S(1)}, u32[]{:S(2)}, u32[]{:S(2)}) collective-permute-start(bf16[128,128]{1,0:T(8,128)(2,1)S(1)} %shard_map.89), channel_id=1, source_target_pairs={{0,4},{2,6},{4,0},{6,2},{1,5},{3,7},{5,1},{7,3},{8,12},{10,14},{12... | collective-permute-start | bytes 98312 | tf_op jit(solution)/shard_map/ppermute | solution.py:30
  69.7 3.5 %collective-permute-done.13 = bf16[128,128]{1,0:T(8,128)(2,1)S(1)} collective-permute-done((bf16[128,128]{1,0:T(8,128)(2,1)S(1)}, bf16[128,128]{1,0:T(8,128)(2,1)S(1)}, u32[]{:S(2)}, u32[]{:S(2)}) %collective-permute-start.13) | collective-permute-done | bytes 32800 | tf_op jit(solution)/shard_map/ppermute | solution.py:30
  75.6 4.8 %all-to-all-start.2 = ((bf16[4,4,64,512]{3,2,1,0:T(8,128)(2,1)}), bf16[4,4,64,512]{3,2,1,0:T(8,128)(2,1)S(1)}, u32[]{:S(2)}, u32[]{:S(2)}) async-start(bf16[4,4,64,512]{3,2,1,0:T(8,128)(2,1)} %copy-done), calls=%async_computation.2 | async-start | bytes 2097152 | tf_op jit(solution)/shard_map/all_to_all | solution.py:38
  80.5 3.5 %collective-permute-start.17 = (bf16[128,256]{1,0:T(8,128)(2,1)S(1)}, bf16[128,256]{1,0:T(8,128)(2,1)S(1)}, u32[]{:S(2)}, u32[]{:S(2)}) collective-permute-start(bf16[128,256]{1,0:T(8,128)(2,1)S(1)} %get-tuple-element.51.own), channel_id=1, source_target_pairs={{0,8},{8,16},{16,24},{24,32},{32,40},{40,48},{48,56},{56,64},{64,7... | collective-permute-start | bytes 196616 | tf_op jit(solution)/shard_map/ppermute | solution.py:50
  83.9 2.4 %collective-permute-start.18 = (bf16[128,256]{1,0:T(8,128)(2,1)S(1)}, bf16[128,256]{1,0:T(8,128)(2,1)S(1)}, u32[]{:S(2)}, u32[]{:S(2)}) collective-permute-start(bf16[128,256]{1,0:T(8,128)(2,1)S(1)} %get-tuple-element.51.own), channel_id=1, source_target_pairs={{8,0},{16,8},{24,16},{32,24},{40,32},{48,40},{56,48},{64,56},{72,6... | collective-permute-start | bytes 196616 | tf_op jit(solution)/shard_map/ppermute | solution.py:54
  86.6 6.3 %collective-permute-done.18.after = bf16[128,256]{1,0:T(8,128)(2,1)S(1)} collective-permute-done((bf16[128,256]{1,0:T(8,128)(2,1)S(1)}, bf16[128,256]{1,0:T(8,128)(2,1)S(1)}, u32[]{:S(2)}, u32[]{:S(2)}) %collective-permute-start.18) | collective-permute-done | bytes 65568 | tf_op jit(solution)/shard_map/ppermute | solution.py:54
  96.0 4.1 %collective-permute-start.21 = (bf16[128,128]{1,0:T(8,128)(2,1)S(1)}, bf16[128,128]{1,0:T(8,128)(2,1)S(1)}, u32[]{:S(2)}, u32[]{:S(2)}) collective-permute-start(bf16[128,128]{1,0:T(8,128)(2,1)S(1)} %get-tuple-element.56), channel_id=1, source_target_pairs={{0,4},{2,6},{4,0},{6,2},{1,5},{3,7},{5,1},{7,3},{8,12},{10,14},{12... | collective-permute-start | bytes 98312 | tf_op jit(solution)/shard_map/ppermute | solution.py:233
  100.6 1.8 %collective-permute-done.21.r2 = bf16[128,128]{1,0:T(8,128)(2,1)S(1)} collective-permute-done((bf16[128,128]{1,0:T(8,128)(2,1)S(1)}, bf16[128,128]{1,0:T(8,128)(2,1)S(1)}, u32[]{:S(2)}, u32[]{:S(2)}) %collective-permute-start.21) | collective-permute-done | bytes 32800 | tf_op jit(solution)/shard_map/ppermute | solution.py:233
  102.3 1.7 %collective-permute-done.22.r3 = bf16[128,128]{1,0:T(8,128)(2,1)S(1)} collective-permute-done((bf16[128,128]{1,0:T(8,128)(2,1)S(1)}, bf16[128,128]{1,0:T(8,128)(2,1)S(1)}, u32[]{:S(2)}, u32[]{:S(2)}) %collective-permute-start.22) | collective-permute-done | bytes 32800 | tf_op jit(solution)/shard_map/ppermute | solution.py:232
  104.1 2.7 %collective-permute-start.24 = (bf16[128,128]{1,0:T(8,128)(2,1)S(1)}, bf16[128,128]{1,0:T(8,128)(2,1)S(1)}, u32[]{:S(2)}, u32[]{:S(2)}) collective-permute-start(bf16[128,128]{1,0:T(8,128)(2,1)S(1)} %shard_map.93), channel_id=1, source_target_pairs={{0,4},{2,6},{4,0},{6,2},{1,5},{3,7},{5,1},{7,3},{8,12},{10,14},{12... | collective-permute-start | bytes 98312 | tf_op jit(solution)/shard_map/ppermute | solution.py:30
  106.8 1.5 %collective-permute-start.25 = (bf16[128,128]{1,0:T(8,128)(2,1)S(1)}, bf16[128,128]{1,0:T(8,128)(2,1)S(1)}, u32[]{:S(2)}, u32[]{:S(2)}) collective-permute-start(bf16[128,128]{1,0:T(8,128)(2,1)S(1)} %shard_map.93), channel_id=1, source_target_pairs={{0,6},{2,0},{4,2},{6,4},{1,7},{3,1},{5,3},{7,5},{8,14},{10,8},{12,... | collective-permute-start | bytes 98312 | tf_op jit(solution)/shard_map/ppermute | solution.py:30
  112.7 1.9 %collective-permute-start.27 = (bf16[128,256]{1,0:T(8,128)(2,1)S(1)}, bf16[128,256]{1,0:T(8,128)(2,1)S(1)}, u32[]{:S(2)}, u32[]{:S(2)}) collective-permute-start(bf16[128,256]{1,0:T(8,128)(2,1)S(1)} %get-tuple-element.60.own), channel_id=1, source_target_pairs={{0,8},{8,16},{16,24},{24,32},{32,40},{40,48},{48,56},{56,64},{64,7... | collective-permute-start | bytes 196616 | tf_op jit(solution)/shard_map/ppermute | solution.py:50
  114.6 3.9 %collective-permute-start.28 = (bf16[128,256]{1,0:T(8,128)(2,1)S(1)}, bf16[128,256]{1,0:T(8,128)(2,1)S(1)}, u32[]{:S(2)}, u32[]{:S(2)}) collective-permute-start(bf16[128,256]{1,0:T(8,128)(2,1)S(1)} %get-tuple-element.60.own), channel_id=1, source_target_pairs={{8,0},{16,8},{24,16},{32,24},{40,32},{48,40},{56,48},{64,56},{72,6... | collective-permute-start | bytes 196616 | tf_op jit(solution)/shard_map/ppermute | solution.py:54
  118.9 4.0 %collective-permute-done.28.after = bf16[128,256]{1,0:T(8,128)(2,1)S(1)} collective-permute-done((bf16[128,256]{1,0:T(8,128)(2,1)S(1)}, bf16[128,256]{1,0:T(8,128)(2,1)S(1)}, u32[]{:S(2)}, u32[]{:S(2)}) %collective-permute-start.28) | collective-permute-done | bytes 65568 | tf_op jit(solution)/shard_map/ppermute | solution.py:54
  125.4 1.5 %collective-permute-start.30 = (bf16[128,128]{1,0:T(8,128)(2,1)S(1)}, bf16[128,128]{1,0:T(8,128)(2,1)S(1)}, u32[]{:S(2)}, u32[]{:S(2)}) collective-permute-start(bf16[128,128]{1,0:T(8,128)(2,1)S(1)} %get-tuple-element.64), channel_id=1, source_target_pairs={{0,2},{2,4},{4,6},{6,0},{1,3},{3,5},{5,7},{7,1},{8,10},{10,12},{12... | collective-permute-start | bytes 98312 | tf_op jit(solution)/shard_map/ppermute | solution.py:231
  126.9 2.7 %collective-permute-start.31 = (bf16[128,128]{1,0:T(8,128)(2,1)S(1)}, bf16[128,128]{1,0:T(8,128)(2,1)S(1)}, u32[]{:S(2)}, u32[]{:S(2)}) collective-permute-start(bf16[128,128]{1,0:T(8,128)(2,1)S(1)} %get-tuple-element.65), channel_id=1, source_target_pairs={{0,4},{2,6},{4,0},{6,2},{1,5},{3,7},{5,1},{7,3},{8,12},{10,14},{12... | collective-permute-start | bytes 98312 | tf_op jit(solution)/shard_map/ppermute | solution.py:233
  130.6 1.7 %collective-permute-done.31.r2 = bf16[128,128]{1,0:T(8,128)(2,1)S(1)} collective-permute-done((bf16[128,128]{1,0:T(8,128)(2,1)S(1)}, bf16[128,128]{1,0:T(8,128)(2,1)S(1)}, u32[]{:S(2)}, u32[]{:S(2)}) %collective-permute-start.31) | collective-permute-done | bytes 32800 | tf_op jit(solution)/shard_map/ppermute | solution.py:233
  (69 shorter events, 31.8 us)
Async XLA Ops:
  1.9 22.1 %all-to-all-start = ((bf16[16,64,512]{2,1,0:T(8,128)(2,1)}), bf16[16,64,512]{2,1,0:T(8,128)(2,1)S(1)}, u32[]{:S(2)}, u32[]{:S(2)}) async-start(bf16[16,64,512]{2,1,0:T(8,128)(2,1)} %shard_map.83), calls=%async_computation | async-start | bytes 2097152 | tf_op jit(solution)/shard_map/all_to_all | solution.py:38
  9.9 7.9 %collective-permute-start = (bf16[128,128]{1,0:T(8,128)(2,1)S(1)}, bf16[128,128]{1,0:T(8,128)(2,1)S(1)}, u32[]{:S(2)}, u32[]{:S(2)}) collective-permute-start(bf16[128,128]{1,0:T(8,128)(2,1)S(1)} %copy-done.4), channel_id=1, source_target_pairs={{0,2},{2,4},{4,6},{6,0},{1,3},{3,5},{5,7},{7,1},{8,10},{10,12},{12... | collective-permute-start | bytes 98312 | tf_op jit(solution)/shard_map/ppermute | solution.py:30
  11.5 6.2 %collective-permute-start.1 = (bf16[128,128]{1,0:T(8,128)(2,1)S(1)}, bf16[128,128]{1,0:T(8,128)(2,1)S(1)}, u32[]{:S(2)}, u32[]{:S(2)}) collective-permute-start(bf16[128,128]{1,0:T(8,128)(2,1)S(1)} %copy-done.4), channel_id=1, source_target_pairs={{0,4},{2,6},{4,0},{6,2},{1,5},{3,7},{5,1},{7,3},{8,12},{10,14},{12... | collective-permute-start | bytes 98312 | tf_op jit(solution)/shard_map/ppermute | solution.py:30
  14.4 3.9 %collective-permute-start.2 = (bf16[128,128]{1,0:T(8,128)(2,1)S(1)}, bf16[128,128]{1,0:T(8,128)(2,1)S(1)}, u32[]{:S(2)}, u32[]{:S(2)}) collective-permute-start(bf16[128,128]{1,0:T(8,128)(2,1)S(1)} %copy-done.4), channel_id=1, source_target_pairs={{0,6},{2,0},{4,2},{6,4},{1,7},{3,1},{5,3},{7,5},{8,14},{10,8},{12,... | collective-permute-start | bytes 98312 | tf_op jit(solution)/shard_map/ppermute | solution.py:30
  24.6 50.4 %all-to-all-start.1 = ((bf16[16,64,512]{2,1,0:T(8,128)(2,1)}), bf16[16,64,512]{2,1,0:T(8,128)(2,1)S(1)}, u32[]{:S(2)}, u32[]{:S(2)}) async-start(bf16[16,64,512]{2,1,0:T(8,128)(2,1)} %get-tuple-element.49), calls=%async_computation.1 | async-start | bytes 2097152 | tf_op jit(solution)/shard_map/all_to_all | solution.py:38
  31.7 13.3 %collective-permute-start.4 = (bf16[144,256]{1,0:T(8,128)(2,1)S(1)}, bf16[144,256]{1,0:T(8,128)(2,1)S(1)}, u32[]{:S(2)}, u32[]{:S(2)}) collective-permute-start(bf16[144,256]{1,0:T(8,128)(2,1)S(1)} %get-tuple-element.39.own), channel_id=1, source_target_pairs={{0,8},{8,16},{16,24},{24,32},{32,40},{40,48},{48,56},{56,64},{64,7... | collective-permute-start | bytes 221192 | tf_op jit(solution)/shard_map/ppermute | solution.py:50
  35.1 11.4 %collective-permute-start.5 = (bf16[144,256]{1,0:T(8,128)(2,1)S(1)}, bf16[144,256]{1,0:T(8,128)(2,1)S(1)}, u32[]{:S(2)}, u32[]{:S(2)}) collective-permute-start(bf16[144,256]{1,0:T(8,128)(2,1)S(1)} %get-tuple-element.39.own), channel_id=1, source_target_pairs={{8,0},{16,8},{24,16},{32,24},{40,32},{48,40},{56,48},{64,56},{72,6... | collective-permute-start | bytes 221192 | tf_op jit(solution)/shard_map/ppermute | solution.py:54
  48.1 8.9 %collective-permute-start.9 = (bf16[4,128,128]{2,1,0:T(8,128)(2,1)S(1)}, bf16[4,128,128]{2,1,0:T(8,128)(2,1)S(1)}, u32[]{:S(2)}, u32[]{:S(2)}) collective-permute-start(bf16[4,128,128]{2,1,0:T(8,128)(2,1)S(1)} %get-tuple-element.44), channel_id=1, source_target_pairs={{0,1},{1,0},{2,3},{3,2},{4,5},{5,4},{6,7},{7,6},{8,9},{9,8},{10,11... | collective-permute-start | bytes 393224 | tf_op jit(solution)/shard_map/ppermute | solution.py:46
  48.1 5.0 %collective-permute-start.6 = (bf16[64,512]{1,0:T(8,128)(2,1)S(1)}, bf16[64,512]{1,0:T(8,128)(2,1)S(1)}, u32[]{:S(2)}, u32[]{:S(2)}) collective-permute-start(bf16[64,512]{1,0:T(8,128)(2,1)S(1)} %get-tuple-element.42.p0), channel_id=1, source_target_pairs={{0,8},{8,16},{16,24},{24,0},{1,9},{9,17},{17,25},{25,1},{2,10},{10... | collective-permute-start | bytes 196616 | tf_op jit(solution)/shard_map/ppermute | solution.py:30
  48.8 5.8 %collective-permute-start.7 = (bf16[64,512]{1,0:T(8,128)(2,1)S(1)}, bf16[64,512]{1,0:T(8,128)(2,1)S(1)}, u32[]{:S(2)}, u32[]{:S(2)}) collective-permute-start(bf16[64,512]{1,0:T(8,128)(2,1)S(1)} %get-tuple-element.42.p0), channel_id=1, source_target_pairs={{0,16},{8,24},{16,0},{24,8},{1,17},{9,25},{17,1},{25,9},{2,18},{10... | collective-permute-start | bytes 196616 | tf_op jit(solution)/shard_map/ppermute | solution.py:30
  49.7 6.2 %collective-permute-start.8 = (bf16[64,512]{1,0:T(8,128)(2,1)S(1)}, bf16[64,512]{1,0:T(8,128)(2,1)S(1)}, u32[]{:S(2)}, u32[]{:S(2)}) collective-permute-start(bf16[64,512]{1,0:T(8,128)(2,1)S(1)} %get-tuple-element.42.p0), channel_id=1, source_target_pairs={{0,24},{8,0},{16,8},{24,16},{1,25},{9,1},{17,9},{25,17},{2,26},{10... | collective-permute-start | bytes 196616 | tf_op jit(solution)/shard_map/ppermute | solution.py:30
  57.0 5.9 %collective-permute-start.10 = (bf16[128,128]{1,0:T(8,128)(2,1)S(1)}, bf16[128,128]{1,0:T(8,128)(2,1)S(1)}, u32[]{:S(2)}, u32[]{:S(2)}) collective-permute-start(bf16[128,128]{1,0:T(8,128)(2,1)S(1)} %get-tuple-element.46), channel_id=1, source_target_pairs={{0,2},{2,4},{4,6},{6,0},{1,3},{3,5},{5,7},{7,1},{8,10},{10,12},{12... | collective-permute-start | bytes 98312 | tf_op jit(solution)/shard_map/ppermute | solution.py:231
  58.7 5.4 %collective-permute-start.11 = (bf16[128,128]{1,0:T(8,128)(2,1)S(1)}, bf16[128,128]{1,0:T(8,128)(2,1)S(1)}, u32[]{:S(2)}, u32[]{:S(2)}) collective-permute-start(bf16[128,128]{1,0:T(8,128)(2,1)S(1)} %get-tuple-element.47), channel_id=1, source_target_pairs={{0,4},{2,6},{4,0},{6,2},{1,5},{3,7},{5,1},{7,3},{8,12},{10,14},{12... | collective-permute-start | bytes 98312 | tf_op jit(solution)/shard_map/ppermute | solution.py:233
  61.6 3.9 %collective-permute-start.12 = (bf16[128,128]{1,0:T(8,128)(2,1)S(1)}, bf16[128,128]{1,0:T(8,128)(2,1)S(1)}, u32[]{:S(2)}, u32[]{:S(2)}) collective-permute-start(bf16[128,128]{1,0:T(8,128)(2,1)S(1)} %get-tuple-element.48), channel_id=1, source_target_pairs={{0,6},{2,0},{4,2},{6,4},{1,7},{3,1},{5,3},{7,5},{8,14},{10,8},{12,... | collective-permute-start | bytes 98312 | tf_op jit(solution)/shard_map/ppermute | solution.py:232
  65.5 4.2 %collective-permute-start.15 = (bf16[128,128]{1,0:T(8,128)(2,1)S(1)}, bf16[128,128]{1,0:T(8,128)(2,1)S(1)}, u32[]{:S(2)}, u32[]{:S(2)}) collective-permute-start(bf16[128,128]{1,0:T(8,128)(2,1)S(1)} %shard_map.89), channel_id=1, source_target_pairs={{0,6},{2,0},{4,2},{6,4},{1,7},{3,1},{5,3},{7,5},{8,14},{10,8},{12,... | collective-permute-start | bytes 98312 | tf_op jit(solution)/shard_map/ppermute | solution.py:30
  68.1 5.1 %collective-permute-start.13 = (bf16[128,128]{1,0:T(8,128)(2,1)S(1)}, bf16[128,128]{1,0:T(8,128)(2,1)S(1)}, u32[]{:S(2)}, u32[]{:S(2)}) collective-permute-start(bf16[128,128]{1,0:T(8,128)(2,1)S(1)} %shard_map.89), channel_id=1, source_target_pairs={{0,2},{2,4},{4,6},{6,0},{1,3},{3,5},{5,7},{7,1},{8,10},{10,12},{12... | collective-permute-start | bytes 98312 | tf_op jit(solution)/shard_map/ppermute | solution.py:30
  68.1 5.5 %collective-permute-start.14 = (bf16[128,128]{1,0:T(8,128)(2,1)S(1)}, bf16[128,128]{1,0:T(8,128)(2,1)S(1)}, u32[]{:S(2)}, u32[]{:S(2)}) collective-permute-start(bf16[128,128]{1,0:T(8,128)(2,1)S(1)} %shard_map.89), channel_id=1, source_target_pairs={{0,4},{2,6},{4,0},{6,2},{1,5},{3,7},{5,1},{7,3},{8,12},{10,14},{12... | collective-permute-start | bytes 98312 | tf_op jit(solution)/shard_map/ppermute | solution.py:30
  73.6 1.4 %collective-permute-start.16 = (bf16[4,128,128]{2,1,0:T(8,128)(2,1)S(1)}, bf16[4,128,128]{2,1,0:T(8,128)(2,1)S(1)}, u32[]{:S(2)}, u32[]{:S(2)}) collective-permute-start(bf16[4,128,128]{2,1,0:T(8,128)(2,1)S(1)} %pad_maximum_fusion.1.own), channel_id=1, source_target_pairs={{0,1},{1,0},{2,3},{3,2},{4,5},{5,4},{6,7},{7,6},{8,9},{9,8},{10,11... | collective-permute-start | bytes 393224 | tf_op jit(solution)/shard_map/ppermute | solution.py:46
  75.6 36.5 %all-to-all-start.2 = ((bf16[4,4,64,512]{3,2,1,0:T(8,128)(2,1)}), bf16[4,4,64,512]{3,2,1,0:T(8,128)(2,1)S(1)}, u32[]{:S(2)}, u32[]{:S(2)}) async-start(bf16[4,4,64,512]{3,2,1,0:T(8,128)(2,1)} %copy-done), calls=%async_computation.2 | async-start | bytes 2097152 | tf_op jit(solution)/shard_map/all_to_all | solution.py:38
  80.5 6.1 %collective-permute-start.17 = (bf16[128,256]{1,0:T(8,128)(2,1)S(1)}, bf16[128,256]{1,0:T(8,128)(2,1)S(1)}, u32[]{:S(2)}, u32[]{:S(2)}) collective-permute-start(bf16[128,256]{1,0:T(8,128)(2,1)S(1)} %get-tuple-element.51.own), channel_id=1, source_target_pairs={{0,8},{8,16},{16,24},{24,32},{32,40},{40,48},{48,56},{56,64},{64,7... | collective-permute-start | bytes 196616 | tf_op jit(solution)/shard_map/ppermute | solution.py:50
  83.9 9.0 %collective-permute-start.18 = (bf16[128,256]{1,0:T(8,128)(2,1)S(1)}, bf16[128,256]{1,0:T(8,128)(2,1)S(1)}, u32[]{:S(2)}, u32[]{:S(2)}) collective-permute-start(bf16[128,256]{1,0:T(8,128)(2,1)S(1)} %get-tuple-element.51.own), channel_id=1, source_target_pairs={{8,0},{16,8},{24,16},{32,24},{40,32},{48,40},{56,48},{64,56},{72,6... | collective-permute-start | bytes 196616 | tf_op jit(solution)/shard_map/ppermute | solution.py:54
  95.4 5.2 %collective-permute-start.20 = (bf16[128,128]{1,0:T(8,128)(2,1)S(1)}, bf16[128,128]{1,0:T(8,128)(2,1)S(1)}, u32[]{:S(2)}, u32[]{:S(2)}) collective-permute-start(bf16[128,128]{1,0:T(8,128)(2,1)S(1)} %get-tuple-element.55), channel_id=1, source_target_pairs={{0,2},{2,4},{4,6},{6,0},{1,3},{3,5},{5,7},{7,1},{8,10},{10,12},{12... | collective-permute-start | bytes 98312 | tf_op jit(solution)/shard_map/ppermute | solution.py:231
  96.0 6.4 %collective-permute-start.21 = (bf16[128,128]{1,0:T(8,128)(2,1)S(1)}, bf16[128,128]{1,0:T(8,128)(2,1)S(1)}, u32[]{:S(2)}, u32[]{:S(2)}) collective-permute-start(bf16[128,128]{1,0:T(8,128)(2,1)S(1)} %get-tuple-element.56), channel_id=1, source_target_pairs={{0,4},{2,6},{4,0},{6,2},{1,5},{3,7},{5,1},{7,3},{8,12},{10,14},{12... | collective-permute-start | bytes 98312 | tf_op jit(solution)/shard_map/ppermute | solution.py:233
  100.1 3.9 %collective-permute-start.22 = (bf16[128,128]{1,0:T(8,128)(2,1)S(1)}, bf16[128,128]{1,0:T(8,128)(2,1)S(1)}, u32[]{:S(2)}, u32[]{:S(2)}) collective-permute-start(bf16[128,128]{1,0:T(8,128)(2,1)S(1)} %get-tuple-element.57), channel_id=1, source_target_pairs={{0,6},{2,0},{4,2},{6,4},{1,7},{3,1},{5,3},{7,5},{8,14},{10,8},{12,... | collective-permute-start | bytes 98312 | tf_op jit(solution)/shard_map/ppermute | solution.py:232
  104.0 5.2 %collective-permute-start.23 = (bf16[128,128]{1,0:T(8,128)(2,1)S(1)}, bf16[128,128]{1,0:T(8,128)(2,1)S(1)}, u32[]{:S(2)}, u32[]{:S(2)}) collective-permute-start(bf16[128,128]{1,0:T(8,128)(2,1)S(1)} %shard_map.93), channel_id=1, source_target_pairs={{0,2},{2,4},{4,6},{6,0},{1,3},{3,5},{5,7},{7,1},{8,10},{10,12},{12... | collective-permute-start | bytes 98312 | tf_op jit(solution)/shard_map/ppermute | solution.py:30
  104.1 5.5 %collective-permute-start.24 = (bf16[128,128]{1,0:T(8,128)(2,1)S(1)}, bf16[128,128]{1,0:T(8,128)(2,1)S(1)}, u32[]{:S(2)}, u32[]{:S(2)}) collective-permute-start(bf16[128,128]{1,0:T(8,128)(2,1)S(1)} %shard_map.93), channel_id=1, source_target_pairs={{0,4},{2,6},{4,0},{6,2},{1,5},{3,7},{5,1},{7,3},{8,12},{10,14},{12... | collective-permute-start | bytes 98312 | tf_op jit(solution)/shard_map/ppermute | solution.py:30
  106.8 3.9 %collective-permute-start.25 = (bf16[128,128]{1,0:T(8,128)(2,1)S(1)}, bf16[128,128]{1,0:T(8,128)(2,1)S(1)}, u32[]{:S(2)}, u32[]{:S(2)}) collective-permute-start(bf16[128,128]{1,0:T(8,128)(2,1)S(1)} %shard_map.93), channel_id=1, source_target_pairs={{0,6},{2,0},{4,2},{6,4},{1,7},{3,1},{5,3},{7,5},{8,14},{10,8},{12,... | collective-permute-start | bytes 98312 | tf_op jit(solution)/shard_map/ppermute | solution.py:30
  112.7 6.2 %collective-permute-start.27 = (bf16[128,256]{1,0:T(8,128)(2,1)S(1)}, bf16[128,256]{1,0:T(8,128)(2,1)S(1)}, u32[]{:S(2)}, u32[]{:S(2)}) collective-permute-start(bf16[128,256]{1,0:T(8,128)(2,1)S(1)} %get-tuple-element.60.own), channel_id=1, source_target_pairs={{0,8},{8,16},{16,24},{24,32},{32,40},{40,48},{48,56},{56,64},{64,7... | collective-permute-start | bytes 196616 | tf_op jit(solution)/shard_map/ppermute | solution.py:50
  114.6 8.3 %collective-permute-start.28 = (bf16[128,256]{1,0:T(8,128)(2,1)S(1)}, bf16[128,256]{1,0:T(8,128)(2,1)S(1)}, u32[]{:S(2)}, u32[]{:S(2)}) collective-permute-start(bf16[128,256]{1,0:T(8,128)(2,1)S(1)} %get-tuple-element.60.own), channel_id=1, source_target_pairs={{8,0},{16,8},{24,16},{32,24},{40,32},{48,40},{56,48},{64,56},{72,6... | collective-permute-start | bytes 196616 | tf_op jit(solution)/shard_map/ppermute | solution.py:54
  125.4 5.2 %collective-permute-start.30 = (bf16[128,128]{1,0:T(8,128)(2,1)S(1)}, bf16[128,128]{1,0:T(8,128)(2,1)S(1)}, u32[]{:S(2)}, u32[]{:S(2)}) collective-permute-start(bf16[128,128]{1,0:T(8,128)(2,1)S(1)} %get-tuple-element.64), channel_id=1, source_target_pairs={{0,2},{2,4},{4,6},{6,0},{1,3},{3,5},{5,7},{7,1},{8,10},{10,12},{12... | collective-permute-start | bytes 98312 | tf_op jit(solution)/shard_map/ppermute | solution.py:231
  126.9 5.4 %collective-permute-start.31 = (bf16[128,128]{1,0:T(8,128)(2,1)S(1)}, bf16[128,128]{1,0:T(8,128)(2,1)S(1)}, u32[]{:S(2)}, u32[]{:S(2)}) collective-permute-start(bf16[128,128]{1,0:T(8,128)(2,1)S(1)} %get-tuple-element.65), channel_id=1, source_target_pairs={{0,4},{2,6},{4,0},{6,2},{1,5},{3,7},{5,1},{7,3},{8,12},{10,14},{12... | collective-permute-start | bytes 98312 | tf_op jit(solution)/shard_map/ppermute | solution.py:233
  129.6 3.9 %collective-permute-start.32 = (bf16[128,128]{1,0:T(8,128)(2,1)S(1)}, bf16[128,128]{1,0:T(8,128)(2,1)S(1)}, u32[]{:S(2)}, u32[]{:S(2)}) collective-permute-start(bf16[128,128]{1,0:T(8,128)(2,1)S(1)} %get-tuple-element.66), channel_id=1, source_target_pairs={{0,6},{2,0},{4,2},{6,4},{1,7},{3,1},{5,3},{7,5},{8,14},{10,8},{12,... | collective-permute-start | bytes 98312 | tf_op jit(solution)/shard_map/ppermute | solution.py:232
  (9 other events, 72.8 us)

commit v14 on v8

--- a/solution.py
+++ b/solution.py
@@ -85,9 +85,12 @@
 
 
 def pack_body(wq, wk, wv, wo, first, parts, sems):
-    fetch([(w.at[0], parts.at[n]) for n, w in enumerate((wq, wk, wv, wo))], sems)
+    @pl.when(pl.program_id(0) == 0)
+    def _():
+        fetch([(w.at[0], parts.at[n]) for n, w in enumerate((wq, wk, wv, wo))], sems)
+
     whole = jnp.concatenate([parts[n] for n in range(4)], axis=1)
-    for n in range(16):
+    for n in range(4):
         first[n] = whole
 
 
@@ -220,6 +223,28 @@
         into[...] = share.astype(into.dtype)
 
 
+def attend_halves_body(q, before, own, after, table, weights, mine, theirs, *, layer):
+    parts = [(p[0:128, 0:128], p[0:128, 128:256]) for p in (before, own, after)]
+    attended = attend(q, parts, table.at[2 * layer : 2 * layer + 2])
+    c = lax.axis_index("c")
+    for k in range(4):
+        for into, core in ((mine, c), (theirs, 1 - c)):
+            at = ahead("y", k) * 256 + core * 128
+            rows = weights[pl.ds(pl.multiple_of(at, 128), 128), 384:512]
+            share = lax.dot_general(attended, rows, NT, preferred_element_type=F32)
+            into[k] = share.astype(into.dtype)
+
+
+def join_body(mine, theirs, kept, s1, s2, s3):
+    for k, into in enumerate((kept, s1, s2, s3)):
+        into[...] = (mine[k] + theirs[k].astype(F32)).astype(into.dtype)
+
+
+def total_body(kept, r1, r2, r3, out):
+    total = kept[...] + r1[...].astype(F32) + r2[...].astype(F32) + r3[...].astype(F32)
+    out[...] = total.astype(BF16)
+
+
 def sum_body(kept, r1, r2, r3, out):
     out[...] = kept[...] + r1[...].astype(F32) + r2[...].astype(F32) + r3[...].astype(F32)
 
@@ -228,22 +253,25 @@
     out[...] = (mine[...] + theirs[...]).astype(BF16)
 
 
-def split_body(kept, r1, r2, r3, mine, theirs):
-    c = lax.axis_index("c")
-    for into, core in ((mine, c), (theirs, 1 - c)):
-        at = pl.ds(pl.multiple_of(core * 128, 128), 128)
-        into[...] = (
-            kept[:, at] + r1[:, at].astype(F32) + r2[:, at].astype(F32) + r3[:, at].astype(F32)
-        )
-
-
-def scattered(body, *args):
-    outs = [shaped(128, 256, dtype=F32)] + [shaped(128, 256)] * 3
-    kept, s1, s2, s3 = call(body, outs, *args)
+def turned(s1, s2, s3):
     r1 = lax.ppermute(s1, "y", turn(1))
     r3 = lax.ppermute(s3, "y", turn(3))
     r2 = lax.ppermute(s2, "y", turn(2))
-    return kept, r1, r2, r3
+    return r1, r2, r3
+
+
+def scattered(body, *args):
+    outs = [shaped(128, 256, dtype=F32)] + [shaped(128, 256)] * 3
+    kept, *sent = call(body, outs, *args)
+    return kept, *turned(*sent)
+
+
+def scattered_halves(body, *args):
+    outs = [shaped(4, 128, 128, dtype=F32), shaped(4, 128, 128)]
+    mine, theirs = call(body, outs, *args)
+    outs = [shaped(128, 128, dtype=F32)] + [shaped(128, 128)] * 3
+    kept, *sent = call(join_body, outs, mine, swap(theirs))
+    return call(total_body, shaped(128, 128), kept, *turned(*sent))
 
 
 def local(tokens, norm_gain, w_query, w_key, w_value, w_out, offset_bias, documents):
@@ -254,6 +282,7 @@
     ]
     first = call(
         pack_body, shaped(16, 64, 512), *held, in_specs=[hbm] * 4,
+        grid=(4,), out_specs=pl.BlockSpec((4, 64, 512), lambda n: (n, 0, 0)),
         scratch=[pltpu.VMEM((4, 64, 128), BF16), pltpu.SemaphoreType.DMA((4,))],
     )
     weights = gather_rows(first, SP)
@@ -279,13 +308,17 @@
             many, axes = ((many1, SP), (many2, "z"))[layer]
             next_weights = gather_rows(after_this(many, kv), axes)
         if layer == 0:
-            table = call(table_body, shaped(6, 128, 384, dtype=F32), wide, before, kv, after)
+            table = call(
+                table_body, shaped(6, 128, 384, dtype=F32), wide, before, kv, after,
+            )
+        args = (q, before, kv, after, table, weights)
+        if layer == 2:
+            return scattered_halves(
+                functools.partial(attend_halves_body, layer=layer), *args
+            )
         kept, r1, r2, r3 = scattered(
-            functools.partial(attend_scatter_body, layer=layer),
-            q, before, kv, after, table, weights,
+            functools.partial(attend_scatter_body, layer=layer), *args
         )
-        if layer == 2:
-            break
         if layer == 0:
             kept = after_this(kept, many2)
         half = call(sum_body, shaped(128, 256, dtype=F32), kept, r1, r2, r3)
@@ -296,8 +329,6 @@
             [shaped(128, 128), shaped(128, 256)],
             *in_order(stream, spread(stream, "y")), norm_gain, weights,
         )
-    mine, theirs = call(split_body, [shaped(128, 128, dtype=F32)] * 2, kept, r1, r2, r3)
-    return call(pair_sum_body, shaped(128, 128), mine, swap(theirs))
 
 
 def solution(mesh):

time: 127 us -> 127 us (level)
  the two profiles are of different devices: /device:TPU:39 before, /device:TPU:38 now
where the time goes in v14:
time: 127 us; the launch traced here: 126 us
  starting transfers between devices  68.8 us (54%)
  waiting for transfers between devices  45.6 us (36%)
  Pallas kernels  9.2 us (7%)
  local copies, waits for them, and re-layouts  2 us (2%)
    all_to_all x3, starting transfers between devices, gather_rows(): return lax.all_to_all(a, axes, 0, 0, tiled=True).reshape(1024, 512)  19.6 us
    ppermute x12, starting transfers between devices, spread(): return [lax.ppermute(a, axis, turn(k)) for k in (1, 3, 2)]  17.1 us
    ppermute x3, waiting for transfers between devices, from_after(): return lax.ppermute(a, SP, [(i + 1, i) for i in range(15)])  11.3 us
    ppermute x3, starting transfers between devices, from_before(): return lax.ppermute(a, SP, [(i, i + 1) for i in range(15)])  10.1 us
    pallas_call x16, Pallas kernels, call(): pl.pallas_call(body, out_shape=outs, **specs, scratch_shapes=list(scratch...  9.2 us
    ppermute x3, starting transfers between devices, turned(): r2 = lax.ppermute(s2, 'y', turn(2))  9.17 us
    ppermute x3, starting transfers between devices, from_after(): return lax.ppermute(a, SP, [(i + 1, i) for i in range(15)])  8.31 us
    ppermute x12, waiting for transfers between devices, spread(): return [lax.ppermute(a, axis, turn(k)) for k in (1, 3, 2)]  7.88 us
  transfers between devices with their start and end apart: 34, of which 23 were waited for; matrix products, arithmetic and copies ran while one was open for 0% of the time, Pallas kernels for 3%

profile of v14, /device:TPU:38, one launch (start us, length us, event | category | flops | bytes accessed | tf_op | source)
XLA Modules:
  0.0 125.9 jit_solution(18338657031417143414)
XLA Ops:
  0.0 2.4 %shard_map.83 = bf16[16,64,512]{2,1,0:T(8,128)(2,1)} custom-call(bf16[3,64,128]{2,1,0:T(8,128)(2,1)} %wq.3, bf16[3,64,128]{2,1,0:T(8,128)(2,1)} %wk.3, bf16[3,64,128]{2,1,0:T(8,128)(2,1)} %wv.3, bf16[3,64,128]{2,1,0:T(8,128)(2,1)} %bitcast.16), custom_call_target="tpu_custom_call" | custom-call | tf_op jit(solution)/shard_map/pallas_call | solution.py:66
  2.4 8.0 %all-to-all-start = ((bf16[16,64,512]{2,1,0:T(8,128)(2,1)}), bf16[16,64,512]{2,1,0:T(8,128)(2,1)S(1)}, u32[]{:S(2)}, u32[]{:S(2)}) async-start(bf16[16,64,512]{2,1,0:T(8,128)(2,1)} %shard_map.83), calls=%async_computation | async-start | bytes 2097152 | tf_op jit(solution)/shard_map/all_to_all | solution.py:38
  10.4 1.6 %collective-permute-start = (bf16[128,128]{1,0:T(8,128)(2,1)S(1)}, bf16[128,128]{1,0:T(8,128)(2,1)S(1)}, u32[]{:S(2)}, u32[]{:S(2)}) collective-permute-start(bf16[128,128]{1,0:T(8,128)(2,1)S(1)} %copy-done.5), channel_id=1, source_target_pairs={{0,2},{2,4},{4,6},{6,0},{1,3},{3,5},{5,7},{7,1},{8,10},{10,12},{12... | collective-permute-start | bytes 98312 | tf_op jit(solution)/shard_map/ppermute | solution.py:30
  12.0 2.9 %collective-permute-start.1 = (bf16[128,128]{1,0:T(8,128)(2,1)S(1)}, bf16[128,128]{1,0:T(8,128)(2,1)S(1)}, u32[]{:S(2)}, u32[]{:S(2)}) collective-permute-start(bf16[128,128]{1,0:T(8,128)(2,1)S(1)} %copy-done.5), channel_id=1, source_target_pairs={{0,4},{2,6},{4,0},{6,2},{1,5},{3,7},{5,1},{7,3},{8,12},{10,14},{12... | collective-permute-start | bytes 98312 | tf_op jit(solution)/shard_map/ppermute | solution.py:30
  14.9 1.3 %collective-permute-start.2 = (bf16[128,128]{1,0:T(8,128)(2,1)S(1)}, bf16[128,128]{1,0:T(8,128)(2,1)S(1)}, u32[]{:S(2)}, u32[]{:S(2)}) collective-permute-start(bf16[128,128]{1,0:T(8,128)(2,1)S(1)} %copy-done.5), channel_id=1, source_target_pairs={{0,6},{2,0},{4,2},{6,4},{1,7},{3,1},{5,3},{7,5},{8,14},{10,8},{12,... | collective-permute-start | bytes 98312 | tf_op jit(solution)/shard_map/ppermute | solution.py:30
  19.0 1.3 %collective-permute-done.3.partner = bf16[4,128,128]{2,1,0:T(8,128)(2,1)S(1)} collective-permute-done((bf16[4,128,128]{2,1,0:T(8,128)(2,1)S(1)}, bf16[4,128,128]{2,1,0:T(8,128)(2,1)S(1)}, u32[]{:S(2)}, u32[]{:S(2)}) %collective-permute-start.3) | collective-permute-done | bytes 131104 | tf_op jit(solution)/shard_map/ppermute | solution.py:46
  20.3 4.2 %all-to-all-done = bf16[16,64,512]{2,1,0:T(8,128)(2,1)S(1)} async-done(((bf16[16,64,512]{2,1,0:T(8,128)(2,1)}), bf16[16,64,512]{2,1,0:T(8,128)(2,1)S(1)}, u32[]{:S(2)}, u32[]{:S(2)}) %all-to-all-start) | async-done | bytes 1048608 | tf_op jit(solution)/shard_map/all_to_all | solution.py:38
  25.1 7.1 %all-to-all-start.1 = ((bf16[16,64,512]{2,1,0:T(8,128)(2,1)}), bf16[16,64,512]{2,1,0:T(8,128)(2,1)S(1)}, u32[]{:S(2)}, u32[]{:S(2)}) async-start(bf16[16,64,512]{2,1,0:T(8,128)(2,1)} %copy-done.1), calls=%async_computation.1 | async-start | bytes 2097152 | tf_op jit(solution)/shard_map/all_to_all | solution.py:38
  32.2 3.4 %collective-permute-start.4 = (bf16[144,256]{1,0:T(8,128)(2,1)S(1)}, bf16[144,256]{1,0:T(8,128)(2,1)S(1)}, u32[]{:S(2)}, u32[]{:S(2)}) collective-permute-start(bf16[144,256]{1,0:T(8,128)(2,1)S(1)} %get-tuple-element.35.own), channel_id=1, source_target_pairs={{0,8},{8,16},{16,24},{24,32},{32,40},{40,48},{48,56},{56,64},{64,7... | collective-permute-start | bytes 221192 | tf_op jit(solution)/shard_map/ppermute | solution.py:50
  35.6 2.5 %collective-permute-start.5 = (bf16[144,256]{1,0:T(8,128)(2,1)S(1)}, bf16[144,256]{1,0:T(8,128)(2,1)S(1)}, u32[]{:S(2)}, u32[]{:S(2)}) collective-permute-start(bf16[144,256]{1,0:T(8,128)(2,1)S(1)} %get-tuple-element.35.own), channel_id=1, source_target_pairs={{8,0},{16,8},{24,16},{32,24},{40,32},{48,40},{56,48},{64,56},{72,6... | collective-permute-start | bytes 221192 | tf_op jit(solution)/shard_map/ppermute | solution.py:54
  38.1 2.7 %collective-permute-start.6 = (bf16[64,512]{1,0:T(8,128)(2,1)S(1)}, bf16[64,512]{1,0:T(8,128)(2,1)S(1)}, u32[]{:S(2)}, u32[]{:S(2)}) collective-permute-start(bf16[64,512]{1,0:T(8,128)(2,1)S(1)} %get-tuple-element.38.p0), channel_id=1, source_target_pairs={{0,8},{8,16},{16,24},{24,0},{1,9},{9,17},{17,25},{25,1},{2,10},{10... | collective-permute-start | bytes 196616 | tf_op jit(solution)/shard_map/ppermute | solution.py:30
  41.8 5.0 %collective-permute-done.4.before = bf16[144,256]{1,0:T(8,128)(2,1)S(1)} collective-permute-done((bf16[144,256]{1,0:T(8,128)(2,1)S(1)}, bf16[144,256]{1,0:T(8,128)(2,1)S(1)}, u32[]{:S(2)}, u32[]{:S(2)}) %collective-permute-start.4) | collective-permute-done | bytes 73760 | tf_op jit(solution)/shard_map/ppermute | solution.py:50
  48.5 3.3 %collective-permute-start.10 = (bf16[128,256]{1,0:T(8,128)(2,1)S(1)}, bf16[128,256]{1,0:T(8,128)(2,1)S(1)}, u32[]{:S(2)}, u32[]{:S(2)}) collective-permute-start(bf16[128,256]{1,0:T(8,128)(2,1)S(1)} %get-tuple-element.41), channel_id=1, source_target_pairs={{0,4},{2,6},{4,0},{6,2},{1,5},{3,7},{5,1},{7,3},{8,12},{10,14},{12... | collective-permute-start | bytes 196616 | tf_op jit(solution)/shard_map/ppermute | solution.py:259
  56.0 2.3 %collective-permute-done.9.r1 = bf16[128,256]{1,0:T(8,128)(2,1)S(1)} collective-permute-done((bf16[128,256]{1,0:T(8,128)(2,1)S(1)}, bf16[128,256]{1,0:T(8,128)(2,1)S(1)}, u32[]{:S(2)}, u32[]{:S(2)}) %collective-permute-start.9) | collective-permute-done | bytes 65568 | tf_op jit(solution)/shard_map/ppermute | solution.py:257
  58.4 1.3 %collective-permute-done.12.theirs = f32[128,256]{1,0:T(8,128)S(1)} collective-permute-done((f32[128,256]{1,0:T(8,128)S(1)}, f32[128,256]{1,0:T(8,128)S(1)}, u32[]{:S(2)}, u32[]{:S(2)}) %collective-permute-start.12) | collective-permute-done | bytes 131104 | tf_op jit(solution)/shard_map/ppermute | solution.py:46
  59.9 1.4 %collective-permute-start.14 = (bf16[128,256]{1,0:T(8,128)(2,1)S(1)}, bf16[128,256]{1,0:T(8,128)(2,1)S(1)}, u32[]{:S(2)}, u32[]{:S(2)}) collective-permute-start(bf16[128,256]{1,0:T(8,128)(2,1)S(1)} %shard_map.89.x0), channel_id=1, source_target_pairs={{0,4},{2,6},{4,0},{6,2},{1,5},{3,7},{5,1},{7,3},{8,12},{10,14},{12... | collective-permute-start | bytes 196616 | tf_op jit(solution)/shard_map/ppermute | solution.py:30
  61.3 1.8 %collective-permute-start.15 = (bf16[128,256]{1,0:T(8,128)(2,1)S(1)}, bf16[128,256]{1,0:T(8,128)(2,1)S(1)}, u32[]{:S(2)}, u32[]{:S(2)}) collective-permute-start(bf16[128,256]{1,0:T(8,128)(2,1)S(1)} %shard_map.89.x0), channel_id=1, source_target_pairs={{0,6},{2,0},{4,2},{6,4},{1,7},{3,1},{5,3},{7,5},{8,14},{10,8},{12,... | collective-permute-start | bytes 196616 | tf_op jit(solution)/shard_map/ppermute | solution.py:30
  63.1 3.5 %collective-permute-done.13.x1 = bf16[128,256]{1,0:T(8,128)(2,1)S(1)} collective-permute-done((bf16[128,256]{1,0:T(8,128)(2,1)S(1)}, bf16[128,256]{1,0:T(8,128)(2,1)S(1)}, u32[]{:S(2)}, u32[]{:S(2)}) %collective-permute-start.13) | collective-permute-done | bytes 65568 | tf_op jit(solution)/shard_map/ppermute | solution.py:30
  67.7 4.6 %all-to-all-start.2 = ((bf16[4,4,64,512]{3,2,1,0:T(8,128)(2,1)}), bf16[4,4,64,512]{3,2,1,0:T(8,128)(2,1)S(1)}, u32[]{:S(2)}, u32[]{:S(2)}) async-start(bf16[4,4,64,512]{3,2,1,0:T(8,128)(2,1)} %copy-done), calls=%async_computation.2 | async-start | bytes 2097152 | tf_op jit(solution)/shard_map/all_to_all | solution.py:38
  72.3 4.8 %collective-permute-start.16 = (bf16[128,256]{1,0:T(8,128)(2,1)S(1)}, bf16[128,256]{1,0:T(8,128)(2,1)S(1)}, u32[]{:S(2)}, u32[]{:S(2)}) collective-permute-start(bf16[128,256]{1,0:T(8,128)(2,1)S(1)} %get-tuple-element.45.own), channel_id=1, source_target_pairs={{0,8},{8,16},{16,24},{24,32},{32,40},{40,48},{48,56},{56,64},{64,7... | collective-permute-start | bytes 196616 | tf_op jit(solution)/shard_map/ppermute | solution.py:50
  77.0 1.9 %collective-permute-start.17 = (bf16[128,256]{1,0:T(8,128)(2,1)S(1)}, bf16[128,256]{1,0:T(8,128)(2,1)S(1)}, u32[]{:S(2)}, u32[]{:S(2)}) collective-permute-start(bf16[128,256]{1,0:T(8,128)(2,1)S(1)} %get-tuple-element.45.own), channel_id=1, source_target_pairs={{8,0},{16,8},{24,16},{32,24},{40,32},{48,40},{56,48},{64,56},{72,6... | collective-permute-start | bytes 196616 | tf_op jit(solution)/shard_map/ppermute | solution.py:54
  79.0 7.0 %collective-permute-done.17.after = bf16[128,256]{1,0:T(8,128)(2,1)S(1)} collective-permute-done((bf16[128,256]{1,0:T(8,128)(2,1)S(1)}, bf16[128,256]{1,0:T(8,128)(2,1)S(1)}, u32[]{:S(2)}, u32[]{:S(2)}) %collective-permute-start.17) | collective-permute-done | bytes 65568 | tf_op jit(solution)/shard_map/ppermute | solution.py:54
  88.0 2.8 %collective-permute-start.19 = (bf16[128,256]{1,0:T(8,128)(2,1)S(1)}, bf16[128,256]{1,0:T(8,128)(2,1)S(1)}, u32[]{:S(2)}, u32[]{:S(2)}) collective-permute-start(bf16[128,256]{1,0:T(8,128)(2,1)S(1)} %get-tuple-element.48), channel_id=1, source_target_pairs={{0,4},{2,6},{4,0},{6,2},{1,5},{3,7},{5,1},{7,3},{8,12},{10,14},{12... | collective-permute-start | bytes 196616 | tf_op jit(solution)/shard_map/ppermute | solution.py:259
  90.9 1.6 %collective-permute-done.18.r1 = bf16[128,256]{1,0:T(8,128)(2,1)S(1)} collective-permute-done((bf16[128,256]{1,0:T(8,128)(2,1)S(1)}, bf16[128,256]{1,0:T(8,128)(2,1)S(1)}, u32[]{:S(2)}, u32[]{:S(2)}) %collective-permute-start.18) | collective-permute-done | bytes 65568 | tf_op jit(solution)/shard_map/ppermute | solution.py:257
  96.9 2.8 %collective-permute-start.23 = (bf16[128,256]{1,0:T(8,128)(2,1)S(1)}, bf16[128,256]{1,0:T(8,128)(2,1)S(1)}, u32[]{:S(2)}, u32[]{:S(2)}) collective-permute-start(bf16[128,256]{1,0:T(8,128)(2,1)S(1)} %shard_map.93.x0), channel_id=1, source_target_pairs={{0,4},{2,6},{4,0},{6,2},{1,5},{3,7},{5,1},{7,3},{8,12},{10,14},{12... | collective-permute-start | bytes 196616 | tf_op jit(solution)/shard_map/ppermute | solution.py:30
  100.8 2.6 %collective-permute-done.22.x1 = bf16[128,256]{1,0:T(8,128)(2,1)S(1)} collective-permute-done((bf16[128,256]{1,0:T(8,128)(2,1)S(1)}, bf16[128,256]{1,0:T(8,128)(2,1)S(1)}, u32[]{:S(2)}, u32[]{:S(2)}) %collective-permute-start.22) | collective-permute-done | bytes 65568 | tf_op jit(solution)/shard_map/ppermute | solution.py:30
  104.5 1.9 %collective-permute-start.25 = (bf16[128,256]{1,0:T(8,128)(2,1)S(1)}, bf16[128,256]{1,0:T(8,128)(2,1)S(1)}, u32[]{:S(2)}, u32[]{:S(2)}) collective-permute-start(bf16[128,256]{1,0:T(8,128)(2,1)S(1)} %get-tuple-element.52.own), channel_id=1, source_target_pairs={{0,8},{8,16},{16,24},{24,32},{32,40},{40,48},{48,56},{56,64},{64,7... | collective-permute-start | bytes 196616 | tf_op jit(solution)/shard_map/ppermute | solution.py:50
  106.5 3.9 %collective-permute-start.26 = (bf16[128,256]{1,0:T(8,128)(2,1)S(1)}, bf16[128,256]{1,0:T(8,128)(2,1)S(1)}, u32[]{:S(2)}, u32[]{:S(2)}) collective-permute-start(bf16[128,256]{1,0:T(8,128)(2,1)S(1)} %get-tuple-element.52.own), channel_id=1, source_target_pairs={{8,0},{16,8},{24,16},{32,24},{40,32},{48,40},{56,48},{64,56},{72,6... | collective-permute-start | bytes 196616 | tf_op jit(solution)/shard_map/ppermute | solution.py:54
  110.7 4.0 %collective-permute-done.26.after = bf16[128,256]{1,0:T(8,128)(2,1)S(1)} collective-permute-done((bf16[128,256]{1,0:T(8,128)(2,1)S(1)}, bf16[128,256]{1,0:T(8,128)(2,1)S(1)}, u32[]{:S(2)}, u32[]{:S(2)}) %collective-permute-start.26) | collective-permute-done | bytes 65568 | tf_op jit(solution)/shard_map/ppermute | solution.py:54
  118.3 3.1 %collective-permute-start.29 = (bf16[128,128]{1,0:T(8,128)(2,1)S(1)}, bf16[128,128]{1,0:T(8,128)(2,1)S(1)}, u32[]{:S(2)}, u32[]{:S(2)}) collective-permute-start(bf16[128,128]{1,0:T(8,128)(2,1)S(1)} %get-tuple-element.57), channel_id=1, source_target_pairs={{0,4},{2,6},{4,0},{6,2},{1,5},{3,7},{5,1},{7,3},{8,12},{10,14},{12... | collective-permute-start | bytes 98312 | tf_op jit(solution)/shard_map/ppermute | solution.py:259
  122.4 1.3 %collective-permute-done.29.r2 = bf16[128,128]{1,0:T(8,128)(2,1)S(1)} collective-permute-done((bf16[128,128]{1,0:T(8,128)(2,1)S(1)}, bf16[128,128]{1,0:T(8,128)(2,1)S(1)}, u32[]{:S(2)}, u32[]{:S(2)}) %collective-permute-start.29) | collective-permute-done | bytes 32800 | tf_op jit(solution)/shard_map/ppermute | solution.py:259
  123.7 1.6 %collective-permute-done.30.r3 = bf16[128,128]{1,0:T(8,128)(2,1)S(1)} collective-permute-done((bf16[128,128]{1,0:T(8,128)(2,1)S(1)}, bf16[128,128]{1,0:T(8,128)(2,1)S(1)}, u32[]{:S(2)}, u32[]{:S(2)}) %collective-permute-start.30) | collective-permute-done | bytes 32800 | tf_op jit(solution)/shard_map/ppermute | solution.py:258
  (65 shorter events, 25.6 us)
Async XLA Ops:
  2.4 22.1 %all-to-all-start = ((bf16[16,64,512]{2,1,0:T(8,128)(2,1)}), bf16[16,64,512]{2,1,0:T(8,128)(2,1)S(1)}, u32[]{:S(2)}, u32[]{:S(2)}) async-start(bf16[16,64,512]{2,1,0:T(8,128)(2,1)} %shard_map.83), calls=%async_computation | async-start | bytes 2097152 | tf_op jit(solution)/shard_map/all_to_all | solution.py:38
  10.4 7.9 %collective-permute-start = (bf16[128,128]{1,0:T(8,128)(2,1)S(1)}, bf16[128,128]{1,0:T(8,128)(2,1)S(1)}, u32[]{:S(2)}, u32[]{:S(2)}) collective-permute-start(bf16[128,128]{1,0:T(8,128)(2,1)S(1)} %copy-done.5), channel_id=1, source_target_pairs={{0,2},{2,4},{4,6},{6,0},{1,3},{3,5},{5,7},{7,1},{8,10},{10,12},{12... | collective-permute-start | bytes 98312 | tf_op jit(solution)/shard_map/ppermute | solution.py:30
  12.0 6.2 %collective-permute-start.1 = (bf16[128,128]{1,0:T(8,128)(2,1)S(1)}, bf16[128,128]{1,0:T(8,128)(2,1)S(1)}, u32[]{:S(2)}, u32[]{:S(2)}) collective-permute-start(bf16[128,128]{1,0:T(8,128)(2,1)S(1)} %copy-done.5), channel_id=1, source_target_pairs={{0,4},{2,6},{4,0},{6,2},{1,5},{3,7},{5,1},{7,3},{8,12},{10,14},{12... | collective-permute-start | bytes 98312 | tf_op jit(solution)/shard_map/ppermute | solution.py:30
  14.9 3.9 %collective-permute-start.2 = (bf16[128,128]{1,0:T(8,128)(2,1)S(1)}, bf16[128,128]{1,0:T(8,128)(2,1)S(1)}, u32[]{:S(2)}, u32[]{:S(2)}) collective-permute-start(bf16[128,128]{1,0:T(8,128)(2,1)S(1)} %copy-done.5), channel_id=1, source_target_pairs={{0,6},{2,0},{4,2},{6,4},{1,7},{3,1},{5,3},{7,5},{8,14},{10,8},{12,... | collective-permute-start | bytes 98312 | tf_op jit(solution)/shard_map/ppermute | solution.py:30
  25.1 42.1 %all-to-all-start.1 = ((bf16[16,64,512]{2,1,0:T(8,128)(2,1)}), bf16[16,64,512]{2,1,0:T(8,128)(2,1)S(1)}, u32[]{:S(2)}, u32[]{:S(2)}) async-start(bf16[16,64,512]{2,1,0:T(8,128)(2,1)} %copy-done.1), calls=%async_computation.1 | async-start | bytes 2097152 | tf_op jit(solution)/shard_map/all_to_all | solution.py:38
  32.2 14.5 %collective-permute-start.4 = (bf16[144,256]{1,0:T(8,128)(2,1)S(1)}, bf16[144,256]{1,0:T(8,128)(2,1)S(1)}, u32[]{:S(2)}, u32[]{:S(2)}) collective-permute-start(bf16[144,256]{1,0:T(8,128)(2,1)S(1)} %get-tuple-element.35.own), channel_id=1, source_target_pairs={{0,8},{8,16},{16,24},{24,32},{32,40},{40,48},{48,56},{56,64},{64,7... | collective-permute-start | bytes 221192 | tf_op jit(solution)/shard_map/ppermute | solution.py:50
  35.6 11.4 %collective-permute-start.5 = (bf16[144,256]{1,0:T(8,128)(2,1)S(1)}, bf16[144,256]{1,0:T(8,128)(2,1)S(1)}, u32[]{:S(2)}, u32[]{:S(2)}) collective-permute-start(bf16[144,256]{1,0:T(8,128)(2,1)S(1)} %get-tuple-element.35.own), channel_id=1, source_target_pairs={{8,0},{16,8},{24,16},{32,24},{40,32},{48,40},{56,48},{64,56},{72,6... | collective-permute-start | bytes 221192 | tf_op jit(solution)/shard_map/ppermute | solution.py:54
  38.1 14.7 %collective-permute-start.6 = (bf16[64,512]{1,0:T(8,128)(2,1)S(1)}, bf16[64,512]{1,0:T(8,128)(2,1)S(1)}, u32[]{:S(2)}, u32[]{:S(2)}) collective-permute-start(bf16[64,512]{1,0:T(8,128)(2,1)S(1)} %get-tuple-element.38.p0), channel_id=1, source_target_pairs={{0,8},{8,16},{16,24},{24,0},{1,9},{9,17},{17,25},{25,1},{2,10},{10... | collective-permute-start | bytes 196616 | tf_op jit(solution)/shard_map/ppermute | solution.py:30
  40.8 13.0 %collective-permute-start.7 = (bf16[64,512]{1,0:T(8,128)(2,1)S(1)}, bf16[64,512]{1,0:T(8,128)(2,1)S(1)}, u32[]{:S(2)}, u32[]{:S(2)}) collective-permute-start(bf16[64,512]{1,0:T(8,128)(2,1)S(1)} %get-tuple-element.38.p0), channel_id=1, source_target_pairs={{0,16},{8,24},{16,0},{24,8},{1,17},{9,25},{17,1},{25,9},{2,18},{10... | collective-permute-start | bytes 196616 | tf_op jit(solution)/shard_map/ppermute | solution.py:30
  41.1 12.7 %collective-permute-start.8 = (bf16[64,512]{1,0:T(8,128)(2,1)S(1)}, bf16[64,512]{1,0:T(8,128)(2,1)S(1)}, u32[]{:S(2)}, u32[]{:S(2)}) collective-permute-start(bf16[64,512]{1,0:T(8,128)(2,1)S(1)} %get-tuple-element.38.p0), channel_id=1, source_target_pairs={{0,24},{8,0},{16,8},{24,16},{1,25},{9,1},{17,9},{25,17},{2,26},{10... | collective-permute-start | bytes 196616 | tf_op jit(solution)/shard_map/ppermute | solution.py:30
  48.5 6.4 %collective-permute-start.10 = (bf16[128,256]{1,0:T(8,128)(2,1)S(1)}, bf16[128,256]{1,0:T(8,128)(2,1)S(1)}, u32[]{:S(2)}, u32[]{:S(2)}) collective-permute-start(bf16[128,256]{1,0:T(8,128)(2,1)S(1)} %get-tuple-element.41), channel_id=1, source_target_pairs={{0,4},{2,6},{4,0},{6,2},{1,5},{3,7},{5,1},{7,3},{8,12},{10,14},{12... | collective-permute-start | bytes 196616 | tf_op jit(solution)/shard_map/ppermute | solution.py:259
  51.8 4.3 %collective-permute-start.11 = (bf16[128,256]{1,0:T(8,128)(2,1)S(1)}, bf16[128,256]{1,0:T(8,128)(2,1)S(1)}, u32[]{:S(2)}, u32[]{:S(2)}) collective-permute-start(bf16[128,256]{1,0:T(8,128)(2,1)S(1)} %get-tuple-element.42), channel_id=1, source_target_pairs={{0,6},{2,0},{4,2},{6,4},{1,7},{3,1},{5,3},{7,5},{8,14},{10,8},{12,... | collective-permute-start | bytes 196616 | tf_op jit(solution)/shard_map/ppermute | solution.py:258
  52.8 5.5 %collective-permute-start.9 = (bf16[128,256]{1,0:T(8,128)(2,1)S(1)}, bf16[128,256]{1,0:T(8,128)(2,1)S(1)}, u32[]{:S(2)}, u32[]{:S(2)}) collective-permute-start(bf16[128,256]{1,0:T(8,128)(2,1)S(1)} %get-tuple-element.40), channel_id=1, source_target_pairs={{0,2},{2,4},{4,6},{6,0},{1,3},{3,5},{5,7},{7,1},{8,10},{10,12},{12... | collective-permute-start | bytes 196616 | tf_op jit(solution)/shard_map/ppermute | solution.py:257
  58.3 1.4 %collective-permute-start.12 = (f32[128,256]{1,0:T(8,128)S(1)}, f32[128,256]{1,0:T(8,128)S(1)}, u32[]{:S(2)}, u32[]{:S(2)}) collective-permute-start(f32[128,256]{1,0:T(8,128)S(1)} %shard_map.88.mine), channel_id=1, source_target_pairs={{0,1},{1,0},{2,3},{3,2},{4,5},{5,4},{6,7},{7,6},{8,9},{9,8},{10,11... | collective-permute-start | bytes 393224 | tf_op jit(solution)/shard_map/ppermute | solution.py:46
  59.8 6.8 %collective-permute-start.13 = (bf16[128,256]{1,0:T(8,128)(2,1)S(1)}, bf16[128,256]{1,0:T(8,128)(2,1)S(1)}, u32[]{:S(2)}, u32[]{:S(2)}) collective-permute-start(bf16[128,256]{1,0:T(8,128)(2,1)S(1)} %shard_map.89.x0), channel_id=1, source_target_pairs={{0,2},{2,4},{4,6},{6,0},{1,3},{3,5},{5,7},{7,1},{8,10},{10,12},{12... | collective-permute-start | bytes 196616 | tf_op jit(solution)/shard_map/ppermute | solution.py:30
  59.9 6.8 %collective-permute-start.14 = (bf16[128,256]{1,0:T(8,128)(2,1)S(1)}, bf16[128,256]{1,0:T(8,128)(2,1)S(1)}, u32[]{:S(2)}, u32[]{:S(2)}) collective-permute-start(bf16[128,256]{1,0:T(8,128)(2,1)S(1)} %shard_map.89.x0), channel_id=1, source_target_pairs={{0,4},{2,6},{4,0},{6,2},{1,5},{3,7},{5,1},{7,3},{8,12},{10,14},{12... | collective-permute-start | bytes 196616 | tf_op jit(solution)/shard_map/ppermute | solution.py:30
  61.3 5.9 %collective-permute-start.15 = (bf16[128,256]{1,0:T(8,128)(2,1)S(1)}, bf16[128,256]{1,0:T(8,128)(2,1)S(1)}, u32[]{:S(2)}, u32[]{:S(2)}) collective-permute-start(bf16[128,256]{1,0:T(8,128)(2,1)S(1)} %shard_map.89.x0), channel_id=1, source_target_pairs={{0,6},{2,0},{4,2},{6,4},{1,7},{3,1},{5,3},{7,5},{8,14},{10,8},{12,... | collective-permute-start | bytes 196616 | tf_op jit(solution)/shard_map/ppermute | solution.py:30
  67.7 36.3 %all-to-all-start.2 = ((bf16[4,4,64,512]{3,2,1,0:T(8,128)(2,1)}), bf16[4,4,64,512]{3,2,1,0:T(8,128)(2,1)S(1)}, u32[]{:S(2)}, u32[]{:S(2)}) async-start(bf16[4,4,64,512]{3,2,1,0:T(8,128)(2,1)} %copy-done), calls=%async_computation.2 | async-start | bytes 2097152 | tf_op jit(solution)/shard_map/all_to_all | solution.py:38
  72.3 6.7 %collective-permute-start.16 = (bf16[128,256]{1,0:T(8,128)(2,1)S(1)}, bf16[128,256]{1,0:T(8,128)(2,1)S(1)}, u32[]{:S(2)}, u32[]{:S(2)}) collective-permute-start(bf16[128,256]{1,0:T(8,128)(2,1)S(1)} %get-tuple-element.45.own), channel_id=1, source_target_pairs={{0,8},{8,16},{16,24},{24,32},{32,40},{40,48},{48,56},{56,64},{64,7... | collective-permute-start | bytes 196616 | tf_op jit(solution)/shard_map/ppermute | solution.py:50
  77.0 9.0 %collective-permute-start.17 = (bf16[128,256]{1,0:T(8,128)(2,1)S(1)}, bf16[128,256]{1,0:T(8,128)(2,1)S(1)}, u32[]{:S(2)}, u32[]{:S(2)}) collective-permute-start(bf16[128,256]{1,0:T(8,128)(2,1)S(1)} %get-tuple-element.45.own), channel_id=1, source_target_pairs={{8,0},{16,8},{24,16},{32,24},{40,32},{48,40},{56,48},{64,56},{72,6... | collective-permute-start | bytes 196616 | tf_op jit(solution)/shard_map/ppermute | solution.py:54
  86.9 5.5 %collective-permute-start.18 = (bf16[128,256]{1,0:T(8,128)(2,1)S(1)}, bf16[128,256]{1,0:T(8,128)(2,1)S(1)}, u32[]{:S(2)}, u32[]{:S(2)}) collective-permute-start(bf16[128,256]{1,0:T(8,128)(2,1)S(1)} %get-tuple-element.47), channel_id=1, source_target_pairs={{0,2},{2,4},{4,6},{6,0},{1,3},{3,5},{5,7},{7,1},{8,10},{10,12},{12... | collective-permute-start | bytes 196616 | tf_op jit(solution)/shard_map/ppermute | solution.py:257
  88.0 5.8 %collective-permute-start.19 = (bf16[128,256]{1,0:T(8,128)(2,1)S(1)}, bf16[128,256]{1,0:T(8,128)(2,1)S(1)}, u32[]{:S(2)}, u32[]{:S(2)}) collective-permute-start(bf16[128,256]{1,0:T(8,128)(2,1)S(1)} %get-tuple-element.48), channel_id=1, source_target_pairs={{0,4},{2,6},{4,0},{6,2},{1,5},{3,7},{5,1},{7,3},{8,12},{10,14},{12... | collective-permute-start | bytes 196616 | tf_op jit(solution)/shard_map/ppermute | solution.py:259
  90.9 4.3 %collective-permute-start.20 = (bf16[128,256]{1,0:T(8,128)(2,1)S(1)}, bf16[128,256]{1,0:T(8,128)(2,1)S(1)}, u32[]{:S(2)}, u32[]{:S(2)}) collective-permute-start(bf16[128,256]{1,0:T(8,128)(2,1)S(1)} %get-tuple-element.49), channel_id=1, source_target_pairs={{0,6},{2,0},{4,2},{6,4},{1,7},{3,1},{5,3},{7,5},{8,14},{10,8},{12,... | collective-permute-start | bytes 196616 | tf_op jit(solution)/shard_map/ppermute | solution.py:258
  95.2 1.4 %collective-permute-start.21 = (f32[128,256]{1,0:T(8,128)S(1)}, f32[128,256]{1,0:T(8,128)S(1)}, u32[]{:S(2)}, u32[]{:S(2)}) collective-permute-start(f32[128,256]{1,0:T(8,128)S(1)} %shard_map.92.mine), channel_id=1, source_target_pairs={{0,1},{1,0},{2,3},{3,2},{4,5},{5,4},{6,7},{7,6},{8,9},{9,8},{10,11... | collective-permute-start | bytes 393224 | tf_op jit(solution)/shard_map/ppermute | solution.py:46
  96.6 6.8 %collective-permute-start.22 = (bf16[128,256]{1,0:T(8,128)(2,1)S(1)}, bf16[128,256]{1,0:T(8,128)(2,1)S(1)}, u32[]{:S(2)}, u32[]{:S(2)}) collective-permute-start(bf16[128,256]{1,0:T(8,128)(2,1)S(1)} %shard_map.93.x0), channel_id=1, source_target_pairs={{0,2},{2,4},{4,6},{6,0},{1,3},{3,5},{5,7},{7,1},{8,10},{10,12},{12... | collective-permute-start | bytes 196616 | tf_op jit(solution)/shard_map/ppermute | solution.py:30
  96.9 6.5 %collective-permute-start.23 = (bf16[128,256]{1,0:T(8,128)(2,1)S(1)}, bf16[128,256]{1,0:T(8,128)(2,1)S(1)}, u32[]{:S(2)}, u32[]{:S(2)}) collective-permute-start(bf16[128,256]{1,0:T(8,128)(2,1)S(1)} %shard_map.93.x0), channel_id=1, source_target_pairs={{0,4},{2,6},{4,0},{6,2},{1,5},{3,7},{5,1},{7,3},{8,12},{10,14},{12... | collective-permute-start | bytes 196616 | tf_op jit(solution)/shard_map/ppermute | solution.py:30
  99.7 4.3 %collective-permute-start.24 = (bf16[128,256]{1,0:T(8,128)(2,1)S(1)}, bf16[128,256]{1,0:T(8,128)(2,1)S(1)}, u32[]{:S(2)}, u32[]{:S(2)}) collective-permute-start(bf16[128,256]{1,0:T(8,128)(2,1)S(1)} %shard_map.93.x0), channel_id=1, source_target_pairs={{0,6},{2,0},{4,2},{6,4},{1,7},{3,1},{5,3},{7,5},{8,14},{10,8},{12,... | collective-permute-start | bytes 196616 | tf_op jit(solution)/shard_map/ppermute | solution.py:30
  104.5 6.2 %collective-permute-start.25 = (bf16[128,256]{1,0:T(8,128)(2,1)S(1)}, bf16[128,256]{1,0:T(8,128)(2,1)S(1)}, u32[]{:S(2)}, u32[]{:S(2)}) collective-permute-start(bf16[128,256]{1,0:T(8,128)(2,1)S(1)} %get-tuple-element.52.own), channel_id=1, source_target_pairs={{0,8},{8,16},{16,24},{24,32},{32,40},{40,48},{48,56},{56,64},{64,7... | collective-permute-start | bytes 196616 | tf_op jit(solution)/shard_map/ppermute | solution.py:50
  106.5 8.3 %collective-permute-start.26 = (bf16[128,256]{1,0:T(8,128)(2,1)S(1)}, bf16[128,256]{1,0:T(8,128)(2,1)S(1)}, u32[]{:S(2)}, u32[]{:S(2)}) collective-permute-start(bf16[128,256]{1,0:T(8,128)(2,1)S(1)} %get-tuple-element.52.own), channel_id=1, source_target_pairs={{8,0},{16,8},{24,16},{32,24},{40,32},{48,40},{56,48},{64,56},{72,6... | collective-permute-start | bytes 196616 | tf_op jit(solution)/shard_map/ppermute | solution.py:54
  117.2 5.2 %collective-permute-start.28 = (bf16[128,128]{1,0:T(8,128)(2,1)S(1)}, bf16[128,128]{1,0:T(8,128)(2,1)S(1)}, u32[]{:S(2)}, u32[]{:S(2)}) collective-permute-start(bf16[128,128]{1,0:T(8,128)(2,1)S(1)} %get-tuple-element.56), channel_id=1, source_target_pairs={{0,2},{2,4},{4,6},{6,0},{1,3},{3,5},{5,7},{7,1},{8,10},{10,12},{12... | collective-permute-start | bytes 98312 | tf_op jit(solution)/shard_map/ppermute | solution.py:257
  118.3 5.4 %collective-permute-start.29 = (bf16[128,128]{1,0:T(8,128)(2,1)S(1)}, bf16[128,128]{1,0:T(8,128)(2,1)S(1)}, u32[]{:S(2)}, u32[]{:S(2)}) collective-permute-start(bf16[128,128]{1,0:T(8,128)(2,1)S(1)} %get-tuple-element.57), channel_id=1, source_target_pairs={{0,4},{2,6},{4,0},{6,2},{1,5},{3,7},{5,1},{7,3},{8,12},{10,14},{12... | collective-permute-start | bytes 98312 | tf_op jit(solution)/shard_map/ppermute | solution.py:259
  121.4 3.9 %collective-permute-start.30 = (bf16[128,128]{1,0:T(8,128)(2,1)S(1)}, bf16[128,128]{1,0:T(8,128)(2,1)S(1)}, u32[]{:S(2)}, u32[]{:S(2)}) collective-permute-start(bf16[128,128]{1,0:T(8,128)(2,1)S(1)} %get-tuple-element.58), channel_id=1, source_target_pairs={{0,6},{2,0},{4,2},{6,4},{1,7},{3,1},{5,3},{7,5},{8,14},{10,8},{12,... | collective-permute-start | bytes 98312 | tf_op jit(solution)/shard_map/ppermute | solution.py:258
  (8 other events, 71.0 us)

commit v15 on v14

--- a/solution.py
+++ b/solution.py
@@ -85,12 +85,9 @@
 
 
 def pack_body(wq, wk, wv, wo, first, parts, sems):
-    @pl.when(pl.program_id(0) == 0)
-    def _():
-        fetch([(w.at[0], parts.at[n]) for n, w in enumerate((wq, wk, wv, wo))], sems)
-
+    fetch([(w.at[0], parts.at[n]) for n, w in enumerate((wq, wk, wv, wo))], sems)
     whole = jnp.concatenate([parts[n] for n in range(4)], axis=1)
-    for n in range(4):
+    for n in range(16):
         first[n] = whole
 
 
@@ -282,7 +279,6 @@
     ]
     first = call(
         pack_body, shaped(16, 64, 512), *held, in_specs=[hbm] * 4,
-        grid=(4,), out_specs=pl.BlockSpec((4, 64, 512), lambda n: (n, 0, 0)),
         scratch=[pltpu.VMEM((4, 64, 128), BF16), pltpu.SemaphoreType.DMA((4,))],
     )
     weights = gather_rows(first, SP)

time: 127 us -> 126 us (level)
  no operation moved by 1% of the time
where the time goes in v15:
time: 126 us; the launch traced here: 125 us
  starting transfers between devices  68.8 us (55%)
  waiting for transfers between devices  45.6 us (36%)
  Pallas kernels  8.74 us (7%)
  local copies, waits for them, and re-layouts  2 us (2%)
    all_to_all x3, starting transfers between devices, gather_rows(): return lax.all_to_all(a, axes, 0, 0, tiled=True).reshape(1024, 512)  19.6 us
    ppermute x12, starting transfers between devices, spread(): return [lax.ppermute(a, axis, turn(k)) for k in (1, 3, 2)]  17.1 us
    ppermute x3, waiting for transfers between devices, from_after(): return lax.ppermute(a, SP, [(i + 1, i) for i in range(15)])  11.3 us
    ppermute x3, starting transfers between devices, from_before(): return lax.ppermute(a, SP, [(i, i + 1) for i in range(15)])  10.1 us
    ppermute x3, starting transfers between devices, turned(): r2 = lax.ppermute(s2, 'y', turn(2))  9.16 us
    pallas_call x16, Pallas kernels, call(): pl.pallas_call(body, out_shape=outs, **specs, scratch_shapes=list(scratch...  8.74 us
    ppermute x3, starting transfers between devices, from_after(): return lax.ppermute(a, SP, [(i + 1, i) for i in range(15)])  8.31 us
    ppermute x12, waiting for transfers between devices, spread(): return [lax.ppermute(a, axis, turn(k)) for k in (1, 3, 2)]  7.89 us
  transfers between devices with their start and end apart: 34, of which 23 were waited for; matrix products, arithmetic and copies ran while one was open for 0% of the time, Pallas kernels for 3%

profile of v15, /device:TPU:38, one launch (start us, length us, event | category | flops | bytes accessed | tf_op | source)
XLA Modules:
  0.0 125.4 jit_solution(11610534351572798168)
XLA Ops:
  0.0 1.9 %shard_map.83 = bf16[16,64,512]{2,1,0:T(8,128)(2,1)} custom-call(bf16[3,64,128]{2,1,0:T(8,128)(2,1)} %wq.3, bf16[3,64,128]{2,1,0:T(8,128)(2,1)} %wk.3, bf16[3,64,128]{2,1,0:T(8,128)(2,1)} %wv.3, bf16[3,64,128]{2,1,0:T(8,128)(2,1)} %bitcast.16), custom_call_target="tpu_custom_call" | custom-call | tf_op jit(solution)/shard_map/pallas_call | solution.py:66
  2.0 8.0 %all-to-all-start = ((bf16[16,64,512]{2,1,0:T(8,128)(2,1)}), bf16[16,64,512]{2,1,0:T(8,128)(2,1)S(1)}, u32[]{:S(2)}, u32[]{:S(2)}) async-start(bf16[16,64,512]{2,1,0:T(8,128)(2,1)} %shard_map.83), calls=%async_computation | async-start | bytes 2097152 | tf_op jit(solution)/shard_map/all_to_all | solution.py:38
  9.9 1.6 %collective-permute-start = (bf16[128,128]{1,0:T(8,128)(2,1)S(1)}, bf16[128,128]{1,0:T(8,128)(2,1)S(1)}, u32[]{:S(2)}, u32[]{:S(2)}) collective-permute-start(bf16[128,128]{1,0:T(8,128)(2,1)S(1)} %copy-done.5), channel_id=1, source_target_pairs={{0,2},{2,4},{4,6},{6,0},{1,3},{3,5},{5,7},{7,1},{8,10},{10,12},{12... | collective-permute-start | bytes 98312 | tf_op jit(solution)/shard_map/ppermute | solution.py:30
  11.6 2.9 %collective-permute-start.1 = (bf16[128,128]{1,0:T(8,128)(2,1)S(1)}, bf16[128,128]{1,0:T(8,128)(2,1)S(1)}, u32[]{:S(2)}, u32[]{:S(2)}) collective-permute-start(bf16[128,128]{1,0:T(8,128)(2,1)S(1)} %copy-done.5), channel_id=1, source_target_pairs={{0,4},{2,6},{4,0},{6,2},{1,5},{3,7},{5,1},{7,3},{8,12},{10,14},{12... | collective-permute-start | bytes 98312 | tf_op jit(solution)/shard_map/ppermute | solution.py:30
  14.5 1.3 %collective-permute-start.2 = (bf16[128,128]{1,0:T(8,128)(2,1)S(1)}, bf16[128,128]{1,0:T(8,128)(2,1)S(1)}, u32[]{:S(2)}, u32[]{:S(2)}) collective-permute-start(bf16[128,128]{1,0:T(8,128)(2,1)S(1)} %copy-done.5), channel_id=1, source_target_pairs={{0,6},{2,0},{4,2},{6,4},{1,7},{3,1},{5,3},{7,5},{8,14},{10,8},{12,... | collective-permute-start | bytes 98312 | tf_op jit(solution)/shard_map/ppermute | solution.py:30
  18.5 1.3 %collective-permute-done.3.partner = bf16[4,128,128]{2,1,0:T(8,128)(2,1)S(1)} collective-permute-done((bf16[4,128,128]{2,1,0:T(8,128)(2,1)S(1)}, bf16[4,128,128]{2,1,0:T(8,128)(2,1)S(1)}, u32[]{:S(2)}, u32[]{:S(2)}) %collective-permute-start.3) | collective-permute-done | bytes 131104 | tf_op jit(solution)/shard_map/ppermute | solution.py:46
  19.8 4.2 %all-to-all-done = bf16[16,64,512]{2,1,0:T(8,128)(2,1)S(1)} async-done(((bf16[16,64,512]{2,1,0:T(8,128)(2,1)}), bf16[16,64,512]{2,1,0:T(8,128)(2,1)S(1)}, u32[]{:S(2)}, u32[]{:S(2)}) %all-to-all-start) | async-done | bytes 1048608 | tf_op jit(solution)/shard_map/all_to_all | solution.py:38
  24.7 7.1 %all-to-all-start.1 = ((bf16[16,64,512]{2,1,0:T(8,128)(2,1)}), bf16[16,64,512]{2,1,0:T(8,128)(2,1)S(1)}, u32[]{:S(2)}, u32[]{:S(2)}) async-start(bf16[16,64,512]{2,1,0:T(8,128)(2,1)} %copy-done.1), calls=%async_computation.1 | async-start | bytes 2097152 | tf_op jit(solution)/shard_map/all_to_all | solution.py:38
  31.8 3.4 %collective-permute-start.4 = (bf16[144,256]{1,0:T(8,128)(2,1)S(1)}, bf16[144,256]{1,0:T(8,128)(2,1)S(1)}, u32[]{:S(2)}, u32[]{:S(2)}) collective-permute-start(bf16[144,256]{1,0:T(8,128)(2,1)S(1)} %get-tuple-element.35.own), channel_id=1, source_target_pairs={{0,8},{8,16},{16,24},{24,32},{32,40},{40,48},{48,56},{56,64},{64,7... | collective-permute-start | bytes 221192 | tf_op jit(solution)/shard_map/ppermute | solution.py:50
  35.1 2.5 %collective-permute-start.5 = (bf16[144,256]{1,0:T(8,128)(2,1)S(1)}, bf16[144,256]{1,0:T(8,128)(2,1)S(1)}, u32[]{:S(2)}, u32[]{:S(2)}) collective-permute-start(bf16[144,256]{1,0:T(8,128)(2,1)S(1)} %get-tuple-element.35.own), channel_id=1, source_target_pairs={{8,0},{16,8},{24,16},{32,24},{40,32},{48,40},{56,48},{64,56},{72,6... | collective-permute-start | bytes 221192 | tf_op jit(solution)/shard_map/ppermute | solution.py:54
  37.6 2.7 %collective-permute-start.6 = (bf16[64,512]{1,0:T(8,128)(2,1)S(1)}, bf16[64,512]{1,0:T(8,128)(2,1)S(1)}, u32[]{:S(2)}, u32[]{:S(2)}) collective-permute-start(bf16[64,512]{1,0:T(8,128)(2,1)S(1)} %get-tuple-element.38.p0), channel_id=1, source_target_pairs={{0,8},{8,16},{16,24},{24,0},{1,9},{9,17},{17,25},{25,1},{2,10},{10... | collective-permute-start | bytes 196616 | tf_op jit(solution)/shard_map/ppermute | solution.py:30
  41.3 5.0 %collective-permute-done.4.before = bf16[144,256]{1,0:T(8,128)(2,1)S(1)} collective-permute-done((bf16[144,256]{1,0:T(8,128)(2,1)S(1)}, bf16[144,256]{1,0:T(8,128)(2,1)S(1)}, u32[]{:S(2)}, u32[]{:S(2)}) %collective-permute-start.4) | collective-permute-done | bytes 73760 | tf_op jit(solution)/shard_map/ppermute | solution.py:50
  48.0 3.3 %collective-permute-start.10 = (bf16[128,256]{1,0:T(8,128)(2,1)S(1)}, bf16[128,256]{1,0:T(8,128)(2,1)S(1)}, u32[]{:S(2)}, u32[]{:S(2)}) collective-permute-start(bf16[128,256]{1,0:T(8,128)(2,1)S(1)} %get-tuple-element.41), channel_id=1, source_target_pairs={{0,4},{2,6},{4,0},{6,2},{1,5},{3,7},{5,1},{7,3},{8,12},{10,14},{12... | collective-permute-start | bytes 196616 | tf_op jit(solution)/shard_map/ppermute | solution.py:256
  55.5 2.3 %collective-permute-done.9.r1 = bf16[128,256]{1,0:T(8,128)(2,1)S(1)} collective-permute-done((bf16[128,256]{1,0:T(8,128)(2,1)S(1)}, bf16[128,256]{1,0:T(8,128)(2,1)S(1)}, u32[]{:S(2)}, u32[]{:S(2)}) %collective-permute-start.9) | collective-permute-done | bytes 65568 | tf_op jit(solution)/shard_map/ppermute | solution.py:254
  57.9 1.3 %collective-permute-done.12.theirs = f32[128,256]{1,0:T(8,128)S(1)} collective-permute-done((f32[128,256]{1,0:T(8,128)S(1)}, f32[128,256]{1,0:T(8,128)S(1)}, u32[]{:S(2)}, u32[]{:S(2)}) %collective-permute-start.12) | collective-permute-done | bytes 131104 | tf_op jit(solution)/shard_map/ppermute | solution.py:46
  59.4 1.4 %collective-permute-start.14 = (bf16[128,256]{1,0:T(8,128)(2,1)S(1)}, bf16[128,256]{1,0:T(8,128)(2,1)S(1)}, u32[]{:S(2)}, u32[]{:S(2)}) collective-permute-start(bf16[128,256]{1,0:T(8,128)(2,1)S(1)} %shard_map.89.x0), channel_id=1, source_target_pairs={{0,4},{2,6},{4,0},{6,2},{1,5},{3,7},{5,1},{7,3},{8,12},{10,14},{12... | collective-permute-start | bytes 196616 | tf_op jit(solution)/shard_map/ppermute | solution.py:30
  60.8 1.8 %collective-permute-start.15 = (bf16[128,256]{1,0:T(8,128)(2,1)S(1)}, bf16[128,256]{1,0:T(8,128)(2,1)S(1)}, u32[]{:S(2)}, u32[]{:S(2)}) collective-permute-start(bf16[128,256]{1,0:T(8,128)(2,1)S(1)} %shard_map.89.x0), channel_id=1, source_target_pairs={{0,6},{2,0},{4,2},{6,4},{1,7},{3,1},{5,3},{7,5},{8,14},{10,8},{12,... | collective-permute-start | bytes 196616 | tf_op jit(solution)/shard_map/ppermute | solution.py:30
  62.6 3.5 %collective-permute-done.13.x1 = bf16[128,256]{1,0:T(8,128)(2,1)S(1)} collective-permute-done((bf16[128,256]{1,0:T(8,128)(2,1)S(1)}, bf16[128,256]{1,0:T(8,128)(2,1)S(1)}, u32[]{:S(2)}, u32[]{:S(2)}) %collective-permute-start.13) | collective-permute-done | bytes 65568 | tf_op jit(solution)/shard_map/ppermute | solution.py:30
  67.2 4.6 %all-to-all-start.2 = ((bf16[4,4,64,512]{3,2,1,0:T(8,128)(2,1)}), bf16[4,4,64,512]{3,2,1,0:T(8,128)(2,1)S(1)}, u32[]{:S(2)}, u32[]{:S(2)}) async-start(bf16[4,4,64,512]{3,2,1,0:T(8,128)(2,1)} %copy-done), calls=%async_computation.2 | async-start | bytes 2097152 | tf_op jit(solution)/shard_map/all_to_all | solution.py:38
  71.8 4.8 %collective-permute-start.16 = (bf16[128,256]{1,0:T(8,128)(2,1)S(1)}, bf16[128,256]{1,0:T(8,128)(2,1)S(1)}, u32[]{:S(2)}, u32[]{:S(2)}) collective-permute-start(bf16[128,256]{1,0:T(8,128)(2,1)S(1)} %get-tuple-element.45.own), channel_id=1, source_target_pairs={{0,8},{8,16},{16,24},{24,32},{32,40},{40,48},{48,56},{56,64},{64,7... | collective-permute-start | bytes 196616 | tf_op jit(solution)/shard_map/ppermute | solution.py:50
  76.6 1.9 %collective-permute-start.17 = (bf16[128,256]{1,0:T(8,128)(2,1)S(1)}, bf16[128,256]{1,0:T(8,128)(2,1)S(1)}, u32[]{:S(2)}, u32[]{:S(2)}) collective-permute-start(bf16[128,256]{1,0:T(8,128)(2,1)S(1)} %get-tuple-element.45.own), channel_id=1, source_target_pairs={{8,0},{16,8},{24,16},{32,24},{40,32},{48,40},{56,48},{64,56},{72,6... | collective-permute-start | bytes 196616 | tf_op jit(solution)/shard_map/ppermute | solution.py:54
  78.5 7.0 %collective-permute-done.17.after = bf16[128,256]{1,0:T(8,128)(2,1)S(1)} collective-permute-done((bf16[128,256]{1,0:T(8,128)(2,1)S(1)}, bf16[128,256]{1,0:T(8,128)(2,1)S(1)}, u32[]{:S(2)}, u32[]{:S(2)}) %collective-permute-start.17) | collective-permute-done | bytes 65568 | tf_op jit(solution)/shard_map/ppermute | solution.py:54
  87.6 2.8 %collective-permute-start.19 = (bf16[128,256]{1,0:T(8,128)(2,1)S(1)}, bf16[128,256]{1,0:T(8,128)(2,1)S(1)}, u32[]{:S(2)}, u32[]{:S(2)}) collective-permute-start(bf16[128,256]{1,0:T(8,128)(2,1)S(1)} %get-tuple-element.48), channel_id=1, source_target_pairs={{0,4},{2,6},{4,0},{6,2},{1,5},{3,7},{5,1},{7,3},{8,12},{10,14},{12... | collective-permute-start | bytes 196616 | tf_op jit(solution)/shard_map/ppermute | solution.py:256
  90.4 1.6 %collective-permute-done.18.r1 = bf16[128,256]{1,0:T(8,128)(2,1)S(1)} collective-permute-done((bf16[128,256]{1,0:T(8,128)(2,1)S(1)}, bf16[128,256]{1,0:T(8,128)(2,1)S(1)}, u32[]{:S(2)}, u32[]{:S(2)}) %collective-permute-start.18) | collective-permute-done | bytes 65568 | tf_op jit(solution)/shard_map/ppermute | solution.py:254
  96.4 2.8 %collective-permute-start.23 = (bf16[128,256]{1,0:T(8,128)(2,1)S(1)}, bf16[128,256]{1,0:T(8,128)(2,1)S(1)}, u32[]{:S(2)}, u32[]{:S(2)}) collective-permute-start(bf16[128,256]{1,0:T(8,128)(2,1)S(1)} %shard_map.93.x0), channel_id=1, source_target_pairs={{0,4},{2,6},{4,0},{6,2},{1,5},{3,7},{5,1},{7,3},{8,12},{10,14},{12... | collective-permute-start | bytes 196616 | tf_op jit(solution)/shard_map/ppermute | solution.py:30
  100.3 2.6 %collective-permute-done.22.x1 = bf16[128,256]{1,0:T(8,128)(2,1)S(1)} collective-permute-done((bf16[128,256]{1,0:T(8,128)(2,1)S(1)}, bf16[128,256]{1,0:T(8,128)(2,1)S(1)}, u32[]{:S(2)}, u32[]{:S(2)}) %collective-permute-start.22) | collective-permute-done | bytes 65568 | tf_op jit(solution)/shard_map/ppermute | solution.py:30
  104.0 1.9 %collective-permute-start.25 = (bf16[128,256]{1,0:T(8,128)(2,1)S(1)}, bf16[128,256]{1,0:T(8,128)(2,1)S(1)}, u32[]{:S(2)}, u32[]{:S(2)}) collective-permute-start(bf16[128,256]{1,0:T(8,128)(2,1)S(1)} %get-tuple-element.52.own), channel_id=1, source_target_pairs={{0,8},{8,16},{16,24},{24,32},{32,40},{40,48},{48,56},{56,64},{64,7... | collective-permute-start | bytes 196616 | tf_op jit(solution)/shard_map/ppermute | solution.py:50
  106.0 3.9 %collective-permute-start.26 = (bf16[128,256]{1,0:T(8,128)(2,1)S(1)}, bf16[128,256]{1,0:T(8,128)(2,1)S(1)}, u32[]{:S(2)}, u32[]{:S(2)}) collective-permute-start(bf16[128,256]{1,0:T(8,128)(2,1)S(1)} %get-tuple-element.52.own), channel_id=1, source_target_pairs={{8,0},{16,8},{24,16},{32,24},{40,32},{48,40},{56,48},{64,56},{72,6... | collective-permute-start | bytes 196616 | tf_op jit(solution)/shard_map/ppermute | solution.py:54
  110.2 4.0 %collective-permute-done.26.after = bf16[128,256]{1,0:T(8,128)(2,1)S(1)} collective-permute-done((bf16[128,256]{1,0:T(8,128)(2,1)S(1)}, bf16[128,256]{1,0:T(8,128)(2,1)S(1)}, u32[]{:S(2)}, u32[]{:S(2)}) %collective-permute-start.26) | collective-permute-done | bytes 65568 | tf_op jit(solution)/shard_map/ppermute | solution.py:54
  117.8 3.1 %collective-permute-start.29 = (bf16[128,128]{1,0:T(8,128)(2,1)S(1)}, bf16[128,128]{1,0:T(8,128)(2,1)S(1)}, u32[]{:S(2)}, u32[]{:S(2)}) collective-permute-start(bf16[128,128]{1,0:T(8,128)(2,1)S(1)} %get-tuple-element.57), channel_id=1, source_target_pairs={{0,4},{2,6},{4,0},{6,2},{1,5},{3,7},{5,1},{7,3},{8,12},{10,14},{12... | collective-permute-start | bytes 98312 | tf_op jit(solution)/shard_map/ppermute | solution.py:256
  121.9 1.3 %collective-permute-done.29.r2 = bf16[128,128]{1,0:T(8,128)(2,1)S(1)} collective-permute-done((bf16[128,128]{1,0:T(8,128)(2,1)S(1)}, bf16[128,128]{1,0:T(8,128)(2,1)S(1)}, u32[]{:S(2)}, u32[]{:S(2)}) %collective-permute-start.29) | collective-permute-done | bytes 32800 | tf_op jit(solution)/shard_map/ppermute | solution.py:256
  123.2 1.6 %collective-permute-done.30.r3 = bf16[128,128]{1,0:T(8,128)(2,1)S(1)} collective-permute-done((bf16[128,128]{1,0:T(8,128)(2,1)S(1)}, bf16[128,128]{1,0:T(8,128)(2,1)S(1)}, u32[]{:S(2)}, u32[]{:S(2)}) %collective-permute-start.30) | collective-permute-done | bytes 32800 | tf_op jit(solution)/shard_map/ppermute | solution.py:255
  (65 shorter events, 25.6 us)
Async XLA Ops:
  2.0 22.1 %all-to-all-start = ((bf16[16,64,512]{2,1,0:T(8,128)(2,1)}), bf16[16,64,512]{2,1,0:T(8,128)(2,1)S(1)}, u32[]{:S(2)}, u32[]{:S(2)}) async-start(bf16[16,64,512]{2,1,0:T(8,128)(2,1)} %shard_map.83), calls=%async_computation | async-start | bytes 2097152 | tf_op jit(solution)/shard_map/all_to_all | solution.py:38
  9.9 7.9 %collective-permute-start = (bf16[128,128]{1,0:T(8,128)(2,1)S(1)}, bf16[128,128]{1,0:T(8,128)(2,1)S(1)}, u32[]{:S(2)}, u32[]{:S(2)}) collective-permute-start(bf16[128,128]{1,0:T(8,128)(2,1)S(1)} %copy-done.5), channel_id=1, source_target_pairs={{0,2},{2,4},{4,6},{6,0},{1,3},{3,5},{5,7},{7,1},{8,10},{10,12},{12... | collective-permute-start | bytes 98312 | tf_op jit(solution)/shard_map/ppermute | solution.py:30
  11.6 6.2 %collective-permute-start.1 = (bf16[128,128]{1,0:T(8,128)(2,1)S(1)}, bf16[128,128]{1,0:T(8,128)(2,1)S(1)}, u32[]{:S(2)}, u32[]{:S(2)}) collective-permute-start(bf16[128,128]{1,0:T(8,128)(2,1)S(1)} %copy-done.5), channel_id=1, source_target_pairs={{0,4},{2,6},{4,0},{6,2},{1,5},{3,7},{5,1},{7,3},{8,12},{10,14},{12... | collective-permute-start | bytes 98312 | tf_op jit(solution)/shard_map/ppermute | solution.py:30
  14.5 3.9 %collective-permute-start.2 = (bf16[128,128]{1,0:T(8,128)(2,1)S(1)}, bf16[128,128]{1,0:T(8,128)(2,1)S(1)}, u32[]{:S(2)}, u32[]{:S(2)}) collective-permute-start(bf16[128,128]{1,0:T(8,128)(2,1)S(1)} %copy-done.5), channel_id=1, source_target_pairs={{0,6},{2,0},{4,2},{6,4},{1,7},{3,1},{5,3},{7,5},{8,14},{10,8},{12,... | collective-permute-start | bytes 98312 | tf_op jit(solution)/shard_map/ppermute | solution.py:30
  18.4 1.4 %collective-permute-start.3 = (bf16[4,128,128]{2,1,0:T(8,128)(2,1)S(1)}, bf16[4,128,128]{2,1,0:T(8,128)(2,1)S(1)}, u32[]{:S(2)}, u32[]{:S(2)}) collective-permute-start(bf16[4,128,128]{2,1,0:T(8,128)(2,1)S(1)} %pad_maximum_fusion.own), channel_id=1, source_target_pairs={{0,1},{1,0},{2,3},{3,2},{4,5},{5,4},{6,7},{7,6},{8,9},{9,8},{10,11... | collective-permute-start | bytes 393224 | tf_op jit(solution)/shard_map/ppermute | solution.py:46
  24.7 42.0 %all-to-all-start.1 = ((bf16[16,64,512]{2,1,0:T(8,128)(2,1)}), bf16[16,64,512]{2,1,0:T(8,128)(2,1)S(1)}, u32[]{:S(2)}, u32[]{:S(2)}) async-start(bf16[16,64,512]{2,1,0:T(8,128)(2,1)} %copy-done.1), calls=%async_computation.1 | async-start | bytes 2097152 | tf_op jit(solution)/shard_map/all_to_all | solution.py:38
  31.8 14.5 %collective-permute-start.4 = (bf16[144,256]{1,0:T(8,128)(2,1)S(1)}, bf16[144,256]{1,0:T(8,128)(2,1)S(1)}, u32[]{:S(2)}, u32[]{:S(2)}) collective-permute-start(bf16[144,256]{1,0:T(8,128)(2,1)S(1)} %get-tuple-element.35.own), channel_id=1, source_target_pairs={{0,8},{8,16},{16,24},{24,32},{32,40},{40,48},{48,56},{56,64},{64,7... | collective-permute-start | bytes 221192 | tf_op jit(solution)/shard_map/ppermute | solution.py:50
  35.1 11.4 %collective-permute-start.5 = (bf16[144,256]{1,0:T(8,128)(2,1)S(1)}, bf16[144,256]{1,0:T(8,128)(2,1)S(1)}, u32[]{:S(2)}, u32[]{:S(2)}) collective-permute-start(bf16[144,256]{1,0:T(8,128)(2,1)S(1)} %get-tuple-element.35.own), channel_id=1, source_target_pairs={{8,0},{16,8},{24,16},{32,24},{40,32},{48,40},{56,48},{64,56},{72,6... | collective-permute-start | bytes 221192 | tf_op jit(solution)/shard_map/ppermute | solution.py:54
  37.6 14.7 %collective-permute-start.6 = (bf16[64,512]{1,0:T(8,128)(2,1)S(1)}, bf16[64,512]{1,0:T(8,128)(2,1)S(1)}, u32[]{:S(2)}, u32[]{:S(2)}) collective-permute-start(bf16[64,512]{1,0:T(8,128)(2,1)S(1)} %get-tuple-element.38.p0), channel_id=1, source_target_pairs={{0,8},{8,16},{16,24},{24,0},{1,9},{9,17},{17,25},{25,1},{2,10},{10... | collective-permute-start | bytes 196616 | tf_op jit(solution)/shard_map/ppermute | solution.py:30
  40.3 13.0 %collective-permute-start.7 = (bf16[64,512]{1,0:T(8,128)(2,1)S(1)}, bf16[64,512]{1,0:T(8,128)(2,1)S(1)}, u32[]{:S(2)}, u32[]{:S(2)}) collective-permute-start(bf16[64,512]{1,0:T(8,128)(2,1)S(1)} %get-tuple-element.38.p0), channel_id=1, source_target_pairs={{0,16},{8,24},{16,0},{24,8},{1,17},{9,25},{17,1},{25,9},{2,18},{10... | collective-permute-start | bytes 196616 | tf_op jit(solution)/shard_map/ppermute | solution.py:30
  40.6 12.7 %collective-permute-start.8 = (bf16[64,512]{1,0:T(8,128)(2,1)S(1)}, bf16[64,512]{1,0:T(8,128)(2,1)S(1)}, u32[]{:S(2)}, u32[]{:S(2)}) collective-permute-start(bf16[64,512]{1,0:T(8,128)(2,1)S(1)} %get-tuple-element.38.p0), channel_id=1, source_target_pairs={{0,24},{8,0},{16,8},{24,16},{1,25},{9,1},{17,9},{25,17},{2,26},{10... | collective-permute-start | bytes 196616 | tf_op jit(solution)/shard_map/ppermute | solution.py:30
  48.0 6.4 %collective-permute-start.10 = (bf16[128,256]{1,0:T(8,128)(2,1)S(1)}, bf16[128,256]{1,0:T(8,128)(2,1)S(1)}, u32[]{:S(2)}, u32[]{:S(2)}) collective-permute-start(bf16[128,256]{1,0:T(8,128)(2,1)S(1)} %get-tuple-element.41), channel_id=1, source_target_pairs={{0,4},{2,6},{4,0},{6,2},{1,5},{3,7},{5,1},{7,3},{8,12},{10,14},{12... | collective-permute-start | bytes 196616 | tf_op jit(solution)/shard_map/ppermute | solution.py:256
  51.3 4.3 %collective-permute-start.11 = (bf16[128,256]{1,0:T(8,128)(2,1)S(1)}, bf16[128,256]{1,0:T(8,128)(2,1)S(1)}, u32[]{:S(2)}, u32[]{:S(2)}) collective-permute-start(bf16[128,256]{1,0:T(8,128)(2,1)S(1)} %get-tuple-element.42), channel_id=1, source_target_pairs={{0,6},{2,0},{4,2},{6,4},{1,7},{3,1},{5,3},{7,5},{8,14},{10,8},{12,... | collective-permute-start | bytes 196616 | tf_op jit(solution)/shard_map/ppermute | solution.py:255
  52.3 5.5 %collective-permute-start.9 = (bf16[128,256]{1,0:T(8,128)(2,1)S(1)}, bf16[128,256]{1,0:T(8,128)(2,1)S(1)}, u32[]{:S(2)}, u32[]{:S(2)}) collective-permute-start(bf16[128,256]{1,0:T(8,128)(2,1)S(1)} %get-tuple-element.40), channel_id=1, source_target_pairs={{0,2},{2,4},{4,6},{6,0},{1,3},{3,5},{5,7},{7,1},{8,10},{10,12},{12... | collective-permute-start | bytes 196616 | tf_op jit(solution)/shard_map/ppermute | solution.py:254
  57.8 1.4 %collective-permute-start.12 = (f32[128,256]{1,0:T(8,128)S(1)}, f32[128,256]{1,0:T(8,128)S(1)}, u32[]{:S(2)}, u32[]{:S(2)}) collective-permute-start(f32[128,256]{1,0:T(8,128)S(1)} %shard_map.88.mine), channel_id=1, source_target_pairs={{0,1},{1,0},{2,3},{3,2},{4,5},{5,4},{6,7},{7,6},{8,9},{9,8},{10,11... | collective-permute-start | bytes 393224 | tf_op jit(solution)/shard_map/ppermute | solution.py:46
  59.3 6.8 %collective-permute-start.13 = (bf16[128,256]{1,0:T(8,128)(2,1)S(1)}, bf16[128,256]{1,0:T(8,128)(2,1)S(1)}, u32[]{:S(2)}, u32[]{:S(2)}) collective-permute-start(bf16[128,256]{1,0:T(8,128)(2,1)S(1)} %shard_map.89.x0), channel_id=1, source_target_pairs={{0,2},{2,4},{4,6},{6,0},{1,3},{3,5},{5,7},{7,1},{8,10},{10,12},{12... | collective-permute-start | bytes 196616 | tf_op jit(solution)/shard_map/ppermute | solution.py:30
  59.4 6.8 %collective-permute-start.14 = (bf16[128,256]{1,0:T(8,128)(2,1)S(1)}, bf16[128,256]{1,0:T(8,128)(2,1)S(1)}, u32[]{:S(2)}, u32[]{:S(2)}) collective-permute-start(bf16[128,256]{1,0:T(8,128)(2,1)S(1)} %shard_map.89.x0), channel_id=1, source_target_pairs={{0,4},{2,6},{4,0},{6,2},{1,5},{3,7},{5,1},{7,3},{8,12},{10,14},{12... | collective-permute-start | bytes 196616 | tf_op jit(solution)/shard_map/ppermute | solution.py:30
  60.8 5.9 %collective-permute-start.15 = (bf16[128,256]{1,0:T(8,128)(2,1)S(1)}, bf16[128,256]{1,0:T(8,128)(2,1)S(1)}, u32[]{:S(2)}, u32[]{:S(2)}) collective-permute-start(bf16[128,256]{1,0:T(8,128)(2,1)S(1)} %shard_map.89.x0), channel_id=1, source_target_pairs={{0,6},{2,0},{4,2},{6,4},{1,7},{3,1},{5,3},{7,5},{8,14},{10,8},{12,... | collective-permute-start | bytes 196616 | tf_op jit(solution)/shard_map/ppermute | solution.py:30
  67.2 36.3 %all-to-all-start.2 = ((bf16[4,4,64,512]{3,2,1,0:T(8,128)(2,1)}), bf16[4,4,64,512]{3,2,1,0:T(8,128)(2,1)S(1)}, u32[]{:S(2)}, u32[]{:S(2)}) async-start(bf16[4,4,64,512]{3,2,1,0:T(8,128)(2,1)} %copy-done), calls=%async_computation.2 | async-start | bytes 2097152 | tf_op jit(solution)/shard_map/all_to_all | solution.py:38
  71.8 6.7 %collective-permute-start.16 = (bf16[128,256]{1,0:T(8,128)(2,1)S(1)}, bf16[128,256]{1,0:T(8,128)(2,1)S(1)}, u32[]{:S(2)}, u32[]{:S(2)}) collective-permute-start(bf16[128,256]{1,0:T(8,128)(2,1)S(1)} %get-tuple-element.45.own), channel_id=1, source_target_pairs={{0,8},{8,16},{16,24},{24,32},{32,40},{40,48},{48,56},{56,64},{64,7... | collective-permute-start | bytes 196616 | tf_op jit(solution)/shard_map/ppermute | solution.py:50
  76.6 9.0 %collective-permute-start.17 = (bf16[128,256]{1,0:T(8,128)(2,1)S(1)}, bf16[128,256]{1,0:T(8,128)(2,1)S(1)}, u32[]{:S(2)}, u32[]{:S(2)}) collective-permute-start(bf16[128,256]{1,0:T(8,128)(2,1)S(1)} %get-tuple-element.45.own), channel_id=1, source_target_pairs={{8,0},{16,8},{24,16},{32,24},{40,32},{48,40},{56,48},{64,56},{72,6... | collective-permute-start | bytes 196616 | tf_op jit(solution)/shard_map/ppermute | solution.py:54
  86.5 5.5 %collective-permute-start.18 = (bf16[128,256]{1,0:T(8,128)(2,1)S(1)}, bf16[128,256]{1,0:T(8,128)(2,1)S(1)}, u32[]{:S(2)}, u32[]{:S(2)}) collective-permute-start(bf16[128,256]{1,0:T(8,128)(2,1)S(1)} %get-tuple-element.47), channel_id=1, source_target_pairs={{0,2},{2,4},{4,6},{6,0},{1,3},{3,5},{5,7},{7,1},{8,10},{10,12},{12... | collective-permute-start | bytes 196616 | tf_op jit(solution)/shard_map/ppermute | solution.py:254
  87.6 5.8 %collective-permute-start.19 = (bf16[128,256]{1,0:T(8,128)(2,1)S(1)}, bf16[128,256]{1,0:T(8,128)(2,1)S(1)}, u32[]{:S(2)}, u32[]{:S(2)}) collective-permute-start(bf16[128,256]{1,0:T(8,128)(2,1)S(1)} %get-tuple-element.48), channel_id=1, source_target_pairs={{0,4},{2,6},{4,0},{6,2},{1,5},{3,7},{5,1},{7,3},{8,12},{10,14},{12... | collective-permute-start | bytes 196616 | tf_op jit(solution)/shard_map/ppermute | solution.py:256
  90.4 4.3 %collective-permute-start.20 = (bf16[128,256]{1,0:T(8,128)(2,1)S(1)}, bf16[128,256]{1,0:T(8,128)(2,1)S(1)}, u32[]{:S(2)}, u32[]{:S(2)}) collective-permute-start(bf16[128,256]{1,0:T(8,128)(2,1)S(1)} %get-tuple-element.49), channel_id=1, source_target_pairs={{0,6},{2,0},{4,2},{6,4},{1,7},{3,1},{5,3},{7,5},{8,14},{10,8},{12,... | collective-permute-start | bytes 196616 | tf_op jit(solution)/shard_map/ppermute | solution.py:255
  96.1 6.8 %collective-permute-start.22 = (bf16[128,256]{1,0:T(8,128)(2,1)S(1)}, bf16[128,256]{1,0:T(8,128)(2,1)S(1)}, u32[]{:S(2)}, u32[]{:S(2)}) collective-permute-start(bf16[128,256]{1,0:T(8,128)(2,1)S(1)} %shard_map.93.x0), channel_id=1, source_target_pairs={{0,2},{2,4},{4,6},{6,0},{1,3},{3,5},{5,7},{7,1},{8,10},{10,12},{12... | collective-permute-start | bytes 196616 | tf_op jit(solution)/shard_map/ppermute | solution.py:30
  96.4 6.5 %collective-permute-start.23 = (bf16[128,256]{1,0:T(8,128)(2,1)S(1)}, bf16[128,256]{1,0:T(8,128)(2,1)S(1)}, u32[]{:S(2)}, u32[]{:S(2)}) collective-permute-start(bf16[128,256]{1,0:T(8,128)(2,1)S(1)} %shard_map.93.x0), channel_id=1, source_target_pairs={{0,4},{2,6},{4,0},{6,2},{1,5},{3,7},{5,1},{7,3},{8,12},{10,14},{12... | collective-permute-start | bytes 196616 | tf_op jit(solution)/shard_map/ppermute | solution.py:30
  99.3 4.3 %collective-permute-start.24 = (bf16[128,256]{1,0:T(8,128)(2,1)S(1)}, bf16[128,256]{1,0:T(8,128)(2,1)S(1)}, u32[]{:S(2)}, u32[]{:S(2)}) collective-permute-start(bf16[128,256]{1,0:T(8,128)(2,1)S(1)} %shard_map.93.x0), channel_id=1, source_target_pairs={{0,6},{2,0},{4,2},{6,4},{1,7},{3,1},{5,3},{7,5},{8,14},{10,8},{12,... | collective-permute-start | bytes 196616 | tf_op jit(solution)/shard_map/ppermute | solution.py:30
  104.0 6.2 %collective-permute-start.25 = (bf16[128,256]{1,0:T(8,128)(2,1)S(1)}, bf16[128,256]{1,0:T(8,128)(2,1)S(1)}, u32[]{:S(2)}, u32[]{:S(2)}) collective-permute-start(bf16[128,256]{1,0:T(8,128)(2,1)S(1)} %get-tuple-element.52.own), channel_id=1, source_target_pairs={{0,8},{8,16},{16,24},{24,32},{32,40},{40,48},{48,56},{56,64},{64,7... | collective-permute-start | bytes 196616 | tf_op jit(solution)/shard_map/ppermute | solution.py:50
  106.0 8.3 %collective-permute-start.26 = (bf16[128,256]{1,0:T(8,128)(2,1)S(1)}, bf16[128,256]{1,0:T(8,128)(2,1)S(1)}, u32[]{:S(2)}, u32[]{:S(2)}) collective-permute-start(bf16[128,256]{1,0:T(8,128)(2,1)S(1)} %get-tuple-element.52.own), channel_id=1, source_target_pairs={{8,0},{16,8},{24,16},{32,24},{40,32},{48,40},{56,48},{64,56},{72,6... | collective-permute-start | bytes 196616 | tf_op jit(solution)/shard_map/ppermute | solution.py:54
  116.7 5.2 %collective-permute-start.28 = (bf16[128,128]{1,0:T(8,128)(2,1)S(1)}, bf16[128,128]{1,0:T(8,128)(2,1)S(1)}, u32[]{:S(2)}, u32[]{:S(2)}) collective-permute-start(bf16[128,128]{1,0:T(8,128)(2,1)S(1)} %get-tuple-element.56), channel_id=1, source_target_pairs={{0,2},{2,4},{4,6},{6,0},{1,3},{3,5},{5,7},{7,1},{8,10},{10,12},{12... | collective-permute-start | bytes 98312 | tf_op jit(solution)/shard_map/ppermute | solution.py:254
  117.8 5.4 %collective-permute-start.29 = (bf16[128,128]{1,0:T(8,128)(2,1)S(1)}, bf16[128,128]{1,0:T(8,128)(2,1)S(1)}, u32[]{:S(2)}, u32[]{:S(2)}) collective-permute-start(bf16[128,128]{1,0:T(8,128)(2,1)S(1)} %get-tuple-element.57), channel_id=1, source_target_pairs={{0,4},{2,6},{4,0},{6,2},{1,5},{3,7},{5,1},{7,3},{8,12},{10,14},{12... | collective-permute-start | bytes 98312 | tf_op jit(solution)/shard_map/ppermute | solution.py:256
  120.9 3.9 %collective-permute-start.30 = (bf16[128,128]{1,0:T(8,128)(2,1)S(1)}, bf16[128,128]{1,0:T(8,128)(2,1)S(1)}, u32[]{:S(2)}, u32[]{:S(2)}) collective-permute-start(bf16[128,128]{1,0:T(8,128)(2,1)S(1)} %get-tuple-element.58), channel_id=1, source_target_pairs={{0,6},{2,0},{4,2},{6,4},{1,7},{3,1},{5,3},{7,5},{8,14},{10,8},{12,... | collective-permute-start | bytes 98312 | tf_op jit(solution)/shard_map/ppermute | solution.py:255
  (8 other events, 71.0 us)
